TPU v7x, 32 devices: a whole 2x2x4 slice. The times are simulated.
32 devices in a mesh: grp: 2 (over x), tp: 4 (over z), dp: 4 (over y, core).
Axes of the slice: x: 2, y: 2, z: 4, core: 2. Of those that a mesh axis runs over, the one named last changes fastest.
Arguments:
- tokens: bfloat16 [32, 4096], P(('grp', 'tp'), 'dp'), parts along dimension 0, may hold values from -30 to 30
- norm_gain: float32 [2, 4096], P(None, 'dp'), may hold values from 0.1 to 1.9
- w_query: bfloat16 [2, 4096, 2048], P(None, 'dp', 'tp'), may hold values from -0.09375 to 0.09375
- w_forget: bfloat16 [2, 4096, 2048], P(None, 'dp', 'tp'), may hold values from -0.09375 to 0.09375
- w_value: bfloat16 [2, 4096, 2048], P(None, 'dp', 'tp'), may hold values from -0.09375 to 0.09375
- w_gate: bfloat16 [2, 4096, 2048], P(None, 'dp', 'tp'), may hold values from -0.09375 to 0.09375
- lower_bound: float32 [2, 2048], P(None, 'tp'), may hold values from 0 to 0.9
- head_gain: float32 [2, 128], replicated, may hold values from 0.1 to 1.9
- w_out: bfloat16 [2, 2048, 4096], P(None, 'tp', 'dp'), may hold values from -0.125 to 0.125
- state: float32 [2, 32, 16, 128, 128], P(None, ('grp', 'dp'), 'tp'), parts along dimension 1, may hold values from -4 to 4
Outputs:
- hidden_out: bfloat16 [32, 4096], P(('grp', 'tp'), 'dp'), parts along dimension 0
- new_state: float32 [2, 32, 16, 128, 128], P(None, ('grp', 'dp'), 'tp'), parts along dimension 1
There are 2 independent parts, one for each index of `grp`. A program takes and returns all parts, laid end to end along the dimension named above; an argument that names none is the same for every part. Nothing has to cross between parts.
All inputs are finite; a program needn't handle non-finite values.
Results may differ from a plain program's by a relative error of at most 0.02.
Values may be sent and summed in bfloat16 or wider, within the bound.
No kernel may reach another device: no remote copies, remote signals or barrier semaphores. Data moves between devices by JAX's collectives and lax.ppermute only.
A program may use at most 64 MiB of HBM per device.

v0:
```python
import jax
import jax.numpy as jnp
from jax import lax
from jax.sharding import PartitionSpec as P

D = 4096
HD = 128


def per_device(
    tokens, norm_gain, w_query, w_forget, w_value, w_gate, lower_bound, head_gain, w_out, state
):
    local_seqs = state.shape[1]
    head_count = state.shape[2]
    offset = lax.axis_index("dp") * local_seqs
    hidden = tokens
    updated = []
    for layer in range(2):
        gathered = lax.all_gather(hidden, "tp", axis=0, tiled=True)
        widened = gathered.astype(jnp.float32)
        squares = jnp.sum(widened * widened, axis=1)
        scaled = (widened * norm_gain[layer]).astype(jnp.bfloat16)
        joined = jnp.concatenate(
            [
                jnp.dot(scaled, weight[layer], preferred_element_type=jnp.float32)
                for weight in (w_query, w_forget, w_value, w_gate)
            ],
            axis=1,
        )
        square_total = lax.psum(squares, "dp")
        own_squares = lax.dynamic_slice_in_dim(square_total, offset, local_seqs, 0)
        payload = (joined,)
        summed = (lax.psum(payload[0].astype(jnp.bfloat16), "dp").astype(jnp.float32),)
        shares = tuple(
            (lax.dynamic_slice_in_dim(member, offset, local_seqs, 0) for member in summed)
        )
        own_proj = shares[0]
        width = own_proj.shape[1] // 4
        factor = lax.rsqrt(own_squares / D + 1e-06)[:, None]
        query, forget_pre, value, gate_pre = (
            own_proj[:, index * width : (index + 1) * width] * factor for index in range(4)
        )
        bound = lower_bound[layer]
        forget = bound + (1.0 - bound) * jax.nn.sigmoid(forget_pre)
        keyvec = (1.0 - bound) * jax.nn.sigmoid(-forget_pre)

        def shaped(array):
            return array.reshape(local_seqs, head_count, HD)

        carried = (
            shaped(forget)[..., None] * state[layer]
            + shaped(keyvec)[..., None] * shaped(value)[..., None, :]
        )
        updated.append(carried)
        readout = jnp.einsum("bhkv,bhk->bhv", carried, shaped(query))
        readout = (
            readout
            * lax.rsqrt(jnp.mean(readout * readout, axis=-1, keepdims=True) + 1e-06)
            * head_gain[layer]
        )
        normed = (readout.reshape(local_seqs, head_count * HD) * jax.nn.sigmoid(gate_pre)).astype(
            jnp.bfloat16
        )
        out_weight = w_out[layer]
        mixed = jnp.dot(
            lax.all_gather(normed, "dp", axis=0, tiled=True),
            out_weight,
            preferred_element_type=jnp.float32,
        )
        mixed_sum = lax.psum_scatter(
            mixed.astype(jnp.bfloat16), "tp", scatter_dimension=0, tiled=True
        ).astype(jnp.float32)
        hidden = (hidden.astype(jnp.float32) + mixed_sum).astype(jnp.bfloat16)
    return (hidden, jnp.stack(updated))


def solution(mesh):
    return jax.shard_map(
        per_device,
        mesh=mesh,
        in_specs=(
            P(("grp", "tp"), "dp"),
            P(None, "dp"),
            P(None, "dp", "tp"),
            P(None, "dp", "tp"),
            P(None, "dp", "tp"),
            P(None, "dp", "tp"),
            P(None, "tp"),
            P(),
            P(None, "tp", "dp"),
            P(None, ("grp", "dp"), "tp", None, None),
        ),
        out_specs=(P(("grp", "tp"), "dp"), P(None, ("grp", "dp"), "tp", None, None)),
        check_vma=False,
    )
```

profile of v0, /device:TPU:0, one launch (start us, length us, event | category | flops | bytes accessed | tf_op | source)
XLA Modules:
  0.0 181.9 jit_solution(1064112044140529132)
XLA Ops:
  7.2 0.9 fusion.47
  8.1 15.1 %all-gather = bf16[4,4,1024]{2,1,0:T(4,128)(2,1)S(1)} all-gather(bf16[1,4,1024]{2,1,0:T(4,128)(2,1)} %bitcast.92), channel_id=1, replica_groups=mesh['grp'=2,'tp'=4,'dp'=4] {'tp'}, dimensions={0}, use_global_device_ids=true | all-gather | bytes 40960 | tf_op jit(solution)/shard_map/all_gather | solution.py:19
  23.2 0.1 multiply_convert_fusion.1
  23.3 1.5 convolution_convert_fusion.6
  24.8 1.5 convolution_convert_fusion.7
  26.3 0.3 convolution_convert_fusion.8
  26.5 1.6 convolution_convert_fusion.9
  28.2 0.7 pad_maximum_fusion.1
  28.9 5.7 %psum.29 = f32[16]{0:T(128)S(1)} all-reduce(f32[16]{0:T(128)S(1)} %get-tuple-element.7), channel_id=1, replica_groups=mesh['grp'=2,'tp'=4,'dp'=4] {'dp'}, use_global_device_ids=true, to_apply=%region_2.0 | all-reduce | flops 16 | bytes 128 | tf_op jit(solution)/shard_map/psum | solution.py:30
  34.7 0.6 dynamic-slice
  35.9 25.6 %all-reduce.5.cloned.1.call-done = bf16[16,2048]{1,0:T(8,128)(2,1)} async-done(((bf16[16,2048]{1,0:T(8,128)(2,1)}), bf16[16,2048]{1,0:T(8,128)(2,1)}) %all-reduce.5.cloned.1.call-update) | async-done | bytes 65552 | tf_op jit(solution)/shard_map/psum | solution.py:33
  61.5 0.8 dynamic-slice_convert_fusion.1
  62.4 1.9 %fusion.10 = f32[4,4,1,128]{3,2,1,0:T(1,128)S(1)} fusion(f32[4,4,128,1]{2,3,1,0:T(1,128)S(1)} %bitcast.100, f32[2,4,4,128,128]{4,3,2,1,0:T(8,128)} %param.19, f32[4,4,128]{2,1,0:T(4,128)S(1)} %mul.268, f32[4,4,128]{2,1,0:T(4,128)S(1)} %mul.265, f32[4,4,128]{2,1,0:T(4,128)S(1)} %mul.261), kind=kOutput, calls=%fused_computation.22 | convolution fusion | flops 1310720 | bytes 1089536 | tf_op jit(solution)/shard_map/bhkv,bhk->bhv/dot_general | solution.py:55
  64.6 5.2 %all-gather.1 = bf16[4,4,512]{2,1,0:T(4,128)(2,1)S(1)} all-gather(bf16[1,4,512]{2,1,0:T(4,128)(2,1)S(1)} %fusion.45), channel_id=1, replica_groups=mesh['grp'=2,'tp'=4,'dp'=4] {'dp'}, dimensions={0}, use_global_device_ids=true | all-gather | bytes 20480 | tf_op jit(solution)/shard_map/all_gather | solution.py:66
  69.9 1.5 convolution_convert_fusion.1
  71.3 19.0 %all-reduce = bf16[16,1024]{1,0:T(8,128)(2,1)S(1)} all-reduce(bf16[16,1024]{1,0:T(8,128)(2,1)S(1)} %convolution_convert_fusion.1), channel_id=2, replica_groups=mesh['grp'=2,'tp'=4,'dp'=4] {'tp'}, use_global_device_ids=true, to_apply=%region_4.0.clone | all-reduce | flops 16384 | bytes 65536
  90.4 13.1 %all-gather.2 = bf16[4,4,1024]{2,1,0:T(4,128)(2,1)S(1)} all-gather(bf16[1,4,1024]{2,1,0:T(4,128)(2,1)S(1)} %fusion.46), channel_id=1, replica_groups=mesh['grp'=2,'tp'=4,'dp'=4] {'tp'}, dimensions={0}, use_global_device_ids=true | all-gather | bytes 40960 | tf_op jit(solution)/shard_map/all_gather | solution.py:19
  103.6 0.2 convolution_convert_fusion.2
  103.9 1.7 convolution_convert_fusion.3
  105.6 0.3 convolution_convert_fusion.4
  105.8 1.5 convolution_convert_fusion.5
  107.3 5.9 %psum.31 = f32[16]{0:T(128)S(1)} all-reduce(f32[16]{0:T(128)S(1)} %get-tuple-element.5), channel_id=1, replica_groups=mesh['grp'=2,'tp'=4,'dp'=4] {'dp'}, use_global_device_ids=true, to_apply=%region_7.0 | all-reduce | flops 16 | bytes 128 | tf_op jit(solution)/shard_map/psum | solution.py:30
  113.1 0.6 pad_maximum_fusion.2
  113.9 28.8 %all-reduce.7.cloned.1.call-done = bf16[16,2048]{1,0:T(8,128)(2,1)} async-done(((bf16[16,2048]{1,0:T(8,128)(2,1)}), bf16[16,2048]{1,0:T(8,128)(2,1)}) %all-reduce.7.cloned.1.call-update) | async-done | bytes 65552 | tf_op jit(solution)/shard_map/psum | solution.py:33
  142.7 0.8 dynamic-slice_convert_fusion
  143.7 2.6 %multiply_add_fusion.1 = (f32[1,4,4,128,128]{4,3,2,1,0:T(8,128)S(1)}, f32[1,4,4,128,128]{4,3,2,1,0:T(8,128)S(1)}) fusion(f32[2,4,4,128,128]{4,3,2,1,0:T(8,128)} %param.19, f32[4,4,128]{2,1,0:T(4,128)S(1)} %mul.268, f32[4,4,128]{2,1,0:T(4,128)S(1)} %mul.265, f32[4,4,128]{2,1,0:T(4,128)S(1)} %mul.261, f32[4,4,128]{2,1,0:T(4,128)S(1)} %mul.296, ...), kind=kLoop, calls=%fused_computation.28 | loop fusion | flops 1572864 | bytes 4243456 | tf_op jit(solution)/shard_map/add | solution.py:51
  146.3 0.7 fusion.2
  147.3 5.2 %all-gather.3 = bf16[4,4,512]{2,1,0:T(4,128)(2,1)S(1)} all-gather(bf16[1,4,512]{2,1,0:T(4,128)(2,1)S(1)} %fusion.44), channel_id=1, replica_groups=mesh['grp'=2,'tp'=4,'dp'=4] {'dp'}, dimensions={0}, use_global_device_ids=true | all-gather | bytes 20480 | tf_op jit(solution)/shard_map/all_gather | solution.py:66
  152.5 1.5 convolution_convert_fusion
  154.0 19.0 %all-reduce.1 = bf16[16,1024]{1,0:T(8,128)(2,1)S(1)} all-reduce(bf16[16,1024]{1,0:T(8,128)(2,1)S(1)} %convolution_convert_fusion), channel_id=3, replica_groups=mesh['grp'=2,'tp'=4,'dp'=4] {'tp'}, use_global_device_ids=true, to_apply=%region_9.0.clone | all-reduce | flops 16384 | bytes 65536
  173.0 0.6 add_convert_fusion
  173.6 1.5 pad_maximum_fusion
  (48 shorter events, 1.3 us)
Async XLA Ops:
  7.2 19.1 %copy-start.1 = (bf16[2,1024,512]{2,1,0:T(8,128)(2,1)S(1)}, bf16[2,1024,512]{2,1,0:T(8,128)(2,1)}, u32[]{:S(2)}) copy-start(bf16[2,1024,512]{2,1,0:T(8,128)(2,1)} %param.13) | copy-start | bytes 6291460
  7.2 54.3 %all-reduce.5.cloned.1.call-start = ((), (), s32[]{:S(2)}) async-start(), calls=%async_computation | async-start | bytes 131072 | tf_op jit(solution)/shard_map/psum | solution.py:33
  23.3 5.6 %copy-start.6 = (f32[2,128]{1,0:T(2,128)S(1)}, f32[2,128]{1,0:T(2,128)}, u32[]{:S(2)}) copy-start(f32[2,128]{1,0:T(2,128)} %param.17) | copy-start | bytes 3076
  23.3 5.6 %copy-start.5 = (f32[2,512]{1,0:T(2,128)S(1)}, f32[2,512]{1,0:T(2,128)}, u32[]{:S(2)}) copy-start(f32[2,512]{1,0:T(2,128)} %param.16) | copy-start | bytes 12292
  23.3 11.4 %copy-start.7 = (u32[32]{0:T(128)S(1)}, u32[32]{0:T(128)}, u32[]{:S(2)}) copy-start(u32[32]{0:T(128)} %constant.30) | copy-start | bytes 388
  26.5 63.8 %copy-start.4 = (bf16[4,1024]{1,0:T(4,128)(2,1)S(1)}, bf16[4,1024]{1,0:T(4,128)(2,1)}, u32[]{:S(2)}) copy-start(bf16[4,1024]{1,0:T(4,128)(2,1)} %param.10) | copy-start | bytes 24580
  26.5 77.1 %copy-start = (bf16[2,1024,512]{2,1,0:T(8,128)(2,1)S(1)}, bf16[2,1024,512]{2,1,0:T(8,128)(2,1)}, u32[]{:S(2)}) copy-start(bf16[2,1024,512]{2,1,0:T(8,128)(2,1)} %param.15) | copy-start | bytes 6291460
  28.8 113.9 %all-reduce.7.cloned.1.call-start = ((), (), s32[]{:S(2)}) async-start(), calls=%async_computation.1 | async-start | bytes 131072 | tf_op jit(solution)/shard_map/psum | solution.py:33
  103.5 2.1 %copy-start.2 = (bf16[2,1024,512]{2,1,0:T(8,128)(2,1)S(1)}, bf16[2,1024,512]{2,1,0:T(8,128)(2,1)}, u32[]{:S(2)}) copy-start(bf16[2,1024,512]{2,1,0:T(8,128)(2,1)} %param.13) | copy-start | bytes 6291460
  143.7 2.6 %copy-start.3 = (f32[2,4,4,128,128]{4,3,2,1,0:T(8,128)S(1)}, f32[2,4,4,128,128]{4,3,2,1,0:T(8,128)}, u32[]{:S(2)}) copy-start(f32[2,4,4,128,128]{4,3,2,1,0:T(8,128)} %param.19) | copy-start | bytes 6291460
Sparse Core Ops, SparseCore 0:
  28.9 32.5 all-reduce.4
  113.9 28.7 all-reduce.6
where the time goes:
time: 182 us
  blocking collectives  88.1 us (48%)
  waiting for transfers between devices  54.5 us (30%)
  between operations  14.9 us (8%)
  matrix products  14.1 us (8%)
  other arithmetic  8.64 us (5%)
    psum x2, waiting for transfers between devices, per_device(): lax.psum(payload[0].astype(jnp.bfloat16), 'dp').astype(jnp.float32)  54.4 us
    unnamed x2, blocking collectives  38 us
    all_gather x2, blocking collectives, per_device(): gathered = lax.all_gather(hidden, 'tp', axis=0, tiled=True)  28.2 us
    psum x2, blocking collectives, per_device(): square_total = lax.psum(squares, 'dp')  11.5 us
    all_gather x2, blocking collectives, per_device(): lax.all_gather(normed, 'dp', axis=0, tiled=True)  10.4 us
    dot_general x8, matrix products, per_device(): jnp.dot(scaled, weight[layer], preferred_element_type=jnp.float32)  8.47 us
  transfers between devices with their start and end apart: 2, of which 2 were waited for; matrix products, arithmetic and copies ran while one was open for 0% of the time, Pallas kernels for 0%

commit v1 on v0

v1 whole, which is shorter than its diff:
```python
import jax
import jax.numpy as jnp
from jax import lax
from jax.sharding import PartitionSpec as P


def partners(n):
    if n & (n - 1) == 0:
        return [[i ^ k for i in range(n)] for k in range(n)]
    return [[(k - i) % n for i in range(n)] for k in range(n)]


def peer_of(n, k, index):
    if n & (n - 1) == 0:
        return jnp.bitwise_xor(index, k)
    return lax.rem(k - index + n, n)


def swap(array, axis, n, k):
    return lax.ppermute(array, axis, list(enumerate(partners(n)[k])))


def per_device(
    features,
    n_tp,
    n_dp,
    tokens,
    norm_gain,
    w_query,
    w_forget,
    w_value,
    w_gate,
    lower_bound,
    head_gain,
    w_out,
    state,
):
    seqs, heads, hd = state.shape[1], state.shape[2], state.shape[3]
    rows = tokens.shape[0]
    total = rows * n_tp
    tp = lax.axis_index("tp")
    dp = lax.axis_index("dp")

    def gather(array, axis, n, index):
        count = array.shape[0]
        out = jnp.zeros((count * n,) + array.shape[1:], array.dtype)
        parts = [array] + [swap(array, axis, n, k) for k in range(1, n)]
        for k, part in enumerate(parts):
            out = lax.dynamic_update_slice_in_dim(out, part, peer_of(n, k, index) * count, 0)
        return out

    def scatter_sum(array, axis, n, index):
        count = array.shape[0] // n
        own = lax.dynamic_slice_in_dim(array, index * count, count, 0)
        for k in range(1, n):
            piece = lax.dynamic_slice_in_dim(array, peer_of(n, k, index) * count, count, 0)
            own = own + swap(piece.astype(jnp.bfloat16), axis, n, k).astype(jnp.float32)
        return own

    hidden = gather(tokens, "tp", n_tp, tp)
    updated = []
    for layer in range(2):
        widened = hidden.astype(jnp.float32)
        squares = jnp.sum(widened * widened, axis=1, keepdims=True)
        scaled = (widened * norm_gain[layer]).astype(jnp.bfloat16)
        high = squares.astype(jnp.bfloat16).astype(jnp.float32)
        middle = (squares - high).astype(jnp.bfloat16).astype(jnp.float32)
        low = squares - high - middle
        joined = jnp.concatenate(
            [
                jnp.dot(scaled, weight[layer], preferred_element_type=jnp.float32)
                for weight in (w_query, w_forget, w_value, w_gate)
            ]
            + [jnp.concatenate([high, middle, low, jnp.zeros((total, 125), jnp.float32)], axis=1)],
            axis=1,
        )
        own = scatter_sum(joined, "dp", n_dp, dp)
        width = heads * hd
        mean = jnp.sum(own[:, 4 * width :], axis=1, keepdims=True) / features
        factor = lax.rsqrt(mean + 1e-06)
        query, forget_pre, value, gate_pre = (
            own[:, index * width : (index + 1) * width] * factor for index in range(4)
        )
        bound = lower_bound[layer]
        forget = bound + (1.0 - bound) * jax.nn.sigmoid(forget_pre)
        keyvec = (1.0 - bound) * jax.nn.sigmoid(-forget_pre)

        def shaped(array):
            return array.reshape(seqs, heads, hd)

        carried = (
            shaped(forget)[..., None] * state[layer]
            + shaped(keyvec)[..., None] * shaped(value)[..., None, :]
        )
        updated.append(carried)
        readout = jnp.einsum("bhkv,bhk->bhv", carried, shaped(query))
        readout = (
            readout
            * lax.rsqrt(jnp.mean(readout * readout, axis=-1, keepdims=True) + 1e-06)
            * head_gain[layer]
        )
        normed = (readout.reshape(seqs, width) * jax.nn.sigmoid(gate_pre)).astype(jnp.bfloat16)
        mixed = jnp.dot(
            gather(normed, "dp", n_dp, dp), w_out[layer], preferred_element_type=jnp.float32
        )
        if layer == 0:
            sent = mixed.astype(jnp.bfloat16)
            for k in range(1, n_tp):
                mixed = mixed + swap(sent, "tp", n_tp, k).astype(jnp.float32)
            hidden = (widened + mixed).astype(jnp.bfloat16)
        else:
            base = lax.dynamic_slice_in_dim(widened, tp * rows, rows, 0)
            hidden = (base + scatter_sum(mixed, "tp", n_tp, tp)).astype(jnp.bfloat16)
    return (hidden, jnp.stack(updated))


def solution(mesh):
    n_tp, n_dp = mesh.shape["tp"], mesh.shape["dp"]

    def body(tokens, *rest):
        return per_device(tokens.shape[1] * n_dp, n_tp, n_dp, tokens, *rest)

    return jax.shard_map(
        body,
        mesh=mesh,
        in_specs=(
            P(("grp", "tp"), "dp"),
            P(None, "dp"),
            P(None, "dp", "tp"),
            P(None, "dp", "tp"),
            P(None, "dp", "tp"),
            P(None, "dp", "tp"),
            P(None, "tp"),
            P(),
            P(None, "tp", "dp"),
            P(None, ("grp", "dp"), "tp", None, None),
        ),
        out_specs=(P(("grp", "tp"), "dp"), P(None, ("grp", "dp"), "tp", None, None)),
        check_vma=False,
    )
```

time: 182 us -> 59.5 us (0.33)
  blocking collectives: 88.1 us -> 0 us
  waiting for transfers between devices: 54.5 us -> 15.3 us
  starting transfers between devices: 0.08 us -> 22.2 us
  between operations: 14.9 us -> 0.94 us
  matrix products: 14.1 us -> 11.4 us
  other arithmetic: 8.64 us -> 6.69 us
    psum x2 -> x0, waiting for transfers between devices: 54.4 us -> none  [per_device(): lax.psum(payload[0].astype(jnp.bfloat16), 'dp').astype(jnp.float32)]
    all_gather x4 -> x0, blocking collectives: 38.6 us -> none  [the longest x2 28.2 us: per_device(): gathered = lax.all_gather(hidden, 'tp', axis=0, tiled=True)]
    unnamed x2 -> x0, blocking collectives: 38 us -> none
    ppermute x0 -> x21, starting transfers between devices: none -> 22.2 us  [swap(): return lax.ppermute(array, axis, list(enumerate(partners(n)[k])))]
    ppermute x0 -> x21, waiting for transfers between devices: none -> 15.3 us  [swap(): return lax.ppermute(array, axis, list(enumerate(partners(n)[k])))]
    psum x2 -> x0, blocking collectives: 11.5 us -> none  [per_device(): square_total = lax.psum(squares, 'dp')]
    dot_general x8, matrix products: 8.47 us -> 5.67 us  [per_device(): jnp.dot(scaled, weight[layer], preferred_element_type=jnp.float32)]
  transfers between devices with their start and end apart: 2 -> 21, of which waited for: 2 -> 11; matrix products, arithmetic and copies ran while one was open for 0% -> 11% of each run, Pallas kernels for 0% -> 0%
where the time goes in v1:
time: 59.5 us; the launch traced here: 59.1 us
  starting transfers between devices  22.2 us (37%)
  waiting for transfers between devices  15.3 us (26%)
  matrix products  11.4 us (19%)
  other arithmetic  6.69 us (11%)
  local copies, waits for them, and re-layouts  2.55 us (4%)
  between operations  0.94 us (2%)
    ppermute x21, starting transfers between devices, swap(): return lax.ppermute(array, axis, list(enumerate(partners(n)[k])))  22.2 us
    ppermute x21, waiting for transfers between devices, swap(): return lax.ppermute(array, axis, list(enumerate(partners(n)[k])))  15.3 us
    dot_general x8, matrix products, per_device(): jnp.dot(scaled, weight[layer], preferred_element_type=jnp.float32)  5.67 us
    dot_general x2, matrix products, per_device(): readout = jnp.einsum('bhkv,bhk->bhv', carried, shaped(query))  4.03 us
    add x1, other arithmetic, per_device(): shaped(forget)[..., None] * state[layer]  2.45 us
    dot_general x2, matrix products, per_device(): jnp.dot(gather(normed, 'dp', n_dp, dp), w_out[layer], preferred_element_t...  1.73 us
    another operation x1, other arithmetic, per_device(): return (hidden, jnp.stack(updated))  1.55 us
  transfers between devices with their start and end apart: 21, of which 11 were waited for; matrix products, arithmetic and copies ran while one was open for 11% of the time, Pallas kernels for 0%

profile of v1, /device:TPU:0, one launch (start us, length us, event | category | flops | bytes accessed | tf_op | source)
XLA Modules:
  0.0 59.1 jit_solution(14553940598794785653)
XLA Ops:
  0.6 3.1 %collective-permute-start = (bf16[4,1024]{1,0:T(4,128)(2,1)}, bf16[4,1024]{1,0:T(4,128)(2,1)S(1)}, u32[]{:S(2)}, u32[]{:S(2)}) collective-permute-start(bf16[4,1024]{1,0:T(4,128)(2,1)} %param.10), channel_id=1, source_target_pairs={{0,4},{4,0},{8,12},{12,8},{1,5},{5,1},{9,13},{13,9},{2,6},{6,2},{1... | collective-permute-start | bytes 24584 | tf_op jit(solution)/shard_map/ppermute | solution.py:20
  3.8 2.5 %collective-permute-start.2 = (bf16[4,1024]{1,0:T(4,128)(2,1)}, bf16[4,1024]{1,0:T(4,128)(2,1)S(1)}, u32[]{:S(2)}, u32[]{:S(2)}) collective-permute-start(bf16[4,1024]{1,0:T(4,128)(2,1)} %param.10), channel_id=1, source_target_pairs={{0,12},{4,8},{8,4},{12,0},{1,13},{5,9},{9,5},{13,1},{2,14},{6,10},... | collective-permute-start | bytes 24584 | tf_op jit(solution)/shard_map/ppermute | solution.py:20
  6.3 0.8 %fusion.70 = (f32[1,512]{1,0:T(1,128)S(1)}, f32[1,512]{1,0:T(1,128)S(1)}, f32[1,512]{1,0:T(1,128)S(1)}, f32[1,512]{1,0:T(1,128)S(1)}) fusion(f32[2,512]{1,0:T(2,128)} %param.16), kind=kLoop, calls=%fused_computation.129 | loop fusion | flops 1024 | bytes 12288 | tf_op jit(solution)/shard_map/slice | solution.py:84
  7.1 0.8 %fusion.69 = (f32[1,1024]{1,0:T(1,128)S(1)}, f32[1,1024]{1,0:T(1,128)S(1)}) fusion(f32[2,1024]{1,0:T(2,128)} %param.11), kind=kLoop, calls=%fused_computation.128 | loop fusion | bytes 16384 | tf_op jit(solution)/shard_map/slice | solution.py:65
  7.9 0.7 %constant_dynamic-update-slice_fusion.11 = bf16[16,1024]{1,0:T(8,128)(2,1)S(1)} fusion(bf16[16,1024]{1,0:T(8,128)(2,1)S(1)} %broadcast_in_dim.2, bf16[4,1024]{1,0:T(4,128)(2,1)} %param.10, s32[]{:T(128)S(6)} %select_n.16), kind=kLoop, calls=%fused_computation.107 | loop fusion | bytes 16388 | tf_op jit(solution)/shard_map/dynamic_update_slice | solution.py:49
  8.7 2.3 %collective-permute-done.1 = bf16[4,1024]{1,0:T(4,128)(2,1)S(1)} collective-permute-done((bf16[4,1024]{1,0:T(4,128)(2,1)}, bf16[4,1024]{1,0:T(4,128)(2,1)S(1)}, u32[]{:S(2)}, u32[]{:S(2)}) %collective-permute-start.1) | collective-permute-done | bytes 8224 | tf_op jit(solution)/shard_map/ppermute | solution.py:20
  11.4 1.5 %fusion.22 = f32[16,512]{1,0:T(8,128)S(1)} fusion(bf16[2,1024,512]{2,1,0:T(8,128)(2,1)} %param.13, bf16[16,1024]{1,0:T(8,128)(2,1)S(1)} %constant_dynamic-update-slice_fusion.8, f32[1024]{0:T(1024)S(1)} %bitcast.106), kind=kOutput, calls=%fused_computation.23 | convolution fusion | flops 16826368 | bytes 1118208 | tf_op jit(solution)/shard_map/dot_general | solution.py:71
  12.9 1.5 %fusion.20 = f32[16,512]{1,0:T(8,128)S(1)} fusion(bf16[2,1024,512]{2,1,0:T(8,128)(2,1)} %param.14, bf16[16,1024]{1,0:T(8,128)(2,1)S(1)} %constant_dynamic-update-slice_fusion.8, f32[1024]{0:T(1024)S(1)} %bitcast.107), kind=kOutput, calls=%fused_computation.21 | convolution fusion | flops 16826368 | bytes 1118208 | tf_op jit(solution)/shard_map/dot_general | solution.py:71
  14.6 1.5 %fusion.24 = f32[16,512]{1,0:T(8,128)S(1)} fusion(bf16[2,1024,512]{2,1,0:T(8,128)(2,1)} %param.12, bf16[16,1024]{1,0:T(8,128)(2,1)S(1)} %constant_dynamic-update-slice_fusion.8, f32[1024]{0:T(1024)S(1)} %bitcast.109), kind=kOutput, calls=%fused_computation.25 | convolution fusion | flops 16826368 | bytes 1118208 | tf_op jit(solution)/shard_map/dot_general | solution.py:71
  16.3 1.6 %collective-permute-start.5 = (bf16[4,2176]{1,0:T(4,128)(2,1)S(1)}, bf16[4,2176]{1,0:T(4,128)(2,1)S(1)}, u32[]{:S(2)}, u32[]{:S(2)}) collective-permute-start(bf16[4,2176]{1,0:T(4,128)(2,1)S(1)} %get-tuple-element.14), channel_id=1, source_target_pairs={{0,3},{1,2},{2,1},{3,0},{4,7},{5,6},{6,5},{7,4},{8,11},{9,10},{10,... | collective-permute-start | bytes 52232 | tf_op jit(solution)/shard_map/ppermute | solution.py:20
  18.5 1.1 %collective-permute-done.5 = bf16[4,2176]{1,0:T(4,128)(2,1)S(1)} collective-permute-done((bf16[4,2176]{1,0:T(4,128)(2,1)S(1)}, bf16[4,2176]{1,0:T(4,128)(2,1)S(1)}, u32[]{:S(2)}, u32[]{:S(2)}) %collective-permute-start.5) | collective-permute-done | bytes 17440 | tf_op jit(solution)/shard_map/ppermute | solution.py:20
  19.6 2.1 %collective-permute-done.4 = bf16[4,2176]{1,0:T(4,128)(2,1)S(1)} collective-permute-done((bf16[4,2176]{1,0:T(4,128)(2,1)S(1)}, bf16[4,2176]{1,0:T(4,128)(2,1)S(1)}, u32[]{:S(2)}, u32[]{:S(2)}) %collective-permute-start.4) | collective-permute-done | bytes 17440 | tf_op jit(solution)/shard_map/ppermute | solution.py:20
  22.0 2.1 %fusion.16 = f32[4,4,1,128]{3,2,1,0:T(1,128)S(1)} fusion(f32[4,4,128,1]{2,3,1,0:T(1,128)S(1)} %bitcast.115, f32[2,4,4,128,128]{4,3,2,1,0:T(8,128)} %param.19, f32[4,4,128]{2,1,0:T(4,128)S(1)} %mul.313, f32[4,4,128]{2,1,0:T(4,128)S(1)} %mul.310, f32[4,4,128]{2,1,0:T(4,128)S(1)} %mul.306), kind=kOutput, calls=%fused_computation.18 | convolution fusion | flops 1310720 | bytes 1089536 | tf_op jit(solution)/shard_map/bhkv,bhk->bhv/dot_general | solution.py:96
  25.0 1.3 %collective-permute-start.8 = (bf16[4,512]{1,0:T(4,128)(2,1)S(1)}, bf16[4,512]{1,0:T(4,128)(2,1)S(1)}, u32[]{:S(2)}, u32[]{:S(2)}) collective-permute-start(bf16[4,512]{1,0:T(4,128)(2,1)S(1)} %get-tuple-element.7), channel_id=1, source_target_pairs={{0,3},{1,2},{2,1},{3,0},{4,7},{5,6},{6,5},{7,4},{8,11},{9,10},{10,... | collective-permute-start | bytes 12296 | tf_op jit(solution)/shard_map/ppermute | solution.py:20
  26.3 1.8 %collective-permute-done.7 = bf16[4,512]{1,0:T(4,128)(2,1)S(1)} collective-permute-done((bf16[4,512]{1,0:T(4,128)(2,1)S(1)}, bf16[4,512]{1,0:T(4,128)(2,1)S(1)}, u32[]{:S(2)}, u32[]{:S(2)}) %collective-permute-start.7) | collective-permute-done | bytes 4128 | tf_op jit(solution)/shard_map/ppermute | solution.py:20
  28.2 1.5 %fusion.71 = (bf16[16,1024]{1,0:T(8,128)(2,1)S(1)}, f32[16,1024]{1,0:T(8,128)S(1)}) fusion(bf16[16,512]{1,0:T(8,128)(2,1)S(1)} %constant_dynamic-update-slice_fusion.4, bf16[2,512,1024]{2,1,0:T(8,128)(2,1)} %param.18), kind=kOutput, calls=%fused_computation.130 | convolution fusion | flops 16793600 | bytes 1163264 | tf_op jit(solution)/shard_map/dot_general | solution.py:103
  29.7 1.4 %collective-permute-start.11 = (bf16[16,1024]{1,0:T(8,128)(2,1)S(1)}, bf16[16,1024]{1,0:T(8,128)(2,1)S(1)}, u32[]{:S(2)}, u32[]{:S(2)}) collective-permute-start(bf16[16,1024]{1,0:T(8,128)(2,1)S(1)} %get-tuple-element.39), channel_id=1, source_target_pairs={{0,12},{4,8},{8,4},{12,0},{1,13},{5,9},{9,5},{13,1},{2,14},{6,10},... | collective-permute-start | bytes 98312 | tf_op jit(solution)/shard_map/ppermute | solution.py:20
  31.0 0.8 %collective-permute-start.10 = (bf16[16,1024]{1,0:T(8,128)(2,1)S(1)}, bf16[16,1024]{1,0:T(8,128)(2,1)S(1)}, u32[]{:S(2)}, u32[]{:S(2)}) collective-permute-start(bf16[16,1024]{1,0:T(8,128)(2,1)S(1)} %get-tuple-element.39), channel_id=1, source_target_pairs={{0,8},{4,12},{8,0},{12,4},{1,9},{5,13},{9,1},{13,5},{2,10},{6,14},... | collective-permute-start | bytes 98312 | tf_op jit(solution)/shard_map/ppermute | solution.py:20
  31.8 2.2 %collective-permute-start.9 = (bf16[16,1024]{1,0:T(8,128)(2,1)S(1)}, bf16[16,1024]{1,0:T(8,128)(2,1)S(1)}, u32[]{:S(2)}, u32[]{:S(2)}) collective-permute-start(bf16[16,1024]{1,0:T(8,128)(2,1)S(1)} %get-tuple-element.39), channel_id=1, source_target_pairs={{0,4},{4,0},{8,12},{12,8},{1,5},{5,1},{9,13},{13,9},{2,6},{6,2},{1... | collective-permute-start | bytes 98312 | tf_op jit(solution)/shard_map/ppermute | solution.py:20
  34.1 1.3 %collective-permute-done.11 = bf16[16,1024]{1,0:T(8,128)(2,1)S(1)} collective-permute-done((bf16[16,1024]{1,0:T(8,128)(2,1)S(1)}, bf16[16,1024]{1,0:T(8,128)(2,1)S(1)}, u32[]{:S(2)}, u32[]{:S(2)}) %collective-permute-start.11) | collective-permute-done | bytes 32800 | tf_op jit(solution)/shard_map/ppermute | solution.py:20
  35.4 0.9 %collective-permute-done.10 = bf16[16,1024]{1,0:T(8,128)(2,1)S(1)} collective-permute-done((bf16[16,1024]{1,0:T(8,128)(2,1)S(1)}, bf16[16,1024]{1,0:T(8,128)(2,1)S(1)}, u32[]{:S(2)}, u32[]{:S(2)}) %collective-permute-start.10) | collective-permute-done | bytes 32800 | tf_op jit(solution)/shard_map/ppermute | solution.py:20
  38.1 1.6 %collective-permute-start.14 = (bf16[4,2176]{1,0:T(4,128)(2,1)S(1)}, bf16[4,2176]{1,0:T(4,128)(2,1)S(1)}, u32[]{:S(2)}, u32[]{:S(2)}) collective-permute-start(bf16[4,2176]{1,0:T(4,128)(2,1)S(1)} %get-tuple-element.11), channel_id=1, source_target_pairs={{0,3},{1,2},{2,1},{3,0},{4,7},{5,6},{6,5},{7,4},{8,11},{9,10},{10,... | collective-permute-start | bytes 52232 | tf_op jit(solution)/shard_map/ppermute | solution.py:20
  40.2 1.1 %collective-permute-done.14 = bf16[4,2176]{1,0:T(4,128)(2,1)S(1)} collective-permute-done((bf16[4,2176]{1,0:T(4,128)(2,1)S(1)}, bf16[4,2176]{1,0:T(4,128)(2,1)S(1)}, u32[]{:S(2)}, u32[]{:S(2)}) %collective-permute-start.14) | collective-permute-done | bytes 17440 | tf_op jit(solution)/shard_map/ppermute | solution.py:20
  41.3 2.1 %collective-permute-done.13 = bf16[4,2176]{1,0:T(4,128)(2,1)S(1)} collective-permute-done((bf16[4,2176]{1,0:T(4,128)(2,1)S(1)}, bf16[4,2176]{1,0:T(4,128)(2,1)S(1)}, u32[]{:S(2)}, u32[]{:S(2)}) %collective-permute-start.13) | collective-permute-done | bytes 17440 | tf_op jit(solution)/shard_map/ppermute | solution.py:20
  43.7 1.9 %fusion.3 = f32[4,4,1,128]{3,2,1,0:T(1,128)S(1)} fusion(f32[4,4,128,1]{2,3,1,0:T(1,128)S(1)} %bitcast.116, f32[2,4,4,128,128]{4,3,2,1,0:T(8,128)} %param.19, f32[4,4,128]{2,1,0:T(4,128)S(1)} %mul.341, f32[4,4,128]{2,1,0:T(4,128)S(1)} %mul.338, f32[4,4,128]{2,1,0:T(4,128)S(1)} %mul.334), kind=kOutput, calls=%fused_computation.5 | convolution fusion | flops 1310720 | bytes 1089536 | tf_op jit(solution)/shard_map/bhkv,bhk->bhv/dot_general | solution.py:96
  46.6 1.6 %collective-permute-start.17 = (bf16[4,512]{1,0:T(4,128)(2,1)S(1)}, bf16[4,512]{1,0:T(4,128)(2,1)S(1)}, u32[]{:S(2)}, u32[]{:S(2)}) collective-permute-start(bf16[4,512]{1,0:T(4,128)(2,1)S(1)} %get-tuple-element.3), channel_id=1, source_target_pairs={{0,3},{1,2},{2,1},{3,0},{4,7},{5,6},{6,5},{7,4},{8,11},{9,10},{10,... | collective-permute-start | bytes 12296 | tf_op jit(solution)/shard_map/ppermute | solution.py:20
  48.2 2.4 %multiply_add_fusion.1 = (f32[1,4,4,128,128]{4,3,2,1,0:T(8,128)S(1)}, f32[1,4,4,128,128]{4,3,2,1,0:T(8,128)S(1)}) fusion(f32[2,4,4,128,128]{4,3,2,1,0:T(8,128)} %param.19, f32[4,4,128]{2,1,0:T(4,128)S(1)} %mul.313, f32[4,4,128]{2,1,0:T(4,128)S(1)} %mul.310, f32[4,4,128]{2,1,0:T(4,128)S(1)} %mul.306, f32[4,4,128]{2,1,0:T(4,128)S(1)} %mul.341, ...), kind=kLoop, calls=%fused_computation.28 | loop fusion | flops 1572864 | bytes 4243456 | tf_op jit(solution)/shard_map/add | solution.py:92
  51.0 1.5 %collective-permute-start.18 = (bf16[4,1024]{1,0:T(4,128)(2,1)S(1)}, bf16[4,1024]{1,0:T(4,128)(2,1)S(1)}, u32[]{:S(2)}, u32[]{:S(2)}) collective-permute-start(bf16[4,1024]{1,0:T(4,128)(2,1)S(1)} %get-tuple-element.16), channel_id=1, source_target_pairs={{0,4},{4,0},{8,12},{12,8},{1,5},{5,1},{9,13},{13,9},{2,6},{6,2},{1... | collective-permute-start | bytes 24584 | tf_op jit(solution)/shard_map/ppermute | solution.py:20
  52.5 1.3 %collective-permute-start.20 = (bf16[4,1024]{1,0:T(4,128)(2,1)S(1)}, bf16[4,1024]{1,0:T(4,128)(2,1)S(1)}, u32[]{:S(2)}, u32[]{:S(2)}) collective-permute-start(bf16[4,1024]{1,0:T(4,128)(2,1)S(1)} %get-tuple-element.17), channel_id=1, source_target_pairs={{0,12},{4,8},{8,4},{12,0},{1,13},{5,9},{9,5},{13,1},{2,14},{6,10},... | collective-permute-start | bytes 24584 | tf_op jit(solution)/shard_map/ppermute | solution.py:20
  53.9 0.7 %collective-permute-start.19 = (bf16[4,1024]{1,0:T(4,128)(2,1)S(1)}, bf16[4,1024]{1,0:T(4,128)(2,1)S(1)}, u32[]{:S(2)}, u32[]{:S(2)}) collective-permute-start(bf16[4,1024]{1,0:T(4,128)(2,1)S(1)} %get-tuple-element.18), channel_id=1, source_target_pairs={{0,8},{4,12},{8,0},{12,4},{1,9},{5,13},{9,1},{13,5},{2,10},{6,14},... | collective-permute-start | bytes 24584 | tf_op jit(solution)/shard_map/ppermute | solution.py:20
  54.6 1.5 %pad_maximum_fusion = f32[2,4,4,128,128]{4,3,2,1,0:T(8,128)} fusion(f32[1,4,4,128,128]{4,3,2,1,0:T(8,128)S(1)} %get-tuple-element.9, f32[1,4,4,128,128]{4,3,2,1,0:T(8,128)S(1)} %get-tuple-element.8), kind=kLoop, calls=%fused_computation | loop fusion | flops 524288 | bytes 4194304 | tf_op jit(solution)/shard_map/stack | solution.py:114
  56.1 1.9 %collective-permute-done.20 = bf16[4,1024]{1,0:T(4,128)(2,1)S(1)} collective-permute-done((bf16[4,1024]{1,0:T(4,128)(2,1)S(1)}, bf16[4,1024]{1,0:T(4,128)(2,1)S(1)}, u32[]{:S(2)}, u32[]{:S(2)}) %collective-permute-start.20) | collective-permute-done | bytes 8224 | tf_op jit(solution)/shard_map/ppermute | solution.py:20
  (96 shorter events, 7.6 us)
Async XLA Ops:
  0.6 13.8 %copy-start = (bf16[2,1024,512]{2,1,0:T(8,128)(2,1)S(1)}, bf16[2,1024,512]{2,1,0:T(8,128)(2,1)}, u32[]{:S(2)}) copy-start(bf16[2,1024,512]{2,1,0:T(8,128)(2,1)} %param.15) | copy-start | bytes 6291460
  0.6 8.0 %collective-permute-start = (bf16[4,1024]{1,0:T(4,128)(2,1)}, bf16[4,1024]{1,0:T(4,128)(2,1)S(1)}, u32[]{:S(2)}, u32[]{:S(2)}) collective-permute-start(bf16[4,1024]{1,0:T(4,128)(2,1)} %param.10), channel_id=1, source_target_pairs={{0,4},{4,0},{8,12},{12,8},{1,5},{5,1},{9,13},{13,9},{2,6},{6,2},{1... | collective-permute-start | bytes 24584 | tf_op jit(solution)/shard_map/ppermute | solution.py:20
  3.8 7.3 %collective-permute-start.2 = (bf16[4,1024]{1,0:T(4,128)(2,1)}, bf16[4,1024]{1,0:T(4,128)(2,1)S(1)}, u32[]{:S(2)}, u32[]{:S(2)}) collective-permute-start(bf16[4,1024]{1,0:T(4,128)(2,1)} %param.10), channel_id=1, source_target_pairs={{0,12},{4,8},{8,4},{12,0},{1,13},{5,9},{9,5},{13,1},{2,14},{6,10},... | collective-permute-start | bytes 24584 | tf_op jit(solution)/shard_map/ppermute | solution.py:20
  6.2 4.8 %collective-permute-start.1 = (bf16[4,1024]{1,0:T(4,128)(2,1)}, bf16[4,1024]{1,0:T(4,128)(2,1)S(1)}, u32[]{:S(2)}, u32[]{:S(2)}) collective-permute-start(bf16[4,1024]{1,0:T(4,128)(2,1)} %param.10), channel_id=1, source_target_pairs={{0,8},{4,12},{8,0},{12,4},{1,9},{5,13},{9,1},{13,5},{2,10},{6,14},... | collective-permute-start | bytes 24584 | tf_op jit(solution)/shard_map/ppermute | solution.py:20
  12.9 5.6 %copy-start.5 = (f32[2,128]{1,0:T(2,128)S(1)}, f32[2,128]{1,0:T(2,128)}, u32[]{:S(2)}) copy-start(f32[2,128]{1,0:T(2,128)} %param.17) | copy-start | bytes 3076
  16.2 2.2 %collective-permute-start.3 = (bf16[4,2176]{1,0:T(4,128)(2,1)S(1)}, bf16[4,2176]{1,0:T(4,128)(2,1)S(1)}, u32[]{:S(2)}, u32[]{:S(2)}) collective-permute-start(bf16[4,2176]{1,0:T(4,128)(2,1)S(1)} %get-tuple-element.13), channel_id=1, source_target_pairs={{0,1},{1,0},{2,3},{3,2},{4,5},{5,4},{6,7},{7,6},{8,9},{9,8},{10,11... | collective-permute-start | bytes 52232 | tf_op jit(solution)/shard_map/ppermute | solution.py:20
  16.3 3.2 %collective-permute-start.5 = (bf16[4,2176]{1,0:T(4,128)(2,1)S(1)}, bf16[4,2176]{1,0:T(4,128)(2,1)S(1)}, u32[]{:S(2)}, u32[]{:S(2)}) collective-permute-start(bf16[4,2176]{1,0:T(4,128)(2,1)S(1)} %get-tuple-element.14), channel_id=1, source_target_pairs={{0,3},{1,2},{2,1},{3,0},{4,7},{5,6},{6,5},{7,4},{8,11},{9,10},{10,... | collective-permute-start | bytes 52232 | tf_op jit(solution)/shard_map/ppermute | solution.py:20
  17.9 3.8 %collective-permute-start.4 = (bf16[4,2176]{1,0:T(4,128)(2,1)S(1)}, bf16[4,2176]{1,0:T(4,128)(2,1)S(1)}, u32[]{:S(2)}, u32[]{:S(2)}) collective-permute-start(bf16[4,2176]{1,0:T(4,128)(2,1)S(1)} %get-tuple-element.15), channel_id=1, source_target_pairs={{0,2},{1,3},{2,0},{3,1},{4,6},{5,7},{6,4},{7,5},{8,10},{9,11},{10,... | collective-permute-start | bytes 52232 | tf_op jit(solution)/shard_map/ppermute | solution.py:20
  22.0 14.8 %copy-start.1 = (bf16[2,1024,512]{2,1,0:T(8,128)(2,1)S(1)}, bf16[2,1024,512]{2,1,0:T(8,128)(2,1)}, u32[]{:S(2)}) copy-start(bf16[2,1024,512]{2,1,0:T(8,128)(2,1)} %param.14) | copy-start | bytes 6291460
  24.1 13.0 %copy-start.2 = (bf16[2,1024,512]{2,1,0:T(8,128)(2,1)S(1)}, bf16[2,1024,512]{2,1,0:T(8,128)(2,1)}, u32[]{:S(2)}) copy-start(bf16[2,1024,512]{2,1,0:T(8,128)(2,1)} %param.13) | copy-start | bytes 6291460
  24.4 1.9 %collective-permute-start.6 = (bf16[4,512]{1,0:T(4,128)(2,1)S(1)}, bf16[4,512]{1,0:T(4,128)(2,1)S(1)}, u32[]{:S(2)}, u32[]{:S(2)}) collective-permute-start(bf16[4,512]{1,0:T(4,128)(2,1)S(1)} %get-tuple-element.7), channel_id=1, source_target_pairs={{0,1},{1,0},{2,3},{3,2},{4,5},{5,4},{6,7},{7,6},{8,9},{9,8},{10,11... | collective-permute-start | bytes 12296 | tf_op jit(solution)/shard_map/ppermute | solution.py:20
  24.5 3.7 %collective-permute-start.7 = (bf16[4,512]{1,0:T(4,128)(2,1)S(1)}, bf16[4,512]{1,0:T(4,128)(2,1)S(1)}, u32[]{:S(2)}, u32[]{:S(2)}) collective-permute-start(bf16[4,512]{1,0:T(4,128)(2,1)S(1)} %get-tuple-element.7), channel_id=1, source_target_pairs={{0,2},{1,3},{2,0},{3,1},{4,6},{5,7},{6,4},{7,5},{8,10},{9,11},{10,... | collective-permute-start | bytes 12296 | tf_op jit(solution)/shard_map/ppermute | solution.py:20
  25.0 3.1 %collective-permute-start.8 = (bf16[4,512]{1,0:T(4,128)(2,1)S(1)}, bf16[4,512]{1,0:T(4,128)(2,1)S(1)}, u32[]{:S(2)}, u32[]{:S(2)}) collective-permute-start(bf16[4,512]{1,0:T(4,128)(2,1)S(1)} %get-tuple-element.7), channel_id=1, source_target_pairs={{0,3},{1,2},{2,1},{3,0},{4,7},{5,6},{6,5},{7,4},{8,11},{9,10},{10,... | collective-permute-start | bytes 12296 | tf_op jit(solution)/shard_map/ppermute | solution.py:20
  29.7 7.7 %copy-start.3 = (bf16[2,1024,512]{2,1,0:T(8,128)(2,1)S(1)}, bf16[2,1024,512]{2,1,0:T(8,128)(2,1)}, u32[]{:S(2)}) copy-start(bf16[2,1024,512]{2,1,0:T(8,128)(2,1)} %param.12) | copy-start | bytes 6291460
  29.7 5.7 %collective-permute-start.11 = (bf16[16,1024]{1,0:T(8,128)(2,1)S(1)}, bf16[16,1024]{1,0:T(8,128)(2,1)S(1)}, u32[]{:S(2)}, u32[]{:S(2)}) collective-permute-start(bf16[16,1024]{1,0:T(8,128)(2,1)S(1)} %get-tuple-element.39), channel_id=1, source_target_pairs={{0,12},{4,8},{8,4},{12,0},{1,13},{5,9},{9,5},{13,1},{2,14},{6,10},... | collective-permute-start | bytes 98312 | tf_op jit(solution)/shard_map/ppermute | solution.py:20
  31.0 5.2 %collective-permute-start.10 = (bf16[16,1024]{1,0:T(8,128)(2,1)S(1)}, bf16[16,1024]{1,0:T(8,128)(2,1)S(1)}, u32[]{:S(2)}, u32[]{:S(2)}) collective-permute-start(bf16[16,1024]{1,0:T(8,128)(2,1)S(1)} %get-tuple-element.39), channel_id=1, source_target_pairs={{0,8},{4,12},{8,0},{12,4},{1,9},{5,13},{9,1},{13,5},{2,10},{6,14},... | collective-permute-start | bytes 98312 | tf_op jit(solution)/shard_map/ppermute | solution.py:20
  31.8 4.6 %collective-permute-start.9 = (bf16[16,1024]{1,0:T(8,128)(2,1)S(1)}, bf16[16,1024]{1,0:T(8,128)(2,1)S(1)}, u32[]{:S(2)}, u32[]{:S(2)}) collective-permute-start(bf16[16,1024]{1,0:T(8,128)(2,1)S(1)} %get-tuple-element.39), channel_id=1, source_target_pairs={{0,4},{4,0},{8,12},{12,8},{1,5},{5,1},{9,13},{13,9},{2,6},{6,2},{1... | collective-permute-start | bytes 98312 | tf_op jit(solution)/shard_map/ppermute | solution.py:20
  38.0 2.2 %collective-permute-start.12 = (bf16[4,2176]{1,0:T(4,128)(2,1)S(1)}, bf16[4,2176]{1,0:T(4,128)(2,1)S(1)}, u32[]{:S(2)}, u32[]{:S(2)}) collective-permute-start(bf16[4,2176]{1,0:T(4,128)(2,1)S(1)} %get-tuple-element.10), channel_id=1, source_target_pairs={{0,1},{1,0},{2,3},{3,2},{4,5},{5,4},{6,7},{7,6},{8,9},{9,8},{10,11... | collective-permute-start | bytes 52232 | tf_op jit(solution)/shard_map/ppermute | solution.py:20
  38.1 3.2 %collective-permute-start.14 = (bf16[4,2176]{1,0:T(4,128)(2,1)S(1)}, bf16[4,2176]{1,0:T(4,128)(2,1)S(1)}, u32[]{:S(2)}, u32[]{:S(2)}) collective-permute-start(bf16[4,2176]{1,0:T(4,128)(2,1)S(1)} %get-tuple-element.11), channel_id=1, source_target_pairs={{0,3},{1,2},{2,1},{3,0},{4,7},{5,6},{6,5},{7,4},{8,11},{9,10},{10,... | collective-permute-start | bytes 52232 | tf_op jit(solution)/shard_map/ppermute | solution.py:20
  39.7 3.8 %collective-permute-start.13 = (bf16[4,2176]{1,0:T(4,128)(2,1)S(1)}, bf16[4,2176]{1,0:T(4,128)(2,1)S(1)}, u32[]{:S(2)}, u32[]{:S(2)}) collective-permute-start(bf16[4,2176]{1,0:T(4,128)(2,1)S(1)} %get-tuple-element.12), channel_id=1, source_target_pairs={{0,2},{1,3},{2,0},{3,1},{4,6},{5,7},{6,4},{7,5},{8,10},{9,11},{10,... | collective-permute-start | bytes 52232 | tf_op jit(solution)/shard_map/ppermute | solution.py:20
  46.0 4.8 %copy-start.4 = (bf16[2,512,1024]{2,1,0:T(8,128)(2,1)S(1)}, bf16[2,512,1024]{2,1,0:T(8,128)(2,1)}, u32[]{:S(2)}) copy-start(bf16[2,512,1024]{2,1,0:T(8,128)(2,1)} %param.18) | copy-start | bytes 6291460
  46.0 4.7 %collective-permute-start.16 = (bf16[4,512]{1,0:T(4,128)(2,1)S(1)}, bf16[4,512]{1,0:T(4,128)(2,1)S(1)}, u32[]{:S(2)}, u32[]{:S(2)}) collective-permute-start(bf16[4,512]{1,0:T(4,128)(2,1)S(1)} %get-tuple-element.3), channel_id=1, source_target_pairs={{0,2},{1,3},{2,0},{3,1},{4,6},{5,7},{6,4},{7,5},{8,10},{9,11},{10,... | collective-permute-start | bytes 12296 | tf_op jit(solution)/shard_map/ppermute | solution.py:20
  46.6 4.1 %collective-permute-start.15 = (bf16[4,512]{1,0:T(4,128)(2,1)S(1)}, bf16[4,512]{1,0:T(4,128)(2,1)S(1)}, u32[]{:S(2)}, u32[]{:S(2)}) collective-permute-start(bf16[4,512]{1,0:T(4,128)(2,1)S(1)} %get-tuple-element.3), channel_id=1, source_target_pairs={{0,1},{1,0},{2,3},{3,2},{4,5},{5,4},{6,7},{7,6},{8,9},{9,8},{10,11... | collective-permute-start | bytes 12296 | tf_op jit(solution)/shard_map/ppermute | solution.py:20
  46.6 4.2 %collective-permute-start.17 = (bf16[4,512]{1,0:T(4,128)(2,1)S(1)}, bf16[4,512]{1,0:T(4,128)(2,1)S(1)}, u32[]{:S(2)}, u32[]{:S(2)}) collective-permute-start(bf16[4,512]{1,0:T(4,128)(2,1)S(1)} %get-tuple-element.3), channel_id=1, source_target_pairs={{0,3},{1,2},{2,1},{3,0},{4,7},{5,6},{6,5},{7,4},{8,11},{9,10},{10,... | collective-permute-start | bytes 12296 | tf_op jit(solution)/shard_map/ppermute | solution.py:20
  51.0 5.1 %collective-permute-start.18 = (bf16[4,1024]{1,0:T(4,128)(2,1)S(1)}, bf16[4,1024]{1,0:T(4,128)(2,1)S(1)}, u32[]{:S(2)}, u32[]{:S(2)}) collective-permute-start(bf16[4,1024]{1,0:T(4,128)(2,1)S(1)} %get-tuple-element.16), channel_id=1, source_target_pairs={{0,4},{4,0},{8,12},{12,8},{1,5},{5,1},{9,13},{13,9},{2,6},{6,2},{1... | collective-permute-start | bytes 24584 | tf_op jit(solution)/shard_map/ppermute | solution.py:20
  52.5 5.4 %collective-permute-start.20 = (bf16[4,1024]{1,0:T(4,128)(2,1)S(1)}, bf16[4,1024]{1,0:T(4,128)(2,1)S(1)}, u32[]{:S(2)}, u32[]{:S(2)}) collective-permute-start(bf16[4,1024]{1,0:T(4,128)(2,1)S(1)} %get-tuple-element.17), channel_id=1, source_target_pairs={{0,12},{4,8},{8,4},{12,0},{1,13},{5,9},{9,5},{13,1},{2,14},{6,10},... | collective-permute-start | bytes 24584 | tf_op jit(solution)/shard_map/ppermute | solution.py:20
  53.9 4.5 %collective-permute-start.19 = (bf16[4,1024]{1,0:T(4,128)(2,1)S(1)}, bf16[4,1024]{1,0:T(4,128)(2,1)S(1)}, u32[]{:S(2)}, u32[]{:S(2)}) collective-permute-start(bf16[4,1024]{1,0:T(4,128)(2,1)S(1)} %get-tuple-element.18), channel_id=1, source_target_pairs={{0,8},{4,12},{8,0},{12,4},{1,9},{5,13},{9,1},{13,5},{2,10},{6,14},... | collective-permute-start | bytes 24584 | tf_op jit(solution)/shard_map/ppermute | solution.py:20

commit v2 on v1

v2 whole, which is shorter than its diff:
```python
import functools

import jax
import jax.numpy as jnp
from jax import lax
from jax.experimental import pallas as pl
from jax.experimental.pallas import tpu as pltpu
from jax.sharding import PartitionSpec as P

F32, BF16 = jnp.float32, jnp.bfloat16
LANES = 128
VMEM = pl.BlockSpec(memory_space=pltpu.VMEM)
ANY = pl.BlockSpec(memory_space=pl.ANY)


def peer_of(n, k, index):
    if n & (n - 1) == 0:
        return index ^ k
    return (index + k) % n


def swap(array, axis, n, k):
    return lax.ppermute(array, axis, [(peer_of(n, k, i), i) for i in range(n)])


def send(array, axis, n, k):
    return lax.ppermute(array, axis, [(i, peer_of(n, k, i)) for i in range(n)])


def slot_rows(total, n, index):
    size = total // n
    row = jnp.arange(total, dtype=jnp.int32)
    return peer_of(n, row // size, index) * size + row % size


def split(array):
    high = array.astype(BF16)
    return high, (array - high.astype(F32)).astype(BF16)


def finish_projection(base, gain_ref, layer, weights, outs):
    count = outs[0].shape[0]
    squares = jnp.sum(base * base, axis=1, keepdims=True)
    scaled = (base * gain_ref[layer : layer + 1, :]).astype(BF16)
    high, rest = split(squares)
    high = high.astype(F32)
    middle, low = split(squares - high)
    lane = lax.broadcasted_iota(jnp.int32, (base.shape[0], LANES), 1)
    zero = jnp.zeros((base.shape[0], LANES), F32)
    tail = jnp.where(lane == 0, high, zero)
    tail = jnp.where(lane == 1, middle.astype(F32), tail)
    tail = jnp.where(lane == 2, low.astype(F32), tail)
    width = weights[0].shape[-1]
    for index, weight in enumerate(weights):
        product = jnp.dot(scaled, weight[0], preferred_element_type=F32)
        for k, out in enumerate(outs):
            out[:, index * width : (index + 1) * width] = product[
                k * count : (k + 1) * count
            ].astype(out.dtype)
    for k, out in enumerate(outs):
        out[:, 4 * width :] = tail[k * count : (k + 1) * count].astype(out.dtype)


def project_first(n_tp, n_dp, layer, *refs):
    parts, (order, gain), weights = refs[:n_tp], refs[n_tp : n_tp + 2], refs[n_tp + 2 : n_tp + 6]
    base_out, outs, slots = refs[n_tp + 6], refs[n_tp + 7 : -1], refs[-1]
    rows = parts[0].shape[0]
    for k, part in enumerate(parts):
        slots[k * rows : (k + 1) * rows, :] = part[...].astype(F32)
    base = jnp.dot(order[...], slots[...].astype(BF16), preferred_element_type=F32)
    base_out[...] = base.astype(BF16)
    finish_projection(base, gain, layer, weights, outs)


def project_next(n_tp, n_dp, layer, *refs):
    (base_in, mixed), parts = refs[:2], refs[2 : n_tp + 1]
    gain, weights = refs[n_tp + 1], refs[n_tp + 2 : n_tp + 6]
    base_out, outs = refs[n_tp + 6], refs[n_tp + 7 :]
    base = base_in[...].astype(F32) + mixed[...]
    for part in parts:
        base = base + part[...].astype(F32)
    rounded = base.astype(BF16)
    base_out[...] = rounded
    finish_projection(rounded.astype(F32), gain, layer, weights, outs)


def recur(n_dp, layer, features, *refs):
    own, parts = refs[0], refs[1:n_dp]
    bound_ref, head_gain, state, normed, gates = refs[n_dp:]
    seqs, heads, hd = state.shape[1], state.shape[2], state.shape[3]
    width = heads * hd
    total = own[...]
    for part in parts:
        total = total + part[...].astype(F32)
    mean = jnp.sum(total[:, 4 * width :], axis=1, keepdims=True) / features
    factor = lax.rsqrt(mean + 1e-06)
    query, forget_pre, value, gate_pre = (
        total[:, index * width : (index + 1) * width] * factor for index in range(4)
    )
    bound = bound_ref[layer : layer + 1, :]
    forget = bound + (1.0 - bound) * jax.nn.sigmoid(forget_pre)
    keyvec = (1.0 - bound) * jax.nn.sigmoid(-forget_pre)
    for seq in range(seqs):
        for index, vector in enumerate((forget, keyvec, value)):
            gates[seq, index : index + 1, :] = vector[seq : seq + 1]
    gate = jax.nn.sigmoid(gate_pre)
    weighted = query * forget
    shared = query * keyvec
    row = lax.broadcasted_iota(jnp.int32, (seqs, hd), 0)
    for head in range(heads):
        cols = slice(head * hd, (head + 1) * hd)
        readout = jnp.sum(shared[:, cols], axis=1, keepdims=True) * value[:, cols]
        for seq in range(seqs):
            high, low = split(jnp.where(row == seq, weighted[:, cols], 0.0))
            stored = state[0, seq, head].astype(BF16)
            readout = readout + jnp.dot(high, stored, preferred_element_type=F32)
            readout = readout + jnp.dot(low, stored, preferred_element_type=F32)
        scale = lax.rsqrt(jnp.mean(readout * readout, axis=1, keepdims=True) + 1e-06)
        normed[:, cols] = (
            readout * scale * head_gain[layer : layer + 1, :] * gate[:, cols]
        ).astype(BF16)


def update(gates, state, *refs):
    out = refs[-1]
    heads, hd = state.shape[2], state.shape[3]
    for head in range(heads):
        cols = slice(head * hd, (head + 1) * hd)
        forget, keyvec, value = (gates[0, index : index + 1, cols] for index in range(3))
        forget = jnp.transpose(jnp.broadcast_to(forget, (hd, hd)))
        keyvec = jnp.transpose(jnp.broadcast_to(keyvec, (hd, hd)))
        out[0, 0, head] = forget * state[0, 0, head] + keyvec * value


def gather_rows(parts, slots):
    rows = parts[0].shape[0]
    for k, part in enumerate(parts):
        slots[k * rows : (k + 1) * rows, :] = part[...].astype(F32)
    return slots[...].astype(BF16)


def mix_next(n_dp, *refs):
    parts, (weight, mixed, sent, slots) = refs[:n_dp], refs[n_dp:]
    product = jnp.dot(gather_rows(parts, slots), weight[0], preferred_element_type=F32)
    mixed[...] = product
    sent[...] = product.astype(BF16)


def mix_last(n_dp, *refs):
    parts, (weight, base, order) = refs[:n_dp], refs[n_dp : n_dp + 3]
    own, outs, slots = refs[n_dp + 3], refs[n_dp + 4 : -1], refs[-1]
    rows = own.shape[0]
    product = jnp.dot(gather_rows(parts, slots), weight[0], preferred_element_type=F32)
    high, low = split(product)
    moved = jnp.dot(order[...], high, preferred_element_type=F32)
    first = order[:rows, :]
    own[...] = (
        moved[:rows]
        + jnp.dot(first, low, preferred_element_type=F32)
        + jnp.dot(first, base[...], preferred_element_type=F32)
    )
    for k, out in enumerate(outs):
        out[...] = moved[(k + 1) * rows : (k + 2) * rows].astype(BF16)


def close(own, *refs):
    total = own[...]
    for part in refs[:-1]:
        total = total + part[...].astype(F32)
    refs[-1][...] = total.astype(BF16)


def layer_block(array, layer):
    zeros = (0,) * (array.ndim - 1)
    return pl.BlockSpec((1,) + array.shape[1:], lambda step: (layer,) + zeros)


def call(body, name, args, in_specs, outs, scratch=()):
    return pl.pallas_call(
        body,
        name=name,
        grid=(1,),
        out_shape=[jax.ShapeDtypeStruct(shape, dtype) for shape, dtype in outs],
        in_specs=in_specs,
        out_specs=[VMEM] * len(outs),
        scratch_shapes=[pltpu.VMEM(shape, dtype) for shape, dtype in scratch],
    )(*args)


def per_device(
    n_tp,
    n_dp,
    tokens,
    norm_gain,
    w_query,
    w_forget,
    w_value,
    w_gate,
    lower_bound,
    head_gain,
    w_out,
    state,
):
    seqs, heads, hd = state.shape[1], state.shape[2], state.shape[3]
    rows, local = tokens.shape
    features = local * n_dp
    total = rows * n_tp
    width = heads * hd
    weights = (w_query, w_forget, w_value, w_gate)
    tp_rows = slot_rows(total, n_tp, lax.axis_index("tp"))
    dp_rows = slot_rows(total, n_dp, lax.axis_index("dp"))
    order_in = (dp_rows[:, None] == tp_rows[None, :]).astype(BF16)
    order_out = (tp_rows[:, None] == dp_rows[None, :]).astype(BF16)

    parts = [tokens] + [swap(tokens, "tp", n_tp, k) for k in range(1, n_tp)]
    base = mixed = None
    new_state = None
    for layer in range(2):
        outs = [((total, local), BF16), ((seqs, 4 * width + LANES), F32)]
        outs += [((seqs, 4 * width + LANES), BF16)] * (n_dp - 1)
        specs = [layer_block(weight, layer) for weight in weights]
        if layer == 0:
            base, own, *sent = call(
                functools.partial(project_first, n_tp, n_dp, layer),
                "project_first",
                (*parts, order_in, norm_gain, *weights),
                [VMEM] * (n_tp + 2) + specs,
                outs,
                [((total, local), F32)],
            )
        else:
            base, own, *sent = call(
                functools.partial(project_next, n_tp, n_dp, layer),
                "project_next",
                (base, mixed, *parts, norm_gain, *weights),
                [VMEM] * (n_tp + 2) + specs,
                outs,
            )
        parts = [send(sent[k - 1], "dp", n_dp, k) for k in range(1, n_dp)]
        normed, gates = call(
            functools.partial(recur, n_dp, layer, features),
            "recur",
            (own, *parts, lower_bound, head_gain, state),
            [VMEM] * (n_dp + 2) + [layer_block(state, layer)],
            [((seqs, width), BF16), ((seqs, 3, width), F32)],
        )
        parts = [normed] + [swap(normed, "dp", n_dp, k) for k in range(1, n_dp)]
        block = pl.BlockSpec(
            (1, 1, heads, hd, hd), lambda seq, layer=layer: (layer, seq, 0, 0, 0)
        )
        gate_block = pl.BlockSpec((1, 3, width), lambda seq: (seq, 0, 0))
        new_state = pl.pallas_call(
            update,
            name="update",
            grid=(seqs,),
            out_shape=jax.ShapeDtypeStruct(state.shape, F32),
            in_specs=[gate_block, block] + ([ANY] if layer else []),
            out_specs=block,
            input_output_aliases={2: 0} if layer else {},
        )(gates, state, *((new_state,) if layer else ()))
        if layer == 0:
            mixed, sent = call(
                functools.partial(mix_next, n_dp),
                "mix_next",
                (*parts, w_out),
                [VMEM] * n_dp + [layer_block(w_out, layer)],
                [((total, local), F32), ((total, local), BF16)],
                [((total, width), F32)],
            )
            parts = [swap(sent, "tp", n_tp, k) for k in range(1, n_tp)]
        else:
            own, *sent = call(
                functools.partial(mix_last, n_dp),
                "mix_last",
                (*parts, w_out, base, order_out),
                [VMEM] * n_dp + [layer_block(w_out, layer)] + [VMEM] * 2,
                [((rows, local), F32)] + [((rows, local), BF16)] * (n_tp - 1),
                [((total, width), F32)],
            )
            parts = [send(sent[k - 1], "tp", n_tp, k) for k in range(1, n_tp)]
    (hidden,) = call(
        close, "close", (own, *parts), [VMEM] * n_tp, [((rows, local), BF16)]
    )
    return (hidden, new_state)


def solution(mesh):
    n_tp, n_dp = mesh.shape["tp"], mesh.shape["dp"]
    return jax.shard_map(
        functools.partial(per_device, n_tp, n_dp),
        mesh=mesh,
        in_specs=(
            P(("grp", "tp"), "dp"),
            P(None, "dp"),
            P(None, "dp", "tp"),
            P(None, "dp", "tp"),
            P(None, "dp", "tp"),
            P(None, "dp", "tp"),
            P(None, "tp"),
            P(),
            P(None, "tp", "dp"),
            P(None, ("grp", "dp"), "tp", None, None),
        ),
        out_specs=(P(("grp", "tp"), "dp"), P(None, ("grp", "dp"), "tp", None, None)),
        check_vma=False,
    )
```

time: 59.5 us -> 72 us (1.21)
  Pallas kernels: 0 us -> 25.5 us
  matrix products: 11.4 us -> 0 us
  other arithmetic: 6.69 us -> 0.67 us
  waiting for transfers between devices: 15.3 us -> 18 us
  local copies, waits for them, and re-layouts: 2.55 us -> 4.75 us
    pallas_call x0 -> x9, Pallas kernels: none -> 25.5 us  [the longest x7 18 us: call(): pl.pallas_call(body, name=name, grid=(1,), out_shape=[jax.ShapeDtypeStruc...]
    dot_general x12 -> x0, matrix products: 11.4 us -> none  [the longest x8 5.67 us: per_device(): jnp.dot(scaled, weight[layer], preferred_element_type=jnp.float32)]
    unnamed x12 -> x42, local copies, waits for them, and re-layouts: 0.03 us -> 4.75 us
    ppermute x21, waiting for transfers between devices: 15.3 us -> 18 us  [the longest x12 11.9 us: swap(): return lax.ppermute(array, axis, [(peer_of(n, k, i), i) for i in range(n)])]
    add x5 -> x1, other arithmetic: 2.69 us -> 0.01 us  [slot_rows(): return peer_of(n, row // size, index) * size + row % size]
    another operation x1 -> x0, other arithmetic: 1.55 us -> none  [per_device(): return (hidden, jnp.stack(updated))]
    dynamic_update_slice x10 -> x0, local copies, waits for them, and re-layouts: 0.85 us -> none  [gather(): lax.dynamic_update_slice_in_dim(out, part, peer_of(n, k, index) * count, 0)]
    slice x1 -> x0, local copies, waits for them, and re-layouts: 0.78 us -> none  [per_device(): scaled = (widened * norm_gain[layer]).astype(jnp.bfloat16)]
  transfers between devices with their start and end apart: 21 -> 21, of which waited for: 11 -> 12; matrix products, arithmetic and copies ran while one was open for 11% -> 1% of each run, Pallas kernels for 0% -> 11%
where the time goes in v2:
time: 72 us; the launch traced here: 71.6 us
  Pallas kernels  25.5 us (35%)
  starting transfers between devices  22 us (31%)
  waiting for transfers between devices  18 us (25%)
  local copies, waits for them, and re-layouts  4.75 us (7%)
    pallas_call x7, Pallas kernels, call(): pl.pallas_call(body, name=name, grid=(1,), out_shape=[jax.ShapeDtypeStruc...  18 us
    ppermute x12, starting transfers between devices, swap(): return lax.ppermute(array, axis, [(peer_of(n, k, i), i) for i in range(n)])  13.8 us
    ppermute x12, waiting for transfers between devices, swap(): return lax.ppermute(array, axis, [(peer_of(n, k, i), i) for i in range(n)])  11.9 us
    ppermute x9, starting transfers between devices, send(): return lax.ppermute(array, axis, [(i, peer_of(n, k, i)) for i in range(n)])  8.14 us
    pallas_call x2, Pallas kernels, per_device(): pl.pallas_call(update, name='update', grid=(seqs,), out_shape=jax.ShapeDt...  7.53 us
    ppermute x9, waiting for transfers between devices, send(): return lax.ppermute(array, axis, [(i, peer_of(n, k, i)) for i in range(n)])  6.07 us
    unnamed x42, local copies, waits for them, and re-layouts  4.75 us
  transfers between devices with their start and end apart: 21, of which 12 were waited for; matrix products, arithmetic and copies ran while one was open for 1% of the time, Pallas kernels for 11%

profile of v2, /device:TPU:0, one launch (start us, length us, event | category | flops | bytes accessed | tf_op | source)
XLA Modules:
  0.0 71.6 jit_solution(15227150127850653436)
XLA Ops:
  0.6 4.1 %collective-permute-start.1 = (bf16[4,1024]{1,0:T(4,128)(2,1)}, bf16[4,1024]{1,0:T(4,128)(2,1)S(1)}, u32[]{:S(2)}, u32[]{:S(2)}) collective-permute-start(bf16[4,1024]{1,0:T(4,128)(2,1)} %refs_0_.1), channel_id=1, source_target_pairs={{8,0},{12,4},{0,8},{4,12},{9,1},{13,5},{1,9},{5,13},{10,2},{14,6},... | collective-permute-start | bytes 24584 | tf_op jit(solution)/shard_map/ppermute | solution.py:23
  4.8 1.6 %collective-permute-start = (bf16[4,1024]{1,0:T(4,128)(2,1)}, bf16[4,1024]{1,0:T(4,128)(2,1)S(1)}, u32[]{:S(2)}, u32[]{:S(2)}) collective-permute-start(bf16[4,1024]{1,0:T(4,128)(2,1)} %refs_0_.1), channel_id=1, source_target_pairs={{4,0},{0,4},{12,8},{8,12},{5,1},{1,5},{13,9},{9,13},{6,2},{2,6},{1... | collective-permute-start | bytes 24584 | tf_op jit(solution)/shard_map/ppermute | solution.py:23
  6.3 0.7 compare_convert_fusion
  7.0 1.6 %collective-permute-done.refs_1_ = bf16[4,1024]{1,0:T(4,128)(2,1)S(1)} collective-permute-done((bf16[4,1024]{1,0:T(4,128)(2,1)}, bf16[4,1024]{1,0:T(4,128)(2,1)S(1)}, u32[]{:S(2)}, u32[]{:S(2)}) %collective-permute-start) | collective-permute-done | bytes 8224 | tf_op jit(solution)/shard_map/ppermute | solution.py:23
  8.6 3.4 %collective-permute-done.2.refs_3_ = bf16[4,1024]{1,0:T(4,128)(2,1)S(1)} collective-permute-done((bf16[4,1024]{1,0:T(4,128)(2,1)}, bf16[4,1024]{1,0:T(4,128)(2,1)S(1)}, u32[]{:S(2)}, u32[]{:S(2)}) %collective-permute-start.2) | collective-permute-done | bytes 8224 | tf_op jit(solution)/shard_map/ppermute | solution.py:23
  12.6 3.6 %project_first.1 = (bf16[16,1024]{1,0:T(8,128)(2,1)}, f32[4,2176]{1,0:T(4,128)}, bf16[4,2176]{1,0:T(4,128)(2,1)}, bf16[4,2176]{1,0:T(4,128)(2,1)}, bf16[4,2176]{1,0:T(4,128)(2,1)}) custom-call(bf16[4,1024]{1,0:T(4,128)(2,1)} %refs_0_.1, bf16[4,1024]{1,0:T(4,128)(2,1)} %copy-done.10, bf16[4,1024]{1,0:T(4,128)(2,1)} %copy-done.9, bf16[4,1024]{1,0:T(4,128)(2,1)} %copy-done.11, ...), custom_call_target="tpu_custom_call" | custom-call | tf_op jit(solution)/shard_map/project_first/pallas_call | solution.py:179
  16.2 1.6 %collective-permute-start.4 = (bf16[4,2176]{1,0:T(4,128)(2,1)}, bf16[4,2176]{1,0:T(4,128)(2,1)S(1)}, u32[]{:S(2)}, u32[]{:S(2)}) collective-permute-start(bf16[4,2176]{1,0:T(4,128)(2,1)} %get-tuple-element.25), channel_id=1, source_target_pairs={{0,2},{1,3},{2,0},{3,1},{4,6},{5,7},{6,4},{7,5},{8,10},{9,11},{10,... | collective-permute-start | bytes 52232 | tf_op jit(solution)/shard_map/ppermute | solution.py:27
  18.1 2.2 %collective-permute-done.4.refs_2_ = bf16[4,2176]{1,0:T(4,128)(2,1)S(1)} collective-permute-done((bf16[4,2176]{1,0:T(4,128)(2,1)}, bf16[4,2176]{1,0:T(4,128)(2,1)S(1)}, u32[]{:S(2)}, u32[]{:S(2)}) %collective-permute-start.4) | collective-permute-done | bytes 17440 | tf_op jit(solution)/shard_map/ppermute | solution.py:27
  20.3 0.9 %collective-permute-done.5.refs_3_ = bf16[4,2176]{1,0:T(4,128)(2,1)S(1)} collective-permute-done((bf16[4,2176]{1,0:T(4,128)(2,1)}, bf16[4,2176]{1,0:T(4,128)(2,1)S(1)}, u32[]{:S(2)}, u32[]{:S(2)}) %collective-permute-start.5) | collective-permute-done | bytes 17440 | tf_op jit(solution)/shard_map/ppermute | solution.py:27
  21.8 2.5 %recur.2 = (bf16[4,512]{1,0:T(4,128)(2,1)}, f32[4,3,512]{2,1,0:T(4,128)}) custom-call(f32[4,2176]{1,0:T(4,128)} %get-tuple-element.23.refs_0_, bf16[4,2176]{1,0:T(4,128)(2,1)} %copy-done.3, bf16[4,2176]{1,0:T(4,128)(2,1)} %copy-done.5, bf16[4,2176]{1,0:T(4,128)(2,1)} %copy-done.7, f32[2,512]{1,0:T(2,128)} %refs_4_.6, f32[2,128]{1,0:T(2,128)} %refs_5_.7, ...), custom_call_target="tpu_custom_call" | custom-call | tf_op jit(solution)/shard_map/recur/pallas_call | solution.py:179
  24.7 1.4 %collective-permute-start.7 = (bf16[4,512]{1,0:T(4,128)(2,1)}, bf16[4,512]{1,0:T(4,128)(2,1)S(1)}, u32[]{:S(2)}, u32[]{:S(2)}) collective-permute-start(bf16[4,512]{1,0:T(4,128)(2,1)} %get-tuple-element.27.refs_0_), channel_id=1, source_target_pairs={{2,0},{3,1},{0,2},{1,3},{6,4},{7,5},{4,6},{5,7},{10,8},{11,9},{8,1... | collective-permute-start | bytes 12296 | tf_op jit(solution)/shard_map/ppermute | solution.py:23
  26.2 1.4 %collective-permute-done.8.refs_3_ = bf16[4,512]{1,0:T(4,128)(2,1)S(1)} collective-permute-done((bf16[4,512]{1,0:T(4,128)(2,1)}, bf16[4,512]{1,0:T(4,128)(2,1)S(1)}, u32[]{:S(2)}, u32[]{:S(2)}) %collective-permute-start.8) | collective-permute-done | bytes 4128 | tf_op jit(solution)/shard_map/ppermute | solution.py:23
  27.5 1.0 %collective-permute-done.7.refs_2_ = bf16[4,512]{1,0:T(4,128)(2,1)S(1)} collective-permute-done((bf16[4,512]{1,0:T(4,128)(2,1)}, bf16[4,512]{1,0:T(4,128)(2,1)S(1)}, u32[]{:S(2)}, u32[]{:S(2)}) %collective-permute-start.7) | collective-permute-done | bytes 4128 | tf_op jit(solution)/shard_map/ppermute | solution.py:23
  29.7 2.1 %mix_next.1 = (f32[16,1024]{1,0:T(8,128)}, bf16[16,1024]{1,0:T(8,128)(2,1)}) custom-call(bf16[4,512]{1,0:T(4,128)(2,1)} %get-tuple-element.27.refs_0_, bf16[4,512]{1,0:T(4,128)(2,1)} %copy-done.20, bf16[4,512]{1,0:T(4,128)(2,1)} %copy-done.19, bf16[4,512]{1,0:T(4,128)(2,1)} %copy-done.17, bf16[2,512,1024]{2,1,0:T(8,128)(2,1)} %refs_4_.7), custom_call_target="tpu_custom_call" | custom-call | tf_op jit(solution)/shard_map/mix_next/pallas_call | solution.py:179
  31.9 4.3 %collective-permute-start.9 = (bf16[16,1024]{1,0:T(8,128)(2,1)}, bf16[16,1024]{1,0:T(8,128)(2,1)S(1)}, u32[]{:S(2)}, u32[]{:S(2)}) collective-permute-start(bf16[16,1024]{1,0:T(8,128)(2,1)} %get-tuple-element.29), channel_id=1, source_target_pairs={{4,0},{0,4},{12,8},{8,12},{5,1},{1,5},{13,9},{9,13},{6,2},{2,6},{1... | collective-permute-start | bytes 98312 | tf_op jit(solution)/shard_map/ppermute | solution.py:23
  36.2 1.5 %collective-permute-done.11.refs_4_ = bf16[16,1024]{1,0:T(8,128)(2,1)S(1)} collective-permute-done((bf16[16,1024]{1,0:T(8,128)(2,1)}, bf16[16,1024]{1,0:T(8,128)(2,1)S(1)}, u32[]{:S(2)}, u32[]{:S(2)}) %collective-permute-start.11) | collective-permute-done | bytes 32800 | tf_op jit(solution)/shard_map/ppermute | solution.py:23
  37.8 0.6 collective-permute-done.9.refs_2_
  39.0 3.6 %project_next.1 = (bf16[16,1024]{1,0:T(8,128)(2,1)}, f32[4,2176]{1,0:T(4,128)}, bf16[4,2176]{1,0:T(4,128)(2,1)}, bf16[4,2176]{1,0:T(4,128)(2,1)}, bf16[4,2176]{1,0:T(4,128)(2,1)}) custom-call(bf16[16,1024]{1,0:T(8,128)(2,1)} %get-tuple-element.22.refs_0_, f32[16,1024]{1,0:T(8,128)} %get-tuple-element.28.refs_1_, bf16[16,1024]{1,0:T(8,128)(2,1)} %copy-done.2, ...), custom_call_target="tpu_custom_call" | custom-call | tf_op jit(solution)/shard_map/project_next/pallas_call | solution.py:179
  42.6 1.4 %collective-permute-start.13 = (bf16[4,2176]{1,0:T(4,128)(2,1)}, bf16[4,2176]{1,0:T(4,128)(2,1)S(1)}, u32[]{:S(2)}, u32[]{:S(2)}) collective-permute-start(bf16[4,2176]{1,0:T(4,128)(2,1)} %get-tuple-element.32), channel_id=1, source_target_pairs={{0,2},{1,3},{2,0},{3,1},{4,6},{5,7},{6,4},{7,5},{8,10},{9,11},{10,... | collective-permute-start | bytes 52232 | tf_op jit(solution)/shard_map/ppermute | solution.py:27
  44.4 2.2 %collective-permute-done.13.refs_2_ = bf16[4,2176]{1,0:T(4,128)(2,1)S(1)} collective-permute-done((bf16[4,2176]{1,0:T(4,128)(2,1)}, bf16[4,2176]{1,0:T(4,128)(2,1)S(1)}, u32[]{:S(2)}, u32[]{:S(2)}) %collective-permute-start.13) | collective-permute-done | bytes 17440 | tf_op jit(solution)/shard_map/ppermute | solution.py:27
  46.6 0.8 %collective-permute-done.14.refs_3_ = bf16[4,2176]{1,0:T(4,128)(2,1)S(1)} collective-permute-done((bf16[4,2176]{1,0:T(4,128)(2,1)}, bf16[4,2176]{1,0:T(4,128)(2,1)S(1)}, u32[]{:S(2)}, u32[]{:S(2)}) %collective-permute-start.14) | collective-permute-done | bytes 17440 | tf_op jit(solution)/shard_map/ppermute | solution.py:27
  48.0 2.5 %recur.3 = (bf16[4,512]{1,0:T(4,128)(2,1)}, f32[4,3,512]{2,1,0:T(4,128)}) custom-call(f32[4,2176]{1,0:T(4,128)} %get-tuple-element.30.refs_0_, bf16[4,2176]{1,0:T(4,128)(2,1)} %copy-done.4, bf16[4,2176]{1,0:T(4,128)(2,1)} %copy-done.6, bf16[4,2176]{1,0:T(4,128)(2,1)} %copy-done.8, f32[2,512]{1,0:T(2,128)} %refs_4_.6, f32[2,128]{1,0:T(2,128)} %refs_5_.7, ...), custom_call_target="tpu_custom_call" | custom-call | tf_op jit(solution)/shard_map/recur/pallas_call | solution.py:179
  51.0 1.3 %collective-permute-start.16 = (bf16[4,512]{1,0:T(4,128)(2,1)}, bf16[4,512]{1,0:T(4,128)(2,1)S(1)}, u32[]{:S(2)}, u32[]{:S(2)}) collective-permute-start(bf16[4,512]{1,0:T(4,128)(2,1)} %get-tuple-element.34.refs_0_), channel_id=1, source_target_pairs={{2,0},{3,1},{0,2},{1,3},{6,4},{7,5},{4,6},{5,7},{10,8},{11,9},{8,1... | collective-permute-start | bytes 12296 | tf_op jit(solution)/shard_map/ppermute | solution.py:23
  52.3 1.4 %collective-permute-done.17.refs_3_ = bf16[4,512]{1,0:T(4,128)(2,1)S(1)} collective-permute-done((bf16[4,512]{1,0:T(4,128)(2,1)}, bf16[4,512]{1,0:T(4,128)(2,1)S(1)}, u32[]{:S(2)}, u32[]{:S(2)}) %collective-permute-start.17) | collective-permute-done | bytes 4128 | tf_op jit(solution)/shard_map/ppermute | solution.py:23
  53.7 1.1 %collective-permute-done.16.refs_2_ = bf16[4,512]{1,0:T(4,128)(2,1)S(1)} collective-permute-done((bf16[4,512]{1,0:T(4,128)(2,1)}, bf16[4,512]{1,0:T(4,128)(2,1)S(1)}, u32[]{:S(2)}, u32[]{:S(2)}) %collective-permute-start.16) | collective-permute-done | bytes 4128 | tf_op jit(solution)/shard_map/ppermute | solution.py:23
  55.4 2.3 %mix_last.1 = (f32[4,1024]{1,0:T(4,128)}, bf16[4,1024]{1,0:T(4,128)(2,1)}, bf16[4,1024]{1,0:T(4,128)(2,1)}, bf16[4,1024]{1,0:T(4,128)(2,1)}) custom-call(bf16[4,512]{1,0:T(4,128)(2,1)} %get-tuple-element.34.refs_0_, bf16[4,512]{1,0:T(4,128)(2,1)} %copy-done.18, bf16[4,512]{1,0:T(4,128)(2,1)} %copy-done.16, bf16[4,512]{1,0:T(4,128)(2,1)} %copy-done.15, ...), custom_call_target="tpu_custom_call" | custom-call | tf_op jit(solution)/shard_map/mix_last/pallas_call | solution.py:179
  57.7 2.0 %collective-permute-start.18 = (bf16[4,1024]{1,0:T(4,128)(2,1)}, bf16[4,1024]{1,0:T(4,128)(2,1)S(1)}, u32[]{:S(2)}, u32[]{:S(2)}) collective-permute-start(bf16[4,1024]{1,0:T(4,128)(2,1)} %get-tuple-element.37), channel_id=1, source_target_pairs={{0,4},{4,0},{8,12},{12,8},{1,5},{5,1},{9,13},{13,9},{2,6},{6,2},{1... | collective-permute-start | bytes 24584 | tf_op jit(solution)/shard_map/ppermute | solution.py:27
  59.7 0.9 %collective-permute-start.19 = (bf16[4,1024]{1,0:T(4,128)(2,1)}, bf16[4,1024]{1,0:T(4,128)(2,1)S(1)}, u32[]{:S(2)}, u32[]{:S(2)}) collective-permute-start(bf16[4,1024]{1,0:T(4,128)(2,1)} %get-tuple-element.38), channel_id=1, source_target_pairs={{0,8},{4,12},{8,0},{12,4},{1,9},{5,13},{9,1},{13,5},{2,10},{6,14},... | collective-permute-start | bytes 24584 | tf_op jit(solution)/shard_map/ppermute | solution.py:27
  60.6 1.5 %collective-permute-start.20 = (bf16[4,1024]{1,0:T(4,128)(2,1)}, bf16[4,1024]{1,0:T(4,128)(2,1)S(1)}, u32[]{:S(2)}, u32[]{:S(2)}) collective-permute-start(bf16[4,1024]{1,0:T(4,128)(2,1)} %get-tuple-element.39), channel_id=1, source_target_pairs={{0,12},{4,8},{8,4},{12,0},{1,13},{5,9},{9,5},{13,1},{2,14},{6,10},... | collective-permute-start | bytes 24584 | tf_op jit(solution)/shard_map/ppermute | solution.py:27
  62.1 3.8 %update.2.refs_0_ = f32[2,4,4,128,128]{4,3,2,1,0:T(8,128)} custom-call(f32[4,3,512]{2,1,0:T(4,128)} %get-tuple-element.41.gates, f32[2,4,4,128,128]{4,3,2,1,0:T(8,128)} %state.3), custom_call_target="tpu_custom_call" | custom-call | tf_op jit(solution)/shard_map/update/pallas_call | solution.py:252
  65.9 3.8 %update.3 = f32[2,4,4,128,128]{4,3,2,1,0:T(8,128)} custom-call(f32[4,3,512]{2,1,0:T(4,128)} %get-tuple-element.40.gates, f32[2,4,4,128,128]{4,3,2,1,0:T(8,128)} %state.3, f32[2,4,4,128,128]{4,3,2,1,0:T(8,128)} %update.2.refs_0_), custom_call_target="tpu_custom_call", output_to_operand_aliasing={{}: (2, {})} | custom-call | tf_op jit(solution)/shard_map/update/pallas_call | solution.py:252
  70.2 1.4 %close.1 = bf16[4,1024]{1,0:T(4,128)(2,1)} custom-call(f32[4,1024]{1,0:T(4,128)} %get-tuple-element.36.own, bf16[4,1024]{1,0:T(4,128)(2,1)} %copy-done.12, bf16[4,1024]{1,0:T(4,128)(2,1)} %copy-done.13, bf16[4,1024]{1,0:T(4,128)(2,1)} %copy-done.14), custom_call_target="tpu_custom_call" | custom-call | tf_op jit(solution)/shard_map/close/pallas_call | solution.py:179
  (63 shorter events, 6.6 us)
Async XLA Ops:
  0.6 6.4 %collective-permute-start.1 = (bf16[4,1024]{1,0:T(4,128)(2,1)}, bf16[4,1024]{1,0:T(4,128)(2,1)S(1)}, u32[]{:S(2)}, u32[]{:S(2)}) collective-permute-start(bf16[4,1024]{1,0:T(4,128)(2,1)} %refs_0_.1), channel_id=1, source_target_pairs={{8,0},{12,4},{0,8},{4,12},{9,1},{13,5},{1,9},{5,13},{10,2},{14,6},... | collective-permute-start | bytes 24584 | tf_op jit(solution)/shard_map/ppermute | solution.py:23
  4.8 3.9 %collective-permute-start = (bf16[4,1024]{1,0:T(4,128)(2,1)}, bf16[4,1024]{1,0:T(4,128)(2,1)S(1)}, u32[]{:S(2)}, u32[]{:S(2)}) collective-permute-start(bf16[4,1024]{1,0:T(4,128)(2,1)} %refs_0_.1), channel_id=1, source_target_pairs={{4,0},{0,4},{12,8},{8,12},{5,1},{1,5},{13,9},{9,13},{6,2},{2,6},{1... | collective-permute-start | bytes 24584 | tf_op jit(solution)/shard_map/ppermute | solution.py:23
  6.3 5.7 %collective-permute-start.2 = (bf16[4,1024]{1,0:T(4,128)(2,1)}, bf16[4,1024]{1,0:T(4,128)(2,1)S(1)}, u32[]{:S(2)}, u32[]{:S(2)}) collective-permute-start(bf16[4,1024]{1,0:T(4,128)(2,1)} %refs_0_.1), channel_id=1, source_target_pairs={{12,0},{8,4},{4,8},{0,12},{13,1},{9,5},{5,9},{1,13},{14,2},{10,6},... | collective-permute-start | bytes 24584 | tf_op jit(solution)/shard_map/ppermute | solution.py:23
  7.0 5.0 %copy-start.9 = (bf16[4,1024]{1,0:T(4,128)(2,1)}, bf16[4,1024]{1,0:T(4,128)(2,1)S(1)}, u32[]{:S(2)}) copy-start(bf16[4,1024]{1,0:T(4,128)(2,1)S(1)} %collective-permute-done.1.refs_2_) | copy-start | bytes 24580
  8.6 3.4 %copy-start.10 = (bf16[4,1024]{1,0:T(4,128)(2,1)}, bf16[4,1024]{1,0:T(4,128)(2,1)S(1)}, u32[]{:S(2)}) copy-start(bf16[4,1024]{1,0:T(4,128)(2,1)S(1)} %collective-permute-done.refs_1_) | copy-start | bytes 24580
  16.2 1.9 %collective-permute-start.3 = (bf16[4,2176]{1,0:T(4,128)(2,1)}, bf16[4,2176]{1,0:T(4,128)(2,1)S(1)}, u32[]{:S(2)}, u32[]{:S(2)}) collective-permute-start(bf16[4,2176]{1,0:T(4,128)(2,1)} %get-tuple-element.24), channel_id=1, source_target_pairs={{0,1},{1,0},{2,3},{3,2},{4,5},{5,4},{6,7},{7,6},{8,9},{9,8},{10,11... | collective-permute-start | bytes 52232 | tf_op jit(solution)/shard_map/ppermute | solution.py:27
  16.2 4.0 %collective-permute-start.4 = (bf16[4,2176]{1,0:T(4,128)(2,1)}, bf16[4,2176]{1,0:T(4,128)(2,1)S(1)}, u32[]{:S(2)}, u32[]{:S(2)}) collective-permute-start(bf16[4,2176]{1,0:T(4,128)(2,1)} %get-tuple-element.25), channel_id=1, source_target_pairs={{0,2},{1,3},{2,0},{3,1},{4,6},{5,7},{6,4},{7,5},{8,10},{9,11},{10,... | collective-permute-start | bytes 52232 | tf_op jit(solution)/shard_map/ppermute | solution.py:27
  17.8 3.4 %collective-permute-start.5 = (bf16[4,2176]{1,0:T(4,128)(2,1)}, bf16[4,2176]{1,0:T(4,128)(2,1)S(1)}, u32[]{:S(2)}, u32[]{:S(2)}) collective-permute-start(bf16[4,2176]{1,0:T(4,128)(2,1)} %get-tuple-element.26), channel_id=1, source_target_pairs={{0,3},{1,2},{2,1},{3,0},{4,7},{5,6},{6,5},{7,4},{8,11},{9,10},{10,... | collective-permute-start | bytes 52232 | tf_op jit(solution)/shard_map/ppermute | solution.py:27
  18.1 3.1 %copy-start.3 = (bf16[4,2176]{1,0:T(4,128)(2,1)}, bf16[4,2176]{1,0:T(4,128)(2,1)S(1)}, u32[]{:S(2)}) copy-start(bf16[4,2176]{1,0:T(4,128)(2,1)S(1)} %collective-permute-done.3.refs_1_) | copy-start | bytes 52228
  20.3 1.0 %copy-start.5 = (bf16[4,2176]{1,0:T(4,128)(2,1)}, bf16[4,2176]{1,0:T(4,128)(2,1)S(1)}, u32[]{:S(2)}) copy-start(bf16[4,2176]{1,0:T(4,128)(2,1)S(1)} %collective-permute-done.4.refs_2_) | copy-start | bytes 52228
  24.3 3.2 %collective-permute-start.8 = (bf16[4,512]{1,0:T(4,128)(2,1)}, bf16[4,512]{1,0:T(4,128)(2,1)S(1)}, u32[]{:S(2)}, u32[]{:S(2)}) collective-permute-start(bf16[4,512]{1,0:T(4,128)(2,1)} %get-tuple-element.27.refs_0_), channel_id=1, source_target_pairs={{3,0},{2,1},{1,2},{0,3},{7,4},{6,5},{5,6},{4,7},{11,8},{10,9},{9,1... | collective-permute-start | bytes 12296 | tf_op jit(solution)/shard_map/ppermute | solution.py:23
  24.7 3.8 %collective-permute-start.7 = (bf16[4,512]{1,0:T(4,128)(2,1)}, bf16[4,512]{1,0:T(4,128)(2,1)S(1)}, u32[]{:S(2)}, u32[]{:S(2)}) collective-permute-start(bf16[4,512]{1,0:T(4,128)(2,1)} %get-tuple-element.27.refs_0_), channel_id=1, source_target_pairs={{2,0},{3,1},{0,2},{1,3},{6,4},{7,5},{4,6},{5,7},{10,8},{11,9},{8,1... | collective-permute-start | bytes 12296 | tf_op jit(solution)/shard_map/ppermute | solution.py:23
  26.1 2.4 %collective-permute-start.6 = (bf16[4,512]{1,0:T(4,128)(2,1)}, bf16[4,512]{1,0:T(4,128)(2,1)S(1)}, u32[]{:S(2)}, u32[]{:S(2)}) collective-permute-start(bf16[4,512]{1,0:T(4,128)(2,1)} %get-tuple-element.27.refs_0_), channel_id=1, source_target_pairs={{1,0},{0,1},{3,2},{2,3},{5,4},{4,5},{7,6},{6,7},{9,8},{8,9},{11,10... | collective-permute-start | bytes 12296 | tf_op jit(solution)/shard_map/ppermute | solution.py:23
  27.5 1.0 %copy-start.17 = (bf16[4,512]{1,0:T(4,128)(2,1)}, bf16[4,512]{1,0:T(4,128)(2,1)S(1)}, u32[]{:S(2)}) copy-start(bf16[4,512]{1,0:T(4,128)(2,1)S(1)} %collective-permute-done.8.refs_3_) | copy-start | bytes 12292
  31.8 5.9 %collective-permute-start.11 = (bf16[16,1024]{1,0:T(8,128)(2,1)}, bf16[16,1024]{1,0:T(8,128)(2,1)S(1)}, u32[]{:S(2)}, u32[]{:S(2)}) collective-permute-start(bf16[16,1024]{1,0:T(8,128)(2,1)} %get-tuple-element.29), channel_id=1, source_target_pairs={{12,0},{8,4},{4,8},{0,12},{13,1},{9,5},{5,9},{1,13},{14,2},{10,6},... | collective-permute-start | bytes 98312 | tf_op jit(solution)/shard_map/ppermute | solution.py:23
  31.9 5.8 %collective-permute-start.10 = (bf16[16,1024]{1,0:T(8,128)(2,1)}, bf16[16,1024]{1,0:T(8,128)(2,1)S(1)}, u32[]{:S(2)}, u32[]{:S(2)}) collective-permute-start(bf16[16,1024]{1,0:T(8,128)(2,1)} %get-tuple-element.29), channel_id=1, source_target_pairs={{8,0},{12,4},{0,8},{4,12},{9,1},{13,5},{1,9},{5,13},{10,2},{14,6},... | collective-permute-start | bytes 98312 | tf_op jit(solution)/shard_map/ppermute | solution.py:23
  31.9 6.4 %collective-permute-start.9 = (bf16[16,1024]{1,0:T(8,128)(2,1)}, bf16[16,1024]{1,0:T(8,128)(2,1)S(1)}, u32[]{:S(2)}, u32[]{:S(2)}) collective-permute-start(bf16[16,1024]{1,0:T(8,128)(2,1)} %get-tuple-element.29), channel_id=1, source_target_pairs={{4,0},{0,4},{12,8},{8,12},{5,1},{1,5},{13,9},{9,13},{6,2},{2,6},{1... | collective-permute-start | bytes 98312 | tf_op jit(solution)/shard_map/ppermute | solution.py:23
  37.8 0.6 copy-start
  37.8 0.6 copy-start.1
  38.4 0.6 copy-start.2
  42.6 1.9 %collective-permute-start.12 = (bf16[4,2176]{1,0:T(4,128)(2,1)}, bf16[4,2176]{1,0:T(4,128)(2,1)S(1)}, u32[]{:S(2)}, u32[]{:S(2)}) collective-permute-start(bf16[4,2176]{1,0:T(4,128)(2,1)} %get-tuple-element.31), channel_id=1, source_target_pairs={{0,1},{1,0},{2,3},{3,2},{4,5},{5,4},{6,7},{7,6},{8,9},{9,8},{10,11... | collective-permute-start | bytes 52232 | tf_op jit(solution)/shard_map/ppermute | solution.py:27
  42.6 4.0 %collective-permute-start.13 = (bf16[4,2176]{1,0:T(4,128)(2,1)}, bf16[4,2176]{1,0:T(4,128)(2,1)S(1)}, u32[]{:S(2)}, u32[]{:S(2)}) collective-permute-start(bf16[4,2176]{1,0:T(4,128)(2,1)} %get-tuple-element.32), channel_id=1, source_target_pairs={{0,2},{1,3},{2,0},{3,1},{4,6},{5,7},{6,4},{7,5},{8,10},{9,11},{10,... | collective-permute-start | bytes 52232 | tf_op jit(solution)/shard_map/ppermute | solution.py:27
  44.0 3.4 %collective-permute-start.14 = (bf16[4,2176]{1,0:T(4,128)(2,1)}, bf16[4,2176]{1,0:T(4,128)(2,1)S(1)}, u32[]{:S(2)}, u32[]{:S(2)}) collective-permute-start(bf16[4,2176]{1,0:T(4,128)(2,1)} %get-tuple-element.33), channel_id=1, source_target_pairs={{0,3},{1,2},{2,1},{3,0},{4,7},{5,6},{6,5},{7,4},{8,11},{9,10},{10,... | collective-permute-start | bytes 52232 | tf_op jit(solution)/shard_map/ppermute | solution.py:27
  44.4 3.0 %copy-start.4 = (bf16[4,2176]{1,0:T(4,128)(2,1)}, bf16[4,2176]{1,0:T(4,128)(2,1)S(1)}, u32[]{:S(2)}) copy-start(bf16[4,2176]{1,0:T(4,128)(2,1)S(1)} %collective-permute-done.12.refs_1_) | copy-start | bytes 52228
  46.6 0.8 %copy-start.6 = (bf16[4,2176]{1,0:T(4,128)(2,1)}, bf16[4,2176]{1,0:T(4,128)(2,1)S(1)}, u32[]{:S(2)}) copy-start(bf16[4,2176]{1,0:T(4,128)(2,1)S(1)} %collective-permute-done.13.refs_2_) | copy-start | bytes 52228
  50.5 3.2 %collective-permute-start.17 = (bf16[4,512]{1,0:T(4,128)(2,1)}, bf16[4,512]{1,0:T(4,128)(2,1)S(1)}, u32[]{:S(2)}, u32[]{:S(2)}) collective-permute-start(bf16[4,512]{1,0:T(4,128)(2,1)} %get-tuple-element.34.refs_0_), channel_id=1, source_target_pairs={{3,0},{2,1},{1,2},{0,3},{7,4},{6,5},{5,6},{4,7},{11,8},{10,9},{9,1... | collective-permute-start | bytes 12296 | tf_op jit(solution)/shard_map/ppermute | solution.py:23
  51.0 3.8 %collective-permute-start.16 = (bf16[4,512]{1,0:T(4,128)(2,1)}, bf16[4,512]{1,0:T(4,128)(2,1)S(1)}, u32[]{:S(2)}, u32[]{:S(2)}) collective-permute-start(bf16[4,512]{1,0:T(4,128)(2,1)} %get-tuple-element.34.refs_0_), channel_id=1, source_target_pairs={{2,0},{3,1},{0,2},{1,3},{6,4},{7,5},{4,6},{5,7},{10,8},{11,9},{8,1... | collective-permute-start | bytes 12296 | tf_op jit(solution)/shard_map/ppermute | solution.py:23
  52.3 2.5 %collective-permute-start.15 = (bf16[4,512]{1,0:T(4,128)(2,1)}, bf16[4,512]{1,0:T(4,128)(2,1)S(1)}, u32[]{:S(2)}, u32[]{:S(2)}) collective-permute-start(bf16[4,512]{1,0:T(4,128)(2,1)} %get-tuple-element.34.refs_0_), channel_id=1, source_target_pairs={{1,0},{0,1},{3,2},{2,3},{5,4},{4,5},{7,6},{6,7},{9,8},{8,9},{11,10... | collective-permute-start | bytes 12296 | tf_op jit(solution)/shard_map/ppermute | solution.py:23
  53.7 1.1 %copy-start.15 = (bf16[4,512]{1,0:T(4,128)(2,1)}, bf16[4,512]{1,0:T(4,128)(2,1)S(1)}, u32[]{:S(2)}) copy-start(bf16[4,512]{1,0:T(4,128)(2,1)S(1)} %collective-permute-done.17.refs_3_) | copy-start | bytes 12292
  57.7 12.0 %collective-permute-start.18 = (bf16[4,1024]{1,0:T(4,128)(2,1)}, bf16[4,1024]{1,0:T(4,128)(2,1)S(1)}, u32[]{:S(2)}, u32[]{:S(2)}) collective-permute-start(bf16[4,1024]{1,0:T(4,128)(2,1)} %get-tuple-element.37), channel_id=1, source_target_pairs={{0,4},{4,0},{8,12},{12,8},{1,5},{5,1},{9,13},{13,9},{2,6},{6,2},{1... | collective-permute-start | bytes 24584 | tf_op jit(solution)/shard_map/ppermute | solution.py:27
  59.7 10.0 %collective-permute-start.19 = (bf16[4,1024]{1,0:T(4,128)(2,1)}, bf16[4,1024]{1,0:T(4,128)(2,1)S(1)}, u32[]{:S(2)}, u32[]{:S(2)}) collective-permute-start(bf16[4,1024]{1,0:T(4,128)(2,1)} %get-tuple-element.38), channel_id=1, source_target_pairs={{0,8},{4,12},{8,0},{12,4},{1,9},{5,13},{9,1},{13,5},{2,10},{6,14},... | collective-permute-start | bytes 24584 | tf_op jit(solution)/shard_map/ppermute | solution.py:27
  60.6 9.1 %collective-permute-start.20 = (bf16[4,1024]{1,0:T(4,128)(2,1)}, bf16[4,1024]{1,0:T(4,128)(2,1)S(1)}, u32[]{:S(2)}, u32[]{:S(2)}) collective-permute-start(bf16[4,1024]{1,0:T(4,128)(2,1)} %get-tuple-element.39), channel_id=1, source_target_pairs={{0,12},{4,8},{8,4},{12,0},{1,13},{5,9},{9,5},{13,1},{2,14},{6,10},... | collective-permute-start | bytes 24584 | tf_op jit(solution)/shard_map/ppermute | solution.py:27
  (10 other events, 5.9 us)

commit v3 on v2

--- a/solution.py
+++ b/solution.py
@@ -25,12 +25,6 @@
 
 def send(array, axis, n, k):
     return lax.ppermute(array, axis, [(i, peer_of(n, k, i)) for i in range(n)])
-
-
-def slot_rows(total, n, index):
-    size = total // n
-    row = jnp.arange(total, dtype=jnp.int32)
-    return peer_of(n, row // size, index) * size + row % size
 
 
 def split(array):
@@ -52,7 +46,7 @@
     tail = jnp.where(lane == 2, low.astype(F32), tail)
     width = weights[0].shape[-1]
     for index, weight in enumerate(weights):
-        product = jnp.dot(scaled, weight[0], preferred_element_type=F32)
+        product = jnp.dot(scaled, weight[layer], preferred_element_type=F32)
         for k, out in enumerate(outs):
             out[:, index * width : (index + 1) * width] = product[
                 k * count : (k + 1) * count
@@ -112,7 +106,7 @@
         readout = jnp.sum(shared[:, cols], axis=1, keepdims=True) * value[:, cols]
         for seq in range(seqs):
             high, low = split(jnp.where(row == seq, weighted[:, cols], 0.0))
-            stored = state[0, seq, head].astype(BF16)
+            stored = state[layer, seq, head].astype(BF16)
             readout = readout + jnp.dot(high, stored, preferred_element_type=F32)
             readout = readout + jnp.dot(low, stored, preferred_element_type=F32)
         scale = lax.rsqrt(jnp.mean(readout * readout, axis=1, keepdims=True) + 1e-06)
@@ -121,15 +115,21 @@
         ).astype(BF16)
 
 
-def update(gates, state, *refs):
-    out = refs[-1]
-    heads, hd = state.shape[2], state.shape[3]
-    for head in range(heads):
-        cols = slice(head * hd, (head + 1) * hd)
-        forget, keyvec, value = (gates[0, index : index + 1, cols] for index in range(3))
-        forget = jnp.transpose(jnp.broadcast_to(forget, (hd, hd)))
-        keyvec = jnp.transpose(jnp.broadcast_to(keyvec, (hd, hd)))
-        out[0, 0, head] = forget * state[0, 0, head] + keyvec * value
+def update(layer, gates, state, *refs):
+    out, staged, sems = refs[-3:]
+    seqs, heads, hd = state.shape[1], state.shape[2], state.shape[3]
+    copies = []
+    for seq in range(seqs):
+        for head in range(heads):
+            cols = slice(head * hd, (head + 1) * hd)
+            forget, keyvec, value = (gates[seq, index : index + 1, cols] for index in range(3))
+            forget = jnp.transpose(jnp.broadcast_to(forget, (hd, hd)))
+            keyvec = jnp.transpose(jnp.broadcast_to(keyvec, (hd, hd)))
+            staged[seq, head] = forget * state[layer, seq, head] + keyvec * value
+        copies.append(pltpu.make_async_copy(staged.at[seq], out.at[layer, seq], sems.at[seq]))
+        copies[-1].start()
+    for copy in copies:
+        copy.wait()
 
 
 def gather_rows(parts, slots):
@@ -139,18 +139,18 @@
     return slots[...].astype(BF16)
 
 
-def mix_next(n_dp, *refs):
+def mix_next(n_dp, layer, *refs):
     parts, (weight, mixed, sent, slots) = refs[:n_dp], refs[n_dp:]
-    product = jnp.dot(gather_rows(parts, slots), weight[0], preferred_element_type=F32)
+    product = jnp.dot(gather_rows(parts, slots), weight[layer], preferred_element_type=F32)
     mixed[...] = product
     sent[...] = product.astype(BF16)
 
 
-def mix_last(n_dp, *refs):
+def mix_last(n_dp, layer, *refs):
     parts, (weight, base, order) = refs[:n_dp], refs[n_dp : n_dp + 3]
     own, outs, slots = refs[n_dp + 3], refs[n_dp + 4 : -1], refs[-1]
     rows = own.shape[0]
-    product = jnp.dot(gather_rows(parts, slots), weight[0], preferred_element_type=F32)
+    product = jnp.dot(gather_rows(parts, slots), weight[layer], preferred_element_type=F32)
     high, low = split(product)
     moved = jnp.dot(order[...], high, preferred_element_type=F32)
     first = order[:rows, :]
@@ -170,21 +170,35 @@
     refs[-1][...] = total.astype(BF16)
 
 
-def layer_block(array, layer):
-    zeros = (0,) * (array.ndim - 1)
-    return pl.BlockSpec((1,) + array.shape[1:], lambda step: (layer,) + zeros)
-
-
-def call(body, name, args, in_specs, outs, scratch=()):
+def in_vmem(array):
+    return pltpu.with_memory_space_constraint(array, pltpu.VMEM)
+
+
+def stage(n_tp, n_dp, tokens, tokens_out, order_in, order_out):
+    tokens_out[...] = tokens[...]
+    total = order_in.shape[0]
+
+    def held(dim, n, index):
+        row = lax.broadcasted_iota(jnp.int32, (total, total), dim)
+        size = total // n
+        return peer_of(n, row // size, index) * size + row % size
+
+    tp, dp = lax.axis_index("tp"), lax.axis_index("dp")
+    order_in[...] = jnp.where(held(0, n_dp, dp) == held(1, n_tp, tp), 1.0, 0.0).astype(BF16)
+    order_out[...] = jnp.where(held(0, n_tp, tp) == held(1, n_dp, dp), 1.0, 0.0).astype(BF16)
+
+
+def call(body, name, args, in_specs, outs, scratch=(), flops=None):
     return pl.pallas_call(
         body,
         name=name,
-        grid=(1,),
-        out_shape=[jax.ShapeDtypeStruct(shape, dtype) for shape, dtype in outs],
+        out_shape=[pltpu.VMEM(shape, dtype) for shape, dtype in outs],
         in_specs=in_specs,
         out_specs=[VMEM] * len(outs),
         scratch_shapes=[pltpu.VMEM(shape, dtype) for shape, dtype in scratch],
-    )(*args)
+        compiler_params=pltpu.CompilerParams(vmem_limit_bytes=8 << 20),
+        cost_estimate=flops and pl.CostEstimate(flops=flops, bytes_accessed=0, transcendentals=0),
+    )(*map(in_vmem, args))
 
 
 def per_device(
@@ -207,18 +221,21 @@
     total = rows * n_tp
     width = heads * hd
     weights = (w_query, w_forget, w_value, w_gate)
-    tp_rows = slot_rows(total, n_tp, lax.axis_index("tp"))
-    dp_rows = slot_rows(total, n_dp, lax.axis_index("dp"))
-    order_in = (dp_rows[:, None] == tp_rows[None, :]).astype(BF16)
-    order_out = (tp_rows[:, None] == dp_rows[None, :]).astype(BF16)
-
+    tokens, order_in, order_out = call(
+        functools.partial(stage, n_tp, n_dp),
+        "stage",
+        (tokens,),
+        [VMEM],
+        [((rows, local), BF16)] + [((total, total), BF16)] * 2,
+        flops=20_000_000_000,
+    )
     parts = [tokens] + [swap(tokens, "tp", n_tp, k) for k in range(1, n_tp)]
     base = mixed = None
     new_state = None
     for layer in range(2):
         outs = [((total, local), BF16), ((seqs, 4 * width + LANES), F32)]
         outs += [((seqs, 4 * width + LANES), BF16)] * (n_dp - 1)
-        specs = [layer_block(weight, layer) for weight in weights]
+        specs = [VMEM] * 4
         if layer == 0:
             base, own, *sent = call(
                 functools.partial(project_first, n_tp, n_dp, layer),
@@ -241,46 +258,51 @@
             functools.partial(recur, n_dp, layer, features),
             "recur",
             (own, *parts, lower_bound, head_gain, state),
-            [VMEM] * (n_dp + 2) + [layer_block(state, layer)],
+            [VMEM] * (n_dp + 2) + [VMEM],
             [((seqs, width), BF16), ((seqs, 3, width), F32)],
         )
         parts = [normed] + [swap(normed, "dp", n_dp, k) for k in range(1, n_dp)]
-        block = pl.BlockSpec(
-            (1, 1, heads, hd, hd), lambda seq, layer=layer: (layer, seq, 0, 0, 0)
-        )
-        gate_block = pl.BlockSpec((1, 3, width), lambda seq: (seq, 0, 0))
         new_state = pl.pallas_call(
-            update,
+            functools.partial(update, layer),
             name="update",
-            grid=(seqs,),
             out_shape=jax.ShapeDtypeStruct(state.shape, F32),
-            in_specs=[gate_block, block] + ([ANY] if layer else []),
-            out_specs=block,
+            in_specs=[VMEM, VMEM] + ([ANY] if layer else []),
+            out_specs=ANY,
             input_output_aliases={2: 0} if layer else {},
-        )(gates, state, *((new_state,) if layer else ()))
+            scratch_shapes=[
+                pltpu.VMEM((seqs, heads, hd, hd), F32),
+                pltpu.SemaphoreType.DMA((seqs,)),
+            ],
+            compiler_params=pltpu.CompilerParams(vmem_limit_bytes=4 << 20),
+        )(in_vmem(gates), in_vmem(state), *((new_state,) if layer else ()))
         if layer == 0:
             mixed, sent = call(
-                functools.partial(mix_next, n_dp),
+                functools.partial(mix_next, n_dp, layer),
                 "mix_next",
                 (*parts, w_out),
-                [VMEM] * n_dp + [layer_block(w_out, layer)],
+                [VMEM] * n_dp + [VMEM],
                 [((total, local), F32), ((total, local), BF16)],
                 [((total, width), F32)],
             )
             parts = [swap(sent, "tp", n_tp, k) for k in range(1, n_tp)]
         else:
             own, *sent = call(
-                functools.partial(mix_last, n_dp),
+                functools.partial(mix_last, n_dp, layer),
                 "mix_last",
                 (*parts, w_out, base, order_out),
-                [VMEM] * n_dp + [layer_block(w_out, layer)] + [VMEM] * 2,
+                [VMEM] * n_dp + [VMEM] + [VMEM] * 2,
                 [((rows, local), F32)] + [((rows, local), BF16)] * (n_tp - 1),
                 [((total, width), F32)],
             )
             parts = [send(sent[k - 1], "tp", n_tp, k) for k in range(1, n_tp)]
-    (hidden,) = call(
-        close, "close", (own, *parts), [VMEM] * n_tp, [((rows, local), BF16)]
-    )
+    hidden = pl.pallas_call(
+        close,
+        name="close",
+        out_shape=jax.ShapeDtypeStruct((rows, local), BF16),
+        in_specs=[VMEM] * n_tp,
+        out_specs=VMEM,
+        compiler_params=pltpu.CompilerParams(vmem_limit_bytes=4 << 20),
+    )(*map(in_vmem, (own, *parts)))
     return (hidden, new_state)
 
 

time: 72 us -> 47.9 us (0.67)
  Pallas kernels: 25.5 us -> 6.49 us
  local copies, waits for them, and re-layouts: 4.75 us -> 0.88 us
    pallas_call x9 -> x10, Pallas kernels: 25.5 us -> 6.49 us  [the longest x7 3.18 us: call(): pl.pallas_call(body, name=name, out_shape=[pltpu.VMEM(shape, dtype) for s...]
    unnamed x42 -> x20, local copies, waits for them, and re-layouts: 4.75 us -> 0.88 us
    ppermute x12, waiting for transfers between devices: 11.9 us -> 10.5 us  [swap(): return lax.ppermute(array, axis, [(peer_of(n, k, i), i) for i in range(n)])]
    ppermute x9, waiting for transfers between devices: 6.07 us -> 6.91 us  [send(): return lax.ppermute(array, axis, [(i, peer_of(n, k, i)) for i in range(n)])]
  transfers between devices with their start and end apart: 21 -> 21, of which waited for: 12 -> 14; matrix products, arithmetic and copies ran while one was open for 1% -> 0% of each run, Pallas kernels for 11% -> 6%
where the time goes in v3:
time: 47.9 us; the launch traced here: 47.7 us
  starting transfers between devices  22.1 us (46%)
  waiting for transfers between devices  17.4 us (36%)
  Pallas kernels  6.49 us (14%)
  local copies, waits for them, and re-layouts  0.88 us (2%)
  between operations  0.81 us (2%)
    ppermute x12, starting transfers between devices, swap(): return lax.ppermute(array, axis, [(peer_of(n, k, i), i) for i in range(n)])  13.9 us
    ppermute x12, waiting for transfers between devices, swap(): return lax.ppermute(array, axis, [(peer_of(n, k, i), i) for i in range(n)])  10.5 us
    ppermute x9, starting transfers between devices, send(): return lax.ppermute(array, axis, [(i, peer_of(n, k, i)) for i in range(n)])  8.18 us
    ppermute x9, waiting for transfers between devices, send(): return lax.ppermute(array, axis, [(i, peer_of(n, k, i)) for i in range(n)])  6.91 us
    pallas_call x7, Pallas kernels, call(): pl.pallas_call(body, name=name, out_shape=[pltpu.VMEM(shape, dtype) for s...  3.18 us
    pallas_call x2, Pallas kernels, per_device(): pl.pallas_call(functools.partial(update, layer), name='update', out_shape...  2.69 us
  transfers between devices with their start and end apart: 21, of which 14 were waited for; matrix products, arithmetic and copies ran while one was open for 0% of the time, Pallas kernels for 6%

profile of v3, /device:TPU:0, one launch (start us, length us, event | category | flops | bytes accessed | tf_op | source)
XLA Modules:
  0.0 47.7 jit_solution(305184659033133540)
XLA Ops:
  0.7 0.8 %copy-done.9 = bf16[4,1024]{1,0:T(4,128)(2,1)S(1)} copy-done((bf16[4,1024]{1,0:T(4,128)(2,1)S(1)}, bf16[4,1024]{1,0:T(4,128)(2,1)}, u32[]{:S(2)}) %copy-start.9) | copy-done | bytes 8216
  1.5 5.1 %collective-permute-start.2 = (bf16[4,1024]{1,0:T(4,128)(2,1)S(1)}, bf16[4,1024]{1,0:T(4,128)(2,1)S(1)}, u32[]{:S(2)}, u32[]{:S(2)}) collective-permute-start(bf16[4,1024]{1,0:T(4,128)(2,1)S(1)} %get-tuple-element.25.refs_0_), channel_id=1, source_target_pairs={{12,0},{8,4},{4,8},{0,12},{13,1},{9,5},{5,9},{1,13},{14,2},{10,6},... | collective-permute-start | bytes 24584 | tf_op jit(solution)/shard_map/ppermute | solution.py:23
  6.7 0.6 %collective-permute-start = (bf16[4,1024]{1,0:T(4,128)(2,1)S(1)}, bf16[4,1024]{1,0:T(4,128)(2,1)S(1)}, u32[]{:S(2)}, u32[]{:S(2)}) collective-permute-start(bf16[4,1024]{1,0:T(4,128)(2,1)S(1)} %get-tuple-element.25.refs_0_), channel_id=1, source_target_pairs={{4,0},{0,4},{12,8},{8,12},{5,1},{1,5},{13,9},{9,13},{6,2},{2,6},{1... | collective-permute-start | bytes 24584 | tf_op jit(solution)/shard_map/ppermute | solution.py:23
  7.3 1.0 %collective-permute-done.2.refs_3_ = bf16[4,1024]{1,0:T(4,128)(2,1)S(1)} collective-permute-done((bf16[4,1024]{1,0:T(4,128)(2,1)S(1)}, bf16[4,1024]{1,0:T(4,128)(2,1)S(1)}, u32[]{:S(2)}, u32[]{:S(2)}) %collective-permute-start.2) | collective-permute-done | bytes 8224 | tf_op jit(solution)/shard_map/ppermute | solution.py:23
  8.3 2.9 %collective-permute-done.1.refs_2_ = bf16[4,1024]{1,0:T(4,128)(2,1)S(1)} collective-permute-done((bf16[4,1024]{1,0:T(4,128)(2,1)S(1)}, bf16[4,1024]{1,0:T(4,128)(2,1)S(1)}, u32[]{:S(2)}, u32[]{:S(2)}) %collective-permute-start.1) | collective-permute-done | bytes 8224 | tf_op jit(solution)/shard_map/ppermute | solution.py:23
  11.3 0.8 %project_first.1 = (bf16[16,1024]{1,0:T(8,128)(2,1)S(1)}, f32[4,2176]{1,0:T(4,128)S(1)}, bf16[4,2176]{1,0:T(4,128)(2,1)S(1)}, bf16[4,2176]{1,0:T(4,128)(2,1)S(1)}, bf16[4,2176]{1,0:T(4,128)(2,1)S(1)}) custom-call(bf16[4,1024]{1,0:T(4,128)(2,1)S(1)} %get-tuple-element.25.refs_0_, bf16[4,1024]{1,0:T(4,128)(2,1)S(1)} %collective-permute-done.refs_1_, ...), custom_call_target="tpu_custom_call" | custom-call | tf_op jit(solution)/shard_map/project_first/pallas_call | solution.py:192
  12.1 1.6 %collective-permute-start.4 = (bf16[4,2176]{1,0:T(4,128)(2,1)S(1)}, bf16[4,2176]{1,0:T(4,128)(2,1)S(1)}, u32[]{:S(2)}, u32[]{:S(2)}) collective-permute-start(bf16[4,2176]{1,0:T(4,128)(2,1)S(1)} %get-tuple-element.30), channel_id=1, source_target_pairs={{0,2},{1,3},{2,0},{3,1},{4,6},{5,7},{6,4},{7,5},{8,10},{9,11},{10,... | collective-permute-start | bytes 52232 | tf_op jit(solution)/shard_map/ppermute | solution.py:27
  14.0 2.0 %collective-permute-done.4.refs_2_ = bf16[4,2176]{1,0:T(4,128)(2,1)S(1)} collective-permute-done((bf16[4,2176]{1,0:T(4,128)(2,1)S(1)}, bf16[4,2176]{1,0:T(4,128)(2,1)S(1)}, u32[]{:S(2)}, u32[]{:S(2)}) %collective-permute-start.4) | collective-permute-done | bytes 17440 | tf_op jit(solution)/shard_map/ppermute | solution.py:27
  15.9 0.9 %collective-permute-done.5.refs_3_ = bf16[4,2176]{1,0:T(4,128)(2,1)S(1)} collective-permute-done((bf16[4,2176]{1,0:T(4,128)(2,1)S(1)}, bf16[4,2176]{1,0:T(4,128)(2,1)S(1)}, u32[]{:S(2)}, u32[]{:S(2)}) %collective-permute-start.5) | collective-permute-done | bytes 17440 | tf_op jit(solution)/shard_map/ppermute | solution.py:27
  16.9 0.6 %recur.2 = (bf16[4,512]{1,0:T(4,128)(2,1)S(1)}, f32[4,3,512]{2,1,0:T(4,128)S(1)}) custom-call(f32[4,2176]{1,0:T(4,128)S(1)} %get-tuple-element.28.refs_0_, bf16[4,2176]{1,0:T(4,128)(2,1)S(1)} %collective-permute-done.3.refs_1_, bf16[4,2176]{1,0:T(4,128)(2,1)S(1)} %collective-permute-done.4.refs_2_, bf16[4,2176]{1,0:T(4,128)(2,1)S(1)} %collective-permute-done.5.refs_3_, ...), custom_call_target="tpu_custom_call" | custom-call | tf_op jit(solution)/shard_map/recur/pallas_call | solution.py:192
  17.8 1.4 %collective-permute-start.7 = (bf16[4,512]{1,0:T(4,128)(2,1)S(1)}, bf16[4,512]{1,0:T(4,128)(2,1)S(1)}, u32[]{:S(2)}, u32[]{:S(2)}) collective-permute-start(bf16[4,512]{1,0:T(4,128)(2,1)S(1)} %get-tuple-element.32.refs_0_), channel_id=1, source_target_pairs={{2,0},{3,1},{0,2},{1,3},{6,4},{7,5},{4,6},{5,7},{10,8},{11,9},{8,1... | collective-permute-start | bytes 12296 | tf_op jit(solution)/shard_map/ppermute | solution.py:23
  19.3 1.2 %collective-permute-done.8.refs_3_ = bf16[4,512]{1,0:T(4,128)(2,1)S(1)} collective-permute-done((bf16[4,512]{1,0:T(4,128)(2,1)S(1)}, bf16[4,512]{1,0:T(4,128)(2,1)S(1)}, u32[]{:S(2)}, u32[]{:S(2)}) %collective-permute-start.8) | collective-permute-done | bytes 4128 | tf_op jit(solution)/shard_map/ppermute | solution.py:23
  20.5 1.0 %collective-permute-done.7.refs_2_ = bf16[4,512]{1,0:T(4,128)(2,1)S(1)} collective-permute-done((bf16[4,512]{1,0:T(4,128)(2,1)S(1)}, bf16[4,512]{1,0:T(4,128)(2,1)S(1)}, u32[]{:S(2)}, u32[]{:S(2)}) %collective-permute-start.7) | collective-permute-done | bytes 4128 | tf_op jit(solution)/shard_map/ppermute | solution.py:23
  21.7 1.5 %collective-permute-start.11 = (bf16[16,1024]{1,0:T(8,128)(2,1)S(1)}, bf16[16,1024]{1,0:T(8,128)(2,1)S(1)}, u32[]{:S(2)}, u32[]{:S(2)}) collective-permute-start(bf16[16,1024]{1,0:T(8,128)(2,1)S(1)} %get-tuple-element.34), channel_id=1, source_target_pairs={{12,0},{8,4},{4,8},{0,12},{13,1},{9,5},{5,9},{1,13},{14,2},{10,6},... | collective-permute-start | bytes 98312 | tf_op jit(solution)/shard_map/ppermute | solution.py:23
  23.2 0.6 %collective-permute-start.10 = (bf16[16,1024]{1,0:T(8,128)(2,1)S(1)}, bf16[16,1024]{1,0:T(8,128)(2,1)S(1)}, u32[]{:S(2)}, u32[]{:S(2)}) collective-permute-start(bf16[16,1024]{1,0:T(8,128)(2,1)S(1)} %get-tuple-element.34), channel_id=1, source_target_pairs={{8,0},{12,4},{0,8},{4,12},{9,1},{13,5},{1,9},{5,13},{10,2},{14,6},... | collective-permute-start | bytes 98312 | tf_op jit(solution)/shard_map/ppermute | solution.py:23
  23.8 2.3 %collective-permute-start.9 = (bf16[16,1024]{1,0:T(8,128)(2,1)S(1)}, bf16[16,1024]{1,0:T(8,128)(2,1)S(1)}, u32[]{:S(2)}, u32[]{:S(2)}) collective-permute-start(bf16[16,1024]{1,0:T(8,128)(2,1)S(1)} %get-tuple-element.34), channel_id=1, source_target_pairs={{4,0},{0,4},{12,8},{8,12},{5,1},{1,5},{13,9},{9,13},{6,2},{2,6},{1... | collective-permute-start | bytes 98312 | tf_op jit(solution)/shard_map/ppermute | solution.py:23
  26.1 1.4 %collective-permute-done.11.refs_4_ = bf16[16,1024]{1,0:T(8,128)(2,1)S(1)} collective-permute-done((bf16[16,1024]{1,0:T(8,128)(2,1)S(1)}, bf16[16,1024]{1,0:T(8,128)(2,1)S(1)}, u32[]{:S(2)}, u32[]{:S(2)}) %collective-permute-start.11) | collective-permute-done | bytes 32800 | tf_op jit(solution)/shard_map/ppermute | solution.py:23
  28.3 0.7 %project_next.1 = (bf16[16,1024]{1,0:T(8,128)(2,1)S(1)}, f32[4,2176]{1,0:T(4,128)S(1)}, bf16[4,2176]{1,0:T(4,128)(2,1)S(1)}, bf16[4,2176]{1,0:T(4,128)(2,1)S(1)}, bf16[4,2176]{1,0:T(4,128)(2,1)S(1)}) custom-call(bf16[16,1024]{1,0:T(8,128)(2,1)S(1)} %get-tuple-element.27.refs_0_, f32[16,1024]{1,0:T(8,128)S(1)} %get-tuple-element.33.refs_1_, ...), custom_call_target="tpu_custom_call" | custom-call | tf_op jit(solution)/shard_map/project_next/pallas_call | solution.py:192
  29.0 1.4 %collective-permute-start.13 = (bf16[4,2176]{1,0:T(4,128)(2,1)S(1)}, bf16[4,2176]{1,0:T(4,128)(2,1)S(1)}, u32[]{:S(2)}, u32[]{:S(2)}) collective-permute-start(bf16[4,2176]{1,0:T(4,128)(2,1)S(1)} %get-tuple-element.37), channel_id=1, source_target_pairs={{0,2},{1,3},{2,0},{3,1},{4,6},{5,7},{6,4},{7,5},{8,10},{9,11},{10,... | collective-permute-start | bytes 52232 | tf_op jit(solution)/shard_map/ppermute | solution.py:27
  30.9 1.9 %collective-permute-done.13.refs_2_ = bf16[4,2176]{1,0:T(4,128)(2,1)S(1)} collective-permute-done((bf16[4,2176]{1,0:T(4,128)(2,1)S(1)}, bf16[4,2176]{1,0:T(4,128)(2,1)S(1)}, u32[]{:S(2)}, u32[]{:S(2)}) %collective-permute-start.13) | collective-permute-done | bytes 17440 | tf_op jit(solution)/shard_map/ppermute | solution.py:27
  32.8 0.8 %collective-permute-done.14.refs_3_ = bf16[4,2176]{1,0:T(4,128)(2,1)S(1)} collective-permute-done((bf16[4,2176]{1,0:T(4,128)(2,1)S(1)}, bf16[4,2176]{1,0:T(4,128)(2,1)S(1)}, u32[]{:S(2)}, u32[]{:S(2)}) %collective-permute-start.14) | collective-permute-done | bytes 17440 | tf_op jit(solution)/shard_map/ppermute | solution.py:27
  33.6 0.6 %recur.3 = (bf16[4,512]{1,0:T(4,128)(2,1)S(1)}, f32[4,3,512]{2,1,0:T(4,128)S(1)}) custom-call(f32[4,2176]{1,0:T(4,128)S(1)} %get-tuple-element.35.refs_0_, bf16[4,2176]{1,0:T(4,128)(2,1)S(1)} %collective-permute-done.12.refs_1_, bf16[4,2176]{1,0:T(4,128)(2,1)S(1)} %collective-permute-done.13.refs_2_, bf16[4,2176]{1,0:T(4,128)(2,1)S(1)} %collective-permute-done.14.refs_3_, ...), custom_call_target="tpu_custom_call" | custom-call | tf_op jit(solution)/shard_map/recur/pallas_call | solution.py:192
  34.7 1.3 %collective-permute-start.16 = (bf16[4,512]{1,0:T(4,128)(2,1)S(1)}, bf16[4,512]{1,0:T(4,128)(2,1)S(1)}, u32[]{:S(2)}, u32[]{:S(2)}) collective-permute-start(bf16[4,512]{1,0:T(4,128)(2,1)S(1)} %get-tuple-element.39.refs_0_), channel_id=1, source_target_pairs={{2,0},{3,1},{0,2},{1,3},{6,4},{7,5},{4,6},{5,7},{10,8},{11,9},{8,1... | collective-permute-start | bytes 12296 | tf_op jit(solution)/shard_map/ppermute | solution.py:23
  36.0 1.2 %collective-permute-done.17.refs_3_ = bf16[4,512]{1,0:T(4,128)(2,1)S(1)} collective-permute-done((bf16[4,512]{1,0:T(4,128)(2,1)S(1)}, bf16[4,512]{1,0:T(4,128)(2,1)S(1)}, u32[]{:S(2)}, u32[]{:S(2)}) %collective-permute-start.17) | collective-permute-done | bytes 4128 | tf_op jit(solution)/shard_map/ppermute | solution.py:23
  37.2 1.1 %collective-permute-done.16.refs_2_ = bf16[4,512]{1,0:T(4,128)(2,1)S(1)} collective-permute-done((bf16[4,512]{1,0:T(4,128)(2,1)S(1)}, bf16[4,512]{1,0:T(4,128)(2,1)S(1)}, u32[]{:S(2)}, u32[]{:S(2)}) %collective-permute-start.16) | collective-permute-done | bytes 4128 | tf_op jit(solution)/shard_map/ppermute | solution.py:23
  38.7 1.8 %collective-permute-start.18 = (bf16[4,1024]{1,0:T(4,128)(2,1)S(1)}, bf16[4,1024]{1,0:T(4,128)(2,1)S(1)}, u32[]{:S(2)}, u32[]{:S(2)}) collective-permute-start(bf16[4,1024]{1,0:T(4,128)(2,1)S(1)} %get-tuple-element.43), channel_id=1, source_target_pairs={{0,4},{4,0},{8,12},{12,8},{1,5},{5,1},{9,13},{13,9},{2,6},{6,2},{1... | collective-permute-start | bytes 24584 | tf_op jit(solution)/shard_map/ppermute | solution.py:27
  40.4 1.2 %collective-permute-start.19 = (bf16[4,1024]{1,0:T(4,128)(2,1)S(1)}, bf16[4,1024]{1,0:T(4,128)(2,1)S(1)}, u32[]{:S(2)}, u32[]{:S(2)}) collective-permute-start(bf16[4,1024]{1,0:T(4,128)(2,1)S(1)} %get-tuple-element.44), channel_id=1, source_target_pairs={{0,8},{4,12},{8,0},{12,4},{1,9},{5,13},{9,1},{13,5},{2,10},{6,14},... | collective-permute-start | bytes 24584 | tf_op jit(solution)/shard_map/ppermute | solution.py:27
  41.7 1.5 %collective-permute-start.20 = (bf16[4,1024]{1,0:T(4,128)(2,1)S(1)}, bf16[4,1024]{1,0:T(4,128)(2,1)S(1)}, u32[]{:S(2)}, u32[]{:S(2)}) collective-permute-start(bf16[4,1024]{1,0:T(4,128)(2,1)S(1)} %get-tuple-element.45), channel_id=1, source_target_pairs={{0,12},{4,8},{8,4},{12,0},{1,13},{5,9},{9,5},{13,1},{2,14},{6,10},... | collective-permute-start | bytes 24584 | tf_op jit(solution)/shard_map/ppermute | solution.py:27
  43.1 1.3 %update.2.refs_0_ = f32[2,4,4,128,128]{4,3,2,1,0:T(8,128)} custom-call(f32[4,3,512]{2,1,0:T(4,128)S(1)} %get-tuple-element.47.gates, f32[2,4,4,128,128]{4,3,2,1,0:T(8,128)S(1)} %copy-done), custom_call_target="tpu_custom_call" | custom-call | tf_op jit(solution)/shard_map/update/pallas_call | solution.py:265
  44.5 1.4 %update.3 = f32[2,4,4,128,128]{4,3,2,1,0:T(8,128)} custom-call(f32[4,3,512]{2,1,0:T(4,128)S(1)} %get-tuple-element.46.gates, f32[2,4,4,128,128]{4,3,2,1,0:T(8,128)S(1)} %copy-done, f32[2,4,4,128,128]{4,3,2,1,0:T(8,128)} %update.2.refs_0_), custom_call_target="tpu_custom_call", output_to_operand_aliasing={{}: (2, {})} | custom-call | tf_op jit(solution)/shard_map/update/pallas_call | solution.py:265
  45.9 1.3 %collective-permute-done.20.refs_2_ = bf16[4,1024]{1,0:T(4,128)(2,1)S(1)} collective-permute-done((bf16[4,1024]{1,0:T(4,128)(2,1)S(1)}, bf16[4,1024]{1,0:T(4,128)(2,1)S(1)}, u32[]{:S(2)}, u32[]{:S(2)}) %collective-permute-start.20) | collective-permute-done | bytes 8224 | tf_op jit(solution)/shard_map/ppermute | solution.py:27
  47.1 0.6 %close.1 = bf16[4,1024]{1,0:T(4,128)(2,1)} custom-call(f32[4,1024]{1,0:T(4,128)S(1)} %get-tuple-element.42.own, bf16[4,1024]{1,0:T(4,128)(2,1)S(1)} %collective-permute-done.18.refs_0_, bf16[4,1024]{1,0:T(4,128)(2,1)S(1)} %collective-permute-done.19.refs_1_, bf16[4,1024]{1,0:T(4,128)(2,1)S(1)} %collective-permute-done.20.refs_2_), custom_call_target="tpu_custom_call" | custom-call | tf_op jit(solution)/shard_map/close/pallas_call | solution.py:298
  (40 shorter events, 3.3 us)
Async XLA Ops:
  0.6 10.6 %copy-start.4 = (bf16[2,1024,512]{2,1,0:T(8,128)(2,1)S(1)}, bf16[2,1024,512]{2,1,0:T(8,128)(2,1)}, u32[]{:S(2)}) copy-start(bf16[2,1024,512]{2,1,0:T(8,128)(2,1)} %refs_9_.3) | copy-start | bytes 6291460
  0.6 10.6 %copy-start.3 = (bf16[2,1024,512]{2,1,0:T(8,128)(2,1)S(1)}, bf16[2,1024,512]{2,1,0:T(8,128)(2,1)}, u32[]{:S(2)}) copy-start(bf16[2,1024,512]{2,1,0:T(8,128)(2,1)} %refs_8_.3) | copy-start | bytes 6291460
  0.7 10.6 %copy-start.2 = (bf16[2,1024,512]{2,1,0:T(8,128)(2,1)S(1)}, bf16[2,1024,512]{2,1,0:T(8,128)(2,1)}, u32[]{:S(2)}) copy-start(bf16[2,1024,512]{2,1,0:T(8,128)(2,1)} %refs_7_.3) | copy-start | bytes 6291460
  0.7 10.6 %copy-start.1 = (bf16[2,1024,512]{2,1,0:T(8,128)(2,1)S(1)}, bf16[2,1024,512]{2,1,0:T(8,128)(2,1)}, u32[]{:S(2)}) copy-start(bf16[2,1024,512]{2,1,0:T(8,128)(2,1)} %refs_6_.6) | copy-start | bytes 6291460
  0.7 10.6 %copy-start.6 = (f32[2,1024]{1,0:T(2,128)S(1)}, f32[2,1024]{1,0:T(2,128)}, u32[]{:S(2)}) copy-start(f32[2,1024]{1,0:T(2,128)} %refs_5_.6) | copy-start | bytes 24580
  0.7 0.8 %copy-start.9 = (bf16[4,1024]{1,0:T(4,128)(2,1)S(1)}, bf16[4,1024]{1,0:T(4,128)(2,1)}, u32[]{:S(2)}) copy-start(bf16[4,1024]{1,0:T(4,128)(2,1)} %tokens.1) | copy-start | bytes 24580
  1.5 6.8 %collective-permute-start.2 = (bf16[4,1024]{1,0:T(4,128)(2,1)S(1)}, bf16[4,1024]{1,0:T(4,128)(2,1)S(1)}, u32[]{:S(2)}, u32[]{:S(2)}) collective-permute-start(bf16[4,1024]{1,0:T(4,128)(2,1)S(1)} %get-tuple-element.25.refs_0_), channel_id=1, source_target_pairs={{12,0},{8,4},{4,8},{0,12},{13,1},{9,5},{5,9},{1,13},{14,2},{10,6},... | collective-permute-start | bytes 24584 | tf_op jit(solution)/shard_map/ppermute | solution.py:23
  6.7 4.5 %collective-permute-start.1 = (bf16[4,1024]{1,0:T(4,128)(2,1)S(1)}, bf16[4,1024]{1,0:T(4,128)(2,1)S(1)}, u32[]{:S(2)}, u32[]{:S(2)}) collective-permute-start(bf16[4,1024]{1,0:T(4,128)(2,1)S(1)} %get-tuple-element.25.refs_0_), channel_id=1, source_target_pairs={{8,0},{12,4},{0,8},{4,12},{9,1},{13,5},{1,9},{5,13},{10,2},{14,6},... | collective-permute-start | bytes 24584 | tf_op jit(solution)/shard_map/ppermute | solution.py:23
  6.7 4.5 %collective-permute-start = (bf16[4,1024]{1,0:T(4,128)(2,1)S(1)}, bf16[4,1024]{1,0:T(4,128)(2,1)S(1)}, u32[]{:S(2)}, u32[]{:S(2)}) collective-permute-start(bf16[4,1024]{1,0:T(4,128)(2,1)S(1)} %get-tuple-element.25.refs_0_), channel_id=1, source_target_pairs={{4,0},{0,4},{12,8},{8,12},{5,1},{1,5},{13,9},{9,13},{6,2},{2,6},{1... | collective-permute-start | bytes 24584 | tf_op jit(solution)/shard_map/ppermute | solution.py:23
  11.3 5.6 %copy-start = (f32[2,4,4,128,128]{4,3,2,1,0:T(8,128)S(1)}, f32[2,4,4,128,128]{4,3,2,1,0:T(8,128)}, u32[]{:S(2)}) copy-start(f32[2,4,4,128,128]{4,3,2,1,0:T(8,128)} %state.3) | copy-start | bytes 6291460
  11.3 5.6 %copy-start.7 = (f32[2,512]{1,0:T(2,128)S(1)}, f32[2,512]{1,0:T(2,128)}, u32[]{:S(2)}) copy-start(f32[2,512]{1,0:T(2,128)} %refs_4_.6) | copy-start | bytes 12292
  11.3 5.6 %copy-start.8 = (f32[2,128]{1,0:T(2,128)S(1)}, f32[2,128]{1,0:T(2,128)}, u32[]{:S(2)}) copy-start(f32[2,128]{1,0:T(2,128)} %refs_5_.7) | copy-start | bytes 3076
  12.1 9.4 %copy-start.5 = (bf16[2,512,1024]{2,1,0:T(8,128)(2,1)S(1)}, bf16[2,512,1024]{2,1,0:T(8,128)(2,1)}, u32[]{:S(2)}) copy-start(bf16[2,512,1024]{2,1,0:T(8,128)(2,1)} %refs_4_.7) | copy-start | bytes 6291460
  12.1 1.9 %collective-permute-start.3 = (bf16[4,2176]{1,0:T(4,128)(2,1)S(1)}, bf16[4,2176]{1,0:T(4,128)(2,1)S(1)}, u32[]{:S(2)}, u32[]{:S(2)}) collective-permute-start(bf16[4,2176]{1,0:T(4,128)(2,1)S(1)} %get-tuple-element.29), channel_id=1, source_target_pairs={{0,1},{1,0},{2,3},{3,2},{4,5},{5,4},{6,7},{7,6},{8,9},{9,8},{10,11... | collective-permute-start | bytes 52232 | tf_op jit(solution)/shard_map/ppermute | solution.py:27
  12.1 3.8 %collective-permute-start.4 = (bf16[4,2176]{1,0:T(4,128)(2,1)S(1)}, bf16[4,2176]{1,0:T(4,128)(2,1)S(1)}, u32[]{:S(2)}, u32[]{:S(2)}) collective-permute-start(bf16[4,2176]{1,0:T(4,128)(2,1)S(1)} %get-tuple-element.30), channel_id=1, source_target_pairs={{0,2},{1,3},{2,0},{3,1},{4,6},{5,7},{6,4},{7,5},{8,10},{9,11},{10,... | collective-permute-start | bytes 52232 | tf_op jit(solution)/shard_map/ppermute | solution.py:27
  13.7 3.2 %collective-permute-start.5 = (bf16[4,2176]{1,0:T(4,128)(2,1)S(1)}, bf16[4,2176]{1,0:T(4,128)(2,1)S(1)}, u32[]{:S(2)}, u32[]{:S(2)}) collective-permute-start(bf16[4,2176]{1,0:T(4,128)(2,1)S(1)} %get-tuple-element.31), channel_id=1, source_target_pairs={{0,3},{1,2},{2,1},{3,0},{4,7},{5,6},{6,5},{7,4},{8,11},{9,10},{10,... | collective-permute-start | bytes 52232 | tf_op jit(solution)/shard_map/ppermute | solution.py:27
  17.4 3.0 %collective-permute-start.8 = (bf16[4,512]{1,0:T(4,128)(2,1)S(1)}, bf16[4,512]{1,0:T(4,128)(2,1)S(1)}, u32[]{:S(2)}, u32[]{:S(2)}) collective-permute-start(bf16[4,512]{1,0:T(4,128)(2,1)S(1)} %get-tuple-element.32.refs_0_), channel_id=1, source_target_pairs={{3,0},{2,1},{1,2},{0,3},{7,4},{6,5},{5,6},{4,7},{11,8},{10,9},{9,1... | collective-permute-start | bytes 12296 | tf_op jit(solution)/shard_map/ppermute | solution.py:23
  17.8 3.6 %collective-permute-start.7 = (bf16[4,512]{1,0:T(4,128)(2,1)S(1)}, bf16[4,512]{1,0:T(4,128)(2,1)S(1)}, u32[]{:S(2)}, u32[]{:S(2)}) collective-permute-start(bf16[4,512]{1,0:T(4,128)(2,1)S(1)} %get-tuple-element.32.refs_0_), channel_id=1, source_target_pairs={{2,0},{3,1},{0,2},{1,3},{6,4},{7,5},{4,6},{5,7},{10,8},{11,9},{8,1... | collective-permute-start | bytes 12296 | tf_op jit(solution)/shard_map/ppermute | solution.py:23
  19.2 2.2 %collective-permute-start.6 = (bf16[4,512]{1,0:T(4,128)(2,1)S(1)}, bf16[4,512]{1,0:T(4,128)(2,1)S(1)}, u32[]{:S(2)}, u32[]{:S(2)}) collective-permute-start(bf16[4,512]{1,0:T(4,128)(2,1)S(1)} %get-tuple-element.32.refs_0_), channel_id=1, source_target_pairs={{1,0},{0,1},{3,2},{2,3},{5,4},{4,5},{7,6},{6,7},{9,8},{8,9},{11,10... | collective-permute-start | bytes 12296 | tf_op jit(solution)/shard_map/ppermute | solution.py:23
  21.7 5.8 %collective-permute-start.11 = (bf16[16,1024]{1,0:T(8,128)(2,1)S(1)}, bf16[16,1024]{1,0:T(8,128)(2,1)S(1)}, u32[]{:S(2)}, u32[]{:S(2)}) collective-permute-start(bf16[16,1024]{1,0:T(8,128)(2,1)S(1)} %get-tuple-element.34), channel_id=1, source_target_pairs={{12,0},{8,4},{4,8},{0,12},{13,1},{9,5},{5,9},{1,13},{14,2},{10,6},... | collective-permute-start | bytes 98312 | tf_op jit(solution)/shard_map/ppermute | solution.py:23
  23.2 4.8 %collective-permute-start.10 = (bf16[16,1024]{1,0:T(8,128)(2,1)S(1)}, bf16[16,1024]{1,0:T(8,128)(2,1)S(1)}, u32[]{:S(2)}, u32[]{:S(2)}) collective-permute-start(bf16[16,1024]{1,0:T(8,128)(2,1)S(1)} %get-tuple-element.34), channel_id=1, source_target_pairs={{8,0},{12,4},{0,8},{4,12},{9,1},{13,5},{1,9},{5,13},{10,2},{14,6},... | collective-permute-start | bytes 98312 | tf_op jit(solution)/shard_map/ppermute | solution.py:23
  23.8 4.6 %collective-permute-start.9 = (bf16[16,1024]{1,0:T(8,128)(2,1)S(1)}, bf16[16,1024]{1,0:T(8,128)(2,1)S(1)}, u32[]{:S(2)}, u32[]{:S(2)}) collective-permute-start(bf16[16,1024]{1,0:T(8,128)(2,1)S(1)} %get-tuple-element.34), channel_id=1, source_target_pairs={{4,0},{0,4},{12,8},{8,12},{5,1},{1,5},{13,9},{9,13},{6,2},{2,6},{1... | collective-permute-start | bytes 98312 | tf_op jit(solution)/shard_map/ppermute | solution.py:23
  29.0 1.9 %collective-permute-start.12 = (bf16[4,2176]{1,0:T(4,128)(2,1)S(1)}, bf16[4,2176]{1,0:T(4,128)(2,1)S(1)}, u32[]{:S(2)}, u32[]{:S(2)}) collective-permute-start(bf16[4,2176]{1,0:T(4,128)(2,1)S(1)} %get-tuple-element.36), channel_id=1, source_target_pairs={{0,1},{1,0},{2,3},{3,2},{4,5},{5,4},{6,7},{7,6},{8,9},{9,8},{10,11... | collective-permute-start | bytes 52232 | tf_op jit(solution)/shard_map/ppermute | solution.py:27
  29.0 3.8 %collective-permute-start.13 = (bf16[4,2176]{1,0:T(4,128)(2,1)S(1)}, bf16[4,2176]{1,0:T(4,128)(2,1)S(1)}, u32[]{:S(2)}, u32[]{:S(2)}) collective-permute-start(bf16[4,2176]{1,0:T(4,128)(2,1)S(1)} %get-tuple-element.37), channel_id=1, source_target_pairs={{0,2},{1,3},{2,0},{3,1},{4,6},{5,7},{6,4},{7,5},{8,10},{9,11},{10,... | collective-permute-start | bytes 52232 | tf_op jit(solution)/shard_map/ppermute | solution.py:27
  30.4 3.2 %collective-permute-start.14 = (bf16[4,2176]{1,0:T(4,128)(2,1)S(1)}, bf16[4,2176]{1,0:T(4,128)(2,1)S(1)}, u32[]{:S(2)}, u32[]{:S(2)}) collective-permute-start(bf16[4,2176]{1,0:T(4,128)(2,1)S(1)} %get-tuple-element.38), channel_id=1, source_target_pairs={{0,3},{1,2},{2,1},{3,0},{4,7},{5,6},{6,5},{7,4},{8,11},{9,10},{10,... | collective-permute-start | bytes 52232 | tf_op jit(solution)/shard_map/ppermute | solution.py:27
  34.2 3.0 %collective-permute-start.17 = (bf16[4,512]{1,0:T(4,128)(2,1)S(1)}, bf16[4,512]{1,0:T(4,128)(2,1)S(1)}, u32[]{:S(2)}, u32[]{:S(2)}) collective-permute-start(bf16[4,512]{1,0:T(4,128)(2,1)S(1)} %get-tuple-element.39.refs_0_), channel_id=1, source_target_pairs={{3,0},{2,1},{1,2},{0,3},{7,4},{6,5},{5,6},{4,7},{11,8},{10,9},{9,1... | collective-permute-start | bytes 12296 | tf_op jit(solution)/shard_map/ppermute | solution.py:23
  34.7 3.6 %collective-permute-start.16 = (bf16[4,512]{1,0:T(4,128)(2,1)S(1)}, bf16[4,512]{1,0:T(4,128)(2,1)S(1)}, u32[]{:S(2)}, u32[]{:S(2)}) collective-permute-start(bf16[4,512]{1,0:T(4,128)(2,1)S(1)} %get-tuple-element.39.refs_0_), channel_id=1, source_target_pairs={{2,0},{3,1},{0,2},{1,3},{6,4},{7,5},{4,6},{5,7},{10,8},{11,9},{8,1... | collective-permute-start | bytes 12296 | tf_op jit(solution)/shard_map/ppermute | solution.py:23
  36.0 2.3 %collective-permute-start.15 = (bf16[4,512]{1,0:T(4,128)(2,1)S(1)}, bf16[4,512]{1,0:T(4,128)(2,1)S(1)}, u32[]{:S(2)}, u32[]{:S(2)}) collective-permute-start(bf16[4,512]{1,0:T(4,128)(2,1)S(1)} %get-tuple-element.39.refs_0_), channel_id=1, source_target_pairs={{1,0},{0,1},{3,2},{2,3},{5,4},{4,5},{7,6},{6,7},{9,8},{8,9},{11,10... | collective-permute-start | bytes 12296 | tf_op jit(solution)/shard_map/ppermute | solution.py:23
  38.7 7.2 %collective-permute-start.18 = (bf16[4,1024]{1,0:T(4,128)(2,1)S(1)}, bf16[4,1024]{1,0:T(4,128)(2,1)S(1)}, u32[]{:S(2)}, u32[]{:S(2)}) collective-permute-start(bf16[4,1024]{1,0:T(4,128)(2,1)S(1)} %get-tuple-element.43), channel_id=1, source_target_pairs={{0,4},{4,0},{8,12},{12,8},{1,5},{5,1},{9,13},{13,9},{2,6},{6,2},{1... | collective-permute-start | bytes 24584 | tf_op jit(solution)/shard_map/ppermute | solution.py:27
  40.4 5.4 %collective-permute-start.19 = (bf16[4,1024]{1,0:T(4,128)(2,1)S(1)}, bf16[4,1024]{1,0:T(4,128)(2,1)S(1)}, u32[]{:S(2)}, u32[]{:S(2)}) collective-permute-start(bf16[4,1024]{1,0:T(4,128)(2,1)S(1)} %get-tuple-element.44), channel_id=1, source_target_pairs={{0,8},{4,12},{8,0},{12,4},{1,9},{5,13},{9,1},{13,5},{2,10},{6,14},... | collective-permute-start | bytes 24584 | tf_op jit(solution)/shard_map/ppermute | solution.py:27
  41.7 5.4 %collective-permute-start.20 = (bf16[4,1024]{1,0:T(4,128)(2,1)S(1)}, bf16[4,1024]{1,0:T(4,128)(2,1)S(1)}, u32[]{:S(2)}, u32[]{:S(2)}) collective-permute-start(bf16[4,1024]{1,0:T(4,128)(2,1)S(1)} %get-tuple-element.45), channel_id=1, source_target_pairs={{0,12},{4,8},{8,4},{12,0},{1,13},{5,9},{9,5},{13,1},{2,14},{6,10},... | collective-permute-start | bytes 24584 | tf_op jit(solution)/shard_map/ppermute | solution.py:27

commit v4 on v3

--- a/solution.py
+++ b/solution.py
@@ -7,6 +7,7 @@
 from jax.experimental.pallas import tpu as pltpu
 from jax.sharding import PartitionSpec as P
 
+
 F32, BF16 = jnp.float32, jnp.bfloat16
 LANES = 128
 VMEM = pl.BlockSpec(memory_space=pltpu.VMEM)
@@ -19,12 +20,18 @@
     return (index + k) % n
 
 
-def swap(array, axis, n, k):
-    return lax.ppermute(array, axis, [(peer_of(n, k, i), i) for i in range(n)])
-
-
-def send(array, axis, n, k):
-    return lax.ppermute(array, axis, [(i, peer_of(n, k, i)) for i in range(n)])
+def exchange(axis, n, arrays, inward=False):
+    parts = [None] * (n - 1)
+    for k in reversed(range(1, n)):
+        pairs = [(i, peer_of(n, k, i)) for i in range(n)]
+        parts[k - 1] = lax.ppermute(
+            arrays[k - 1], axis, [(b, a) for a, b in pairs] if inward else pairs
+        )
+    return parts
+
+
+def gather(axis, n, array):
+    return [array] + exchange(axis, n, [array] * (n - 1), inward=True)
 
 
 def split(array):
@@ -36,7 +43,7 @@
     count = outs[0].shape[0]
     squares = jnp.sum(base * base, axis=1, keepdims=True)
     scaled = (base * gain_ref[layer : layer + 1, :]).astype(BF16)
-    high, rest = split(squares)
+    high, _ = split(squares)
     high = high.astype(F32)
     middle, low = split(squares - high)
     lane = lax.broadcasted_iota(jnp.int32, (base.shape[0], LANES), 1)
@@ -55,7 +62,7 @@
         out[:, 4 * width :] = tail[k * count : (k + 1) * count].astype(out.dtype)
 
 
-def project_first(n_tp, n_dp, layer, *refs):
+def project_first(n_tp, layer, *refs):
     parts, (order, gain), weights = refs[:n_tp], refs[n_tp : n_tp + 2], refs[n_tp + 2 : n_tp + 6]
     base_out, outs, slots = refs[n_tp + 6], refs[n_tp + 7 : -1], refs[-1]
     rows = parts[0].shape[0]
@@ -66,7 +73,7 @@
     finish_projection(base, gain, layer, weights, outs)
 
 
-def project_next(n_tp, n_dp, layer, *refs):
+def project_next(n_tp, layer, *refs):
     (base_in, mixed), parts = refs[:2], refs[2 : n_tp + 1]
     gain, weights = refs[n_tp + 1], refs[n_tp + 2 : n_tp + 6]
     base_out, outs = refs[n_tp + 6], refs[n_tp + 7 :]
@@ -188,10 +195,9 @@
     order_out[...] = jnp.where(held(0, n_tp, tp) == held(1, n_dp, dp), 1.0, 0.0).astype(BF16)
 
 
-def call(body, name, args, in_specs, outs, scratch=(), flops=None):
+def call(body, args, in_specs, outs, scratch=(), flops=None):
     return pl.pallas_call(
         body,
-        name=name,
         out_shape=[pltpu.VMEM(shape, dtype) for shape, dtype in outs],
         in_specs=in_specs,
         out_specs=[VMEM] * len(outs),
@@ -223,13 +229,12 @@
     weights = (w_query, w_forget, w_value, w_gate)
     tokens, order_in, order_out = call(
         functools.partial(stage, n_tp, n_dp),
-        "stage",
         (tokens,),
         [VMEM],
         [((rows, local), BF16)] + [((total, total), BF16)] * 2,
         flops=20_000_000_000,
     )
-    parts = [tokens] + [swap(tokens, "tp", n_tp, k) for k in range(1, n_tp)]
+    parts = gather("tp", n_tp, tokens)
     base = mixed = None
     new_state = None
     for layer in range(2):
@@ -238,8 +243,7 @@
         specs = [VMEM] * 4
         if layer == 0:
             base, own, *sent = call(
-                functools.partial(project_first, n_tp, n_dp, layer),
-                "project_first",
+                functools.partial(project_first, n_tp, layer),
                 (*parts, order_in, norm_gain, *weights),
                 [VMEM] * (n_tp + 2) + specs,
                 outs,
@@ -247,21 +251,19 @@
             )
         else:
             base, own, *sent = call(
-                functools.partial(project_next, n_tp, n_dp, layer),
-                "project_next",
+                functools.partial(project_next, n_tp, layer),
                 (base, mixed, *parts, norm_gain, *weights),
                 [VMEM] * (n_tp + 2) + specs,
                 outs,
             )
-        parts = [send(sent[k - 1], "dp", n_dp, k) for k in range(1, n_dp)]
+        parts = exchange("dp", n_dp, sent)
         normed, gates = call(
             functools.partial(recur, n_dp, layer, features),
-            "recur",
             (own, *parts, lower_bound, head_gain, state),
             [VMEM] * (n_dp + 2) + [VMEM],
             [((seqs, width), BF16), ((seqs, 3, width), F32)],
         )
-        parts = [normed] + [swap(normed, "dp", n_dp, k) for k in range(1, n_dp)]
+        parts = gather("dp", n_dp, normed)
         new_state = pl.pallas_call(
             functools.partial(update, layer),
             name="update",
@@ -278,23 +280,21 @@
         if layer == 0:
             mixed, sent = call(
                 functools.partial(mix_next, n_dp, layer),
-                "mix_next",
                 (*parts, w_out),
                 [VMEM] * n_dp + [VMEM],
                 [((total, local), F32), ((total, local), BF16)],
                 [((total, width), F32)],
             )
-            parts = [swap(sent, "tp", n_tp, k) for k in range(1, n_tp)]
+            parts = exchange("tp", n_tp, [sent] * (n_tp - 1))
         else:
             own, *sent = call(
                 functools.partial(mix_last, n_dp, layer),
-                "mix_last",
                 (*parts, w_out, base, order_out),
                 [VMEM] * n_dp + [VMEM] + [VMEM] * 2,
                 [((rows, local), F32)] + [((rows, local), BF16)] * (n_tp - 1),
                 [((total, width), F32)],
             )
-            parts = [send(sent[k - 1], "tp", n_tp, k) for k in range(1, n_tp)]
+            parts = exchange("tp", n_tp, sent)
     hidden = pl.pallas_call(
         close,
         name="close",
@@ -308,8 +308,12 @@
 
 def solution(mesh):
     n_tp, n_dp = mesh.shape["tp"], mesh.shape["dp"]
+
+    def body(*args):
+        return per_device(n_tp, n_dp, *args)
+
     return jax.shard_map(
-        functools.partial(per_device, n_tp, n_dp),
+        body,
         mesh=mesh,
         in_specs=(
             P(("grp", "tp"), "dp"),

time: 47.9 us -> 47.9 us (level)
  no operation moved by 1% of the time
where the time goes in v4:
time: 47.9 us; the launch traced here: 47.7 us
  starting transfers between devices  22.1 us (46%)
  waiting for transfers between devices  17.4 us (36%)
  Pallas kernels  6.49 us (14%)
  local copies, waits for them, and re-layouts  0.88 us (2%)
  between operations  0.81 us (2%)
    ppermute x21, starting transfers between devices, exchange(): lax.ppermute(arrays[k - 1], axis, [(b, a) for a, b in pairs] if inward el...  22.1 us
    ppermute x21, waiting for transfers between devices, exchange(): lax.ppermute(arrays[k - 1], axis, [(b, a) for a, b in pairs] if inward el...  17.4 us
    pallas_call x7, Pallas kernels, call(): pl.pallas_call(body, out_shape=[pltpu.VMEM(shape, dtype) for shape, dtype...  3.18 us
    pallas_call x2, Pallas kernels, per_device(): pl.pallas_call(functools.partial(update, layer), name='update', out_shape...  2.69 us
  transfers between devices with their start and end apart: 21, of which 14 were waited for; matrix products, arithmetic and copies ran while one was open for 0% of the time, Pallas kernels for 6%

profile of v4, /device:TPU:0, one launch (start us, length us, event | category | flops | bytes accessed | tf_op | source)
XLA Modules:
  0.0 47.7 jit_solution(305184659033133540)
XLA Ops:
  0.7 0.8 %copy-done.9 = bf16[4,1024]{1,0:T(4,128)(2,1)S(1)} copy-done((bf16[4,1024]{1,0:T(4,128)(2,1)S(1)}, bf16[4,1024]{1,0:T(4,128)(2,1)}, u32[]{:S(2)}) %copy-start.9) | copy-done | bytes 8216
  1.5 5.1 %collective-permute-start.2 = (bf16[4,1024]{1,0:T(4,128)(2,1)S(1)}, bf16[4,1024]{1,0:T(4,128)(2,1)S(1)}, u32[]{:S(2)}, u32[]{:S(2)}) collective-permute-start(bf16[4,1024]{1,0:T(4,128)(2,1)S(1)} %get-tuple-element.25.refs_0_), channel_id=1, source_target_pairs={{12,0},{8,4},{4,8},{0,12},{13,1},{9,5},{5,9},{1,13},{14,2},{10,6},... | collective-permute-start | bytes 24584 | tf_op jit(solution)/shard_map/ppermute | solution.py:27
  6.7 0.6 %collective-permute-start = (bf16[4,1024]{1,0:T(4,128)(2,1)S(1)}, bf16[4,1024]{1,0:T(4,128)(2,1)S(1)}, u32[]{:S(2)}, u32[]{:S(2)}) collective-permute-start(bf16[4,1024]{1,0:T(4,128)(2,1)S(1)} %get-tuple-element.25.refs_0_), channel_id=1, source_target_pairs={{4,0},{0,4},{12,8},{8,12},{5,1},{1,5},{13,9},{9,13},{6,2},{2,6},{1... | collective-permute-start | bytes 24584 | tf_op jit(solution)/shard_map/ppermute | solution.py:27
  7.3 1.0 %collective-permute-done.2.refs_3_ = bf16[4,1024]{1,0:T(4,128)(2,1)S(1)} collective-permute-done((bf16[4,1024]{1,0:T(4,128)(2,1)S(1)}, bf16[4,1024]{1,0:T(4,128)(2,1)S(1)}, u32[]{:S(2)}, u32[]{:S(2)}) %collective-permute-start.2) | collective-permute-done | bytes 8224 | tf_op jit(solution)/shard_map/ppermute | solution.py:27
  8.3 2.9 %collective-permute-done.1.refs_2_ = bf16[4,1024]{1,0:T(4,128)(2,1)S(1)} collective-permute-done((bf16[4,1024]{1,0:T(4,128)(2,1)S(1)}, bf16[4,1024]{1,0:T(4,128)(2,1)S(1)}, u32[]{:S(2)}, u32[]{:S(2)}) %collective-permute-start.1) | collective-permute-done | bytes 8224 | tf_op jit(solution)/shard_map/ppermute | solution.py:27
  11.3 0.8 %shard_map.114 = (bf16[16,1024]{1,0:T(8,128)(2,1)S(1)}, f32[4,2176]{1,0:T(4,128)S(1)}, bf16[4,2176]{1,0:T(4,128)(2,1)S(1)}, bf16[4,2176]{1,0:T(4,128)(2,1)S(1)}, bf16[4,2176]{1,0:T(4,128)(2,1)S(1)}) custom-call(bf16[4,1024]{1,0:T(4,128)(2,1)S(1)} %get-tuple-element.25.refs_0_, bf16[4,1024]{1,0:T(4,128)(2,1)S(1)} %collective-permute-done.refs_1_, ...), custom_call_target="tpu_custom_call" | custom-call | tf_op jit(solution)/shard_map/pallas_call | solution.py:199
  12.1 1.6 %collective-permute-start.4 = (bf16[4,2176]{1,0:T(4,128)(2,1)S(1)}, bf16[4,2176]{1,0:T(4,128)(2,1)S(1)}, u32[]{:S(2)}, u32[]{:S(2)}) collective-permute-start(bf16[4,2176]{1,0:T(4,128)(2,1)S(1)} %get-tuple-element.30), channel_id=1, source_target_pairs={{0,2},{1,3},{2,0},{3,1},{4,6},{5,7},{6,4},{7,5},{8,10},{9,11},{10,... | collective-permute-start | bytes 52232 | tf_op jit(solution)/shard_map/ppermute | solution.py:27
  14.0 2.0 %collective-permute-done.4.refs_2_ = bf16[4,2176]{1,0:T(4,128)(2,1)S(1)} collective-permute-done((bf16[4,2176]{1,0:T(4,128)(2,1)S(1)}, bf16[4,2176]{1,0:T(4,128)(2,1)S(1)}, u32[]{:S(2)}, u32[]{:S(2)}) %collective-permute-start.4) | collective-permute-done | bytes 17440 | tf_op jit(solution)/shard_map/ppermute | solution.py:27
  15.9 0.9 %collective-permute-done.5.refs_3_ = bf16[4,2176]{1,0:T(4,128)(2,1)S(1)} collective-permute-done((bf16[4,2176]{1,0:T(4,128)(2,1)S(1)}, bf16[4,2176]{1,0:T(4,128)(2,1)S(1)}, u32[]{:S(2)}, u32[]{:S(2)}) %collective-permute-start.5) | collective-permute-done | bytes 17440 | tf_op jit(solution)/shard_map/ppermute | solution.py:27
  16.9 0.6 %shard_map.115 = (bf16[4,512]{1,0:T(4,128)(2,1)S(1)}, f32[4,3,512]{2,1,0:T(4,128)S(1)}) custom-call(f32[4,2176]{1,0:T(4,128)S(1)} %get-tuple-element.28.refs_0_, bf16[4,2176]{1,0:T(4,128)(2,1)S(1)} %collective-permute-done.3.refs_1_, bf16[4,2176]{1,0:T(4,128)(2,1)S(1)} %collective-permute-done.4.refs_2_, bf16[4,2176]{1,0:T(4,128)(2,1)S(1)} %collective-permute-done.5.refs_3_, ...), custom_call_target="tpu_custom_call" | custom-call | tf_op jit(solution)/shard_map/pallas_call | solution.py:199
  17.8 1.4 %collective-permute-start.7 = (bf16[4,512]{1,0:T(4,128)(2,1)S(1)}, bf16[4,512]{1,0:T(4,128)(2,1)S(1)}, u32[]{:S(2)}, u32[]{:S(2)}) collective-permute-start(bf16[4,512]{1,0:T(4,128)(2,1)S(1)} %get-tuple-element.32.refs_0_), channel_id=1, source_target_pairs={{2,0},{3,1},{0,2},{1,3},{6,4},{7,5},{4,6},{5,7},{10,8},{11,9},{8,1... | collective-permute-start | bytes 12296 | tf_op jit(solution)/shard_map/ppermute | solution.py:27
  19.3 1.2 %collective-permute-done.8.refs_3_ = bf16[4,512]{1,0:T(4,128)(2,1)S(1)} collective-permute-done((bf16[4,512]{1,0:T(4,128)(2,1)S(1)}, bf16[4,512]{1,0:T(4,128)(2,1)S(1)}, u32[]{:S(2)}, u32[]{:S(2)}) %collective-permute-start.8) | collective-permute-done | bytes 4128 | tf_op jit(solution)/shard_map/ppermute | solution.py:27
  20.5 1.0 %collective-permute-done.7.refs_2_ = bf16[4,512]{1,0:T(4,128)(2,1)S(1)} collective-permute-done((bf16[4,512]{1,0:T(4,128)(2,1)S(1)}, bf16[4,512]{1,0:T(4,128)(2,1)S(1)}, u32[]{:S(2)}, u32[]{:S(2)}) %collective-permute-start.7) | collective-permute-done | bytes 4128 | tf_op jit(solution)/shard_map/ppermute | solution.py:27
  21.7 1.5 %collective-permute-start.11 = (bf16[16,1024]{1,0:T(8,128)(2,1)S(1)}, bf16[16,1024]{1,0:T(8,128)(2,1)S(1)}, u32[]{:S(2)}, u32[]{:S(2)}) collective-permute-start(bf16[16,1024]{1,0:T(8,128)(2,1)S(1)} %get-tuple-element.34), channel_id=1, source_target_pairs={{0,12},{4,8},{8,4},{12,0},{1,13},{5,9},{9,5},{13,1},{2,14},{6,10},... | collective-permute-start | bytes 98312 | tf_op jit(solution)/shard_map/ppermute | solution.py:27
  23.2 0.6 %collective-permute-start.10 = (bf16[16,1024]{1,0:T(8,128)(2,1)S(1)}, bf16[16,1024]{1,0:T(8,128)(2,1)S(1)}, u32[]{:S(2)}, u32[]{:S(2)}) collective-permute-start(bf16[16,1024]{1,0:T(8,128)(2,1)S(1)} %get-tuple-element.34), channel_id=1, source_target_pairs={{0,8},{4,12},{8,0},{12,4},{1,9},{5,13},{9,1},{13,5},{2,10},{6,14},... | collective-permute-start | bytes 98312 | tf_op jit(solution)/shard_map/ppermute | solution.py:27
  23.8 2.3 %collective-permute-start.9 = (bf16[16,1024]{1,0:T(8,128)(2,1)S(1)}, bf16[16,1024]{1,0:T(8,128)(2,1)S(1)}, u32[]{:S(2)}, u32[]{:S(2)}) collective-permute-start(bf16[16,1024]{1,0:T(8,128)(2,1)S(1)} %get-tuple-element.34), channel_id=1, source_target_pairs={{0,4},{4,0},{8,12},{12,8},{1,5},{5,1},{9,13},{13,9},{2,6},{6,2},{1... | collective-permute-start | bytes 98312 | tf_op jit(solution)/shard_map/ppermute | solution.py:27
  26.1 1.4 %collective-permute-done.11.refs_4_ = bf16[16,1024]{1,0:T(8,128)(2,1)S(1)} collective-permute-done((bf16[16,1024]{1,0:T(8,128)(2,1)S(1)}, bf16[16,1024]{1,0:T(8,128)(2,1)S(1)}, u32[]{:S(2)}, u32[]{:S(2)}) %collective-permute-start.11) | collective-permute-done | bytes 32800 | tf_op jit(solution)/shard_map/ppermute | solution.py:27
  28.3 0.7 %shard_map.117 = (bf16[16,1024]{1,0:T(8,128)(2,1)S(1)}, f32[4,2176]{1,0:T(4,128)S(1)}, bf16[4,2176]{1,0:T(4,128)(2,1)S(1)}, bf16[4,2176]{1,0:T(4,128)(2,1)S(1)}, bf16[4,2176]{1,0:T(4,128)(2,1)S(1)}) custom-call(bf16[16,1024]{1,0:T(8,128)(2,1)S(1)} %get-tuple-element.27.refs_0_, f32[16,1024]{1,0:T(8,128)S(1)} %get-tuple-element.33.refs_1_, ...), custom_call_target="tpu_custom_call" | custom-call | tf_op jit(solution)/shard_map/pallas_call | solution.py:199
  29.0 1.4 %collective-permute-start.13 = (bf16[4,2176]{1,0:T(4,128)(2,1)S(1)}, bf16[4,2176]{1,0:T(4,128)(2,1)S(1)}, u32[]{:S(2)}, u32[]{:S(2)}) collective-permute-start(bf16[4,2176]{1,0:T(4,128)(2,1)S(1)} %get-tuple-element.37), channel_id=1, source_target_pairs={{0,2},{1,3},{2,0},{3,1},{4,6},{5,7},{6,4},{7,5},{8,10},{9,11},{10,... | collective-permute-start | bytes 52232 | tf_op jit(solution)/shard_map/ppermute | solution.py:27
  30.9 1.9 %collective-permute-done.13.refs_2_ = bf16[4,2176]{1,0:T(4,128)(2,1)S(1)} collective-permute-done((bf16[4,2176]{1,0:T(4,128)(2,1)S(1)}, bf16[4,2176]{1,0:T(4,128)(2,1)S(1)}, u32[]{:S(2)}, u32[]{:S(2)}) %collective-permute-start.13) | collective-permute-done | bytes 17440 | tf_op jit(solution)/shard_map/ppermute | solution.py:27
  32.8 0.8 %collective-permute-done.14.refs_3_ = bf16[4,2176]{1,0:T(4,128)(2,1)S(1)} collective-permute-done((bf16[4,2176]{1,0:T(4,128)(2,1)S(1)}, bf16[4,2176]{1,0:T(4,128)(2,1)S(1)}, u32[]{:S(2)}, u32[]{:S(2)}) %collective-permute-start.14) | collective-permute-done | bytes 17440 | tf_op jit(solution)/shard_map/ppermute | solution.py:27
  33.6 0.6 %shard_map.118 = (bf16[4,512]{1,0:T(4,128)(2,1)S(1)}, f32[4,3,512]{2,1,0:T(4,128)S(1)}) custom-call(f32[4,2176]{1,0:T(4,128)S(1)} %get-tuple-element.35.refs_0_, bf16[4,2176]{1,0:T(4,128)(2,1)S(1)} %collective-permute-done.12.refs_1_, bf16[4,2176]{1,0:T(4,128)(2,1)S(1)} %collective-permute-done.13.refs_2_, ...), custom_call_target="tpu_custom_call" | custom-call | tf_op jit(solution)/shard_map/pallas_call | solution.py:199
  34.7 1.3 %collective-permute-start.16 = (bf16[4,512]{1,0:T(4,128)(2,1)S(1)}, bf16[4,512]{1,0:T(4,128)(2,1)S(1)}, u32[]{:S(2)}, u32[]{:S(2)}) collective-permute-start(bf16[4,512]{1,0:T(4,128)(2,1)S(1)} %get-tuple-element.39.refs_0_), channel_id=1, source_target_pairs={{2,0},{3,1},{0,2},{1,3},{6,4},{7,5},{4,6},{5,7},{10,8},{11,9},{8,1... | collective-permute-start | bytes 12296 | tf_op jit(solution)/shard_map/ppermute | solution.py:27
  36.0 1.2 %collective-permute-done.17.refs_3_ = bf16[4,512]{1,0:T(4,128)(2,1)S(1)} collective-permute-done((bf16[4,512]{1,0:T(4,128)(2,1)S(1)}, bf16[4,512]{1,0:T(4,128)(2,1)S(1)}, u32[]{:S(2)}, u32[]{:S(2)}) %collective-permute-start.17) | collective-permute-done | bytes 4128 | tf_op jit(solution)/shard_map/ppermute | solution.py:27
  37.2 1.1 %collective-permute-done.16.refs_2_ = bf16[4,512]{1,0:T(4,128)(2,1)S(1)} collective-permute-done((bf16[4,512]{1,0:T(4,128)(2,1)S(1)}, bf16[4,512]{1,0:T(4,128)(2,1)S(1)}, u32[]{:S(2)}, u32[]{:S(2)}) %collective-permute-start.16) | collective-permute-done | bytes 4128 | tf_op jit(solution)/shard_map/ppermute | solution.py:27
  38.7 1.8 %collective-permute-start.18 = (bf16[4,1024]{1,0:T(4,128)(2,1)S(1)}, bf16[4,1024]{1,0:T(4,128)(2,1)S(1)}, u32[]{:S(2)}, u32[]{:S(2)}) collective-permute-start(bf16[4,1024]{1,0:T(4,128)(2,1)S(1)} %get-tuple-element.43), channel_id=1, source_target_pairs={{0,4},{4,0},{8,12},{12,8},{1,5},{5,1},{9,13},{13,9},{2,6},{6,2},{1... | collective-permute-start | bytes 24584 | tf_op jit(solution)/shard_map/ppermute | solution.py:27
  40.4 1.2 %collective-permute-start.19 = (bf16[4,1024]{1,0:T(4,128)(2,1)S(1)}, bf16[4,1024]{1,0:T(4,128)(2,1)S(1)}, u32[]{:S(2)}, u32[]{:S(2)}) collective-permute-start(bf16[4,1024]{1,0:T(4,128)(2,1)S(1)} %get-tuple-element.44), channel_id=1, source_target_pairs={{0,8},{4,12},{8,0},{12,4},{1,9},{5,13},{9,1},{13,5},{2,10},{6,14},... | collective-permute-start | bytes 24584 | tf_op jit(solution)/shard_map/ppermute | solution.py:27
  41.7 1.5 %collective-permute-start.20 = (bf16[4,1024]{1,0:T(4,128)(2,1)S(1)}, bf16[4,1024]{1,0:T(4,128)(2,1)S(1)}, u32[]{:S(2)}, u32[]{:S(2)}) collective-permute-start(bf16[4,1024]{1,0:T(4,128)(2,1)S(1)} %get-tuple-element.45), channel_id=1, source_target_pairs={{0,12},{4,8},{8,4},{12,0},{1,13},{5,9},{9,5},{13,1},{2,14},{6,10},... | collective-permute-start | bytes 24584 | tf_op jit(solution)/shard_map/ppermute | solution.py:27
  43.1 1.3 %update.2.refs_0_ = f32[2,4,4,128,128]{4,3,2,1,0:T(8,128)} custom-call(f32[4,3,512]{2,1,0:T(4,128)S(1)} %get-tuple-element.47.gates, f32[2,4,4,128,128]{4,3,2,1,0:T(8,128)S(1)} %copy-done), custom_call_target="tpu_custom_call" | custom-call | tf_op jit(solution)/shard_map/update/pallas_call | solution.py:267
  44.5 1.4 %update.3 = f32[2,4,4,128,128]{4,3,2,1,0:T(8,128)} custom-call(f32[4,3,512]{2,1,0:T(4,128)S(1)} %get-tuple-element.46.gates, f32[2,4,4,128,128]{4,3,2,1,0:T(8,128)S(1)} %copy-done, f32[2,4,4,128,128]{4,3,2,1,0:T(8,128)} %update.2.refs_0_), custom_call_target="tpu_custom_call", output_to_operand_aliasing={{}: (2, {})} | custom-call | tf_op jit(solution)/shard_map/update/pallas_call | solution.py:267
  45.9 1.3 %collective-permute-done.20.refs_2_ = bf16[4,1024]{1,0:T(4,128)(2,1)S(1)} collective-permute-done((bf16[4,1024]{1,0:T(4,128)(2,1)S(1)}, bf16[4,1024]{1,0:T(4,128)(2,1)S(1)}, u32[]{:S(2)}, u32[]{:S(2)}) %collective-permute-start.20) | collective-permute-done | bytes 8224 | tf_op jit(solution)/shard_map/ppermute | solution.py:27
  47.1 0.6 %close.1 = bf16[4,1024]{1,0:T(4,128)(2,1)} custom-call(f32[4,1024]{1,0:T(4,128)S(1)} %get-tuple-element.42.own, bf16[4,1024]{1,0:T(4,128)(2,1)S(1)} %collective-permute-done.18.refs_0_, bf16[4,1024]{1,0:T(4,128)(2,1)S(1)} %collective-permute-done.19.refs_1_, bf16[4,1024]{1,0:T(4,128)(2,1)S(1)} %collective-permute-done.20.refs_2_), custom_call_target="tpu_custom_call" | custom-call | tf_op jit(solution)/shard_map/close/pallas_call | solution.py:298
  (40 shorter events, 3.3 us)
Async XLA Ops:
  0.6 10.6 %copy-start.4 = (bf16[2,1024,512]{2,1,0:T(8,128)(2,1)S(1)}, bf16[2,1024,512]{2,1,0:T(8,128)(2,1)}, u32[]{:S(2)}) copy-start(bf16[2,1024,512]{2,1,0:T(8,128)(2,1)} %refs_9_.3) | copy-start | bytes 6291460
  0.6 10.6 %copy-start.3 = (bf16[2,1024,512]{2,1,0:T(8,128)(2,1)S(1)}, bf16[2,1024,512]{2,1,0:T(8,128)(2,1)}, u32[]{:S(2)}) copy-start(bf16[2,1024,512]{2,1,0:T(8,128)(2,1)} %refs_8_.3) | copy-start | bytes 6291460
  0.7 10.6 %copy-start.2 = (bf16[2,1024,512]{2,1,0:T(8,128)(2,1)S(1)}, bf16[2,1024,512]{2,1,0:T(8,128)(2,1)}, u32[]{:S(2)}) copy-start(bf16[2,1024,512]{2,1,0:T(8,128)(2,1)} %refs_7_.3) | copy-start | bytes 6291460
  0.7 10.6 %copy-start.1 = (bf16[2,1024,512]{2,1,0:T(8,128)(2,1)S(1)}, bf16[2,1024,512]{2,1,0:T(8,128)(2,1)}, u32[]{:S(2)}) copy-start(bf16[2,1024,512]{2,1,0:T(8,128)(2,1)} %refs_6_.6) | copy-start | bytes 6291460
  0.7 10.6 %copy-start.6 = (f32[2,1024]{1,0:T(2,128)S(1)}, f32[2,1024]{1,0:T(2,128)}, u32[]{:S(2)}) copy-start(f32[2,1024]{1,0:T(2,128)} %refs_5_.6) | copy-start | bytes 24580
  0.7 0.8 %copy-start.9 = (bf16[4,1024]{1,0:T(4,128)(2,1)S(1)}, bf16[4,1024]{1,0:T(4,128)(2,1)}, u32[]{:S(2)}) copy-start(bf16[4,1024]{1,0:T(4,128)(2,1)} %tokens.1) | copy-start | bytes 24580
  1.5 6.8 %collective-permute-start.2 = (bf16[4,1024]{1,0:T(4,128)(2,1)S(1)}, bf16[4,1024]{1,0:T(4,128)(2,1)S(1)}, u32[]{:S(2)}, u32[]{:S(2)}) collective-permute-start(bf16[4,1024]{1,0:T(4,128)(2,1)S(1)} %get-tuple-element.25.refs_0_), channel_id=1, source_target_pairs={{12,0},{8,4},{4,8},{0,12},{13,1},{9,5},{5,9},{1,13},{14,2},{10,6},... | collective-permute-start | bytes 24584 | tf_op jit(solution)/shard_map/ppermute | solution.py:27
  6.7 4.5 %collective-permute-start.1 = (bf16[4,1024]{1,0:T(4,128)(2,1)S(1)}, bf16[4,1024]{1,0:T(4,128)(2,1)S(1)}, u32[]{:S(2)}, u32[]{:S(2)}) collective-permute-start(bf16[4,1024]{1,0:T(4,128)(2,1)S(1)} %get-tuple-element.25.refs_0_), channel_id=1, source_target_pairs={{8,0},{12,4},{0,8},{4,12},{9,1},{13,5},{1,9},{5,13},{10,2},{14,6},... | collective-permute-start | bytes 24584 | tf_op jit(solution)/shard_map/ppermute | solution.py:27
  6.7 4.5 %collective-permute-start = (bf16[4,1024]{1,0:T(4,128)(2,1)S(1)}, bf16[4,1024]{1,0:T(4,128)(2,1)S(1)}, u32[]{:S(2)}, u32[]{:S(2)}) collective-permute-start(bf16[4,1024]{1,0:T(4,128)(2,1)S(1)} %get-tuple-element.25.refs_0_), channel_id=1, source_target_pairs={{4,0},{0,4},{12,8},{8,12},{5,1},{1,5},{13,9},{9,13},{6,2},{2,6},{1... | collective-permute-start | bytes 24584 | tf_op jit(solution)/shard_map/ppermute | solution.py:27
  11.3 5.6 %copy-start = (f32[2,4,4,128,128]{4,3,2,1,0:T(8,128)S(1)}, f32[2,4,4,128,128]{4,3,2,1,0:T(8,128)}, u32[]{:S(2)}) copy-start(f32[2,4,4,128,128]{4,3,2,1,0:T(8,128)} %state.3) | copy-start | bytes 6291460
  11.3 5.6 %copy-start.7 = (f32[2,512]{1,0:T(2,128)S(1)}, f32[2,512]{1,0:T(2,128)}, u32[]{:S(2)}) copy-start(f32[2,512]{1,0:T(2,128)} %refs_4_.6) | copy-start | bytes 12292
  11.3 5.6 %copy-start.8 = (f32[2,128]{1,0:T(2,128)S(1)}, f32[2,128]{1,0:T(2,128)}, u32[]{:S(2)}) copy-start(f32[2,128]{1,0:T(2,128)} %refs_5_.7) | copy-start | bytes 3076
  12.1 9.4 %copy-start.5 = (bf16[2,512,1024]{2,1,0:T(8,128)(2,1)S(1)}, bf16[2,512,1024]{2,1,0:T(8,128)(2,1)}, u32[]{:S(2)}) copy-start(bf16[2,512,1024]{2,1,0:T(8,128)(2,1)} %refs_4_.7) | copy-start | bytes 6291460
  12.1 1.9 %collective-permute-start.3 = (bf16[4,2176]{1,0:T(4,128)(2,1)S(1)}, bf16[4,2176]{1,0:T(4,128)(2,1)S(1)}, u32[]{:S(2)}, u32[]{:S(2)}) collective-permute-start(bf16[4,2176]{1,0:T(4,128)(2,1)S(1)} %get-tuple-element.29), channel_id=1, source_target_pairs={{0,1},{1,0},{2,3},{3,2},{4,5},{5,4},{6,7},{7,6},{8,9},{9,8},{10,11... | collective-permute-start | bytes 52232 | tf_op jit(solution)/shard_map/ppermute | solution.py:27
  12.1 3.8 %collective-permute-start.4 = (bf16[4,2176]{1,0:T(4,128)(2,1)S(1)}, bf16[4,2176]{1,0:T(4,128)(2,1)S(1)}, u32[]{:S(2)}, u32[]{:S(2)}) collective-permute-start(bf16[4,2176]{1,0:T(4,128)(2,1)S(1)} %get-tuple-element.30), channel_id=1, source_target_pairs={{0,2},{1,3},{2,0},{3,1},{4,6},{5,7},{6,4},{7,5},{8,10},{9,11},{10,... | collective-permute-start | bytes 52232 | tf_op jit(solution)/shard_map/ppermute | solution.py:27
  13.7 3.2 %collective-permute-start.5 = (bf16[4,2176]{1,0:T(4,128)(2,1)S(1)}, bf16[4,2176]{1,0:T(4,128)(2,1)S(1)}, u32[]{:S(2)}, u32[]{:S(2)}) collective-permute-start(bf16[4,2176]{1,0:T(4,128)(2,1)S(1)} %get-tuple-element.31), channel_id=1, source_target_pairs={{0,3},{1,2},{2,1},{3,0},{4,7},{5,6},{6,5},{7,4},{8,11},{9,10},{10,... | collective-permute-start | bytes 52232 | tf_op jit(solution)/shard_map/ppermute | solution.py:27
  17.4 3.0 %collective-permute-start.8 = (bf16[4,512]{1,0:T(4,128)(2,1)S(1)}, bf16[4,512]{1,0:T(4,128)(2,1)S(1)}, u32[]{:S(2)}, u32[]{:S(2)}) collective-permute-start(bf16[4,512]{1,0:T(4,128)(2,1)S(1)} %get-tuple-element.32.refs_0_), channel_id=1, source_target_pairs={{3,0},{2,1},{1,2},{0,3},{7,4},{6,5},{5,6},{4,7},{11,8},{10,9},{9,1... | collective-permute-start | bytes 12296 | tf_op jit(solution)/shard_map/ppermute | solution.py:27
  17.8 3.6 %collective-permute-start.7 = (bf16[4,512]{1,0:T(4,128)(2,1)S(1)}, bf16[4,512]{1,0:T(4,128)(2,1)S(1)}, u32[]{:S(2)}, u32[]{:S(2)}) collective-permute-start(bf16[4,512]{1,0:T(4,128)(2,1)S(1)} %get-tuple-element.32.refs_0_), channel_id=1, source_target_pairs={{2,0},{3,1},{0,2},{1,3},{6,4},{7,5},{4,6},{5,7},{10,8},{11,9},{8,1... | collective-permute-start | bytes 12296 | tf_op jit(solution)/shard_map/ppermute | solution.py:27
  19.2 2.2 %collective-permute-start.6 = (bf16[4,512]{1,0:T(4,128)(2,1)S(1)}, bf16[4,512]{1,0:T(4,128)(2,1)S(1)}, u32[]{:S(2)}, u32[]{:S(2)}) collective-permute-start(bf16[4,512]{1,0:T(4,128)(2,1)S(1)} %get-tuple-element.32.refs_0_), channel_id=1, source_target_pairs={{1,0},{0,1},{3,2},{2,3},{5,4},{4,5},{7,6},{6,7},{9,8},{8,9},{11,10... | collective-permute-start | bytes 12296 | tf_op jit(solution)/shard_map/ppermute | solution.py:27
  21.7 5.8 %collective-permute-start.11 = (bf16[16,1024]{1,0:T(8,128)(2,1)S(1)}, bf16[16,1024]{1,0:T(8,128)(2,1)S(1)}, u32[]{:S(2)}, u32[]{:S(2)}) collective-permute-start(bf16[16,1024]{1,0:T(8,128)(2,1)S(1)} %get-tuple-element.34), channel_id=1, source_target_pairs={{0,12},{4,8},{8,4},{12,0},{1,13},{5,9},{9,5},{13,1},{2,14},{6,10},... | collective-permute-start | bytes 98312 | tf_op jit(solution)/shard_map/ppermute | solution.py:27
  23.2 4.8 %collective-permute-start.10 = (bf16[16,1024]{1,0:T(8,128)(2,1)S(1)}, bf16[16,1024]{1,0:T(8,128)(2,1)S(1)}, u32[]{:S(2)}, u32[]{:S(2)}) collective-permute-start(bf16[16,1024]{1,0:T(8,128)(2,1)S(1)} %get-tuple-element.34), channel_id=1, source_target_pairs={{0,8},{4,12},{8,0},{12,4},{1,9},{5,13},{9,1},{13,5},{2,10},{6,14},... | collective-permute-start | bytes 98312 | tf_op jit(solution)/shard_map/ppermute | solution.py:27
  23.8 4.6 %collective-permute-start.9 = (bf16[16,1024]{1,0:T(8,128)(2,1)S(1)}, bf16[16,1024]{1,0:T(8,128)(2,1)S(1)}, u32[]{:S(2)}, u32[]{:S(2)}) collective-permute-start(bf16[16,1024]{1,0:T(8,128)(2,1)S(1)} %get-tuple-element.34), channel_id=1, source_target_pairs={{0,4},{4,0},{8,12},{12,8},{1,5},{5,1},{9,13},{13,9},{2,6},{6,2},{1... | collective-permute-start | bytes 98312 | tf_op jit(solution)/shard_map/ppermute | solution.py:27
  29.0 1.9 %collective-permute-start.12 = (bf16[4,2176]{1,0:T(4,128)(2,1)S(1)}, bf16[4,2176]{1,0:T(4,128)(2,1)S(1)}, u32[]{:S(2)}, u32[]{:S(2)}) collective-permute-start(bf16[4,2176]{1,0:T(4,128)(2,1)S(1)} %get-tuple-element.36), channel_id=1, source_target_pairs={{0,1},{1,0},{2,3},{3,2},{4,5},{5,4},{6,7},{7,6},{8,9},{9,8},{10,11... | collective-permute-start | bytes 52232 | tf_op jit(solution)/shard_map/ppermute | solution.py:27
  29.0 3.8 %collective-permute-start.13 = (bf16[4,2176]{1,0:T(4,128)(2,1)S(1)}, bf16[4,2176]{1,0:T(4,128)(2,1)S(1)}, u32[]{:S(2)}, u32[]{:S(2)}) collective-permute-start(bf16[4,2176]{1,0:T(4,128)(2,1)S(1)} %get-tuple-element.37), channel_id=1, source_target_pairs={{0,2},{1,3},{2,0},{3,1},{4,6},{5,7},{6,4},{7,5},{8,10},{9,11},{10,... | collective-permute-start | bytes 52232 | tf_op jit(solution)/shard_map/ppermute | solution.py:27
  30.4 3.2 %collective-permute-start.14 = (bf16[4,2176]{1,0:T(4,128)(2,1)S(1)}, bf16[4,2176]{1,0:T(4,128)(2,1)S(1)}, u32[]{:S(2)}, u32[]{:S(2)}) collective-permute-start(bf16[4,2176]{1,0:T(4,128)(2,1)S(1)} %get-tuple-element.38), channel_id=1, source_target_pairs={{0,3},{1,2},{2,1},{3,0},{4,7},{5,6},{6,5},{7,4},{8,11},{9,10},{10,... | collective-permute-start | bytes 52232 | tf_op jit(solution)/shard_map/ppermute | solution.py:27
  34.2 3.0 %collective-permute-start.17 = (bf16[4,512]{1,0:T(4,128)(2,1)S(1)}, bf16[4,512]{1,0:T(4,128)(2,1)S(1)}, u32[]{:S(2)}, u32[]{:S(2)}) collective-permute-start(bf16[4,512]{1,0:T(4,128)(2,1)S(1)} %get-tuple-element.39.refs_0_), channel_id=1, source_target_pairs={{3,0},{2,1},{1,2},{0,3},{7,4},{6,5},{5,6},{4,7},{11,8},{10,9},{9,1... | collective-permute-start | bytes 12296 | tf_op jit(solution)/shard_map/ppermute | solution.py:27
  34.7 3.6 %collective-permute-start.16 = (bf16[4,512]{1,0:T(4,128)(2,1)S(1)}, bf16[4,512]{1,0:T(4,128)(2,1)S(1)}, u32[]{:S(2)}, u32[]{:S(2)}) collective-permute-start(bf16[4,512]{1,0:T(4,128)(2,1)S(1)} %get-tuple-element.39.refs_0_), channel_id=1, source_target_pairs={{2,0},{3,1},{0,2},{1,3},{6,4},{7,5},{4,6},{5,7},{10,8},{11,9},{8,1... | collective-permute-start | bytes 12296 | tf_op jit(solution)/shard_map/ppermute | solution.py:27
  36.0 2.3 %collective-permute-start.15 = (bf16[4,512]{1,0:T(4,128)(2,1)S(1)}, bf16[4,512]{1,0:T(4,128)(2,1)S(1)}, u32[]{:S(2)}, u32[]{:S(2)}) collective-permute-start(bf16[4,512]{1,0:T(4,128)(2,1)S(1)} %get-tuple-element.39.refs_0_), channel_id=1, source_target_pairs={{1,0},{0,1},{3,2},{2,3},{5,4},{4,5},{7,6},{6,7},{9,8},{8,9},{11,10... | collective-permute-start | bytes 12296 | tf_op jit(solution)/shard_map/ppermute | solution.py:27
  38.7 7.2 %collective-permute-start.18 = (bf16[4,1024]{1,0:T(4,128)(2,1)S(1)}, bf16[4,1024]{1,0:T(4,128)(2,1)S(1)}, u32[]{:S(2)}, u32[]{:S(2)}) collective-permute-start(bf16[4,1024]{1,0:T(4,128)(2,1)S(1)} %get-tuple-element.43), channel_id=1, source_target_pairs={{0,4},{4,0},{8,12},{12,8},{1,5},{5,1},{9,13},{13,9},{2,6},{6,2},{1... | collective-permute-start | bytes 24584 | tf_op jit(solution)/shard_map/ppermute | solution.py:27
  40.4 5.4 %collective-permute-start.19 = (bf16[4,1024]{1,0:T(4,128)(2,1)S(1)}, bf16[4,1024]{1,0:T(4,128)(2,1)S(1)}, u32[]{:S(2)}, u32[]{:S(2)}) collective-permute-start(bf16[4,1024]{1,0:T(4,128)(2,1)S(1)} %get-tuple-element.44), channel_id=1, source_target_pairs={{0,8},{4,12},{8,0},{12,4},{1,9},{5,13},{9,1},{13,5},{2,10},{6,14},... | collective-permute-start | bytes 24584 | tf_op jit(solution)/shard_map/ppermute | solution.py:27
  41.7 5.4 %collective-permute-start.20 = (bf16[4,1024]{1,0:T(4,128)(2,1)S(1)}, bf16[4,1024]{1,0:T(4,128)(2,1)S(1)}, u32[]{:S(2)}, u32[]{:S(2)}) collective-permute-start(bf16[4,1024]{1,0:T(4,128)(2,1)S(1)} %get-tuple-element.45), channel_id=1, source_target_pairs={{0,12},{4,8},{8,4},{12,0},{1,13},{5,9},{9,5},{13,1},{2,14},{6,10},... | collective-permute-start | bytes 24584 | tf_op jit(solution)/shard_map/ppermute | solution.py:27

commit v5 on v4

--- a/solution.py
+++ b/solution.py
@@ -181,8 +181,7 @@
     return pltpu.with_memory_space_constraint(array, pltpu.VMEM)
 
 
-def stage(n_tp, n_dp, tokens, tokens_out, order_in, order_out):
-    tokens_out[...] = tokens[...]
+def stage(n_tp, n_dp, order_in, order_out):
     total = order_in.shape[0]
 
     def held(dim, n, index):
@@ -227,11 +226,11 @@
     total = rows * n_tp
     width = heads * hd
     weights = (w_query, w_forget, w_value, w_gate)
-    tokens, order_in, order_out = call(
+    order_in, order_out = call(
         functools.partial(stage, n_tp, n_dp),
-        (tokens,),
-        [VMEM],
-        [((rows, local), BF16)] + [((total, total), BF16)] * 2,
+        (),
+        [],
+        [((total, total), BF16)] * 2,
         flops=20_000_000_000,
     )
     parts = gather("tp", n_tp, tokens)

time: 47.9 us -> 48.3 us (level)
  waiting for transfers between devices: 17.4 us -> 18.7 us
  local copies, waits for them, and re-layouts: 0.88 us -> 0.05 us
    ppermute x21, waiting for transfers between devices: 17.4 us -> 18.7 us  [exchange(): lax.ppermute(arrays[k - 1], axis, [(b, a) for a, b in pairs] if inward el...]
    unnamed x20, local copies, waits for them, and re-layouts: 0.88 us -> 0.05 us
where the time goes in v5:
time: 48.3 us; the launch traced here: 48.2 us
  starting transfers between devices  22.1 us (46%)
  waiting for transfers between devices  18.7 us (39%)
  Pallas kernels  6.49 us (13%)
  between operations  0.81 us (2%)
    ppermute x21, starting transfers between devices, exchange(): lax.ppermute(arrays[k - 1], axis, [(b, a) for a, b in pairs] if inward el...  22.1 us
    ppermute x21, waiting for transfers between devices, exchange(): lax.ppermute(arrays[k - 1], axis, [(b, a) for a, b in pairs] if inward el...  18.7 us
    pallas_call x7, Pallas kernels, call(): pl.pallas_call(body, out_shape=[pltpu.VMEM(shape, dtype) for shape, dtype...  3.18 us
    pallas_call x2, Pallas kernels, per_device(): pl.pallas_call(functools.partial(update, layer), name='update', out_shape...  2.69 us
  transfers between devices with their start and end apart: 21, of which 14 were waited for; matrix products, arithmetic and copies ran while one was open for 0% of the time, Pallas kernels for 6%

profile of v5, /device:TPU:0, one launch (start us, length us, event | category | flops | bytes accessed | tf_op | source)
XLA Modules:
  0.0 48.2 jit_solution(12436249651618746868)
XLA Ops:
  0.7 4.1 %collective-permute-start.1 = (bf16[4,1024]{1,0:T(4,128)(2,1)}, bf16[4,1024]{1,0:T(4,128)(2,1)S(1)}, u32[]{:S(2)}, u32[]{:S(2)}) collective-permute-start(bf16[4,1024]{1,0:T(4,128)(2,1)} %refs_0_.1), channel_id=1, source_target_pairs={{8,0},{12,4},{0,8},{4,12},{9,1},{13,5},{1,9},{5,13},{10,2},{14,6},... | collective-permute-start | bytes 24584 | tf_op jit(solution)/shard_map/ppermute | solution.py:27
  4.8 1.6 %collective-permute-start = (bf16[4,1024]{1,0:T(4,128)(2,1)}, bf16[4,1024]{1,0:T(4,128)(2,1)S(1)}, u32[]{:S(2)}, u32[]{:S(2)}) collective-permute-start(bf16[4,1024]{1,0:T(4,128)(2,1)} %refs_0_.1), channel_id=1, source_target_pairs={{4,0},{0,4},{12,8},{8,12},{5,1},{1,5},{13,9},{9,13},{6,2},{2,6},{1... | collective-permute-start | bytes 24584 | tf_op jit(solution)/shard_map/ppermute | solution.py:27
  6.7 2.0 %collective-permute-done.refs_1_ = bf16[4,1024]{1,0:T(4,128)(2,1)S(1)} collective-permute-done((bf16[4,1024]{1,0:T(4,128)(2,1)}, bf16[4,1024]{1,0:T(4,128)(2,1)S(1)}, u32[]{:S(2)}, u32[]{:S(2)}) %collective-permute-start) | collective-permute-done | bytes 8224 | tf_op jit(solution)/shard_map/ppermute | solution.py:27
  8.7 3.4 %collective-permute-done.2.refs_3_ = bf16[4,1024]{1,0:T(4,128)(2,1)S(1)} collective-permute-done((bf16[4,1024]{1,0:T(4,128)(2,1)}, bf16[4,1024]{1,0:T(4,128)(2,1)S(1)}, u32[]{:S(2)}, u32[]{:S(2)}) %collective-permute-start.2) | collective-permute-done | bytes 8224 | tf_op jit(solution)/shard_map/ppermute | solution.py:27
  12.1 0.8 %shard_map.114 = (bf16[16,1024]{1,0:T(8,128)(2,1)S(1)}, f32[4,2176]{1,0:T(4,128)S(1)}, bf16[4,2176]{1,0:T(4,128)(2,1)S(1)}, bf16[4,2176]{1,0:T(4,128)(2,1)S(1)}, bf16[4,2176]{1,0:T(4,128)(2,1)S(1)}) custom-call(bf16[4,1024]{1,0:T(4,128)(2,1)S(1)} %copy-done.8, bf16[4,1024]{1,0:T(4,128)(2,1)S(1)} %collective-permute-done.refs_1_, ...), custom_call_target="tpu_custom_call" | custom-call | tf_op jit(solution)/shard_map/pallas_call | solution.py:198
  12.9 1.6 %collective-permute-start.4 = (bf16[4,2176]{1,0:T(4,128)(2,1)S(1)}, bf16[4,2176]{1,0:T(4,128)(2,1)S(1)}, u32[]{:S(2)}, u32[]{:S(2)}) collective-permute-start(bf16[4,2176]{1,0:T(4,128)(2,1)S(1)} %get-tuple-element.28), channel_id=1, source_target_pairs={{0,2},{1,3},{2,0},{3,1},{4,6},{5,7},{6,4},{7,5},{8,10},{9,11},{10,... | collective-permute-start | bytes 52232 | tf_op jit(solution)/shard_map/ppermute | solution.py:27
  14.8 2.0 %collective-permute-done.4.refs_2_ = bf16[4,2176]{1,0:T(4,128)(2,1)S(1)} collective-permute-done((bf16[4,2176]{1,0:T(4,128)(2,1)S(1)}, bf16[4,2176]{1,0:T(4,128)(2,1)S(1)}, u32[]{:S(2)}, u32[]{:S(2)}) %collective-permute-start.4) | collective-permute-done | bytes 17440 | tf_op jit(solution)/shard_map/ppermute | solution.py:27
  16.7 0.9 %collective-permute-done.5.refs_3_ = bf16[4,2176]{1,0:T(4,128)(2,1)S(1)} collective-permute-done((bf16[4,2176]{1,0:T(4,128)(2,1)S(1)}, bf16[4,2176]{1,0:T(4,128)(2,1)S(1)}, u32[]{:S(2)}, u32[]{:S(2)}) %collective-permute-start.5) | collective-permute-done | bytes 17440 | tf_op jit(solution)/shard_map/ppermute | solution.py:27
  17.7 0.6 %shard_map.115 = (bf16[4,512]{1,0:T(4,128)(2,1)S(1)}, f32[4,3,512]{2,1,0:T(4,128)S(1)}) custom-call(f32[4,2176]{1,0:T(4,128)S(1)} %get-tuple-element.26.refs_0_, bf16[4,2176]{1,0:T(4,128)(2,1)S(1)} %collective-permute-done.3.refs_1_, bf16[4,2176]{1,0:T(4,128)(2,1)S(1)} %collective-permute-done.4.refs_2_, bf16[4,2176]{1,0:T(4,128)(2,1)S(1)} %collective-permute-done.5.refs_3_, ...), custom_call_target="tpu_custom_call" | custom-call | tf_op jit(solution)/shard_map/pallas_call | solution.py:198
  18.7 1.4 %collective-permute-start.7 = (bf16[4,512]{1,0:T(4,128)(2,1)S(1)}, bf16[4,512]{1,0:T(4,128)(2,1)S(1)}, u32[]{:S(2)}, u32[]{:S(2)}) collective-permute-start(bf16[4,512]{1,0:T(4,128)(2,1)S(1)} %get-tuple-element.30.refs_0_), channel_id=1, source_target_pairs={{2,0},{3,1},{0,2},{1,3},{6,4},{7,5},{4,6},{5,7},{10,8},{11,9},{8,1... | collective-permute-start | bytes 12296 | tf_op jit(solution)/shard_map/ppermute | solution.py:27
  20.1 1.2 %collective-permute-done.8.refs_3_ = bf16[4,512]{1,0:T(4,128)(2,1)S(1)} collective-permute-done((bf16[4,512]{1,0:T(4,128)(2,1)S(1)}, bf16[4,512]{1,0:T(4,128)(2,1)S(1)}, u32[]{:S(2)}, u32[]{:S(2)}) %collective-permute-start.8) | collective-permute-done | bytes 4128 | tf_op jit(solution)/shard_map/ppermute | solution.py:27
  21.3 1.0 %collective-permute-done.7.refs_2_ = bf16[4,512]{1,0:T(4,128)(2,1)S(1)} collective-permute-done((bf16[4,512]{1,0:T(4,128)(2,1)S(1)}, bf16[4,512]{1,0:T(4,128)(2,1)S(1)}, u32[]{:S(2)}, u32[]{:S(2)}) %collective-permute-start.7) | collective-permute-done | bytes 4128 | tf_op jit(solution)/shard_map/ppermute | solution.py:27
  22.7 4.3 %collective-permute-start.9 = (bf16[16,1024]{1,0:T(8,128)(2,1)S(1)}, bf16[16,1024]{1,0:T(8,128)(2,1)S(1)}, u32[]{:S(2)}, u32[]{:S(2)}) collective-permute-start(bf16[16,1024]{1,0:T(8,128)(2,1)S(1)} %get-tuple-element.32), channel_id=1, source_target_pairs={{0,4},{4,0},{8,12},{12,8},{1,5},{5,1},{9,13},{13,9},{2,6},{6,2},{1... | collective-permute-start | bytes 98312 | tf_op jit(solution)/shard_map/ppermute | solution.py:27
  26.9 1.3 %collective-permute-done.11.refs_4_ = bf16[16,1024]{1,0:T(8,128)(2,1)S(1)} collective-permute-done((bf16[16,1024]{1,0:T(8,128)(2,1)S(1)}, bf16[16,1024]{1,0:T(8,128)(2,1)S(1)}, u32[]{:S(2)}, u32[]{:S(2)}) %collective-permute-start.11) | collective-permute-done | bytes 32800 | tf_op jit(solution)/shard_map/ppermute | solution.py:27
  28.3 0.6 %collective-permute-done.9.refs_2_ = bf16[16,1024]{1,0:T(8,128)(2,1)S(1)} collective-permute-done((bf16[16,1024]{1,0:T(8,128)(2,1)S(1)}, bf16[16,1024]{1,0:T(8,128)(2,1)S(1)}, u32[]{:S(2)}, u32[]{:S(2)}) %collective-permute-start.9) | collective-permute-done | bytes 32800 | tf_op jit(solution)/shard_map/ppermute | solution.py:27
  28.8 0.7 %shard_map.117 = (bf16[16,1024]{1,0:T(8,128)(2,1)S(1)}, f32[4,2176]{1,0:T(4,128)S(1)}, bf16[4,2176]{1,0:T(4,128)(2,1)S(1)}, bf16[4,2176]{1,0:T(4,128)(2,1)S(1)}, bf16[4,2176]{1,0:T(4,128)(2,1)S(1)}) custom-call(bf16[16,1024]{1,0:T(8,128)(2,1)S(1)} %get-tuple-element.25.refs_0_, f32[16,1024]{1,0:T(8,128)S(1)} %get-tuple-element.31.refs_1_, ...), custom_call_target="tpu_custom_call" | custom-call | tf_op jit(solution)/shard_map/pallas_call | solution.py:198
  29.5 1.4 %collective-permute-start.13 = (bf16[4,2176]{1,0:T(4,128)(2,1)S(1)}, bf16[4,2176]{1,0:T(4,128)(2,1)S(1)}, u32[]{:S(2)}, u32[]{:S(2)}) collective-permute-start(bf16[4,2176]{1,0:T(4,128)(2,1)S(1)} %get-tuple-element.35), channel_id=1, source_target_pairs={{0,2},{1,3},{2,0},{3,1},{4,6},{5,7},{6,4},{7,5},{8,10},{9,11},{10,... | collective-permute-start | bytes 52232 | tf_op jit(solution)/shard_map/ppermute | solution.py:27
  30.9 0.4 collective-permute-start.14
  31.4 1.9 %collective-permute-done.13.refs_2_ = bf16[4,2176]{1,0:T(4,128)(2,1)S(1)} collective-permute-done((bf16[4,2176]{1,0:T(4,128)(2,1)S(1)}, bf16[4,2176]{1,0:T(4,128)(2,1)S(1)}, u32[]{:S(2)}, u32[]{:S(2)}) %collective-permute-start.13) | collective-permute-done | bytes 17440 | tf_op jit(solution)/shard_map/ppermute | solution.py:27
  33.3 0.8 %collective-permute-done.14.refs_3_ = bf16[4,2176]{1,0:T(4,128)(2,1)S(1)} collective-permute-done((bf16[4,2176]{1,0:T(4,128)(2,1)S(1)}, bf16[4,2176]{1,0:T(4,128)(2,1)S(1)}, u32[]{:S(2)}, u32[]{:S(2)}) %collective-permute-start.14) | collective-permute-done | bytes 17440 | tf_op jit(solution)/shard_map/ppermute | solution.py:27
  34.1 0.6 %shard_map.118 = (bf16[4,512]{1,0:T(4,128)(2,1)S(1)}, f32[4,3,512]{2,1,0:T(4,128)S(1)}) custom-call(f32[4,2176]{1,0:T(4,128)S(1)} %get-tuple-element.33.refs_0_, bf16[4,2176]{1,0:T(4,128)(2,1)S(1)} %collective-permute-done.12.refs_1_, bf16[4,2176]{1,0:T(4,128)(2,1)S(1)} %collective-permute-done.13.refs_2_, ...), custom_call_target="tpu_custom_call" | custom-call | tf_op jit(solution)/shard_map/pallas_call | solution.py:198
  34.6 0.5 %collective-permute-start.17 = (bf16[4,512]{1,0:T(4,128)(2,1)S(1)}, bf16[4,512]{1,0:T(4,128)(2,1)S(1)}, u32[]{:S(2)}, u32[]{:S(2)}) collective-permute-start(bf16[4,512]{1,0:T(4,128)(2,1)S(1)} %get-tuple-element.37.refs_0_), channel_id=1, source_target_pairs={{3,0},{2,1},{1,2},{0,3},{7,4},{6,5},{5,6},{4,7},{11,8},{10,9},{9,1... | collective-permute-start | bytes 12296 | tf_op jit(solution)/shard_map/ppermute | solution.py:27
  35.1 1.3 %collective-permute-start.16 = (bf16[4,512]{1,0:T(4,128)(2,1)S(1)}, bf16[4,512]{1,0:T(4,128)(2,1)S(1)}, u32[]{:S(2)}, u32[]{:S(2)}) collective-permute-start(bf16[4,512]{1,0:T(4,128)(2,1)S(1)} %get-tuple-element.37.refs_0_), channel_id=1, source_target_pairs={{2,0},{3,1},{0,2},{1,3},{6,4},{7,5},{4,6},{5,7},{10,8},{11,9},{8,1... | collective-permute-start | bytes 12296 | tf_op jit(solution)/shard_map/ppermute | solution.py:27
  36.5 1.2 %collective-permute-done.17.refs_3_ = bf16[4,512]{1,0:T(4,128)(2,1)S(1)} collective-permute-done((bf16[4,512]{1,0:T(4,128)(2,1)S(1)}, bf16[4,512]{1,0:T(4,128)(2,1)S(1)}, u32[]{:S(2)}, u32[]{:S(2)}) %collective-permute-start.17) | collective-permute-done | bytes 4128 | tf_op jit(solution)/shard_map/ppermute | solution.py:27
  37.7 1.1 %collective-permute-done.16.refs_2_ = bf16[4,512]{1,0:T(4,128)(2,1)S(1)} collective-permute-done((bf16[4,512]{1,0:T(4,128)(2,1)S(1)}, bf16[4,512]{1,0:T(4,128)(2,1)S(1)}, u32[]{:S(2)}, u32[]{:S(2)}) %collective-permute-start.16) | collective-permute-done | bytes 4128 | tf_op jit(solution)/shard_map/ppermute | solution.py:27
  39.1 2.1 %collective-permute-start.18 = (bf16[4,1024]{1,0:T(4,128)(2,1)S(1)}, bf16[4,1024]{1,0:T(4,128)(2,1)S(1)}, u32[]{:S(2)}, u32[]{:S(2)}) collective-permute-start(bf16[4,1024]{1,0:T(4,128)(2,1)S(1)} %get-tuple-element.41), channel_id=1, source_target_pairs={{0,4},{4,0},{8,12},{12,8},{1,5},{5,1},{9,13},{13,9},{2,6},{6,2},{1... | collective-permute-start | bytes 24584 | tf_op jit(solution)/shard_map/ppermute | solution.py:27
  41.2 0.9 %collective-permute-start.19 = (bf16[4,1024]{1,0:T(4,128)(2,1)S(1)}, bf16[4,1024]{1,0:T(4,128)(2,1)S(1)}, u32[]{:S(2)}, u32[]{:S(2)}) collective-permute-start(bf16[4,1024]{1,0:T(4,128)(2,1)S(1)} %get-tuple-element.42), channel_id=1, source_target_pairs={{0,8},{4,12},{8,0},{12,4},{1,9},{5,13},{9,1},{13,5},{2,10},{6,14},... | collective-permute-start | bytes 24584 | tf_op jit(solution)/shard_map/ppermute | solution.py:27
  42.1 1.5 %collective-permute-start.20 = (bf16[4,1024]{1,0:T(4,128)(2,1)S(1)}, bf16[4,1024]{1,0:T(4,128)(2,1)S(1)}, u32[]{:S(2)}, u32[]{:S(2)}) collective-permute-start(bf16[4,1024]{1,0:T(4,128)(2,1)S(1)} %get-tuple-element.43), channel_id=1, source_target_pairs={{0,12},{4,8},{8,4},{12,0},{1,13},{5,9},{9,5},{13,1},{2,14},{6,10},... | collective-permute-start | bytes 24584 | tf_op jit(solution)/shard_map/ppermute | solution.py:27
  43.7 1.3 %update.2.refs_0_ = f32[2,4,4,128,128]{4,3,2,1,0:T(8,128)} custom-call(f32[4,3,512]{2,1,0:T(4,128)S(1)} %get-tuple-element.45.gates, f32[2,4,4,128,128]{4,3,2,1,0:T(8,128)S(1)} %copy-done), custom_call_target="tpu_custom_call" | custom-call | tf_op jit(solution)/shard_map/update/pallas_call | solution.py:266
  45.0 1.4 %update.3 = f32[2,4,4,128,128]{4,3,2,1,0:T(8,128)} custom-call(f32[4,3,512]{2,1,0:T(4,128)S(1)} %get-tuple-element.44.gates, f32[2,4,4,128,128]{4,3,2,1,0:T(8,128)S(1)} %copy-done, f32[2,4,4,128,128]{4,3,2,1,0:T(8,128)} %update.2.refs_0_), custom_call_target="tpu_custom_call", output_to_operand_aliasing={{}: (2, {})} | custom-call | tf_op jit(solution)/shard_map/update/pallas_call | solution.py:266
  46.4 1.2 %collective-permute-done.20.refs_2_ = bf16[4,1024]{1,0:T(4,128)(2,1)S(1)} collective-permute-done((bf16[4,1024]{1,0:T(4,128)(2,1)S(1)}, bf16[4,1024]{1,0:T(4,128)(2,1)S(1)}, u32[]{:S(2)}, u32[]{:S(2)}) %collective-permute-start.20) | collective-permute-done | bytes 8224 | tf_op jit(solution)/shard_map/ppermute | solution.py:27
  47.6 0.6 %close.1 = bf16[4,1024]{1,0:T(4,128)(2,1)} custom-call(f32[4,1024]{1,0:T(4,128)S(1)} %get-tuple-element.40.own, bf16[4,1024]{1,0:T(4,128)(2,1)S(1)} %collective-permute-done.18.refs_0_, bf16[4,1024]{1,0:T(4,128)(2,1)S(1)} %collective-permute-done.19.refs_1_, bf16[4,1024]{1,0:T(4,128)(2,1)S(1)} %collective-permute-done.20.refs_2_), custom_call_target="tpu_custom_call" | custom-call | tf_op jit(solution)/shard_map/close/pallas_call | solution.py:297
  (40 shorter events, 1.9 us)
Async XLA Ops:
  0.6 11.4 %copy-start.8 = (bf16[4,1024]{1,0:T(4,128)(2,1)S(1)}, bf16[4,1024]{1,0:T(4,128)(2,1)}, u32[]{:S(2)}) copy-start(bf16[4,1024]{1,0:T(4,128)(2,1)} %refs_0_.1) | copy-start | bytes 24580
  0.6 11.4 %copy-start.4 = (bf16[2,1024,512]{2,1,0:T(8,128)(2,1)S(1)}, bf16[2,1024,512]{2,1,0:T(8,128)(2,1)}, u32[]{:S(2)}) copy-start(bf16[2,1024,512]{2,1,0:T(8,128)(2,1)} %refs_9_.3) | copy-start | bytes 6291460
  0.7 11.4 %copy-start.3 = (bf16[2,1024,512]{2,1,0:T(8,128)(2,1)S(1)}, bf16[2,1024,512]{2,1,0:T(8,128)(2,1)}, u32[]{:S(2)}) copy-start(bf16[2,1024,512]{2,1,0:T(8,128)(2,1)} %refs_8_.3) | copy-start | bytes 6291460
  0.7 11.4 %copy-start.2 = (bf16[2,1024,512]{2,1,0:T(8,128)(2,1)S(1)}, bf16[2,1024,512]{2,1,0:T(8,128)(2,1)}, u32[]{:S(2)}) copy-start(bf16[2,1024,512]{2,1,0:T(8,128)(2,1)} %refs_7_.3) | copy-start | bytes 6291460
  0.7 11.4 %copy-start.1 = (bf16[2,1024,512]{2,1,0:T(8,128)(2,1)S(1)}, bf16[2,1024,512]{2,1,0:T(8,128)(2,1)}, u32[]{:S(2)}) copy-start(bf16[2,1024,512]{2,1,0:T(8,128)(2,1)} %refs_6_.6) | copy-start | bytes 6291460
  0.7 11.4 %copy-start.6 = (f32[2,1024]{1,0:T(2,128)S(1)}, f32[2,1024]{1,0:T(2,128)}, u32[]{:S(2)}) copy-start(f32[2,1024]{1,0:T(2,128)} %refs_5_.6) | copy-start | bytes 24580
  0.7 6.0 %collective-permute-start.1 = (bf16[4,1024]{1,0:T(4,128)(2,1)}, bf16[4,1024]{1,0:T(4,128)(2,1)S(1)}, u32[]{:S(2)}, u32[]{:S(2)}) collective-permute-start(bf16[4,1024]{1,0:T(4,128)(2,1)} %refs_0_.1), channel_id=1, source_target_pairs={{8,0},{12,4},{0,8},{4,12},{9,1},{13,5},{1,9},{5,13},{10,2},{14,6},... | collective-permute-start | bytes 24584 | tf_op jit(solution)/shard_map/ppermute | solution.py:27
  4.8 3.9 %collective-permute-start = (bf16[4,1024]{1,0:T(4,128)(2,1)}, bf16[4,1024]{1,0:T(4,128)(2,1)S(1)}, u32[]{:S(2)}, u32[]{:S(2)}) collective-permute-start(bf16[4,1024]{1,0:T(4,128)(2,1)} %refs_0_.1), channel_id=1, source_target_pairs={{4,0},{0,4},{12,8},{8,12},{5,1},{1,5},{13,9},{9,13},{6,2},{2,6},{1... | collective-permute-start | bytes 24584 | tf_op jit(solution)/shard_map/ppermute | solution.py:27
  6.4 5.7 %collective-permute-start.2 = (bf16[4,1024]{1,0:T(4,128)(2,1)}, bf16[4,1024]{1,0:T(4,128)(2,1)S(1)}, u32[]{:S(2)}, u32[]{:S(2)}) collective-permute-start(bf16[4,1024]{1,0:T(4,128)(2,1)} %refs_0_.1), channel_id=1, source_target_pairs={{12,0},{8,4},{4,8},{0,12},{13,1},{9,5},{5,9},{1,13},{14,2},{10,6},... | collective-permute-start | bytes 24584 | tf_op jit(solution)/shard_map/ppermute | solution.py:27
  12.1 5.6 %copy-start = (f32[2,4,4,128,128]{4,3,2,1,0:T(8,128)S(1)}, f32[2,4,4,128,128]{4,3,2,1,0:T(8,128)}, u32[]{:S(2)}) copy-start(f32[2,4,4,128,128]{4,3,2,1,0:T(8,128)} %state.3) | copy-start | bytes 6291460
  12.1 5.6 %copy-start.7 = (f32[2,512]{1,0:T(2,128)S(1)}, f32[2,512]{1,0:T(2,128)}, u32[]{:S(2)}) copy-start(f32[2,512]{1,0:T(2,128)} %refs_4_.6) | copy-start | bytes 12292
  12.1 5.6 %copy-start.9 = (f32[2,128]{1,0:T(2,128)S(1)}, f32[2,128]{1,0:T(2,128)}, u32[]{:S(2)}) copy-start(f32[2,128]{1,0:T(2,128)} %refs_5_.7) | copy-start | bytes 3076
  12.9 9.4 %copy-start.5 = (bf16[2,512,1024]{2,1,0:T(8,128)(2,1)S(1)}, bf16[2,512,1024]{2,1,0:T(8,128)(2,1)}, u32[]{:S(2)}) copy-start(bf16[2,512,1024]{2,1,0:T(8,128)(2,1)} %refs_4_.7) | copy-start | bytes 6291460
  12.9 1.9 %collective-permute-start.3 = (bf16[4,2176]{1,0:T(4,128)(2,1)S(1)}, bf16[4,2176]{1,0:T(4,128)(2,1)S(1)}, u32[]{:S(2)}, u32[]{:S(2)}) collective-permute-start(bf16[4,2176]{1,0:T(4,128)(2,1)S(1)} %get-tuple-element.27), channel_id=1, source_target_pairs={{0,1},{1,0},{2,3},{3,2},{4,5},{5,4},{6,7},{7,6},{8,9},{9,8},{10,11... | collective-permute-start | bytes 52232 | tf_op jit(solution)/shard_map/ppermute | solution.py:27
  12.9 3.8 %collective-permute-start.4 = (bf16[4,2176]{1,0:T(4,128)(2,1)S(1)}, bf16[4,2176]{1,0:T(4,128)(2,1)S(1)}, u32[]{:S(2)}, u32[]{:S(2)}) collective-permute-start(bf16[4,2176]{1,0:T(4,128)(2,1)S(1)} %get-tuple-element.28), channel_id=1, source_target_pairs={{0,2},{1,3},{2,0},{3,1},{4,6},{5,7},{6,4},{7,5},{8,10},{9,11},{10,... | collective-permute-start | bytes 52232 | tf_op jit(solution)/shard_map/ppermute | solution.py:27
  14.5 3.2 %collective-permute-start.5 = (bf16[4,2176]{1,0:T(4,128)(2,1)S(1)}, bf16[4,2176]{1,0:T(4,128)(2,1)S(1)}, u32[]{:S(2)}, u32[]{:S(2)}) collective-permute-start(bf16[4,2176]{1,0:T(4,128)(2,1)S(1)} %get-tuple-element.29), channel_id=1, source_target_pairs={{0,3},{1,2},{2,1},{3,0},{4,7},{5,6},{6,5},{7,4},{8,11},{9,10},{10,... | collective-permute-start | bytes 52232 | tf_op jit(solution)/shard_map/ppermute | solution.py:27
  18.2 3.0 %collective-permute-start.8 = (bf16[4,512]{1,0:T(4,128)(2,1)S(1)}, bf16[4,512]{1,0:T(4,128)(2,1)S(1)}, u32[]{:S(2)}, u32[]{:S(2)}) collective-permute-start(bf16[4,512]{1,0:T(4,128)(2,1)S(1)} %get-tuple-element.30.refs_0_), channel_id=1, source_target_pairs={{3,0},{2,1},{1,2},{0,3},{7,4},{6,5},{5,6},{4,7},{11,8},{10,9},{9,1... | collective-permute-start | bytes 12296 | tf_op jit(solution)/shard_map/ppermute | solution.py:27
  18.7 3.6 %collective-permute-start.7 = (bf16[4,512]{1,0:T(4,128)(2,1)S(1)}, bf16[4,512]{1,0:T(4,128)(2,1)S(1)}, u32[]{:S(2)}, u32[]{:S(2)}) collective-permute-start(bf16[4,512]{1,0:T(4,128)(2,1)S(1)} %get-tuple-element.30.refs_0_), channel_id=1, source_target_pairs={{2,0},{3,1},{0,2},{1,3},{6,4},{7,5},{4,6},{5,7},{10,8},{11,9},{8,1... | collective-permute-start | bytes 12296 | tf_op jit(solution)/shard_map/ppermute | solution.py:27
  20.0 2.2 %collective-permute-start.6 = (bf16[4,512]{1,0:T(4,128)(2,1)S(1)}, bf16[4,512]{1,0:T(4,128)(2,1)S(1)}, u32[]{:S(2)}, u32[]{:S(2)}) collective-permute-start(bf16[4,512]{1,0:T(4,128)(2,1)S(1)} %get-tuple-element.30.refs_0_), channel_id=1, source_target_pairs={{1,0},{0,1},{3,2},{2,3},{5,4},{4,5},{7,6},{6,7},{9,8},{8,9},{11,10... | collective-permute-start | bytes 12296 | tf_op jit(solution)/shard_map/ppermute | solution.py:27
  22.5 5.7 %collective-permute-start.11 = (bf16[16,1024]{1,0:T(8,128)(2,1)S(1)}, bf16[16,1024]{1,0:T(8,128)(2,1)S(1)}, u32[]{:S(2)}, u32[]{:S(2)}) collective-permute-start(bf16[16,1024]{1,0:T(8,128)(2,1)S(1)} %get-tuple-element.32), channel_id=1, source_target_pairs={{0,12},{4,8},{8,4},{12,0},{1,13},{5,9},{9,5},{13,1},{2,14},{6,10},... | collective-permute-start | bytes 98312 | tf_op jit(solution)/shard_map/ppermute | solution.py:27
  22.6 5.6 %collective-permute-start.10 = (bf16[16,1024]{1,0:T(8,128)(2,1)S(1)}, bf16[16,1024]{1,0:T(8,128)(2,1)S(1)}, u32[]{:S(2)}, u32[]{:S(2)}) collective-permute-start(bf16[16,1024]{1,0:T(8,128)(2,1)S(1)} %get-tuple-element.32), channel_id=1, source_target_pairs={{0,8},{4,12},{8,0},{12,4},{1,9},{5,13},{9,1},{13,5},{2,10},{6,14},... | collective-permute-start | bytes 98312 | tf_op jit(solution)/shard_map/ppermute | solution.py:27
  22.7 6.2 %collective-permute-start.9 = (bf16[16,1024]{1,0:T(8,128)(2,1)S(1)}, bf16[16,1024]{1,0:T(8,128)(2,1)S(1)}, u32[]{:S(2)}, u32[]{:S(2)}) collective-permute-start(bf16[16,1024]{1,0:T(8,128)(2,1)S(1)} %get-tuple-element.32), channel_id=1, source_target_pairs={{0,4},{4,0},{8,12},{12,8},{1,5},{5,1},{9,13},{13,9},{2,6},{6,2},{1... | collective-permute-start | bytes 98312 | tf_op jit(solution)/shard_map/ppermute | solution.py:27
  29.5 1.9 %collective-permute-start.12 = (bf16[4,2176]{1,0:T(4,128)(2,1)S(1)}, bf16[4,2176]{1,0:T(4,128)(2,1)S(1)}, u32[]{:S(2)}, u32[]{:S(2)}) collective-permute-start(bf16[4,2176]{1,0:T(4,128)(2,1)S(1)} %get-tuple-element.34), channel_id=1, source_target_pairs={{0,1},{1,0},{2,3},{3,2},{4,5},{5,4},{6,7},{7,6},{8,9},{9,8},{10,11... | collective-permute-start | bytes 52232 | tf_op jit(solution)/shard_map/ppermute | solution.py:27
  29.5 3.8 %collective-permute-start.13 = (bf16[4,2176]{1,0:T(4,128)(2,1)S(1)}, bf16[4,2176]{1,0:T(4,128)(2,1)S(1)}, u32[]{:S(2)}, u32[]{:S(2)}) collective-permute-start(bf16[4,2176]{1,0:T(4,128)(2,1)S(1)} %get-tuple-element.35), channel_id=1, source_target_pairs={{0,2},{1,3},{2,0},{3,1},{4,6},{5,7},{6,4},{7,5},{8,10},{9,11},{10,... | collective-permute-start | bytes 52232 | tf_op jit(solution)/shard_map/ppermute | solution.py:27
  30.9 3.2 %collective-permute-start.14 = (bf16[4,2176]{1,0:T(4,128)(2,1)S(1)}, bf16[4,2176]{1,0:T(4,128)(2,1)S(1)}, u32[]{:S(2)}, u32[]{:S(2)}) collective-permute-start(bf16[4,2176]{1,0:T(4,128)(2,1)S(1)} %get-tuple-element.36), channel_id=1, source_target_pairs={{0,3},{1,2},{2,1},{3,0},{4,7},{5,6},{6,5},{7,4},{8,11},{9,10},{10,... | collective-permute-start | bytes 52232 | tf_op jit(solution)/shard_map/ppermute | solution.py:27
  34.6 3.0 %collective-permute-start.17 = (bf16[4,512]{1,0:T(4,128)(2,1)S(1)}, bf16[4,512]{1,0:T(4,128)(2,1)S(1)}, u32[]{:S(2)}, u32[]{:S(2)}) collective-permute-start(bf16[4,512]{1,0:T(4,128)(2,1)S(1)} %get-tuple-element.37.refs_0_), channel_id=1, source_target_pairs={{3,0},{2,1},{1,2},{0,3},{7,4},{6,5},{5,6},{4,7},{11,8},{10,9},{9,1... | collective-permute-start | bytes 12296 | tf_op jit(solution)/shard_map/ppermute | solution.py:27
  35.1 3.6 %collective-permute-start.16 = (bf16[4,512]{1,0:T(4,128)(2,1)S(1)}, bf16[4,512]{1,0:T(4,128)(2,1)S(1)}, u32[]{:S(2)}, u32[]{:S(2)}) collective-permute-start(bf16[4,512]{1,0:T(4,128)(2,1)S(1)} %get-tuple-element.37.refs_0_), channel_id=1, source_target_pairs={{2,0},{3,1},{0,2},{1,3},{6,4},{7,5},{4,6},{5,7},{10,8},{11,9},{8,1... | collective-permute-start | bytes 12296 | tf_op jit(solution)/shard_map/ppermute | solution.py:27
  36.5 2.3 %collective-permute-start.15 = (bf16[4,512]{1,0:T(4,128)(2,1)S(1)}, bf16[4,512]{1,0:T(4,128)(2,1)S(1)}, u32[]{:S(2)}, u32[]{:S(2)}) collective-permute-start(bf16[4,512]{1,0:T(4,128)(2,1)S(1)} %get-tuple-element.37.refs_0_), channel_id=1, source_target_pairs={{1,0},{0,1},{3,2},{2,3},{5,4},{4,5},{7,6},{6,7},{9,8},{8,9},{11,10... | collective-permute-start | bytes 12296 | tf_op jit(solution)/shard_map/ppermute | solution.py:27
  39.1 7.2 %collective-permute-start.18 = (bf16[4,1024]{1,0:T(4,128)(2,1)S(1)}, bf16[4,1024]{1,0:T(4,128)(2,1)S(1)}, u32[]{:S(2)}, u32[]{:S(2)}) collective-permute-start(bf16[4,1024]{1,0:T(4,128)(2,1)S(1)} %get-tuple-element.41), channel_id=1, source_target_pairs={{0,4},{4,0},{8,12},{12,8},{1,5},{5,1},{9,13},{13,9},{2,6},{6,2},{1... | collective-permute-start | bytes 24584 | tf_op jit(solution)/shard_map/ppermute | solution.py:27
  41.2 5.2 %collective-permute-start.19 = (bf16[4,1024]{1,0:T(4,128)(2,1)S(1)}, bf16[4,1024]{1,0:T(4,128)(2,1)S(1)}, u32[]{:S(2)}, u32[]{:S(2)}) collective-permute-start(bf16[4,1024]{1,0:T(4,128)(2,1)S(1)} %get-tuple-element.42), channel_id=1, source_target_pairs={{0,8},{4,12},{8,0},{12,4},{1,9},{5,13},{9,1},{13,5},{2,10},{6,14},... | collective-permute-start | bytes 24584 | tf_op jit(solution)/shard_map/ppermute | solution.py:27
  42.1 5.4 %collective-permute-start.20 = (bf16[4,1024]{1,0:T(4,128)(2,1)S(1)}, bf16[4,1024]{1,0:T(4,128)(2,1)S(1)}, u32[]{:S(2)}, u32[]{:S(2)}) collective-permute-start(bf16[4,1024]{1,0:T(4,128)(2,1)S(1)} %get-tuple-element.43), channel_id=1, source_target_pairs={{0,12},{4,8},{8,4},{12,0},{1,13},{5,9},{9,5},{13,1},{2,14},{6,10},... | collective-permute-start | bytes 24584 | tf_op jit(solution)/shard_map/ppermute | solution.py:27

commit v6 on v5

--- a/solution.py
+++ b/solution.py
@@ -28,6 +28,34 @@
             arrays[k - 1], axis, [(b, a) for a, b in pairs] if inward else pairs
         )
     return parts
+
+
+def core_flip(n_dp):
+    return int(n_dp > 1 and n_dp & (n_dp - 1) == 0)
+
+
+def cross_pairs(n_tp, n_dp, k):
+    flip = core_flip(n_dp)
+    return [
+        (t * n_dp + d, peer_of(n_tp, k, t) * n_dp + (d ^ flip))
+        for t in range(n_tp)
+        for d in range(n_dp)
+    ]
+
+
+def cross_exchange(n_tp, n_dp, arrays):
+    parts = [None] * (n_tp - 1)
+    for k in reversed(range(1, n_tp)):
+        parts[k - 1] = lax.ppermute(
+            arrays[k - 1], ("tp", "dp"), cross_pairs(n_tp, n_dp, k)
+        )
+    return parts
+
+
+def cross_weight(n_dp, array):
+    if not core_flip(n_dp):
+        return array
+    return lax.ppermute(array, "dp", [(d, d ^ 1) for d in range(n_dp)])
 
 
 def gather(axis, n, array):
@@ -87,7 +115,7 @@
 
 def recur(n_dp, layer, features, *refs):
     own, parts = refs[0], refs[1:n_dp]
-    bound_ref, head_gain, state, normed, gates = refs[n_dp:]
+    bound_ref, head_gain, state, normed, gates, left = refs[n_dp:]
     seqs, heads, hd = state.shape[1], state.shape[2], state.shape[3]
     width = heads * hd
     total = own[...]
@@ -108,18 +136,41 @@
     weighted = query * forget
     shared = query * keyvec
     row = lax.broadcasted_iota(jnp.int32, (seqs, hd), 0)
-    for head in range(heads):
-        cols = slice(head * hd, (head + 1) * hd)
-        readout = jnp.sum(shared[:, cols], axis=1, keepdims=True) * value[:, cols]
-        for seq in range(seqs):
-            high, low = split(jnp.where(row == seq, weighted[:, cols], 0.0))
-            stored = state[layer, seq, head].astype(BF16)
-            readout = readout + jnp.dot(high, stored, preferred_element_type=F32)
-            readout = readout + jnp.dot(low, stored, preferred_element_type=F32)
-        scale = lax.rsqrt(jnp.mean(readout * readout, axis=1, keepdims=True) + 1e-06)
-        normed[:, cols] = (
-            readout * scale * head_gain[layer : layer + 1, :] * gate[:, cols]
-        ).astype(BF16)
+    terms = [term.astype(F32) for term in split(weighted)]
+    group = 2 if heads % 2 == 0 else 1
+    for first in range(0, heads, group):
+        for index in range(group):
+            cols = slice((first + index) * hd, (first + index + 1) * hd)
+            for part, term in enumerate(terms):
+                top = (index * 2 + part) * seqs
+                for seq in range(seqs):
+                    left[top : top + seqs, seq * hd : (seq + 1) * hd] = jnp.where(
+                        row == seq, term[:, cols], 0.0
+                    )
+        right = jnp.concatenate(
+            [
+                jnp.concatenate(
+                    [state[layer, seq, first + index].astype(BF16) for seq in range(seqs)], axis=0
+                )
+                for index in range(group)
+            ],
+            axis=1,
+        )
+        product = jnp.dot(
+            left[: 2 * group * seqs, :].astype(BF16), right, preferred_element_type=F32
+        )
+        for index in range(group):
+            head = first + index
+            cols = slice(head * hd, (head + 1) * hd)
+            own_cols = slice(index * hd, (index + 1) * hd)
+            readout = jnp.sum(shared[:, cols], axis=1, keepdims=True) * value[:, cols]
+            for part in range(2):
+                top = (index * 2 + part) * seqs
+                readout = readout + product[top : top + seqs, own_cols]
+            scale = lax.rsqrt(jnp.mean(readout * readout, axis=1, keepdims=True) + 1e-06)
+            normed[:, cols] = (
+                readout * scale * head_gain[layer : layer + 1, :] * gate[:, cols]
+            ).astype(BF16)
 
 
 def update(layer, gates, state, *refs):
@@ -147,27 +198,26 @@
 
 
 def mix_next(n_dp, layer, *refs):
-    parts, (weight, mixed, sent, slots) = refs[:n_dp], refs[n_dp:]
-    product = jnp.dot(gather_rows(parts, slots), weight[layer], preferred_element_type=F32)
-    mixed[...] = product
-    sent[...] = product.astype(BF16)
+    parts, (weight, crossed, mixed, sent, slots) = refs[:n_dp], refs[n_dp:]
+    facing = [parts[k ^ core_flip(n_dp)] for k in range(n_dp)]
+    rows = gather_rows(facing, slots)
+    sent[...] = jnp.dot(rows, crossed[layer], preferred_element_type=F32).astype(BF16)
+    rows = gather_rows(parts, slots)
+    mixed[...] = jnp.dot(rows, weight[layer], preferred_element_type=F32)
 
 
 def mix_last(n_dp, layer, *refs):
-    parts, (weight, base, order) = refs[:n_dp], refs[n_dp : n_dp + 3]
-    own, outs, slots = refs[n_dp + 3], refs[n_dp + 4 : -1], refs[-1]
+    parts, (weight, crossed, base, order) = refs[:n_dp], refs[n_dp : n_dp + 4]
+    own, outs, slots = refs[n_dp + 4], refs[n_dp + 5 : -1], refs[-1]
     rows = own.shape[0]
-    product = jnp.dot(gather_rows(parts, slots), weight[layer], preferred_element_type=F32)
-    high, low = split(product)
-    moved = jnp.dot(order[...], high, preferred_element_type=F32)
-    first = order[:rows, :]
-    own[...] = (
-        moved[:rows]
-        + jnp.dot(first, low, preferred_element_type=F32)
-        + jnp.dot(first, base[...], preferred_element_type=F32)
+    moved = jnp.dot(order[...], gather_rows(parts, slots), preferred_element_type=F32)
+    moved = moved.astype(BF16)
+    product = jnp.dot(moved, crossed[layer], preferred_element_type=F32)
+    for k, out in enumerate(outs):
+        out[...] = product[(k + 1) * rows : (k + 2) * rows].astype(BF16)
+    own[...] = jnp.dot(moved, weight[layer], preferred_element_type=F32)[:rows] + jnp.dot(
+        order[:rows, :], base[...], preferred_element_type=F32
     )
-    for k, out in enumerate(outs):
-        out[...] = moved[(k + 1) * rows : (k + 2) * rows].astype(BF16)
 
 
 def close(own, *refs):
@@ -234,6 +284,7 @@
         flops=20_000_000_000,
     )
     parts = gather("tp", n_tp, tokens)
+    crossed = cross_weight(n_dp, w_out)
     base = mixed = None
     new_state = None
     for layer in range(2):
@@ -261,6 +312,7 @@
             (own, *parts, lower_bound, head_gain, state),
             [VMEM] * (n_dp + 2) + [VMEM],
             [((seqs, width), BF16), ((seqs, 3, width), F32)],
+            [((4 * seqs, seqs * hd), F32)],
         )
         parts = gather("dp", n_dp, normed)
         new_state = pl.pallas_call(
@@ -279,21 +331,21 @@
         if layer == 0:
             mixed, sent = call(
                 functools.partial(mix_next, n_dp, layer),
-                (*parts, w_out),
-                [VMEM] * n_dp + [VMEM],
+                (*parts, w_out, crossed),
+                [VMEM] * (n_dp + 2),
                 [((total, local), F32), ((total, local), BF16)],
                 [((total, width), F32)],
             )
-            parts = exchange("tp", n_tp, [sent] * (n_tp - 1))
+            parts = cross_exchange(n_tp, n_dp, [sent] * (n_tp - 1))
         else:
             own, *sent = call(
                 functools.partial(mix_last, n_dp, layer),
-                (*parts, w_out, base, order_out),
-                [VMEM] * n_dp + [VMEM] + [VMEM] * 2,
+                (*parts, w_out, crossed, base, order_out),
+                [VMEM] * (n_dp + 4),
                 [((rows, local), F32)] + [((rows, local), BF16)] * (n_tp - 1),
                 [((total, width), F32)],
             )
-            parts = exchange("tp", n_tp, sent)
+            parts = cross_exchange(n_tp, n_dp, sent)
     hidden = pl.pallas_call(
         close,
         name="close",

time: 48.3 us -> 47.9 us (level)
  starting transfers between devices: 22.1 us -> 21.1 us
  waiting for transfers between devices: 18.7 us -> 19.4 us
    ppermute x21 -> x15, starting transfers between devices: 22.1 us -> 12.8 us  [exchange(): lax.ppermute(arrays[k - 1], axis, [(b, a) for a, b in pairs] if inward el...]
    ppermute x0 -> x7, starting transfers between devices: none -> 8.25 us  [the longest x6 7.69 us: cross_exchange(): lax.ppermute(arrays[k - 1], ('tp', 'dp'), cross_pairs(n_tp, n_dp, k))]
    ppermute x0 -> x7, waiting for transfers between devices: none -> 3.74 us  [the longest x6 3.74 us: cross_exchange(): lax.ppermute(arrays[k - 1], ('tp', 'dp'), cross_pairs(n_tp, n_dp, k))]
    ppermute x21 -> x15, waiting for transfers between devices: 18.7 us -> 15.7 us  [exchange(): lax.ppermute(arrays[k - 1], axis, [(b, a) for a, b in pairs] if inward el...]
  transfers between devices with their start and end apart: 21 -> 22, of which waited for: 14 -> 13; matrix products, arithmetic and copies ran while one was open for 0% -> 0% of each run, Pallas kernels for 6% -> 8%
where the time goes in v6:
time: 47.9 us; the launch traced here: 47.7 us
  starting transfers between devices  21.1 us (44%)
  waiting for transfers between devices  19.4 us (41%)
  Pallas kernels  6.34 us (13%)
  between operations  0.82 us (2%)
    ppermute x15, waiting for transfers between devices, exchange(): lax.ppermute(arrays[k - 1], axis, [(b, a) for a, b in pairs] if inward el...  15.7 us
    ppermute x15, starting transfers between devices, exchange(): lax.ppermute(arrays[k - 1], axis, [(b, a) for a, b in pairs] if inward el...  12.8 us
    ppermute x6, starting transfers between devices, cross_exchange(): lax.ppermute(arrays[k - 1], ('tp', 'dp'), cross_pairs(n_tp, n_dp, k))  7.69 us
    ppermute x6, waiting for transfers between devices, cross_exchange(): lax.ppermute(arrays[k - 1], ('tp', 'dp'), cross_pairs(n_tp, n_dp, k))  3.74 us
    pallas_call x7, Pallas kernels, call(): pl.pallas_call(body, out_shape=[pltpu.VMEM(shape, dtype) for shape, dtype...  3.04 us
    pallas_call x2, Pallas kernels, per_device(): pl.pallas_call(functools.partial(update, layer), name='update', out_shape...  2.69 us
  transfers between devices with their start and end apart: 22, of which 13 were waited for; matrix products, arithmetic and copies ran while one was open for 0% of the time, Pallas kernels for 8%

profile of v6, /device:TPU:0, one launch (start us, length us, event | category | flops | bytes accessed | tf_op | source)
XLA Modules:
  0.0 47.7 jit_solution(15485553627111982511)
XLA Ops:
  0.7 0.6 %collective-permute-start.9 = (bf16[2,512,1024]{2,1,0:T(8,128)(2,1)}, bf16[2,512,1024]{2,1,0:T(8,128)(2,1)S(1)}, u32[]{:S(2)}, u32[]{:S(2)}) collective-permute-start(bf16[2,512,1024]{2,1,0:T(8,128)(2,1)} %refs_4_.7), channel_id=1, source_target_pairs={{0,1},{1,0},{2,3},{3,2},{4,5},{5,4},{6,7},{7,6},{8,9},{9,8},{10,11... | collective-permute-start | bytes 6291464 | tf_op jit(solution)/shard_map/ppermute | solution.py:58
  1.2 2.6 %collective-permute-start = (bf16[4,1024]{1,0:T(4,128)(2,1)}, bf16[4,1024]{1,0:T(4,128)(2,1)S(1)}, u32[]{:S(2)}, u32[]{:S(2)}) collective-permute-start(bf16[4,1024]{1,0:T(4,128)(2,1)} %refs_0_.1), channel_id=1, source_target_pairs={{4,0},{0,4},{12,8},{8,12},{5,1},{1,5},{13,9},{9,13},{6,2},{2,6},{1... | collective-permute-start | bytes 24584 | tf_op jit(solution)/shard_map/ppermute | solution.py:27
  3.9 2.6 %collective-permute-start.1 = (bf16[4,1024]{1,0:T(4,128)(2,1)}, bf16[4,1024]{1,0:T(4,128)(2,1)S(1)}, u32[]{:S(2)}, u32[]{:S(2)}) collective-permute-start(bf16[4,1024]{1,0:T(4,128)(2,1)} %refs_0_.1), channel_id=1, source_target_pairs={{8,0},{12,4},{0,8},{4,12},{9,1},{13,5},{1,9},{5,13},{10,2},{14,6},... | collective-permute-start | bytes 24584 | tf_op jit(solution)/shard_map/ppermute | solution.py:27
  6.5 2.1 %collective-permute-done.1.refs_2_ = bf16[4,1024]{1,0:T(4,128)(2,1)S(1)} collective-permute-done((bf16[4,1024]{1,0:T(4,128)(2,1)}, bf16[4,1024]{1,0:T(4,128)(2,1)S(1)}, u32[]{:S(2)}, u32[]{:S(2)}) %collective-permute-start.1) | collective-permute-done | bytes 8224 | tf_op jit(solution)/shard_map/ppermute | solution.py:27
  8.7 3.5 %collective-permute-done.2.refs_3_ = bf16[4,1024]{1,0:T(4,128)(2,1)S(1)} collective-permute-done((bf16[4,1024]{1,0:T(4,128)(2,1)}, bf16[4,1024]{1,0:T(4,128)(2,1)S(1)}, u32[]{:S(2)}, u32[]{:S(2)}) %collective-permute-start.2) | collective-permute-done | bytes 8224 | tf_op jit(solution)/shard_map/ppermute | solution.py:27
  12.2 0.8 %shard_map.114 = (bf16[16,1024]{1,0:T(8,128)(2,1)S(1)}, f32[4,2176]{1,0:T(4,128)S(1)}, bf16[4,2176]{1,0:T(4,128)(2,1)S(1)}, bf16[4,2176]{1,0:T(4,128)(2,1)S(1)}, bf16[4,2176]{1,0:T(4,128)(2,1)S(1)}) custom-call(bf16[4,1024]{1,0:T(4,128)(2,1)S(1)} %copy-done.8, bf16[4,1024]{1,0:T(4,128)(2,1)S(1)} %collective-permute-done.refs_1_, ...), custom_call_target="tpu_custom_call" | custom-call | tf_op jit(solution)/shard_map/pallas_call | solution.py:248
  13.0 1.6 %collective-permute-start.4 = (bf16[4,2176]{1,0:T(4,128)(2,1)S(1)}, bf16[4,2176]{1,0:T(4,128)(2,1)S(1)}, u32[]{:S(2)}, u32[]{:S(2)}) collective-permute-start(bf16[4,2176]{1,0:T(4,128)(2,1)S(1)} %get-tuple-element.28), channel_id=1, source_target_pairs={{0,2},{1,3},{2,0},{3,1},{4,6},{5,7},{6,4},{7,5},{8,10},{9,11},{10,... | collective-permute-start | bytes 52232 | tf_op jit(solution)/shard_map/ppermute | solution.py:27
  14.9 2.0 %collective-permute-done.4.refs_2_ = bf16[4,2176]{1,0:T(4,128)(2,1)S(1)} collective-permute-done((bf16[4,2176]{1,0:T(4,128)(2,1)S(1)}, bf16[4,2176]{1,0:T(4,128)(2,1)S(1)}, u32[]{:S(2)}, u32[]{:S(2)}) %collective-permute-start.4) | collective-permute-done | bytes 17440 | tf_op jit(solution)/shard_map/ppermute | solution.py:27
  16.8 0.9 %collective-permute-done.5.refs_3_ = bf16[4,2176]{1,0:T(4,128)(2,1)S(1)} collective-permute-done((bf16[4,2176]{1,0:T(4,128)(2,1)S(1)}, bf16[4,2176]{1,0:T(4,128)(2,1)S(1)}, u32[]{:S(2)}, u32[]{:S(2)}) %collective-permute-start.5) | collective-permute-done | bytes 17440 | tf_op jit(solution)/shard_map/ppermute | solution.py:27
  18.4 0.6 %collective-permute-start.7 = (bf16[4,512]{1,0:T(4,128)(2,1)S(1)}, bf16[4,512]{1,0:T(4,128)(2,1)S(1)}, u32[]{:S(2)}, u32[]{:S(2)}) collective-permute-start(bf16[4,512]{1,0:T(4,128)(2,1)S(1)} %get-tuple-element.30.refs_0_), channel_id=1, source_target_pairs={{2,0},{3,1},{0,2},{1,3},{6,4},{7,5},{4,6},{5,7},{10,8},{11,9},{8,1... | collective-permute-start | bytes 12296 | tf_op jit(solution)/shard_map/ppermute | solution.py:27
  19.0 1.1 %collective-permute-start.8 = (bf16[4,512]{1,0:T(4,128)(2,1)S(1)}, bf16[4,512]{1,0:T(4,128)(2,1)S(1)}, u32[]{:S(2)}, u32[]{:S(2)}) collective-permute-start(bf16[4,512]{1,0:T(4,128)(2,1)S(1)} %get-tuple-element.30.refs_0_), channel_id=1, source_target_pairs={{3,0},{2,1},{1,2},{0,3},{7,4},{6,5},{5,6},{4,7},{11,8},{10,9},{9,1... | collective-permute-start | bytes 12296 | tf_op jit(solution)/shard_map/ppermute | solution.py:27
  20.1 1.9 %collective-permute-done.7.refs_2_ = bf16[4,512]{1,0:T(4,128)(2,1)S(1)} collective-permute-done((bf16[4,512]{1,0:T(4,128)(2,1)S(1)}, bf16[4,512]{1,0:T(4,128)(2,1)S(1)}, u32[]{:S(2)}, u32[]{:S(2)}) %collective-permute-start.7) | collective-permute-done | bytes 4128 | tf_op jit(solution)/shard_map/ppermute | solution.py:27
  22.4 0.5 collective-permute-start.11
  22.9 3.4 %collective-permute-start.12 = (bf16[16,1024]{1,0:T(8,128)(2,1)S(1)}, bf16[16,1024]{1,0:T(8,128)(2,1)S(1)}, u32[]{:S(2)}, u32[]{:S(2)}) collective-permute-start(bf16[16,1024]{1,0:T(8,128)(2,1)S(1)} %get-tuple-element.32), channel_id=1, source_target_pairs={{0,13},{1,12},{2,15},{3,14},{4,9},{5,8},{6,11},{7,10},{8,5},{9,4},... | collective-permute-start | bytes 98312 | tf_op jit(solution)/shard_map/ppermute | solution.py:49
  26.3 0.5 collective-permute-done.11.refs_3_
  26.8 1.7 %collective-permute-done.12.refs_4_ = bf16[16,1024]{1,0:T(8,128)(2,1)S(1)} collective-permute-done((bf16[16,1024]{1,0:T(8,128)(2,1)S(1)}, bf16[16,1024]{1,0:T(8,128)(2,1)S(1)}, u32[]{:S(2)}, u32[]{:S(2)}) %collective-permute-start.12) | collective-permute-done | bytes 32800 | tf_op jit(solution)/shard_map/ppermute | solution.py:49
  28.5 0.7 %shard_map.117 = (bf16[16,1024]{1,0:T(8,128)(2,1)S(1)}, f32[4,2176]{1,0:T(4,128)S(1)}, bf16[4,2176]{1,0:T(4,128)(2,1)S(1)}, bf16[4,2176]{1,0:T(4,128)(2,1)S(1)}, bf16[4,2176]{1,0:T(4,128)(2,1)S(1)}) custom-call(bf16[16,1024]{1,0:T(8,128)(2,1)S(1)} %get-tuple-element.25.refs_0_, f32[16,1024]{1,0:T(8,128)S(1)} %get-tuple-element.31.refs_1_, ...), custom_call_target="tpu_custom_call" | custom-call | tf_op jit(solution)/shard_map/pallas_call | solution.py:248
  29.1 0.4 collective-permute-start.13
  29.5 1.4 %collective-permute-start.14 = (bf16[4,2176]{1,0:T(4,128)(2,1)S(1)}, bf16[4,2176]{1,0:T(4,128)(2,1)S(1)}, u32[]{:S(2)}, u32[]{:S(2)}) collective-permute-start(bf16[4,2176]{1,0:T(4,128)(2,1)S(1)} %get-tuple-element.35), channel_id=1, source_target_pairs={{0,2},{1,3},{2,0},{3,1},{4,6},{5,7},{6,4},{7,5},{8,10},{9,11},{10,... | collective-permute-start | bytes 52232 | tf_op jit(solution)/shard_map/ppermute | solution.py:27
  31.0 2.3 %collective-permute-done.14.refs_2_ = bf16[4,2176]{1,0:T(4,128)(2,1)S(1)} collective-permute-done((bf16[4,2176]{1,0:T(4,128)(2,1)S(1)}, bf16[4,2176]{1,0:T(4,128)(2,1)S(1)}, u32[]{:S(2)}, u32[]{:S(2)}) %collective-permute-start.14) | collective-permute-done | bytes 17440 | tf_op jit(solution)/shard_map/ppermute | solution.py:27
  33.3 1.0 %collective-permute-done.15.refs_3_ = bf16[4,2176]{1,0:T(4,128)(2,1)S(1)} collective-permute-done((bf16[4,2176]{1,0:T(4,128)(2,1)S(1)}, bf16[4,2176]{1,0:T(4,128)(2,1)S(1)}, u32[]{:S(2)}, u32[]{:S(2)}) %collective-permute-start.15) | collective-permute-done | bytes 17440 | tf_op jit(solution)/shard_map/ppermute | solution.py:27
  34.8 0.7 %collective-permute-start.17 = (bf16[4,512]{1,0:T(4,128)(2,1)S(1)}, bf16[4,512]{1,0:T(4,128)(2,1)S(1)}, u32[]{:S(2)}, u32[]{:S(2)}) collective-permute-start(bf16[4,512]{1,0:T(4,128)(2,1)S(1)} %get-tuple-element.37.refs_0_), channel_id=1, source_target_pairs={{2,0},{3,1},{0,2},{1,3},{6,4},{7,5},{4,6},{5,7},{10,8},{11,9},{8,1... | collective-permute-start | bytes 12296 | tf_op jit(solution)/shard_map/ppermute | solution.py:27
  35.5 1.1 %collective-permute-start.18 = (bf16[4,512]{1,0:T(4,128)(2,1)S(1)}, bf16[4,512]{1,0:T(4,128)(2,1)S(1)}, u32[]{:S(2)}, u32[]{:S(2)}) collective-permute-start(bf16[4,512]{1,0:T(4,128)(2,1)S(1)} %get-tuple-element.37.refs_0_), channel_id=1, source_target_pairs={{3,0},{2,1},{1,2},{0,3},{7,4},{6,5},{5,6},{4,7},{11,8},{10,9},{9,1... | collective-permute-start | bytes 12296 | tf_op jit(solution)/shard_map/ppermute | solution.py:27
  36.5 1.9 %collective-permute-done.17.refs_2_ = bf16[4,512]{1,0:T(4,128)(2,1)S(1)} collective-permute-done((bf16[4,512]{1,0:T(4,128)(2,1)S(1)}, bf16[4,512]{1,0:T(4,128)(2,1)S(1)}, u32[]{:S(2)}, u32[]{:S(2)}) %collective-permute-start.17) | collective-permute-done | bytes 4128 | tf_op jit(solution)/shard_map/ppermute | solution.py:27
  38.5 0.5 %shard_map.119 = (f32[4,1024]{1,0:T(4,128)S(1)}, bf16[4,1024]{1,0:T(4,128)(2,1)S(1)}, bf16[4,1024]{1,0:T(4,128)(2,1)S(1)}, bf16[4,1024]{1,0:T(4,128)(2,1)S(1)}) custom-call(bf16[4,512]{1,0:T(4,128)(2,1)S(1)} %get-tuple-element.37.refs_0_, bf16[4,512]{1,0:T(4,128)(2,1)S(1)} %collective-permute-done.16.refs_1_, ...), custom_call_target="tpu_custom_call" | custom-call | tf_op jit(solution)/shard_map/pallas_call | solution.py:248
  39.0 0.4 collective-permute-start.19
  39.4 2.8 %collective-permute-start.20 = (bf16[4,1024]{1,0:T(4,128)(2,1)S(1)}, bf16[4,1024]{1,0:T(4,128)(2,1)S(1)}, u32[]{:S(2)}, u32[]{:S(2)}) collective-permute-start(bf16[4,1024]{1,0:T(4,128)(2,1)S(1)} %get-tuple-element.42), channel_id=1, source_target_pairs={{0,9},{1,8},{2,11},{3,10},{4,13},{5,12},{6,15},{7,14},{8,1},{9,0},... | collective-permute-start | bytes 24584 | tf_op jit(solution)/shard_map/ppermute | solution.py:49
  42.2 0.6 %collective-permute-start.21 = (bf16[4,1024]{1,0:T(4,128)(2,1)S(1)}, bf16[4,1024]{1,0:T(4,128)(2,1)S(1)}, u32[]{:S(2)}, u32[]{:S(2)}) collective-permute-start(bf16[4,1024]{1,0:T(4,128)(2,1)S(1)} %get-tuple-element.43), channel_id=1, source_target_pairs={{0,13},{1,12},{2,15},{3,14},{4,9},{5,8},{6,11},{7,10},{8,5},{9,4},... | collective-permute-start | bytes 24584 | tf_op jit(solution)/shard_map/ppermute | solution.py:49
  42.8 1.3 %update.2.refs_0_ = f32[2,4,4,128,128]{4,3,2,1,0:T(8,128)} custom-call(f32[4,3,512]{2,1,0:T(4,128)S(1)} %get-tuple-element.45.gates, f32[2,4,4,128,128]{4,3,2,1,0:T(8,128)S(1)} %copy-done), custom_call_target="tpu_custom_call" | custom-call | tf_op jit(solution)/shard_map/update/pallas_call | solution.py:318
  44.2 1.4 %update.3 = f32[2,4,4,128,128]{4,3,2,1,0:T(8,128)} custom-call(f32[4,3,512]{2,1,0:T(4,128)S(1)} %get-tuple-element.44.gates, f32[2,4,4,128,128]{4,3,2,1,0:T(8,128)S(1)} %copy-done, f32[2,4,4,128,128]{4,3,2,1,0:T(8,128)} %update.2.refs_0_), custom_call_target="tpu_custom_call", output_to_operand_aliasing={{}: (2, {})} | custom-call | tf_op jit(solution)/shard_map/update/pallas_call | solution.py:318
  45.6 1.6 %collective-permute-done.21.refs_2_ = bf16[4,1024]{1,0:T(4,128)(2,1)S(1)} collective-permute-done((bf16[4,1024]{1,0:T(4,128)(2,1)S(1)}, bf16[4,1024]{1,0:T(4,128)(2,1)S(1)}, u32[]{:S(2)}, u32[]{:S(2)}) %collective-permute-start.21) | collective-permute-done | bytes 8224 | tf_op jit(solution)/shard_map/ppermute | solution.py:49
  47.1 0.6 %close.1 = bf16[4,1024]{1,0:T(4,128)(2,1)} custom-call(f32[4,1024]{1,0:T(4,128)S(1)} %get-tuple-element.40.own, bf16[4,1024]{1,0:T(4,128)(2,1)S(1)} %collective-permute-done.19.refs_0_, bf16[4,1024]{1,0:T(4,128)(2,1)S(1)} %collective-permute-done.20.refs_1_, bf16[4,1024]{1,0:T(4,128)(2,1)S(1)} %collective-permute-done.21.refs_2_), custom_call_target="tpu_custom_call" | custom-call | tf_op jit(solution)/shard_map/close/pallas_call | solution.py:349
  (42 shorter events, 2.2 us)
Async XLA Ops:
  0.6 11.5 %copy-start.8 = (bf16[4,1024]{1,0:T(4,128)(2,1)S(1)}, bf16[4,1024]{1,0:T(4,128)(2,1)}, u32[]{:S(2)}) copy-start(bf16[4,1024]{1,0:T(4,128)(2,1)} %refs_0_.1) | copy-start | bytes 24580
  0.6 11.5 %copy-start.6 = (f32[2,1024]{1,0:T(2,128)S(1)}, f32[2,1024]{1,0:T(2,128)}, u32[]{:S(2)}) copy-start(f32[2,1024]{1,0:T(2,128)} %refs_5_.6) | copy-start | bytes 24580
  0.7 11.5 %copy-start.1 = (bf16[2,1024,512]{2,1,0:T(8,128)(2,1)S(1)}, bf16[2,1024,512]{2,1,0:T(8,128)(2,1)}, u32[]{:S(2)}) copy-start(bf16[2,1024,512]{2,1,0:T(8,128)(2,1)} %refs_6_.6) | copy-start | bytes 6291460
  0.7 11.5 %copy-start.2 = (bf16[2,1024,512]{2,1,0:T(8,128)(2,1)S(1)}, bf16[2,1024,512]{2,1,0:T(8,128)(2,1)}, u32[]{:S(2)}) copy-start(bf16[2,1024,512]{2,1,0:T(8,128)(2,1)} %refs_7_.3) | copy-start | bytes 6291460
  0.7 11.5 %copy-start.3 = (bf16[2,1024,512]{2,1,0:T(8,128)(2,1)S(1)}, bf16[2,1024,512]{2,1,0:T(8,128)(2,1)}, u32[]{:S(2)}) copy-start(bf16[2,1024,512]{2,1,0:T(8,128)(2,1)} %refs_8_.3) | copy-start | bytes 6291460
  0.7 11.5 %copy-start.4 = (bf16[2,1024,512]{2,1,0:T(8,128)(2,1)S(1)}, bf16[2,1024,512]{2,1,0:T(8,128)(2,1)}, u32[]{:S(2)}) copy-start(bf16[2,1024,512]{2,1,0:T(8,128)(2,1)} %refs_9_.3) | copy-start | bytes 6291460
  0.7 21.4 %collective-permute-start.9 = (bf16[2,512,1024]{2,1,0:T(8,128)(2,1)}, bf16[2,512,1024]{2,1,0:T(8,128)(2,1)S(1)}, u32[]{:S(2)}, u32[]{:S(2)}) collective-permute-start(bf16[2,512,1024]{2,1,0:T(8,128)(2,1)} %refs_4_.7), channel_id=1, source_target_pairs={{0,1},{1,0},{2,3},{3,2},{4,5},{5,4},{6,7},{7,6},{8,9},{9,8},{10,11... | collective-permute-start | bytes 6291464 | tf_op jit(solution)/shard_map/ppermute | solution.py:58
  1.2 5.3 %collective-permute-start = (bf16[4,1024]{1,0:T(4,128)(2,1)}, bf16[4,1024]{1,0:T(4,128)(2,1)S(1)}, u32[]{:S(2)}, u32[]{:S(2)}) collective-permute-start(bf16[4,1024]{1,0:T(4,128)(2,1)} %refs_0_.1), channel_id=1, source_target_pairs={{4,0},{0,4},{12,8},{8,12},{5,1},{1,5},{13,9},{9,13},{6,2},{2,6},{1... | collective-permute-start | bytes 24584 | tf_op jit(solution)/shard_map/ppermute | solution.py:27
  3.9 4.8 %collective-permute-start.1 = (bf16[4,1024]{1,0:T(4,128)(2,1)}, bf16[4,1024]{1,0:T(4,128)(2,1)S(1)}, u32[]{:S(2)}, u32[]{:S(2)}) collective-permute-start(bf16[4,1024]{1,0:T(4,128)(2,1)} %refs_0_.1), channel_id=1, source_target_pairs={{8,0},{12,4},{0,8},{4,12},{9,1},{13,5},{1,9},{5,13},{10,2},{14,6},... | collective-permute-start | bytes 24584 | tf_op jit(solution)/shard_map/ppermute | solution.py:27
  6.5 5.7 %collective-permute-start.2 = (bf16[4,1024]{1,0:T(4,128)(2,1)}, bf16[4,1024]{1,0:T(4,128)(2,1)S(1)}, u32[]{:S(2)}, u32[]{:S(2)}) collective-permute-start(bf16[4,1024]{1,0:T(4,128)(2,1)} %refs_0_.1), channel_id=1, source_target_pairs={{12,0},{8,4},{4,8},{0,12},{13,1},{9,5},{5,9},{1,13},{14,2},{10,6},... | collective-permute-start | bytes 24584 | tf_op jit(solution)/shard_map/ppermute | solution.py:27
  12.2 5.6 %copy-start = (f32[2,4,4,128,128]{4,3,2,1,0:T(8,128)S(1)}, f32[2,4,4,128,128]{4,3,2,1,0:T(8,128)}, u32[]{:S(2)}) copy-start(f32[2,4,4,128,128]{4,3,2,1,0:T(8,128)} %state.3) | copy-start | bytes 6291460
  12.2 5.6 %copy-start.7 = (f32[2,512]{1,0:T(2,128)S(1)}, f32[2,512]{1,0:T(2,128)}, u32[]{:S(2)}) copy-start(f32[2,512]{1,0:T(2,128)} %refs_4_.6) | copy-start | bytes 12292
  12.2 5.6 %copy-start.9 = (f32[2,128]{1,0:T(2,128)S(1)}, f32[2,128]{1,0:T(2,128)}, u32[]{:S(2)}) copy-start(f32[2,128]{1,0:T(2,128)} %refs_5_.7) | copy-start | bytes 3076
  13.0 9.1 %copy-start.5 = (bf16[2,512,1024]{2,1,0:T(8,128)(2,1)S(1)}, bf16[2,512,1024]{2,1,0:T(8,128)(2,1)}, u32[]{:S(2)}) copy-start(bf16[2,512,1024]{2,1,0:T(8,128)(2,1)} %refs_4_.7) | copy-start | bytes 6291460
  13.0 1.9 %collective-permute-start.3 = (bf16[4,2176]{1,0:T(4,128)(2,1)S(1)}, bf16[4,2176]{1,0:T(4,128)(2,1)S(1)}, u32[]{:S(2)}, u32[]{:S(2)}) collective-permute-start(bf16[4,2176]{1,0:T(4,128)(2,1)S(1)} %get-tuple-element.27), channel_id=1, source_target_pairs={{0,1},{1,0},{2,3},{3,2},{4,5},{5,4},{6,7},{7,6},{8,9},{9,8},{10,11... | collective-permute-start | bytes 52232 | tf_op jit(solution)/shard_map/ppermute | solution.py:27
  13.0 3.8 %collective-permute-start.4 = (bf16[4,2176]{1,0:T(4,128)(2,1)S(1)}, bf16[4,2176]{1,0:T(4,128)(2,1)S(1)}, u32[]{:S(2)}, u32[]{:S(2)}) collective-permute-start(bf16[4,2176]{1,0:T(4,128)(2,1)S(1)} %get-tuple-element.28), channel_id=1, source_target_pairs={{0,2},{1,3},{2,0},{3,1},{4,6},{5,7},{6,4},{7,5},{8,10},{9,11},{10,... | collective-permute-start | bytes 52232 | tf_op jit(solution)/shard_map/ppermute | solution.py:27
  14.6 3.2 %collective-permute-start.5 = (bf16[4,2176]{1,0:T(4,128)(2,1)S(1)}, bf16[4,2176]{1,0:T(4,128)(2,1)S(1)}, u32[]{:S(2)}, u32[]{:S(2)}) collective-permute-start(bf16[4,2176]{1,0:T(4,128)(2,1)S(1)} %get-tuple-element.29), channel_id=1, source_target_pairs={{0,3},{1,2},{2,1},{3,0},{4,7},{5,6},{6,5},{7,4},{8,11},{9,10},{10,... | collective-permute-start | bytes 52232 | tf_op jit(solution)/shard_map/ppermute | solution.py:27
  18.1 1.9 %collective-permute-start.6 = (bf16[4,512]{1,0:T(4,128)(2,1)S(1)}, bf16[4,512]{1,0:T(4,128)(2,1)S(1)}, u32[]{:S(2)}, u32[]{:S(2)}) collective-permute-start(bf16[4,512]{1,0:T(4,128)(2,1)S(1)} %get-tuple-element.30.refs_0_), channel_id=1, source_target_pairs={{1,0},{0,1},{3,2},{2,3},{5,4},{4,5},{7,6},{6,7},{9,8},{8,9},{11,10... | collective-permute-start | bytes 12296 | tf_op jit(solution)/shard_map/ppermute | solution.py:27
  18.4 3.6 %collective-permute-start.7 = (bf16[4,512]{1,0:T(4,128)(2,1)S(1)}, bf16[4,512]{1,0:T(4,128)(2,1)S(1)}, u32[]{:S(2)}, u32[]{:S(2)}) collective-permute-start(bf16[4,512]{1,0:T(4,128)(2,1)S(1)} %get-tuple-element.30.refs_0_), channel_id=1, source_target_pairs={{2,0},{3,1},{0,2},{1,3},{6,4},{7,5},{4,6},{5,7},{10,8},{11,9},{8,1... | collective-permute-start | bytes 12296 | tf_op jit(solution)/shard_map/ppermute | solution.py:27
  19.0 3.0 %collective-permute-start.8 = (bf16[4,512]{1,0:T(4,128)(2,1)S(1)}, bf16[4,512]{1,0:T(4,128)(2,1)S(1)}, u32[]{:S(2)}, u32[]{:S(2)}) collective-permute-start(bf16[4,512]{1,0:T(4,128)(2,1)S(1)} %get-tuple-element.30.refs_0_), channel_id=1, source_target_pairs={{3,0},{2,1},{1,2},{0,3},{7,4},{6,5},{5,6},{4,7},{11,8},{10,9},{9,1... | collective-permute-start | bytes 12296 | tf_op jit(solution)/shard_map/ppermute | solution.py:27
  22.4 3.9 %collective-permute-start.10 = (bf16[16,1024]{1,0:T(8,128)(2,1)S(1)}, bf16[16,1024]{1,0:T(8,128)(2,1)S(1)}, u32[]{:S(2)}, u32[]{:S(2)}) collective-permute-start(bf16[16,1024]{1,0:T(8,128)(2,1)S(1)} %get-tuple-element.32), channel_id=1, source_target_pairs={{0,5},{1,4},{2,7},{3,6},{4,1},{5,0},{6,3},{7,2},{8,13},{9,12},{10,... | collective-permute-start | bytes 98312 | tf_op jit(solution)/shard_map/ppermute | solution.py:49
  22.4 4.3 %collective-permute-start.11 = (bf16[16,1024]{1,0:T(8,128)(2,1)S(1)}, bf16[16,1024]{1,0:T(8,128)(2,1)S(1)}, u32[]{:S(2)}, u32[]{:S(2)}) collective-permute-start(bf16[16,1024]{1,0:T(8,128)(2,1)S(1)} %get-tuple-element.32), channel_id=1, source_target_pairs={{0,9},{1,8},{2,11},{3,10},{4,13},{5,12},{6,15},{7,14},{8,1},{9,0},... | collective-permute-start | bytes 98312 | tf_op jit(solution)/shard_map/ppermute | solution.py:49
  22.9 5.6 %collective-permute-start.12 = (bf16[16,1024]{1,0:T(8,128)(2,1)S(1)}, bf16[16,1024]{1,0:T(8,128)(2,1)S(1)}, u32[]{:S(2)}, u32[]{:S(2)}) collective-permute-start(bf16[16,1024]{1,0:T(8,128)(2,1)S(1)} %get-tuple-element.32), channel_id=1, source_target_pairs={{0,13},{1,12},{2,15},{3,14},{4,9},{5,8},{6,11},{7,10},{8,5},{9,4},... | collective-permute-start | bytes 98312 | tf_op jit(solution)/shard_map/ppermute | solution.py:49
  29.1 1.9 %collective-permute-start.13 = (bf16[4,2176]{1,0:T(4,128)(2,1)S(1)}, bf16[4,2176]{1,0:T(4,128)(2,1)S(1)}, u32[]{:S(2)}, u32[]{:S(2)}) collective-permute-start(bf16[4,2176]{1,0:T(4,128)(2,1)S(1)} %get-tuple-element.34), channel_id=1, source_target_pairs={{0,1},{1,0},{2,3},{3,2},{4,5},{5,4},{6,7},{7,6},{8,9},{9,8},{10,11... | collective-permute-start | bytes 52232 | tf_op jit(solution)/shard_map/ppermute | solution.py:27
  29.5 3.8 %collective-permute-start.14 = (bf16[4,2176]{1,0:T(4,128)(2,1)S(1)}, bf16[4,2176]{1,0:T(4,128)(2,1)S(1)}, u32[]{:S(2)}, u32[]{:S(2)}) collective-permute-start(bf16[4,2176]{1,0:T(4,128)(2,1)S(1)} %get-tuple-element.35), channel_id=1, source_target_pairs={{0,2},{1,3},{2,0},{3,1},{4,6},{5,7},{6,4},{7,5},{8,10},{9,11},{10,... | collective-permute-start | bytes 52232 | tf_op jit(solution)/shard_map/ppermute | solution.py:27
  30.9 3.3 %collective-permute-start.15 = (bf16[4,2176]{1,0:T(4,128)(2,1)S(1)}, bf16[4,2176]{1,0:T(4,128)(2,1)S(1)}, u32[]{:S(2)}, u32[]{:S(2)}) collective-permute-start(bf16[4,2176]{1,0:T(4,128)(2,1)S(1)} %get-tuple-element.36), channel_id=1, source_target_pairs={{0,3},{1,2},{2,1},{3,0},{4,7},{5,6},{6,5},{7,4},{8,11},{9,10},{10,... | collective-permute-start | bytes 52232 | tf_op jit(solution)/shard_map/ppermute | solution.py:27
  34.6 1.9 %collective-permute-start.16 = (bf16[4,512]{1,0:T(4,128)(2,1)S(1)}, bf16[4,512]{1,0:T(4,128)(2,1)S(1)}, u32[]{:S(2)}, u32[]{:S(2)}) collective-permute-start(bf16[4,512]{1,0:T(4,128)(2,1)S(1)} %get-tuple-element.37.refs_0_), channel_id=1, source_target_pairs={{1,0},{0,1},{3,2},{2,3},{5,4},{4,5},{7,6},{6,7},{9,8},{8,9},{11,10... | collective-permute-start | bytes 12296 | tf_op jit(solution)/shard_map/ppermute | solution.py:27
  34.8 3.6 %collective-permute-start.17 = (bf16[4,512]{1,0:T(4,128)(2,1)S(1)}, bf16[4,512]{1,0:T(4,128)(2,1)S(1)}, u32[]{:S(2)}, u32[]{:S(2)}) collective-permute-start(bf16[4,512]{1,0:T(4,128)(2,1)S(1)} %get-tuple-element.37.refs_0_), channel_id=1, source_target_pairs={{2,0},{3,1},{0,2},{1,3},{6,4},{7,5},{4,6},{5,7},{10,8},{11,9},{8,1... | collective-permute-start | bytes 12296 | tf_op jit(solution)/shard_map/ppermute | solution.py:27
  35.5 3.0 %collective-permute-start.18 = (bf16[4,512]{1,0:T(4,128)(2,1)S(1)}, bf16[4,512]{1,0:T(4,128)(2,1)S(1)}, u32[]{:S(2)}, u32[]{:S(2)}) collective-permute-start(bf16[4,512]{1,0:T(4,128)(2,1)S(1)} %get-tuple-element.37.refs_0_), channel_id=1, source_target_pairs={{3,0},{2,1},{1,2},{0,3},{7,4},{6,5},{5,6},{4,7},{11,8},{10,9},{9,1... | collective-permute-start | bytes 12296 | tf_op jit(solution)/shard_map/ppermute | solution.py:27
  39.0 6.6 %collective-permute-start.19 = (bf16[4,1024]{1,0:T(4,128)(2,1)S(1)}, bf16[4,1024]{1,0:T(4,128)(2,1)S(1)}, u32[]{:S(2)}, u32[]{:S(2)}) collective-permute-start(bf16[4,1024]{1,0:T(4,128)(2,1)S(1)} %get-tuple-element.41), channel_id=1, source_target_pairs={{0,5},{1,4},{2,7},{3,6},{4,1},{5,0},{6,3},{7,2},{8,13},{9,12},{10,... | collective-permute-start | bytes 24584 | tf_op jit(solution)/shard_map/ppermute | solution.py:49
  39.4 6.1 %collective-permute-start.20 = (bf16[4,1024]{1,0:T(4,128)(2,1)S(1)}, bf16[4,1024]{1,0:T(4,128)(2,1)S(1)}, u32[]{:S(2)}, u32[]{:S(2)}) collective-permute-start(bf16[4,1024]{1,0:T(4,128)(2,1)S(1)} %get-tuple-element.42), channel_id=1, source_target_pairs={{0,9},{1,8},{2,11},{3,10},{4,13},{5,12},{6,15},{7,14},{8,1},{9,0},... | collective-permute-start | bytes 24584 | tf_op jit(solution)/shard_map/ppermute | solution.py:49
  42.2 4.9 %collective-permute-start.21 = (bf16[4,1024]{1,0:T(4,128)(2,1)S(1)}, bf16[4,1024]{1,0:T(4,128)(2,1)S(1)}, u32[]{:S(2)}, u32[]{:S(2)}) collective-permute-start(bf16[4,1024]{1,0:T(4,128)(2,1)S(1)} %get-tuple-element.43), channel_id=1, source_target_pairs={{0,13},{1,12},{2,15},{3,14},{4,9},{5,8},{6,11},{7,10},{8,5},{9,4},... | collective-permute-start | bytes 24584 | tf_op jit(solution)/shard_map/ppermute | solution.py:49

commit v7 on v6

--- a/solution.py
+++ b/solution.py
@@ -20,14 +20,17 @@
     return (index + k) % n
 
 
-def exchange(axis, n, arrays, inward=False):
-    parts = [None] * (n - 1)
-    for k in reversed(range(1, n)):
+def chip_rounds(n_dp):
+    return list(range(3, n_dp, 2)) if core_flip(n_dp) else list(range(1, n_dp))
+
+
+def exchange(axis, n, arrays, inward=False, rounds=None):
+    rounds = rounds or list(range(1, n))
+    parts = {}
+    for k, array in reversed(list(zip(rounds, arrays))):
         pairs = [(i, peer_of(n, k, i)) for i in range(n)]
-        parts[k - 1] = lax.ppermute(
-            arrays[k - 1], axis, [(b, a) for a, b in pairs] if inward else pairs
-        )
-    return parts
+        parts[k] = lax.ppermute(array, axis, [(b, a) for a, b in pairs] if inward else pairs)
+    return [parts[k] for k in rounds]
 
 
 def core_flip(n_dp):
@@ -52,14 +55,17 @@
     return parts
 
 
-def cross_weight(n_dp, array):
+def cross_copy(n_dp, array):
     if not core_flip(n_dp):
         return array
     return lax.ppermute(array, "dp", [(d, d ^ 1) for d in range(n_dp)])
 
 
-def gather(axis, n, array):
-    return [array] + exchange(axis, n, [array] * (n - 1), inward=True)
+def gather(axis, n, array, rounds=None):
+    rounds = list(range(1, n)) if rounds is None else rounds
+    if not rounds:
+        return [array]
+    return [array] + exchange(axis, n, [array] * len(rounds), True, rounds)
 
 
 def split(array):
@@ -68,7 +74,8 @@
 
 
 def finish_projection(base, gain_ref, layer, weights, outs):
-    count = outs[0].shape[0]
+    count = base.shape[0] // len(outs)
+    group = outs[0].shape[0] // count
     squares = jnp.sum(base * base, axis=1, keepdims=True)
     scaled = (base * gain_ref[layer : layer + 1, :]).astype(BF16)
     high, _ = split(squares)
@@ -83,11 +90,15 @@
     for index, weight in enumerate(weights):
         product = jnp.dot(scaled, weight[layer], preferred_element_type=F32)
         for k, out in enumerate(outs):
-            out[:, index * width : (index + 1) * width] = product[
-                k * count : (k + 1) * count
-            ].astype(out.dtype)
+            for member in range(group):
+                block = slice((k ^ member) * count, ((k ^ member) + 1) * count)
+                rows = slice(member * count, (member + 1) * count)
+                out[rows, index * width : (index + 1) * width] = product[block].astype(out.dtype)
     for k, out in enumerate(outs):
-        out[:, 4 * width :] = tail[k * count : (k + 1) * count].astype(out.dtype)
+        for member in range(group):
+            block = slice((k ^ member) * count, ((k ^ member) + 1) * count)
+            rows = slice(member * count, (member + 1) * count)
+            out[rows, 4 * width :] = tail[block].astype(out.dtype)
 
 
 def project_first(n_tp, layer, *refs):
@@ -102,10 +113,10 @@
 
 
 def project_next(n_tp, layer, *refs):
-    (base_in, mixed), parts = refs[:2], refs[2 : n_tp + 1]
-    gain, weights = refs[n_tp + 1], refs[n_tp + 2 : n_tp + 6]
-    base_out, outs = refs[n_tp + 6], refs[n_tp + 7 :]
-    base = base_in[...].astype(F32) + mixed[...]
+    held, parts = refs[0], refs[1:n_tp]
+    gain, weights = refs[n_tp], refs[n_tp + 1 : n_tp + 5]
+    base_out, outs = refs[n_tp + 5], refs[n_tp + 6 :]
+    base = held[...]
     for part in parts:
         base = base + part[...].astype(F32)
     rounded = base.astype(BF16)
@@ -113,10 +124,12 @@
     finish_projection(rounded.astype(F32), gain, layer, weights, outs)
 
 
-def recur(n_dp, layer, features, *refs):
+def recur(n_dp, layer, features, group, *refs):
     own, parts = refs[0], refs[1:n_dp]
-    bound_ref, head_gain, state, normed, gates, left = refs[n_dp:]
-    seqs, heads, hd = state.shape[1], state.shape[2], state.shape[3]
+    (bound_ref, head_gain), states = refs[n_dp : n_dp + 2], refs[n_dp + 2 : n_dp + 2 + group]
+    normed, gates, left = refs[n_dp + 2 + group :]
+    kept, heads, hd = states[0].shape[1:4]
+    seqs = group * kept
     width = heads * hd
     total = own[...]
     for part in parts:
@@ -129,7 +142,7 @@
     bound = bound_ref[layer : layer + 1, :]
     forget = bound + (1.0 - bound) * jax.nn.sigmoid(forget_pre)
     keyvec = (1.0 - bound) * jax.nn.sigmoid(-forget_pre)
-    for seq in range(seqs):
+    for seq in range(kept):
         for index, vector in enumerate((forget, keyvec, value)):
             gates[seq, index : index + 1, :] = vector[seq : seq + 1]
     gate = jax.nn.sigmoid(gate_pre)
@@ -137,9 +150,9 @@
     shared = query * keyvec
     row = lax.broadcasted_iota(jnp.int32, (seqs, hd), 0)
     terms = [term.astype(F32) for term in split(weighted)]
-    group = 2 if heads % 2 == 0 else 1
-    for first in range(0, heads, group):
-        for index in range(group):
+    wide = 2 if heads % 2 == 0 else 1
+    for first in range(0, heads, wide):
+        for index in range(wide):
             cols = slice((first + index) * hd, (first + index + 1) * hd)
             for part, term in enumerate(terms):
                 top = (index * 2 + part) * seqs
@@ -150,16 +163,20 @@
         right = jnp.concatenate(
             [
                 jnp.concatenate(
-                    [state[layer, seq, first + index].astype(BF16) for seq in range(seqs)], axis=0
+                    [
+                        states[seq // kept][layer, seq % kept, first + index]
+                        for seq in range(seqs)
+                    ],
+                    axis=0,
                 )
-                for index in range(group)
+                for index in range(wide)
             ],
             axis=1,
         )
         product = jnp.dot(
-            left[: 2 * group * seqs, :].astype(BF16), right, preferred_element_type=F32
+            left[: 2 * wide * seqs, :].astype(BF16), right, preferred_element_type=F32
         )
-        for index in range(group):
+        for index in range(wide):
             head = first + index
             cols = slice(head * hd, (head + 1) * hd)
             own_cols = slice(index * hd, (index + 1) * hd)
@@ -190,34 +207,65 @@
         copy.wait()
 
 
+def narrow(state, out, staged, sems):
+    places = [(layer, seq) for layer in range(state.shape[0]) for seq in range(state.shape[1])]
+    copies = [
+        pltpu.make_async_copy(state.at[place], staged.at[place], sems.at[index])
+        for index, place in enumerate(places)
+    ]
+    for copy in copies:
+        copy.start()
+    for copy, place in zip(copies, places):
+        copy.wait()
+        out[place] = staged[place].astype(BF16)
+
+
+def slot_parts(refs, group):
+    count = refs[0].shape[0] // group
+    if group == 1:
+        return [(ref, 0, count) for ref in refs]
+    parts = [(refs[0], 0, count), (refs[0], count, count)]
+    for ref in refs[1:]:
+        parts += [(ref, count, count), (ref, 0, count)]
+    return parts
+
+
 def gather_rows(parts, slots):
-    rows = parts[0].shape[0]
-    for k, part in enumerate(parts):
-        slots[k * rows : (k + 1) * rows, :] = part[...].astype(F32)
+    for k, (ref, top, count) in enumerate(parts):
+        slots[k * count : (k + 1) * count, :] = ref[top : top + count, :].astype(F32)
     return slots[...].astype(BF16)
 
 
-def mix_next(n_dp, layer, *refs):
-    parts, (weight, crossed, mixed, sent, slots) = refs[:n_dp], refs[n_dp:]
-    facing = [parts[k ^ core_flip(n_dp)] for k in range(n_dp)]
+def mix_next(n_chip, group, layer, *refs):
+    parts, (crossed, sent, slots) = slot_parts(refs[:n_chip], group), refs[n_chip:]
+    facing = [parts[k ^ (group - 1)] for k in range(len(parts))]
     rows = gather_rows(facing, slots)
     sent[...] = jnp.dot(rows, crossed[layer], preferred_element_type=F32).astype(BF16)
+
+
+def own_next(n_chip, group, layer, *refs):
+    parts, (weight, base, held, slots) = slot_parts(refs[:n_chip], group), refs[n_chip:]
     rows = gather_rows(parts, slots)
-    mixed[...] = jnp.dot(rows, weight[layer], preferred_element_type=F32)
-
-
-def mix_last(n_dp, layer, *refs):
-    parts, (weight, crossed, base, order) = refs[:n_dp], refs[n_dp : n_dp + 4]
-    own, outs, slots = refs[n_dp + 4], refs[n_dp + 5 : -1], refs[-1]
+    held[...] = base[...].astype(F32) + jnp.dot(rows, weight[layer], preferred_element_type=F32)
+
+
+def mix_last(n_chip, group, layer, *refs):
+    parts, (crossed, order) = slot_parts(refs[:n_chip], group), refs[n_chip : n_chip + 2]
+    outs, slots = refs[n_chip + 2 : -1], refs[-1]
+    rows = outs[0].shape[0]
+    moved = jnp.dot(order[...], gather_rows(parts, slots), preferred_element_type=F32)
+    product = jnp.dot(moved.astype(BF16), crossed[layer], preferred_element_type=F32)
+    for k, out in enumerate(outs):
+        out[...] = product[(k + 1) * rows : (k + 2) * rows].astype(BF16)
+
+
+def own_last(n_chip, group, layer, *refs):
+    parts, (weight, base, order, own, slots) = slot_parts(refs[:n_chip], group), refs[n_chip:]
     rows = own.shape[0]
     moved = jnp.dot(order[...], gather_rows(parts, slots), preferred_element_type=F32)
-    moved = moved.astype(BF16)
-    product = jnp.dot(moved, crossed[layer], preferred_element_type=F32)
-    for k, out in enumerate(outs):
-        out[...] = product[(k + 1) * rows : (k + 2) * rows].astype(BF16)
-    own[...] = jnp.dot(moved, weight[layer], preferred_element_type=F32)[:rows] + jnp.dot(
-        order[:rows, :], base[...], preferred_element_type=F32
-    )
+    own[...] = jnp.dot(moved.astype(BF16), weight[layer], preferred_element_type=F32)[
+        :rows
+    ] + jnp.dot(order[:rows, :], base[...], preferred_element_type=F32)
 
 
 def close(own, *refs):
@@ -284,12 +332,27 @@
         flops=20_000_000_000,
     )
     parts = gather("tp", n_tp, tokens)
-    crossed = cross_weight(n_dp, w_out)
-    base = mixed = None
+    flip = core_flip(n_dp)
+    group, n_chip = flip + 1, n_dp // (flip + 1)
+    narrowed = pl.pallas_call(
+        narrow,
+        name="narrow",
+        out_shape=pltpu.VMEM(state.shape, BF16),
+        in_specs=[ANY],
+        out_specs=VMEM,
+        scratch_shapes=[
+            pltpu.VMEM(state.shape, F32),
+            pltpu.SemaphoreType.DMA((state.shape[0] * seqs,)),
+        ],
+        compiler_params=pltpu.CompilerParams(vmem_limit_bytes=4 << 20),
+    )(pltpu.with_memory_space_constraint(state, pltpu.HBM))
+    states = [narrowed] + [cross_copy(n_dp, narrowed)] * flip
+    crossed = cross_copy(n_dp, w_out)
+    base = held = None
     new_state = None
     for layer in range(2):
-        outs = [((total, local), BF16), ((seqs, 4 * width + LANES), F32)]
-        outs += [((seqs, 4 * width + LANES), BF16)] * (n_dp - 1)
+        message = (group * seqs, 4 * width + LANES)
+        outs = [((total, local), BF16), (message, F32)] + [(message, BF16)] * (n_dp - 1)
         specs = [VMEM] * 4
         if layer == 0:
             base, own, *sent = call(
@@ -302,19 +365,20 @@
         else:
             base, own, *sent = call(
                 functools.partial(project_next, n_tp, layer),
-                (base, mixed, *parts, norm_gain, *weights),
-                [VMEM] * (n_tp + 2) + specs,
+                (held, *parts, norm_gain, *weights),
+                [VMEM] * (n_tp + 1) + specs,
                 outs,
             )
         parts = exchange("dp", n_dp, sent)
         normed, gates = call(
-            functools.partial(recur, n_dp, layer, features),
-            (own, *parts, lower_bound, head_gain, state),
-            [VMEM] * (n_dp + 2) + [VMEM],
-            [((seqs, width), BF16), ((seqs, 3, width), F32)],
-            [((4 * seqs, seqs * hd), F32)],
+            functools.partial(recur, n_dp, layer, features, group),
+            (own, *parts, lower_bound, head_gain, *states),
+            [VMEM] * (n_dp + 2 + group),
+            [((group * seqs, width), BF16), ((seqs, 3, width), F32)],
+            [((4 * group * seqs, group * seqs * hd), F32)],
         )
-        parts = gather("dp", n_dp, normed)
+        read = gather("dp", n_dp, normed, chip_rounds(n_dp))
+        slots = [((total, width), F32)]
         new_state = pl.pallas_call(
             functools.partial(update, layer),
             name="update",
@@ -329,23 +393,37 @@
             compiler_params=pltpu.CompilerParams(vmem_limit_bytes=4 << 20),
         )(in_vmem(gates), in_vmem(state), *((new_state,) if layer else ()))
         if layer == 0:
-            mixed, sent = call(
-                functools.partial(mix_next, n_dp, layer),
-                (*parts, w_out, crossed),
-                [VMEM] * (n_dp + 2),
-                [((total, local), F32), ((total, local), BF16)],
-                [((total, width), F32)],
+            (sent,) = call(
+                functools.partial(mix_next, n_chip, group, layer),
+                (*read, crossed),
+                [VMEM] * (n_chip + 1),
+                [((total, local), BF16)],
+                slots,
             )
             parts = cross_exchange(n_tp, n_dp, [sent] * (n_tp - 1))
+            (held,) = call(
+                functools.partial(own_next, n_chip, group, layer),
+                (*read, w_out, base),
+                [VMEM] * (n_chip + 2),
+                [((total, local), F32)],
+                slots,
+            )
         else:
-            own, *sent = call(
-                functools.partial(mix_last, n_dp, layer),
-                (*parts, w_out, crossed, base, order_out),
-                [VMEM] * (n_dp + 4),
-                [((rows, local), F32)] + [((rows, local), BF16)] * (n_tp - 1),
-                [((total, width), F32)],
+            sent = call(
+                functools.partial(mix_last, n_chip, group, layer),
+                (*read, crossed, order_out),
+                [VMEM] * (n_chip + 2),
+                [((rows, local), BF16)] * (n_tp - 1),
+                slots,
             )
             parts = cross_exchange(n_tp, n_dp, sent)
+            (own,) = call(
+                functools.partial(own_last, n_chip, group, layer),
+                (*read, w_out, base, order_out),
+                [VMEM] * (n_chip + 3),
+                [((rows, local), F32)],
+                slots,
+            )
     hidden = pl.pallas_call(
         close,
         name="close",

time: 47.9 us -> 47.4 us (0.990)
  starting transfers between devices: 21.1 us -> 18.8 us
  Pallas kernels: 6.34 us -> 8.39 us
    ppermute x16 -> x13, starting transfers between devices: 13.4 us -> 11.1 us  [the longest x11 10.5 us: exchange(): lax.ppermute(array, axis, [(b, a) for a, b in pairs] if inward else pairs)]
    pallas_call x0 -> x1, Pallas kernels: none -> 1.58 us  [per_device(): pl.pallas_call(narrow, name='narrow', out_shape=pltpu.VMEM(state.shape, B...]
    ppermute x16 -> x13, waiting for transfers between devices: 15.7 us -> 14.6 us  [the longest x11 14.6 us: exchange(): lax.ppermute(array, axis, [(b, a) for a, b in pairs] if inward else pairs)]
    ppermute x6, waiting for transfers between devices: 3.74 us -> 4.48 us  [cross_exchange(): lax.ppermute(arrays[k - 1], ('tp', 'dp'), cross_pairs(n_tp, n_dp, k))]
    pallas_call x7 -> x9, Pallas kernels: 3.04 us -> 3.5 us  [call(): pl.pallas_call(body, out_shape=[pltpu.VMEM(shape, dtype) for shape, dtype...]
  transfers between devices with their start and end apart: 22 -> 19, of which waited for: 13 -> 10; matrix products, arithmetic and copies ran while one was open for 0% -> 0% of each run, Pallas kernels for 8% -> 13%
where the time goes in v7:
time: 47.4 us; the launch traced here: 47.2 us
  waiting for transfers between devices  19.1 us (40%)
  starting transfers between devices  18.8 us (40%)
  Pallas kernels  8.39 us (18%)
  between operations  0.85 us (2%)
    ppermute x11, waiting for transfers between devices, exchange(): lax.ppermute(array, axis, [(b, a) for a, b in pairs] if inward else pairs)  14.6 us
    ppermute x11, starting transfers between devices, exchange(): lax.ppermute(array, axis, [(b, a) for a, b in pairs] if inward else pairs)  10.5 us
    ppermute x6, starting transfers between devices, cross_exchange(): lax.ppermute(arrays[k - 1], ('tp', 'dp'), cross_pairs(n_tp, n_dp, k))  7.73 us
    ppermute x6, waiting for transfers between devices, cross_exchange(): lax.ppermute(arrays[k - 1], ('tp', 'dp'), cross_pairs(n_tp, n_dp, k))  4.48 us
    pallas_call x9, Pallas kernels, call(): pl.pallas_call(body, out_shape=[pltpu.VMEM(shape, dtype) for shape, dtype...  3.5 us
    pallas_call x2, Pallas kernels, per_device(): pl.pallas_call(functools.partial(update, layer), name='update', out_shape...  2.69 us
    pallas_call x1, Pallas kernels, per_device(): pl.pallas_call(narrow, name='narrow', out_shape=pltpu.VMEM(state.shape, B...  1.58 us
  transfers between devices with their start and end apart: 19, of which 10 were waited for; matrix products, arithmetic and copies ran while one was open for 0% of the time, Pallas kernels for 13%

profile of v7, /device:TPU:0, one launch (start us, length us, event | category | flops | bytes accessed | tf_op | source)
XLA Modules:
  0.0 47.2 jit_solution(16469228133793750262)
XLA Ops:
  0.6 0.6 %collective-permute-start.8 = (bf16[2,512,1024]{2,1,0:T(8,128)(2,1)}, bf16[2,512,1024]{2,1,0:T(8,128)(2,1)S(1)}, u32[]{:S(2)}, u32[]{:S(2)}) collective-permute-start(bf16[2,512,1024]{2,1,0:T(8,128)(2,1)} %refs_2_.3), channel_id=1, source_target_pairs={{0,1},{1,0},{2,3},{3,2},{4,5},{5,4},{6,7},{7,6},{8,9},{9,8},{10,11... | collective-permute-start | bytes 6291464 | tf_op jit(solution)/shard_map/ppermute | solution.py:61
  1.2 2.6 %collective-permute-start = (bf16[4,1024]{1,0:T(4,128)(2,1)}, bf16[4,1024]{1,0:T(4,128)(2,1)S(1)}, u32[]{:S(2)}, u32[]{:S(2)}) collective-permute-start(bf16[4,1024]{1,0:T(4,128)(2,1)} %refs_0_.1), channel_id=1, source_target_pairs={{4,0},{0,4},{12,8},{8,12},{5,1},{1,5},{13,9},{9,13},{6,2},{2,6},{1... | collective-permute-start | bytes 24584 | tf_op jit(solution)/shard_map/ppermute | solution.py:32
  3.8 2.6 %collective-permute-start.1 = (bf16[4,1024]{1,0:T(4,128)(2,1)}, bf16[4,1024]{1,0:T(4,128)(2,1)S(1)}, u32[]{:S(2)}, u32[]{:S(2)}) collective-permute-start(bf16[4,1024]{1,0:T(4,128)(2,1)} %refs_0_.1), channel_id=1, source_target_pairs={{8,0},{12,4},{0,8},{4,12},{9,1},{13,5},{1,9},{5,13},{10,2},{14,6},... | collective-permute-start | bytes 24584 | tf_op jit(solution)/shard_map/ppermute | solution.py:32
  6.4 1.6 %narrow.1.refs_6_ = bf16[2,4,4,128,128]{4,3,2,1,0:T(8,128)(2,1)S(1)} custom-call(f32[2,4,4,128,128]{4,3,2,1,0:T(8,128)} %state.5), custom_call_target="tpu_custom_call" | custom-call | tf_op jit(solution)/shard_map/narrow/pallas_call | solution.py:337
  8.2 0.4 collective-permute-done.1.refs_2_
  8.6 3.5 %collective-permute-done.2.refs_3_ = bf16[4,1024]{1,0:T(4,128)(2,1)S(1)} collective-permute-done((bf16[4,1024]{1,0:T(4,128)(2,1)}, bf16[4,1024]{1,0:T(4,128)(2,1)S(1)}, u32[]{:S(2)}, u32[]{:S(2)}) %collective-permute-start.2) | collective-permute-done | bytes 8224 | tf_op jit(solution)/shard_map/ppermute | solution.py:32
  12.1 0.8 %shard_map.114 = (bf16[16,1024]{1,0:T(8,128)(2,1)S(1)}, f32[8,2176]{1,0:T(8,128)S(1)}, bf16[8,2176]{1,0:T(8,128)(2,1)S(1)}, bf16[8,2176]{1,0:T(8,128)(2,1)S(1)}, bf16[8,2176]{1,0:T(8,128)(2,1)S(1)}) custom-call(bf16[4,1024]{1,0:T(4,128)(2,1)S(1)} %copy-done.8, bf16[4,1024]{1,0:T(4,128)(2,1)S(1)} %collective-permute-done.refs_1_, ...), custom_call_target="tpu_custom_call" | custom-call | tf_op jit(solution)/shard_map/pallas_call | solution.py:296
  12.9 1.6 %collective-permute-start.4 = (bf16[8,2176]{1,0:T(8,128)(2,1)S(1)}, bf16[8,2176]{1,0:T(8,128)(2,1)S(1)}, u32[]{:S(2)}, u32[]{:S(2)}) collective-permute-start(bf16[8,2176]{1,0:T(8,128)(2,1)S(1)} %get-tuple-element.24), channel_id=1, source_target_pairs={{0,2},{1,3},{2,0},{3,1},{4,6},{5,7},{6,4},{7,5},{8,10},{9,11},{10,... | collective-permute-start | bytes 104456 | tf_op jit(solution)/shard_map/ppermute | solution.py:32
  14.8 2.1 %collective-permute-done.4.refs_2_ = bf16[8,2176]{1,0:T(8,128)(2,1)S(1)} collective-permute-done((bf16[8,2176]{1,0:T(8,128)(2,1)S(1)}, bf16[8,2176]{1,0:T(8,128)(2,1)S(1)}, u32[]{:S(2)}, u32[]{:S(2)}) %collective-permute-start.4) | collective-permute-done | bytes 34848 | tf_op jit(solution)/shard_map/ppermute | solution.py:32
  16.9 1.0 %collective-permute-done.5.refs_3_ = bf16[8,2176]{1,0:T(8,128)(2,1)S(1)} collective-permute-done((bf16[8,2176]{1,0:T(8,128)(2,1)S(1)}, bf16[8,2176]{1,0:T(8,128)(2,1)S(1)}, u32[]{:S(2)}, u32[]{:S(2)}) %collective-permute-start.5) | collective-permute-done | bytes 34848 | tf_op jit(solution)/shard_map/ppermute | solution.py:32
  17.9 0.4 shard_map.115
  18.4 0.7 %collective-permute-start.7 = (bf16[8,512]{1,0:T(8,128)(2,1)S(1)}, bf16[8,512]{1,0:T(8,128)(2,1)S(1)}, u32[]{:S(2)}, u32[]{:S(2)}) collective-permute-start(bf16[8,512]{1,0:T(8,128)(2,1)S(1)} %get-tuple-element.26.refs_0_), channel_id=1, source_target_pairs={{3,0},{2,1},{1,2},{0,3},{7,4},{6,5},{5,6},{4,7},{11,8},{10,9},{9,1... | collective-permute-start | bytes 24584 | tf_op jit(solution)/shard_map/ppermute | solution.py:32
  19.1 2.4 %collective-permute-done.7.refs_1_ = bf16[8,512]{1,0:T(8,128)(2,1)S(1)} collective-permute-done((bf16[8,512]{1,0:T(8,128)(2,1)S(1)}, bf16[8,512]{1,0:T(8,128)(2,1)S(1)}, u32[]{:S(2)}, u32[]{:S(2)}) %collective-permute-start.7) | collective-permute-done | bytes 8224 | tf_op jit(solution)/shard_map/ppermute | solution.py:32
  21.8 3.4 %collective-permute-start.10 = (bf16[16,1024]{1,0:T(8,128)(2,1)S(1)}, bf16[16,1024]{1,0:T(8,128)(2,1)S(1)}, u32[]{:S(2)}, u32[]{:S(2)}) collective-permute-start(bf16[16,1024]{1,0:T(8,128)(2,1)S(1)} %shard_map.117), channel_id=1, source_target_pairs={{0,9},{1,8},{2,11},{3,10},{4,13},{5,12},{6,15},{7,14},{8,1},{9,0},... | collective-permute-start | bytes 98312 | tf_op jit(solution)/shard_map/ppermute | solution.py:52
  25.2 0.4 collective-permute-start.11
  25.9 1.0 %collective-permute-done.10.refs_2_ = bf16[16,1024]{1,0:T(8,128)(2,1)S(1)} collective-permute-done((bf16[16,1024]{1,0:T(8,128)(2,1)S(1)}, bf16[16,1024]{1,0:T(8,128)(2,1)S(1)}, u32[]{:S(2)}, u32[]{:S(2)}) %collective-permute-start.10) | collective-permute-done | bytes 32800 | tf_op jit(solution)/shard_map/ppermute | solution.py:52
  26.9 3.4 %collective-permute-done.11.refs_3_ = bf16[16,1024]{1,0:T(8,128)(2,1)S(1)} collective-permute-done((bf16[16,1024]{1,0:T(8,128)(2,1)S(1)}, bf16[16,1024]{1,0:T(8,128)(2,1)S(1)}, u32[]{:S(2)}, u32[]{:S(2)}) %collective-permute-start.11) | collective-permute-done | bytes 32800 | tf_op jit(solution)/shard_map/ppermute | solution.py:52
  30.4 0.7 %shard_map.118 = (bf16[16,1024]{1,0:T(8,128)(2,1)S(1)}, f32[8,2176]{1,0:T(8,128)S(1)}, bf16[8,2176]{1,0:T(8,128)(2,1)S(1)}, bf16[8,2176]{1,0:T(8,128)(2,1)S(1)}, bf16[8,2176]{1,0:T(8,128)(2,1)S(1)}) custom-call(f32[16,1024]{1,0:T(8,128)S(1)} %shard_map.116.refs_0_, bf16[16,1024]{1,0:T(8,128)(2,1)S(1)} %collective-permute-done.9.refs_1_, ...), custom_call_target="tpu_custom_call" | custom-call | tf_op jit(solution)/shard_map/pallas_call | solution.py:296
  31.2 0.9 %collective-permute-start.13 = (bf16[8,2176]{1,0:T(8,128)(2,1)S(1)}, bf16[8,2176]{1,0:T(8,128)(2,1)S(1)}, u32[]{:S(2)}, u32[]{:S(2)}) collective-permute-start(bf16[8,2176]{1,0:T(8,128)(2,1)S(1)} %get-tuple-element.30), channel_id=1, source_target_pairs={{0,2},{1,3},{2,0},{3,1},{4,6},{5,7},{6,4},{7,5},{8,10},{9,11},{10,... | collective-permute-start | bytes 104456 | tf_op jit(solution)/shard_map/ppermute | solution.py:32
  32.1 0.8 %collective-permute-start.14 = (bf16[8,2176]{1,0:T(8,128)(2,1)S(1)}, bf16[8,2176]{1,0:T(8,128)(2,1)S(1)}, u32[]{:S(2)}, u32[]{:S(2)}) collective-permute-start(bf16[8,2176]{1,0:T(8,128)(2,1)S(1)} %get-tuple-element.31), channel_id=1, source_target_pairs={{0,3},{1,2},{2,1},{3,0},{4,7},{5,6},{6,5},{7,4},{8,11},{9,10},{10,... | collective-permute-start | bytes 104456 | tf_op jit(solution)/shard_map/ppermute | solution.py:32
  32.9 2.3 %collective-permute-done.13.refs_2_ = bf16[8,2176]{1,0:T(8,128)(2,1)S(1)} collective-permute-done((bf16[8,2176]{1,0:T(8,128)(2,1)S(1)}, bf16[8,2176]{1,0:T(8,128)(2,1)S(1)}, u32[]{:S(2)}, u32[]{:S(2)}) %collective-permute-start.13) | collective-permute-done | bytes 34848 | tf_op jit(solution)/shard_map/ppermute | solution.py:32
  35.2 0.5 %collective-permute-done.14.refs_3_ = bf16[8,2176]{1,0:T(8,128)(2,1)S(1)} collective-permute-done((bf16[8,2176]{1,0:T(8,128)(2,1)S(1)}, bf16[8,2176]{1,0:T(8,128)(2,1)S(1)}, u32[]{:S(2)}, u32[]{:S(2)}) %collective-permute-start.14) | collective-permute-done | bytes 34848 | tf_op jit(solution)/shard_map/ppermute | solution.py:32
  35.7 0.4 shard_map.119
  36.2 0.8 %collective-permute-start.15 = (bf16[8,512]{1,0:T(8,128)(2,1)S(1)}, bf16[8,512]{1,0:T(8,128)(2,1)S(1)}, u32[]{:S(2)}, u32[]{:S(2)}) collective-permute-start(bf16[8,512]{1,0:T(8,128)(2,1)S(1)} %get-tuple-element.32.refs_0_), channel_id=1, source_target_pairs={{3,0},{2,1},{1,2},{0,3},{7,4},{6,5},{5,6},{4,7},{11,8},{10,9},{9,1... | collective-permute-start | bytes 24584 | tf_op jit(solution)/shard_map/ppermute | solution.py:32
  37.0 2.4 %collective-permute-done.15.refs_1_ = bf16[8,512]{1,0:T(8,128)(2,1)S(1)} collective-permute-done((bf16[8,512]{1,0:T(8,128)(2,1)S(1)}, bf16[8,512]{1,0:T(8,128)(2,1)S(1)}, u32[]{:S(2)}, u32[]{:S(2)}) %collective-permute-start.15) | collective-permute-done | bytes 8224 | tf_op jit(solution)/shard_map/ppermute | solution.py:32
  39.3 0.3 shard_map.121
  39.7 1.1 %collective-permute-start.17 = (bf16[4,1024]{1,0:T(4,128)(2,1)S(1)}, bf16[4,1024]{1,0:T(4,128)(2,1)S(1)}, u32[]{:S(2)}, u32[]{:S(2)}) collective-permute-start(bf16[4,1024]{1,0:T(4,128)(2,1)S(1)} %get-tuple-element.36), channel_id=1, source_target_pairs={{0,9},{1,8},{2,11},{3,10},{4,13},{5,12},{6,15},{7,14},{8,1},{9,0},... | collective-permute-start | bytes 24584 | tf_op jit(solution)/shard_map/ppermute | solution.py:52
  40.8 2.7 %collective-permute-start.18 = (bf16[4,1024]{1,0:T(4,128)(2,1)S(1)}, bf16[4,1024]{1,0:T(4,128)(2,1)S(1)}, u32[]{:S(2)}, u32[]{:S(2)}) collective-permute-start(bf16[4,1024]{1,0:T(4,128)(2,1)S(1)} %get-tuple-element.37), channel_id=1, source_target_pairs={{0,13},{1,12},{2,15},{3,14},{4,9},{5,8},{6,11},{7,10},{8,5},{9,4},... | collective-permute-start | bytes 24584 | tf_op jit(solution)/shard_map/ppermute | solution.py:52
  43.5 1.3 %update.2.refs_0_ = f32[2,4,4,128,128]{4,3,2,1,0:T(8,128)} custom-call(f32[4,3,512]{2,1,0:T(4,128)S(1)} %get-tuple-element.39.gates, f32[2,4,4,128,128]{4,3,2,1,0:T(8,128)S(1)} %copy-done), custom_call_target="tpu_custom_call" | custom-call | tf_op jit(solution)/shard_map/update/pallas_call | solution.py:382
  44.9 1.3 %update.3 = f32[2,4,4,128,128]{4,3,2,1,0:T(8,128)} custom-call(f32[4,3,512]{2,1,0:T(4,128)S(1)} %get-tuple-element.38.gates, f32[2,4,4,128,128]{4,3,2,1,0:T(8,128)S(1)} %copy-done, f32[2,4,4,128,128]{4,3,2,1,0:T(8,128)} %update.2.refs_0_), custom_call_target="tpu_custom_call", output_to_operand_aliasing={{}: (2, {})} | custom-call | tf_op jit(solution)/shard_map/update/pallas_call | solution.py:382
  46.2 0.3 shard_map.120.own
  46.6 0.6 %close.1 = bf16[4,1024]{1,0:T(4,128)(2,1)} custom-call(f32[4,1024]{1,0:T(4,128)S(1)} %shard_map.120.own, bf16[4,1024]{1,0:T(4,128)(2,1)S(1)} %collective-permute-done.16.refs_0_, bf16[4,1024]{1,0:T(4,128)(2,1)S(1)} %collective-permute-done.17.refs_1_, bf16[4,1024]{1,0:T(4,128)(2,1)S(1)} %collective-permute-done.18.refs_2_), custom_call_target="tpu_custom_call" | custom-call | tf_op jit(solution)/shard_map/close/pallas_call | solution.py:427
  (39 shorter events, 1.2 us)
Async XLA Ops:
  0.6 20.9 %collective-permute-start.8 = (bf16[2,512,1024]{2,1,0:T(8,128)(2,1)}, bf16[2,512,1024]{2,1,0:T(8,128)(2,1)S(1)}, u32[]{:S(2)}, u32[]{:S(2)}) collective-permute-start(bf16[2,512,1024]{2,1,0:T(8,128)(2,1)} %refs_2_.3), channel_id=1, source_target_pairs={{0,1},{1,0},{2,3},{3,2},{4,5},{5,4},{6,7},{7,6},{8,9},{9,8},{10,11... | collective-permute-start | bytes 6291464 | tf_op jit(solution)/shard_map/ppermute | solution.py:61
  1.2 7.0 %collective-permute-start = (bf16[4,1024]{1,0:T(4,128)(2,1)}, bf16[4,1024]{1,0:T(4,128)(2,1)S(1)}, u32[]{:S(2)}, u32[]{:S(2)}) collective-permute-start(bf16[4,1024]{1,0:T(4,128)(2,1)} %refs_0_.1), channel_id=1, source_target_pairs={{4,0},{0,4},{12,8},{8,12},{5,1},{1,5},{13,9},{9,13},{6,2},{2,6},{1... | collective-permute-start | bytes 24584 | tf_op jit(solution)/shard_map/ppermute | solution.py:32
  3.8 4.8 %collective-permute-start.1 = (bf16[4,1024]{1,0:T(4,128)(2,1)}, bf16[4,1024]{1,0:T(4,128)(2,1)S(1)}, u32[]{:S(2)}, u32[]{:S(2)}) collective-permute-start(bf16[4,1024]{1,0:T(4,128)(2,1)} %refs_0_.1), channel_id=1, source_target_pairs={{8,0},{12,4},{0,8},{4,12},{9,1},{13,5},{1,9},{5,13},{10,2},{14,6},... | collective-permute-start | bytes 24584 | tf_op jit(solution)/shard_map/ppermute | solution.py:32
  6.4 5.7 %collective-permute-start.2 = (bf16[4,1024]{1,0:T(4,128)(2,1)}, bf16[4,1024]{1,0:T(4,128)(2,1)S(1)}, u32[]{:S(2)}, u32[]{:S(2)}) collective-permute-start(bf16[4,1024]{1,0:T(4,128)(2,1)} %refs_0_.1), channel_id=1, source_target_pairs={{12,0},{8,4},{4,8},{0,12},{13,1},{9,5},{5,9},{1,13},{14,2},{10,6},... | collective-permute-start | bytes 24584 | tf_op jit(solution)/shard_map/ppermute | solution.py:32
  8.0 4.1 %copy-start.1 = (bf16[2,1024,512]{2,1,0:T(8,128)(2,1)S(1)}, bf16[2,1024,512]{2,1,0:T(8,128)(2,1)}, u32[]{:S(2)}) copy-start(bf16[2,1024,512]{2,1,0:T(8,128)(2,1)} %refs_5_.6) | copy-start | bytes 6291460
  8.0 4.1 %copy-start.2 = (bf16[2,1024,512]{2,1,0:T(8,128)(2,1)S(1)}, bf16[2,1024,512]{2,1,0:T(8,128)(2,1)}, u32[]{:S(2)}) copy-start(bf16[2,1024,512]{2,1,0:T(8,128)(2,1)} %refs_6_.3) | copy-start | bytes 6291460
  8.0 4.0 %copy-start.3 = (bf16[2,1024,512]{2,1,0:T(8,128)(2,1)S(1)}, bf16[2,1024,512]{2,1,0:T(8,128)(2,1)}, u32[]{:S(2)}) copy-start(bf16[2,1024,512]{2,1,0:T(8,128)(2,1)} %refs_7_.3) | copy-start | bytes 6291460
  8.0 4.0 %copy-start.4 = (bf16[2,1024,512]{2,1,0:T(8,128)(2,1)S(1)}, bf16[2,1024,512]{2,1,0:T(8,128)(2,1)}, u32[]{:S(2)}) copy-start(bf16[2,1024,512]{2,1,0:T(8,128)(2,1)} %refs_8_.3) | copy-start | bytes 6291460
  8.1 4.0 %copy-start.6 = (f32[2,1024]{1,0:T(2,128)S(1)}, f32[2,1024]{1,0:T(2,128)}, u32[]{:S(2)}) copy-start(f32[2,1024]{1,0:T(2,128)} %refs_4_.4) | copy-start | bytes 24580
  8.1 4.0 %copy-start.8 = (bf16[4,1024]{1,0:T(4,128)(2,1)S(1)}, bf16[4,1024]{1,0:T(4,128)(2,1)}, u32[]{:S(2)}) copy-start(bf16[4,1024]{1,0:T(4,128)(2,1)} %refs_0_.1) | copy-start | bytes 24580
  8.1 9.8 %collective-permute-start.6 = (bf16[2,4,4,128,128]{4,3,2,1,0:T(8,128)(2,1)S(1)}, bf16[2,4,4,128,128]{4,3,2,1,0:T(8,128)(2,1)S(1)}, u32[]{:S(2)}, u32[]{:S(2)}) collective-permute-start(bf16[2,4,4,128,128]{4,3,2,1,0:T(8,128)(2,1)S(1)} %narrow.1.refs_6_), channel_id=1, source_target_pairs={{0,1},{1,0},{2,3},{3,2},{4,5},{5,4},{6,7},{7,6},{8,9},{9,8},{10,11... | collective-permute-start | bytes 3145736 | tf_op jit(solution)/shard_map/ppermute | solution.py:61
  12.1 5.8 %copy-start.7 = (f32[2,512]{1,0:T(2,128)S(1)}, f32[2,512]{1,0:T(2,128)}, u32[]{:S(2)}) copy-start(f32[2,512]{1,0:T(2,128)} %refs_4_.5) | copy-start | bytes 12292
  12.1 5.8 %copy-start.9 = (f32[2,128]{1,0:T(2,128)S(1)}, f32[2,128]{1,0:T(2,128)}, u32[]{:S(2)}) copy-start(f32[2,128]{1,0:T(2,128)} %refs_5_.7) | copy-start | bytes 3076
  12.9 1.9 %collective-permute-start.3 = (bf16[8,2176]{1,0:T(8,128)(2,1)S(1)}, bf16[8,2176]{1,0:T(8,128)(2,1)S(1)}, u32[]{:S(2)}, u32[]{:S(2)}) collective-permute-start(bf16[8,2176]{1,0:T(8,128)(2,1)S(1)} %get-tuple-element.23), channel_id=1, source_target_pairs={{0,1},{1,0},{2,3},{3,2},{4,5},{5,4},{6,7},{7,6},{8,9},{9,8},{10,11... | collective-permute-start | bytes 104456 | tf_op jit(solution)/shard_map/ppermute | solution.py:32
  12.9 4.0 %collective-permute-start.4 = (bf16[8,2176]{1,0:T(8,128)(2,1)S(1)}, bf16[8,2176]{1,0:T(8,128)(2,1)S(1)}, u32[]{:S(2)}, u32[]{:S(2)}) collective-permute-start(bf16[8,2176]{1,0:T(8,128)(2,1)S(1)} %get-tuple-element.24), channel_id=1, source_target_pairs={{0,2},{1,3},{2,0},{3,1},{4,6},{5,7},{6,4},{7,5},{8,10},{9,11},{10,... | collective-permute-start | bytes 104456 | tf_op jit(solution)/shard_map/ppermute | solution.py:32
  14.5 3.4 %collective-permute-start.5 = (bf16[8,2176]{1,0:T(8,128)(2,1)S(1)}, bf16[8,2176]{1,0:T(8,128)(2,1)S(1)}, u32[]{:S(2)}, u32[]{:S(2)}) collective-permute-start(bf16[8,2176]{1,0:T(8,128)(2,1)S(1)} %get-tuple-element.25), channel_id=1, source_target_pairs={{0,3},{1,2},{2,1},{3,0},{4,7},{5,6},{6,5},{7,4},{8,11},{9,10},{10,... | collective-permute-start | bytes 104456 | tf_op jit(solution)/shard_map/ppermute | solution.py:32
  17.9 7.8 %copy-start.5 = (bf16[2,512,1024]{2,1,0:T(8,128)(2,1)S(1)}, bf16[2,512,1024]{2,1,0:T(8,128)(2,1)}, u32[]{:S(2)}) copy-start(bf16[2,512,1024]{2,1,0:T(8,128)(2,1)} %refs_2_.3) | copy-start | bytes 6291460
  18.4 3.1 %collective-permute-start.7 = (bf16[8,512]{1,0:T(8,128)(2,1)S(1)}, bf16[8,512]{1,0:T(8,128)(2,1)S(1)}, u32[]{:S(2)}, u32[]{:S(2)}) collective-permute-start(bf16[8,512]{1,0:T(8,128)(2,1)S(1)} %get-tuple-element.26.refs_0_), channel_id=1, source_target_pairs={{3,0},{2,1},{1,2},{0,3},{7,4},{6,5},{5,6},{4,7},{11,8},{10,9},{9,1... | collective-permute-start | bytes 24584 | tf_op jit(solution)/shard_map/ppermute | solution.py:32
  21.7 4.2 %collective-permute-start.9 = (bf16[16,1024]{1,0:T(8,128)(2,1)S(1)}, bf16[16,1024]{1,0:T(8,128)(2,1)S(1)}, u32[]{:S(2)}, u32[]{:S(2)}) collective-permute-start(bf16[16,1024]{1,0:T(8,128)(2,1)S(1)} %shard_map.117), channel_id=1, source_target_pairs={{0,5},{1,4},{2,7},{3,6},{4,1},{5,0},{6,3},{7,2},{8,13},{9,12},{10,... | collective-permute-start | bytes 98312 | tf_op jit(solution)/shard_map/ppermute | solution.py:52
  21.8 5.2 %collective-permute-start.10 = (bf16[16,1024]{1,0:T(8,128)(2,1)S(1)}, bf16[16,1024]{1,0:T(8,128)(2,1)S(1)}, u32[]{:S(2)}, u32[]{:S(2)}) collective-permute-start(bf16[16,1024]{1,0:T(8,128)(2,1)S(1)} %shard_map.117), channel_id=1, source_target_pairs={{0,9},{1,8},{2,11},{3,10},{4,13},{5,12},{6,15},{7,14},{8,1},{9,0},... | collective-permute-start | bytes 98312 | tf_op jit(solution)/shard_map/ppermute | solution.py:52
  25.2 5.1 %collective-permute-start.11 = (bf16[16,1024]{1,0:T(8,128)(2,1)S(1)}, bf16[16,1024]{1,0:T(8,128)(2,1)S(1)}, u32[]{:S(2)}, u32[]{:S(2)}) collective-permute-start(bf16[16,1024]{1,0:T(8,128)(2,1)S(1)} %shard_map.117), channel_id=1, source_target_pairs={{0,13},{1,12},{2,15},{3,14},{4,9},{5,8},{6,11},{7,10},{8,5},{9,4},... | collective-permute-start | bytes 98312 | tf_op jit(solution)/shard_map/ppermute | solution.py:52
  31.0 1.9 %collective-permute-start.12 = (bf16[8,2176]{1,0:T(8,128)(2,1)S(1)}, bf16[8,2176]{1,0:T(8,128)(2,1)S(1)}, u32[]{:S(2)}, u32[]{:S(2)}) collective-permute-start(bf16[8,2176]{1,0:T(8,128)(2,1)S(1)} %get-tuple-element.29), channel_id=1, source_target_pairs={{0,1},{1,0},{2,3},{3,2},{4,5},{5,4},{6,7},{7,6},{8,9},{9,8},{10,11... | collective-permute-start | bytes 104456 | tf_op jit(solution)/shard_map/ppermute | solution.py:32
  31.2 4.0 %collective-permute-start.13 = (bf16[8,2176]{1,0:T(8,128)(2,1)S(1)}, bf16[8,2176]{1,0:T(8,128)(2,1)S(1)}, u32[]{:S(2)}, u32[]{:S(2)}) collective-permute-start(bf16[8,2176]{1,0:T(8,128)(2,1)S(1)} %get-tuple-element.30), channel_id=1, source_target_pairs={{0,2},{1,3},{2,0},{3,1},{4,6},{5,7},{6,4},{7,5},{8,10},{9,11},{10,... | collective-permute-start | bytes 104456 | tf_op jit(solution)/shard_map/ppermute | solution.py:32
  32.1 3.6 %collective-permute-start.14 = (bf16[8,2176]{1,0:T(8,128)(2,1)S(1)}, bf16[8,2176]{1,0:T(8,128)(2,1)S(1)}, u32[]{:S(2)}, u32[]{:S(2)}) collective-permute-start(bf16[8,2176]{1,0:T(8,128)(2,1)S(1)} %get-tuple-element.31), channel_id=1, source_target_pairs={{0,3},{1,2},{2,1},{3,0},{4,7},{5,6},{6,5},{7,4},{8,11},{9,10},{10,... | collective-permute-start | bytes 104456 | tf_op jit(solution)/shard_map/ppermute | solution.py:32
  35.7 7.8 %copy-start = (f32[2,4,4,128,128]{4,3,2,1,0:T(8,128)S(1)}, f32[2,4,4,128,128]{4,3,2,1,0:T(8,128)}, u32[]{:S(2)}) copy-start(f32[2,4,4,128,128]{4,3,2,1,0:T(8,128)} %state.5) | copy-start | bytes 6291460
  36.2 3.1 %collective-permute-start.15 = (bf16[8,512]{1,0:T(8,128)(2,1)S(1)}, bf16[8,512]{1,0:T(8,128)(2,1)S(1)}, u32[]{:S(2)}, u32[]{:S(2)}) collective-permute-start(bf16[8,512]{1,0:T(8,128)(2,1)S(1)} %get-tuple-element.32.refs_0_), channel_id=1, source_target_pairs={{3,0},{2,1},{1,2},{0,3},{7,4},{6,5},{5,6},{4,7},{11,8},{10,9},{9,1... | collective-permute-start | bytes 24584 | tf_op jit(solution)/shard_map/ppermute | solution.py:32
  39.7 6.9 %collective-permute-start.16 = (bf16[4,1024]{1,0:T(4,128)(2,1)S(1)}, bf16[4,1024]{1,0:T(4,128)(2,1)S(1)}, u32[]{:S(2)}, u32[]{:S(2)}) collective-permute-start(bf16[4,1024]{1,0:T(4,128)(2,1)S(1)} %get-tuple-element.35), channel_id=1, source_target_pairs={{0,5},{1,4},{2,7},{3,6},{4,1},{5,0},{6,3},{7,2},{8,13},{9,12},{10,... | collective-permute-start | bytes 24584 | tf_op jit(solution)/shard_map/ppermute | solution.py:52
  39.7 6.9 %collective-permute-start.17 = (bf16[4,1024]{1,0:T(4,128)(2,1)S(1)}, bf16[4,1024]{1,0:T(4,128)(2,1)S(1)}, u32[]{:S(2)}, u32[]{:S(2)}) collective-permute-start(bf16[4,1024]{1,0:T(4,128)(2,1)S(1)} %get-tuple-element.36), channel_id=1, source_target_pairs={{0,9},{1,8},{2,11},{3,10},{4,13},{5,12},{6,15},{7,14},{8,1},{9,0},... | collective-permute-start | bytes 24584 | tf_op jit(solution)/shard_map/ppermute | solution.py:52
  40.8 5.8 %collective-permute-start.18 = (bf16[4,1024]{1,0:T(4,128)(2,1)S(1)}, bf16[4,1024]{1,0:T(4,128)(2,1)S(1)}, u32[]{:S(2)}, u32[]{:S(2)}) collective-permute-start(bf16[4,1024]{1,0:T(4,128)(2,1)S(1)} %get-tuple-element.37), channel_id=1, source_target_pairs={{0,13},{1,12},{2,15},{3,14},{4,9},{5,8},{6,11},{7,10},{8,5},{9,4},... | collective-permute-start | bytes 24584 | tf_op jit(solution)/shard_map/ppermute | solution.py:52

commit v8 on v7

--- a/solution.py
+++ b/solution.py
@@ -128,7 +128,7 @@
     own, parts = refs[0], refs[1:n_dp]
     (bound_ref, head_gain), states = refs[n_dp : n_dp + 2], refs[n_dp + 2 : n_dp + 2 + group]
     normed, gates, left = refs[n_dp + 2 + group :]
-    kept, heads, hd = states[0].shape[1:4]
+    kept, heads, hd = states[0].shape[:3]
     seqs = group * kept
     width = heads * hd
     total = own[...]
@@ -164,7 +164,7 @@
             [
                 jnp.concatenate(
                     [
-                        states[seq // kept][layer, seq % kept, first + index]
+                        states[seq // kept][seq % kept, first + index]
                         for seq in range(seqs)
                     ],
                     axis=0,
@@ -207,17 +207,16 @@
         copy.wait()
 
 
-def narrow(state, out, staged, sems):
-    places = [(layer, seq) for layer in range(state.shape[0]) for seq in range(state.shape[1])]
+def narrow(layer, state, out, staged, sems):
     copies = [
-        pltpu.make_async_copy(state.at[place], staged.at[place], sems.at[index])
-        for index, place in enumerate(places)
+        pltpu.make_async_copy(state.at[layer, seq], staged.at[seq], sems.at[seq])
+        for seq in range(state.shape[1])
     ]
     for copy in copies:
         copy.start()
-    for copy, place in zip(copies, places):
+    for seq, copy in enumerate(copies):
         copy.wait()
-        out[place] = staged[place].astype(BF16)
+        out[seq] = staged[seq].astype(BF16)
 
 
 def slot_parts(refs, group):
@@ -334,20 +333,22 @@
     parts = gather("tp", n_tp, tokens)
     flip = core_flip(n_dp)
     group, n_chip = flip + 1, n_dp // (flip + 1)
-    narrowed = pl.pallas_call(
-        narrow,
-        name="narrow",
-        out_shape=pltpu.VMEM(state.shape, BF16),
-        in_specs=[ANY],
-        out_specs=VMEM,
-        scratch_shapes=[
-            pltpu.VMEM(state.shape, F32),
-            pltpu.SemaphoreType.DMA((state.shape[0] * seqs,)),
-        ],
-        compiler_params=pltpu.CompilerParams(vmem_limit_bytes=4 << 20),
-    )(pltpu.with_memory_space_constraint(state, pltpu.HBM))
-    states = [narrowed] + [cross_copy(n_dp, narrowed)] * flip
     crossed = cross_copy(n_dp, w_out)
+    states = []
+    for layer in range(2):
+        narrowed = pl.pallas_call(
+            functools.partial(narrow, layer),
+            name="narrow",
+            out_shape=pltpu.VMEM(state.shape[1:], BF16),
+            in_specs=[ANY],
+            out_specs=VMEM,
+            scratch_shapes=[
+                pltpu.VMEM(state.shape[1:], F32),
+                pltpu.SemaphoreType.DMA((seqs,)),
+            ],
+            compiler_params=pltpu.CompilerParams(vmem_limit_bytes=4 << 20),
+        )(pltpu.with_memory_space_constraint(state, pltpu.HBM))
+        states.append([narrowed] + [cross_copy(n_dp, narrowed)] * flip)
     base = held = None
     new_state = None
     for layer in range(2):
@@ -372,7 +373,7 @@
         parts = exchange("dp", n_dp, sent)
         normed, gates = call(
             functools.partial(recur, n_dp, layer, features, group),
-            (own, *parts, lower_bound, head_gain, *states),
+            (own, *parts, lower_bound, head_gain, *states[layer]),
             [VMEM] * (n_dp + 2 + group),
             [((group * seqs, width), BF16), ((seqs, 3, width), F32)],
             [((4 * group * seqs, group * seqs * hd), F32)],

time: 47.4 us -> 49 us (1.034)
  starting transfers between devices: 18.8 us -> 20.4 us
  waiting for transfers between devices: 19.1 us -> 17.9 us
  Pallas kernels: 8.39 us -> 9.27 us
    ppermute x11, waiting for transfers between devices: 14.6 us -> 12.9 us  [exchange(): lax.ppermute(array, axis, [(b, a) for a, b in pairs] if inward else pairs)]
    ppermute x11, starting transfers between devices: 10.5 us -> 11.5 us  [exchange(): lax.ppermute(array, axis, [(b, a) for a, b in pairs] if inward else pairs)]
    pallas_call x1 -> x2, Pallas kernels: 1.58 us -> 2.47 us  [per_device(): pl.pallas_call(functools.partial(narrow, layer), name='narrow', out_shape...]
    ppermute x2 -> x3, starting transfers between devices: 0.63 us -> 1.19 us  [cross_copy(): return lax.ppermute(array, 'dp', [(d, d ^ 1) for d in range(n_dp)])]
  transfers between devices with their start and end apart: 19 -> 20, of which waited for: 10 -> 9; matrix products, arithmetic and copies ran while one was open for 0% -> 0% of each run, Pallas kernels for 13% -> 16%
where the time goes in v8:
time: 49 us; the launch traced here: 48.8 us
  starting transfers between devices  20.4 us (42%)
  waiting for transfers between devices  17.9 us (37%)
  Pallas kernels  9.27 us (19%)
  between operations  0.82 us (2%)
    ppermute x11, waiting for transfers between devices, exchange(): lax.ppermute(array, axis, [(b, a) for a, b in pairs] if inward else pairs)  12.9 us
    ppermute x11, starting transfers between devices, exchange(): lax.ppermute(array, axis, [(b, a) for a, b in pairs] if inward else pairs)  11.5 us
    ppermute x6, starting transfers between devices, cross_exchange(): lax.ppermute(arrays[k - 1], ('tp', 'dp'), cross_pairs(n_tp, n_dp, k))  7.73 us
    ppermute x6, waiting for transfers between devices, cross_exchange(): lax.ppermute(arrays[k - 1], ('tp', 'dp'), cross_pairs(n_tp, n_dp, k))  4.95 us
    pallas_call x9, Pallas kernels, call(): pl.pallas_call(body, out_shape=[pltpu.VMEM(shape, dtype) for shape, dtype...  3.49 us
    pallas_call x2, Pallas kernels, per_device(): pl.pallas_call(functools.partial(update, layer), name='update', out_shape...  2.69 us
    pallas_call x2, Pallas kernels, per_device(): pl.pallas_call(functools.partial(narrow, layer), name='narrow', out_shape...  2.47 us
    ppermute x3, starting transfers between devices, cross_copy(): return lax.ppermute(array, 'dp', [(d, d ^ 1) for d in range(n_dp)])  1.19 us
  transfers between devices with their start and end apart: 20, of which 9 were waited for; matrix products, arithmetic and copies ran while one was open for 0% of the time, Pallas kernels for 16%

profile of v8, /device:TPU:0, one launch (start us, length us, event | category | flops | bytes accessed | tf_op | source)
XLA Modules:
  0.0 48.8 jit_solution(13148988423791599283)
XLA Ops:
  0.6 0.6 %collective-permute-start.8 = (bf16[2,512,1024]{2,1,0:T(8,128)(2,1)}, bf16[2,512,1024]{2,1,0:T(8,128)(2,1)S(1)}, u32[]{:S(2)}, u32[]{:S(2)}) collective-permute-start(bf16[2,512,1024]{2,1,0:T(8,128)(2,1)} %refs_2_.3), channel_id=1, source_target_pairs={{0,1},{1,0},{2,3},{3,2},{4,5},{5,4},{6,7},{7,6},{8,9},{9,8},{10,11... | collective-permute-start | bytes 6291464 | tf_op jit(solution)/shard_map/ppermute | solution.py:61
  1.2 2.6 %collective-permute-start = (bf16[4,1024]{1,0:T(4,128)(2,1)}, bf16[4,1024]{1,0:T(4,128)(2,1)S(1)}, u32[]{:S(2)}, u32[]{:S(2)}) collective-permute-start(bf16[4,1024]{1,0:T(4,128)(2,1)} %refs_0_.1), channel_id=1, source_target_pairs={{4,0},{0,4},{12,8},{8,12},{5,1},{1,5},{13,9},{9,13},{6,2},{2,6},{1... | collective-permute-start | bytes 24584 | tf_op jit(solution)/shard_map/ppermute | solution.py:32
  3.8 2.6 %collective-permute-start.1 = (bf16[4,1024]{1,0:T(4,128)(2,1)}, bf16[4,1024]{1,0:T(4,128)(2,1)S(1)}, u32[]{:S(2)}, u32[]{:S(2)}) collective-permute-start(bf16[4,1024]{1,0:T(4,128)(2,1)} %refs_0_.1), channel_id=1, source_target_pairs={{8,0},{12,4},{0,8},{4,12},{9,1},{13,5},{1,9},{5,13},{10,2},{14,6},... | collective-permute-start | bytes 24584 | tf_op jit(solution)/shard_map/ppermute | solution.py:32
  6.4 1.2 %narrow.2.refs_6_ = bf16[4,4,128,128]{3,2,1,0:T(8,128)(2,1)S(1)} custom-call(f32[2,4,4,128,128]{4,3,2,1,0:T(8,128)} %state.7), custom_call_target="tpu_custom_call" | custom-call | tf_op jit(solution)/shard_map/narrow/pallas_call | solution.py:339
  7.7 1.2 %narrow.3.refs_6_ = bf16[4,4,128,128]{3,2,1,0:T(8,128)(2,1)S(1)} custom-call(f32[2,4,4,128,128]{4,3,2,1,0:T(8,128)} %state.7), custom_call_target="tpu_custom_call" | custom-call | tf_op jit(solution)/shard_map/narrow/pallas_call | solution.py:339
  9.1 0.6 %collective-permute-start.15 = (bf16[4,4,128,128]{3,2,1,0:T(8,128)(2,1)S(1)}, bf16[4,4,128,128]{3,2,1,0:T(8,128)(2,1)S(1)}, u32[]{:S(2)}, u32[]{:S(2)}) collective-permute-start(bf16[4,4,128,128]{3,2,1,0:T(8,128)(2,1)S(1)} %narrow.3.refs_6_), channel_id=1, source_target_pairs={{0,1},{1,0},{2,3},{3,2},{4,5},{5,4},{6,7},{7,6},{8,9},{9,8},{10,11... | collective-permute-start | bytes 1572872 | tf_op jit(solution)/shard_map/ppermute | solution.py:61
  9.7 2.4 %collective-permute-done.2.refs_3_ = bf16[4,1024]{1,0:T(4,128)(2,1)S(1)} collective-permute-done((bf16[4,1024]{1,0:T(4,128)(2,1)}, bf16[4,1024]{1,0:T(4,128)(2,1)S(1)}, u32[]{:S(2)}, u32[]{:S(2)}) %collective-permute-start.2) | collective-permute-done | bytes 8224 | tf_op jit(solution)/shard_map/ppermute | solution.py:32
  12.5 0.8 %shard_map.114 = (bf16[16,1024]{1,0:T(8,128)(2,1)S(1)}, f32[8,2176]{1,0:T(8,128)S(1)}, bf16[8,2176]{1,0:T(8,128)(2,1)S(1)}, bf16[8,2176]{1,0:T(8,128)(2,1)S(1)}, bf16[8,2176]{1,0:T(8,128)(2,1)S(1)}) custom-call(bf16[4,1024]{1,0:T(4,128)(2,1)S(1)} %copy-done.8, bf16[4,1024]{1,0:T(4,128)(2,1)S(1)} %collective-permute-done.refs_1_, ...), custom_call_target="tpu_custom_call" | custom-call | tf_op jit(solution)/shard_map/pallas_call | solution.py:295
  13.2 0.5 %collective-permute-start.3 = (bf16[8,2176]{1,0:T(8,128)(2,1)S(1)}, bf16[8,2176]{1,0:T(8,128)(2,1)S(1)}, u32[]{:S(2)}, u32[]{:S(2)}) collective-permute-start(bf16[8,2176]{1,0:T(8,128)(2,1)S(1)} %get-tuple-element.23), channel_id=1, source_target_pairs={{0,1},{1,0},{2,3},{3,2},{4,5},{5,4},{6,7},{7,6},{8,9},{9,8},{10,11... | collective-permute-start | bytes 104456 | tf_op jit(solution)/shard_map/ppermute | solution.py:32
  13.8 1.7 %collective-permute-start.4 = (bf16[8,2176]{1,0:T(8,128)(2,1)S(1)}, bf16[8,2176]{1,0:T(8,128)(2,1)S(1)}, u32[]{:S(2)}, u32[]{:S(2)}) collective-permute-start(bf16[8,2176]{1,0:T(8,128)(2,1)S(1)} %get-tuple-element.24), channel_id=1, source_target_pairs={{0,2},{1,3},{2,0},{3,1},{4,6},{5,7},{6,4},{7,5},{8,10},{9,11},{10,... | collective-permute-start | bytes 104456 | tf_op jit(solution)/shard_map/ppermute | solution.py:32
  15.5 0.8 %collective-permute-start.5 = (bf16[8,2176]{1,0:T(8,128)(2,1)S(1)}, bf16[8,2176]{1,0:T(8,128)(2,1)S(1)}, u32[]{:S(2)}, u32[]{:S(2)}) collective-permute-start(bf16[8,2176]{1,0:T(8,128)(2,1)S(1)} %get-tuple-element.25), channel_id=1, source_target_pairs={{0,3},{1,2},{2,1},{3,0},{4,7},{5,6},{6,5},{7,4},{8,11},{9,10},{10,... | collective-permute-start | bytes 104456 | tf_op jit(solution)/shard_map/ppermute | solution.py:32
  16.3 1.4 %collective-permute-done.4.refs_2_ = bf16[8,2176]{1,0:T(8,128)(2,1)S(1)} collective-permute-done((bf16[8,2176]{1,0:T(8,128)(2,1)S(1)}, bf16[8,2176]{1,0:T(8,128)(2,1)S(1)}, u32[]{:S(2)}, u32[]{:S(2)}) %collective-permute-start.4) | collective-permute-done | bytes 34848 | tf_op jit(solution)/shard_map/ppermute | solution.py:32
  17.7 1.5 %collective-permute-done.5.refs_3_ = bf16[8,2176]{1,0:T(8,128)(2,1)S(1)} collective-permute-done((bf16[8,2176]{1,0:T(8,128)(2,1)S(1)}, bf16[8,2176]{1,0:T(8,128)(2,1)S(1)}, u32[]{:S(2)}, u32[]{:S(2)}) %collective-permute-start.5) | collective-permute-done | bytes 34848 | tf_op jit(solution)/shard_map/ppermute | solution.py:32
  19.2 0.4 shard_map.115
  19.7 0.5 %collective-permute-start.7 = (bf16[8,512]{1,0:T(8,128)(2,1)S(1)}, bf16[8,512]{1,0:T(8,128)(2,1)S(1)}, u32[]{:S(2)}, u32[]{:S(2)}) collective-permute-start(bf16[8,512]{1,0:T(8,128)(2,1)S(1)} %get-tuple-element.26.refs_0_), channel_id=1, source_target_pairs={{3,0},{2,1},{1,2},{0,3},{7,4},{6,5},{5,6},{4,7},{11,8},{10,9},{9,1... | collective-permute-start | bytes 24584 | tf_op jit(solution)/shard_map/ppermute | solution.py:32
  20.2 2.6 %collective-permute-done.7.refs_1_ = bf16[8,512]{1,0:T(8,128)(2,1)S(1)} collective-permute-done((bf16[8,512]{1,0:T(8,128)(2,1)S(1)}, bf16[8,512]{1,0:T(8,128)(2,1)S(1)}, u32[]{:S(2)}, u32[]{:S(2)}) %collective-permute-start.7) | collective-permute-done | bytes 8224 | tf_op jit(solution)/shard_map/ppermute | solution.py:32
  23.1 0.4 collective-permute-start.9
  23.5 3.5 %collective-permute-start.10 = (bf16[16,1024]{1,0:T(8,128)(2,1)S(1)}, bf16[16,1024]{1,0:T(8,128)(2,1)S(1)}, u32[]{:S(2)}, u32[]{:S(2)}) collective-permute-start(bf16[16,1024]{1,0:T(8,128)(2,1)S(1)} %shard_map.117), channel_id=1, source_target_pairs={{0,9},{1,8},{2,11},{3,10},{4,13},{5,12},{6,15},{7,14},{8,1},{9,0},... | collective-permute-start | bytes 98312 | tf_op jit(solution)/shard_map/ppermute | solution.py:52
  27.2 2.2 %collective-permute-done.10.refs_2_ = bf16[16,1024]{1,0:T(8,128)(2,1)S(1)} collective-permute-done((bf16[16,1024]{1,0:T(8,128)(2,1)S(1)}, bf16[16,1024]{1,0:T(8,128)(2,1)S(1)}, u32[]{:S(2)}, u32[]{:S(2)}) %collective-permute-start.10) | collective-permute-done | bytes 32800 | tf_op jit(solution)/shard_map/ppermute | solution.py:52
  29.4 2.7 %collective-permute-done.11.refs_3_ = bf16[16,1024]{1,0:T(8,128)(2,1)S(1)} collective-permute-done((bf16[16,1024]{1,0:T(8,128)(2,1)S(1)}, bf16[16,1024]{1,0:T(8,128)(2,1)S(1)}, u32[]{:S(2)}, u32[]{:S(2)}) %collective-permute-start.11) | collective-permute-done | bytes 32800 | tf_op jit(solution)/shard_map/ppermute | solution.py:52
  32.2 0.7 %shard_map.118 = (bf16[16,1024]{1,0:T(8,128)(2,1)S(1)}, f32[8,2176]{1,0:T(8,128)S(1)}, bf16[8,2176]{1,0:T(8,128)(2,1)S(1)}, bf16[8,2176]{1,0:T(8,128)(2,1)S(1)}, bf16[8,2176]{1,0:T(8,128)(2,1)S(1)}) custom-call(f32[16,1024]{1,0:T(8,128)S(1)} %shard_map.116.refs_0_, bf16[16,1024]{1,0:T(8,128)(2,1)S(1)} %collective-permute-done.9.refs_1_, ...), custom_call_target="tpu_custom_call" | custom-call | tf_op jit(solution)/shard_map/pallas_call | solution.py:295
  32.9 0.7 %collective-permute-start.13 = (bf16[8,2176]{1,0:T(8,128)(2,1)S(1)}, bf16[8,2176]{1,0:T(8,128)(2,1)S(1)}, u32[]{:S(2)}, u32[]{:S(2)}) collective-permute-start(bf16[8,2176]{1,0:T(8,128)(2,1)S(1)} %get-tuple-element.30), channel_id=1, source_target_pairs={{0,2},{1,3},{2,0},{3,1},{4,6},{5,7},{6,4},{7,5},{8,10},{9,11},{10,... | collective-permute-start | bytes 104456 | tf_op jit(solution)/shard_map/ppermute | solution.py:32
  33.6 1.1 %collective-permute-start.14 = (bf16[8,2176]{1,0:T(8,128)(2,1)S(1)}, bf16[8,2176]{1,0:T(8,128)(2,1)S(1)}, u32[]{:S(2)}, u32[]{:S(2)}) collective-permute-start(bf16[8,2176]{1,0:T(8,128)(2,1)S(1)} %get-tuple-element.31), channel_id=1, source_target_pairs={{0,3},{1,2},{2,1},{3,0},{4,7},{5,6},{6,5},{7,4},{8,11},{9,10},{10,... | collective-permute-start | bytes 104456 | tf_op jit(solution)/shard_map/ppermute | solution.py:32
  34.7 2.4 %collective-permute-done.13.refs_2_ = bf16[8,2176]{1,0:T(8,128)(2,1)S(1)} collective-permute-done((bf16[8,2176]{1,0:T(8,128)(2,1)S(1)}, bf16[8,2176]{1,0:T(8,128)(2,1)S(1)}, u32[]{:S(2)}, u32[]{:S(2)}) %collective-permute-start.13) | collective-permute-done | bytes 34848 | tf_op jit(solution)/shard_map/ppermute | solution.py:32
  37.4 0.4 shard_map.119
  37.8 0.8 %collective-permute-start.16 = (bf16[8,512]{1,0:T(8,128)(2,1)S(1)}, bf16[8,512]{1,0:T(8,128)(2,1)S(1)}, u32[]{:S(2)}, u32[]{:S(2)}) collective-permute-start(bf16[8,512]{1,0:T(8,128)(2,1)S(1)} %get-tuple-element.32.refs_0_), channel_id=1, source_target_pairs={{3,0},{2,1},{1,2},{0,3},{7,4},{6,5},{5,6},{4,7},{11,8},{10,9},{9,1... | collective-permute-start | bytes 24584 | tf_op jit(solution)/shard_map/ppermute | solution.py:32
  38.6 2.3 %collective-permute-done.16.refs_1_ = bf16[8,512]{1,0:T(8,128)(2,1)S(1)} collective-permute-done((bf16[8,512]{1,0:T(8,128)(2,1)S(1)}, bf16[8,512]{1,0:T(8,128)(2,1)S(1)}, u32[]{:S(2)}, u32[]{:S(2)}) %collective-permute-start.16) | collective-permute-done | bytes 8224 | tf_op jit(solution)/shard_map/ppermute | solution.py:32
  41.3 1.1 %collective-permute-start.18 = (bf16[4,1024]{1,0:T(4,128)(2,1)S(1)}, bf16[4,1024]{1,0:T(4,128)(2,1)S(1)}, u32[]{:S(2)}, u32[]{:S(2)}) collective-permute-start(bf16[4,1024]{1,0:T(4,128)(2,1)S(1)} %get-tuple-element.36), channel_id=1, source_target_pairs={{0,9},{1,8},{2,11},{3,10},{4,13},{5,12},{6,15},{7,14},{8,1},{9,0},... | collective-permute-start | bytes 24584 | tf_op jit(solution)/shard_map/ppermute | solution.py:52
  42.4 2.7 %collective-permute-start.19 = (bf16[4,1024]{1,0:T(4,128)(2,1)S(1)}, bf16[4,1024]{1,0:T(4,128)(2,1)S(1)}, u32[]{:S(2)}, u32[]{:S(2)}) collective-permute-start(bf16[4,1024]{1,0:T(4,128)(2,1)S(1)} %get-tuple-element.37), channel_id=1, source_target_pairs={{0,13},{1,12},{2,15},{3,14},{4,9},{5,8},{6,11},{7,10},{8,5},{9,4},... | collective-permute-start | bytes 24584 | tf_op jit(solution)/shard_map/ppermute | solution.py:52
  45.1 1.3 %update.2.refs_0_ = f32[2,4,4,128,128]{4,3,2,1,0:T(8,128)} custom-call(f32[4,3,512]{2,1,0:T(4,128)S(1)} %get-tuple-element.39.gates, f32[2,4,4,128,128]{4,3,2,1,0:T(8,128)S(1)} %copy-done), custom_call_target="tpu_custom_call" | custom-call | tf_op jit(solution)/shard_map/update/pallas_call | solution.py:383
  46.5 1.4 %update.3 = f32[2,4,4,128,128]{4,3,2,1,0:T(8,128)} custom-call(f32[4,3,512]{2,1,0:T(4,128)S(1)} %get-tuple-element.38.gates, f32[2,4,4,128,128]{4,3,2,1,0:T(8,128)S(1)} %copy-done, f32[2,4,4,128,128]{4,3,2,1,0:T(8,128)} %update.2.refs_0_), custom_call_target="tpu_custom_call", output_to_operand_aliasing={{}: (2, {})} | custom-call | tf_op jit(solution)/shard_map/update/pallas_call | solution.py:383
  48.2 0.6 %close.1 = bf16[4,1024]{1,0:T(4,128)(2,1)} custom-call(f32[4,1024]{1,0:T(4,128)S(1)} %shard_map.120.own, bf16[4,1024]{1,0:T(4,128)(2,1)S(1)} %collective-permute-done.17.refs_0_, bf16[4,1024]{1,0:T(4,128)(2,1)S(1)} %collective-permute-done.18.refs_1_, bf16[4,1024]{1,0:T(4,128)(2,1)S(1)} %collective-permute-done.19.refs_2_), custom_call_target="tpu_custom_call" | custom-call | tf_op jit(solution)/shard_map/close/pallas_call | solution.py:428
  (42 shorter events, 2.1 us)
Async XLA Ops:
  0.6 22.2 %collective-permute-start.8 = (bf16[2,512,1024]{2,1,0:T(8,128)(2,1)}, bf16[2,512,1024]{2,1,0:T(8,128)(2,1)S(1)}, u32[]{:S(2)}, u32[]{:S(2)}) collective-permute-start(bf16[2,512,1024]{2,1,0:T(8,128)(2,1)} %refs_2_.3), channel_id=1, source_target_pairs={{0,1},{1,0},{2,3},{3,2},{4,5},{5,4},{6,7},{7,6},{8,9},{9,8},{10,11... | collective-permute-start | bytes 6291464 | tf_op jit(solution)/shard_map/ppermute | solution.py:61
  1.2 7.9 %collective-permute-start = (bf16[4,1024]{1,0:T(4,128)(2,1)}, bf16[4,1024]{1,0:T(4,128)(2,1)S(1)}, u32[]{:S(2)}, u32[]{:S(2)}) collective-permute-start(bf16[4,1024]{1,0:T(4,128)(2,1)} %refs_0_.1), channel_id=1, source_target_pairs={{4,0},{0,4},{12,8},{8,12},{5,1},{1,5},{13,9},{9,13},{6,2},{2,6},{1... | collective-permute-start | bytes 24584 | tf_op jit(solution)/shard_map/ppermute | solution.py:32
  3.8 5.8 %collective-permute-start.1 = (bf16[4,1024]{1,0:T(4,128)(2,1)}, bf16[4,1024]{1,0:T(4,128)(2,1)S(1)}, u32[]{:S(2)}, u32[]{:S(2)}) collective-permute-start(bf16[4,1024]{1,0:T(4,128)(2,1)} %refs_0_.1), channel_id=1, source_target_pairs={{8,0},{12,4},{0,8},{4,12},{9,1},{13,5},{1,9},{5,13},{10,2},{14,6},... | collective-permute-start | bytes 24584 | tf_op jit(solution)/shard_map/ppermute | solution.py:32
  6.4 5.7 %collective-permute-start.2 = (bf16[4,1024]{1,0:T(4,128)(2,1)}, bf16[4,1024]{1,0:T(4,128)(2,1)S(1)}, u32[]{:S(2)}, u32[]{:S(2)}) collective-permute-start(bf16[4,1024]{1,0:T(4,128)(2,1)} %refs_0_.1), channel_id=1, source_target_pairs={{12,0},{8,4},{4,8},{0,12},{13,1},{9,5},{5,9},{1,13},{14,2},{10,6},... | collective-permute-start | bytes 24584 | tf_op jit(solution)/shard_map/ppermute | solution.py:32
  7.7 11.6 %collective-permute-start.6 = (bf16[4,4,128,128]{3,2,1,0:T(8,128)(2,1)S(1)}, bf16[4,4,128,128]{3,2,1,0:T(8,128)(2,1)S(1)}, u32[]{:S(2)}, u32[]{:S(2)}) collective-permute-start(bf16[4,4,128,128]{3,2,1,0:T(8,128)(2,1)S(1)} %narrow.2.refs_6_), channel_id=1, source_target_pairs={{0,1},{1,0},{2,3},{3,2},{4,5},{5,4},{6,7},{7,6},{8,9},{9,8},{10,11... | collective-permute-start | bytes 1572872 | tf_op jit(solution)/shard_map/ppermute | solution.py:61
  9.0 3.1 %copy-start.1 = (bf16[2,1024,512]{2,1,0:T(8,128)(2,1)S(1)}, bf16[2,1024,512]{2,1,0:T(8,128)(2,1)}, u32[]{:S(2)}) copy-start(bf16[2,1024,512]{2,1,0:T(8,128)(2,1)} %refs_5_.6) | copy-start | bytes 6291460
  9.0 3.1 %copy-start.2 = (bf16[2,1024,512]{2,1,0:T(8,128)(2,1)S(1)}, bf16[2,1024,512]{2,1,0:T(8,128)(2,1)}, u32[]{:S(2)}) copy-start(bf16[2,1024,512]{2,1,0:T(8,128)(2,1)} %refs_6_.3) | copy-start | bytes 6291460
  9.0 3.1 %copy-start.3 = (bf16[2,1024,512]{2,1,0:T(8,128)(2,1)S(1)}, bf16[2,1024,512]{2,1,0:T(8,128)(2,1)}, u32[]{:S(2)}) copy-start(bf16[2,1024,512]{2,1,0:T(8,128)(2,1)} %refs_7_.3) | copy-start | bytes 6291460
  9.0 3.4 %copy-start.4 = (bf16[2,1024,512]{2,1,0:T(8,128)(2,1)S(1)}, bf16[2,1024,512]{2,1,0:T(8,128)(2,1)}, u32[]{:S(2)}) copy-start(bf16[2,1024,512]{2,1,0:T(8,128)(2,1)} %refs_8_.3) | copy-start | bytes 6291460
  9.0 3.4 %copy-start.6 = (f32[2,1024]{1,0:T(2,128)S(1)}, f32[2,1024]{1,0:T(2,128)}, u32[]{:S(2)}) copy-start(f32[2,1024]{1,0:T(2,128)} %refs_4_.4) | copy-start | bytes 24580
  9.0 3.4 %copy-start.8 = (bf16[4,1024]{1,0:T(4,128)(2,1)S(1)}, bf16[4,1024]{1,0:T(4,128)(2,1)}, u32[]{:S(2)}) copy-start(bf16[4,1024]{1,0:T(4,128)(2,1)} %refs_0_.1) | copy-start | bytes 24580
  9.1 25.6 %collective-permute-start.15 = (bf16[4,4,128,128]{3,2,1,0:T(8,128)(2,1)S(1)}, bf16[4,4,128,128]{3,2,1,0:T(8,128)(2,1)S(1)}, u32[]{:S(2)}, u32[]{:S(2)}) collective-permute-start(bf16[4,4,128,128]{3,2,1,0:T(8,128)(2,1)S(1)} %narrow.3.refs_6_), channel_id=1, source_target_pairs={{0,1},{1,0},{2,3},{3,2},{4,5},{5,4},{6,7},{7,6},{8,9},{9,8},{10,11... | collective-permute-start | bytes 1572872 | tf_op jit(solution)/shard_map/ppermute | solution.py:61
  12.5 6.7 %copy-start.7 = (f32[2,512]{1,0:T(2,128)S(1)}, f32[2,512]{1,0:T(2,128)}, u32[]{:S(2)}) copy-start(f32[2,512]{1,0:T(2,128)} %refs_4_.5) | copy-start | bytes 12292
  12.5 6.7 %copy-start.9 = (f32[2,128]{1,0:T(2,128)S(1)}, f32[2,128]{1,0:T(2,128)}, u32[]{:S(2)}) copy-start(f32[2,128]{1,0:T(2,128)} %refs_5_.7) | copy-start | bytes 3076
  13.2 13.7 %copy-start.5 = (bf16[2,512,1024]{2,1,0:T(8,128)(2,1)S(1)}, bf16[2,512,1024]{2,1,0:T(8,128)(2,1)}, u32[]{:S(2)}) copy-start(bf16[2,512,1024]{2,1,0:T(8,128)(2,1)} %refs_2_.3) | copy-start | bytes 6291460
  13.2 2.3 %collective-permute-start.3 = (bf16[8,2176]{1,0:T(8,128)(2,1)S(1)}, bf16[8,2176]{1,0:T(8,128)(2,1)S(1)}, u32[]{:S(2)}, u32[]{:S(2)}) collective-permute-start(bf16[8,2176]{1,0:T(8,128)(2,1)S(1)} %get-tuple-element.23), channel_id=1, source_target_pairs={{0,1},{1,0},{2,3},{3,2},{4,5},{5,4},{6,7},{7,6},{8,9},{9,8},{10,11... | collective-permute-start | bytes 104456 | tf_op jit(solution)/shard_map/ppermute | solution.py:32
  13.8 3.9 %collective-permute-start.4 = (bf16[8,2176]{1,0:T(8,128)(2,1)S(1)}, bf16[8,2176]{1,0:T(8,128)(2,1)S(1)}, u32[]{:S(2)}, u32[]{:S(2)}) collective-permute-start(bf16[8,2176]{1,0:T(8,128)(2,1)S(1)} %get-tuple-element.24), channel_id=1, source_target_pairs={{0,2},{1,3},{2,0},{3,1},{4,6},{5,7},{6,4},{7,5},{8,10},{9,11},{10,... | collective-permute-start | bytes 104456 | tf_op jit(solution)/shard_map/ppermute | solution.py:32
  15.5 3.7 %collective-permute-start.5 = (bf16[8,2176]{1,0:T(8,128)(2,1)S(1)}, bf16[8,2176]{1,0:T(8,128)(2,1)S(1)}, u32[]{:S(2)}, u32[]{:S(2)}) collective-permute-start(bf16[8,2176]{1,0:T(8,128)(2,1)S(1)} %get-tuple-element.25), channel_id=1, source_target_pairs={{0,3},{1,2},{2,1},{3,0},{4,7},{5,6},{6,5},{7,4},{8,11},{9,10},{10,... | collective-permute-start | bytes 104456 | tf_op jit(solution)/shard_map/ppermute | solution.py:32
  19.7 3.1 %collective-permute-start.7 = (bf16[8,512]{1,0:T(8,128)(2,1)S(1)}, bf16[8,512]{1,0:T(8,128)(2,1)S(1)}, u32[]{:S(2)}, u32[]{:S(2)}) collective-permute-start(bf16[8,512]{1,0:T(8,128)(2,1)S(1)} %get-tuple-element.26.refs_0_), channel_id=1, source_target_pairs={{3,0},{2,1},{1,2},{0,3},{7,4},{6,5},{5,6},{4,7},{11,8},{10,9},{9,1... | collective-permute-start | bytes 24584 | tf_op jit(solution)/shard_map/ppermute | solution.py:32
  23.1 4.2 %collective-permute-start.9 = (bf16[16,1024]{1,0:T(8,128)(2,1)S(1)}, bf16[16,1024]{1,0:T(8,128)(2,1)S(1)}, u32[]{:S(2)}, u32[]{:S(2)}) collective-permute-start(bf16[16,1024]{1,0:T(8,128)(2,1)S(1)} %shard_map.117), channel_id=1, source_target_pairs={{0,5},{1,4},{2,7},{3,6},{4,1},{5,0},{6,3},{7,2},{8,13},{9,12},{10,... | collective-permute-start | bytes 98312 | tf_op jit(solution)/shard_map/ppermute | solution.py:52
  23.5 5.9 %collective-permute-start.10 = (bf16[16,1024]{1,0:T(8,128)(2,1)S(1)}, bf16[16,1024]{1,0:T(8,128)(2,1)S(1)}, u32[]{:S(2)}, u32[]{:S(2)}) collective-permute-start(bf16[16,1024]{1,0:T(8,128)(2,1)S(1)} %shard_map.117), channel_id=1, source_target_pairs={{0,9},{1,8},{2,11},{3,10},{4,13},{5,12},{6,15},{7,14},{8,1},{9,0},... | collective-permute-start | bytes 98312 | tf_op jit(solution)/shard_map/ppermute | solution.py:52
  27.0 5.2 %collective-permute-start.11 = (bf16[16,1024]{1,0:T(8,128)(2,1)S(1)}, bf16[16,1024]{1,0:T(8,128)(2,1)S(1)}, u32[]{:S(2)}, u32[]{:S(2)}) collective-permute-start(bf16[16,1024]{1,0:T(8,128)(2,1)S(1)} %shard_map.117), channel_id=1, source_target_pairs={{0,13},{1,12},{2,15},{3,14},{4,9},{5,8},{6,11},{7,10},{8,5},{9,4},... | collective-permute-start | bytes 98312 | tf_op jit(solution)/shard_map/ppermute | solution.py:52
  32.8 12.3 %copy-start = (f32[2,4,4,128,128]{4,3,2,1,0:T(8,128)S(1)}, f32[2,4,4,128,128]{4,3,2,1,0:T(8,128)}, u32[]{:S(2)}) copy-start(f32[2,4,4,128,128]{4,3,2,1,0:T(8,128)} %state.7) | copy-start | bytes 6291460
  32.8 1.9 %collective-permute-start.12 = (bf16[8,2176]{1,0:T(8,128)(2,1)S(1)}, bf16[8,2176]{1,0:T(8,128)(2,1)S(1)}, u32[]{:S(2)}, u32[]{:S(2)}) collective-permute-start(bf16[8,2176]{1,0:T(8,128)(2,1)S(1)} %get-tuple-element.29), channel_id=1, source_target_pairs={{0,1},{1,0},{2,3},{3,2},{4,5},{5,4},{6,7},{7,6},{8,9},{9,8},{10,11... | collective-permute-start | bytes 104456 | tf_op jit(solution)/shard_map/ppermute | solution.py:32
  32.9 4.2 %collective-permute-start.13 = (bf16[8,2176]{1,0:T(8,128)(2,1)S(1)}, bf16[8,2176]{1,0:T(8,128)(2,1)S(1)}, u32[]{:S(2)}, u32[]{:S(2)}) collective-permute-start(bf16[8,2176]{1,0:T(8,128)(2,1)S(1)} %get-tuple-element.30), channel_id=1, source_target_pairs={{0,2},{1,3},{2,0},{3,1},{4,6},{5,7},{6,4},{7,5},{8,10},{9,11},{10,... | collective-permute-start | bytes 104456 | tf_op jit(solution)/shard_map/ppermute | solution.py:32
  33.6 3.7 %collective-permute-start.14 = (bf16[8,2176]{1,0:T(8,128)(2,1)S(1)}, bf16[8,2176]{1,0:T(8,128)(2,1)S(1)}, u32[]{:S(2)}, u32[]{:S(2)}) collective-permute-start(bf16[8,2176]{1,0:T(8,128)(2,1)S(1)} %get-tuple-element.31), channel_id=1, source_target_pairs={{0,3},{1,2},{2,1},{3,0},{4,7},{5,6},{6,5},{7,4},{8,11},{9,10},{10,... | collective-permute-start | bytes 104456 | tf_op jit(solution)/shard_map/ppermute | solution.py:32
  37.8 3.1 %collective-permute-start.16 = (bf16[8,512]{1,0:T(8,128)(2,1)S(1)}, bf16[8,512]{1,0:T(8,128)(2,1)S(1)}, u32[]{:S(2)}, u32[]{:S(2)}) collective-permute-start(bf16[8,512]{1,0:T(8,128)(2,1)S(1)} %get-tuple-element.32.refs_0_), channel_id=1, source_target_pairs={{3,0},{2,1},{1,2},{0,3},{7,4},{6,5},{5,6},{4,7},{11,8},{10,9},{9,1... | collective-permute-start | bytes 24584 | tf_op jit(solution)/shard_map/ppermute | solution.py:32
  41.3 6.9 %collective-permute-start.17 = (bf16[4,1024]{1,0:T(4,128)(2,1)S(1)}, bf16[4,1024]{1,0:T(4,128)(2,1)S(1)}, u32[]{:S(2)}, u32[]{:S(2)}) collective-permute-start(bf16[4,1024]{1,0:T(4,128)(2,1)S(1)} %get-tuple-element.35), channel_id=1, source_target_pairs={{0,5},{1,4},{2,7},{3,6},{4,1},{5,0},{6,3},{7,2},{8,13},{9,12},{10,... | collective-permute-start | bytes 24584 | tf_op jit(solution)/shard_map/ppermute | solution.py:52
  41.3 6.9 %collective-permute-start.18 = (bf16[4,1024]{1,0:T(4,128)(2,1)S(1)}, bf16[4,1024]{1,0:T(4,128)(2,1)S(1)}, u32[]{:S(2)}, u32[]{:S(2)}) collective-permute-start(bf16[4,1024]{1,0:T(4,128)(2,1)S(1)} %get-tuple-element.36), channel_id=1, source_target_pairs={{0,9},{1,8},{2,11},{3,10},{4,13},{5,12},{6,15},{7,14},{8,1},{9,0},... | collective-permute-start | bytes 24584 | tf_op jit(solution)/shard_map/ppermute | solution.py:52
  42.4 5.8 %collective-permute-start.19 = (bf16[4,1024]{1,0:T(4,128)(2,1)S(1)}, bf16[4,1024]{1,0:T(4,128)(2,1)S(1)}, u32[]{:S(2)}, u32[]{:S(2)}) collective-permute-start(bf16[4,1024]{1,0:T(4,128)(2,1)S(1)} %get-tuple-element.37), channel_id=1, source_target_pairs={{0,13},{1,12},{2,15},{3,14},{4,9},{5,8},{6,11},{7,10},{8,5},{9,4},... | collective-permute-start | bytes 24584 | tf_op jit(solution)/shard_map/ppermute | solution.py:52

commit v9 on v8

--- a/solution.py
+++ b/solution.py
@@ -207,16 +207,8 @@
         copy.wait()
 
 
-def narrow(layer, state, out, staged, sems):
-    copies = [
-        pltpu.make_async_copy(state.at[layer, seq], staged.at[seq], sems.at[seq])
-        for seq in range(state.shape[1])
-    ]
-    for copy in copies:
-        copy.start()
-    for seq, copy in enumerate(copies):
-        copy.wait()
-        out[seq] = staged[seq].astype(BF16)
+def narrow(layer, state, out):
+    out[...] = state[layer].astype(BF16)
 
 
 def slot_parts(refs, group):
@@ -336,18 +328,9 @@
     crossed = cross_copy(n_dp, w_out)
     states = []
     for layer in range(2):
-        narrowed = pl.pallas_call(
-            functools.partial(narrow, layer),
-            name="narrow",
-            out_shape=pltpu.VMEM(state.shape[1:], BF16),
-            in_specs=[ANY],
-            out_specs=VMEM,
-            scratch_shapes=[
-                pltpu.VMEM(state.shape[1:], F32),
-                pltpu.SemaphoreType.DMA((seqs,)),
-            ],
-            compiler_params=pltpu.CompilerParams(vmem_limit_bytes=4 << 20),
-        )(pltpu.with_memory_space_constraint(state, pltpu.HBM))
+        (narrowed,) = call(
+            functools.partial(narrow, layer), (state,), [VMEM], [(state.shape[1:], BF16)]
+        )
         states.append([narrowed] + [cross_copy(n_dp, narrowed)] * flip)
     base = held = None
     new_state = None

time: 49 us -> 48.2 us (0.984)
  Pallas kernels: 9.27 us -> 6.91 us
  local copies, waits for them, and re-layouts: 0.43 us -> 1.65 us
  waiting for transfers between devices: 17.9 us -> 18.4 us
    pallas_call x2 -> x0, Pallas kernels: 2.47 us -> none  [per_device(): pl.pallas_call(functools.partial(narrow, layer), name='narrow', out_shape...]
    unnamed x20 -> x22, local copies, waits for them, and re-layouts: 0.43 us -> 1.65 us
    ppermute x11, waiting for transfers between devices: 12.9 us -> 13.5 us  [exchange(): lax.ppermute(array, axis, [(b, a) for a, b in pairs] if inward else pairs)]
    pallas_call x9 -> x11, Pallas kernels: 3.49 us -> 3.6 us  [call(): pl.pallas_call(body, out_shape=[pltpu.VMEM(shape, dtype) for shape, dtype...]
  transfers between devices with their start and end apart: 20 -> 20, of which waited for: 9 -> 9; matrix products, arithmetic and copies ran while one was open for 0% -> 0% of each run, Pallas kernels for 16% -> 11%
where the time goes in v9:
time: 48.2 us; the launch traced here: 48.1 us
  starting transfers between devices  20.2 us (42%)
  waiting for transfers between devices  18.4 us (38%)
  Pallas kernels  6.91 us (14%)
  local copies, waits for them, and re-layouts  1.65 us (3%)
  between operations  0.85 us (2%)
    ppermute x11, waiting for transfers between devices, exchange(): lax.ppermute(array, axis, [(b, a) for a, b in pairs] if inward else pairs)  13.5 us
    ppermute x11, starting transfers between devices, exchange(): lax.ppermute(array, axis, [(b, a) for a, b in pairs] if inward else pairs)  11.2 us
    ppermute x6, starting transfers between devices, cross_exchange(): lax.ppermute(arrays[k - 1], ('tp', 'dp'), cross_pairs(n_tp, n_dp, k))  7.85 us
    ppermute x6, waiting for transfers between devices, cross_exchange(): lax.ppermute(arrays[k - 1], ('tp', 'dp'), cross_pairs(n_tp, n_dp, k))  4.95 us
    pallas_call x11, Pallas kernels, call(): pl.pallas_call(body, out_shape=[pltpu.VMEM(shape, dtype) for shape, dtype...  3.6 us
    pallas_call x2, Pallas kernels, per_device(): pl.pallas_call(functools.partial(update, layer), name='update', out_shape...  2.7 us
    unnamed x22, local copies, waits for them, and re-layouts  1.65 us
    ppermute x3, starting transfers between devices, cross_copy(): return lax.ppermute(array, 'dp', [(d, d ^ 1) for d in range(n_dp)])  1.19 us
  transfers between devices with their start and end apart: 20, of which 9 were waited for; matrix products, arithmetic and copies ran while one was open for 0% of the time, Pallas kernels for 11%

profile of v9, /device:TPU:0, one launch (start us, length us, event | category | flops | bytes accessed | tf_op | source)
XLA Modules:
  0.0 48.1 jit_solution(12433535796641692090)
XLA Ops:
  0.6 0.6 %collective-permute-start.8 = (bf16[2,512,1024]{2,1,0:T(8,128)(2,1)}, bf16[2,512,1024]{2,1,0:T(8,128)(2,1)S(1)}, u32[]{:S(2)}, u32[]{:S(2)}) collective-permute-start(bf16[2,512,1024]{2,1,0:T(8,128)(2,1)} %refs_2_.3), channel_id=1, source_target_pairs={{0,1},{1,0},{2,3},{3,2},{4,5},{5,4},{6,7},{7,6},{8,9},{9,8},{10,11... | collective-permute-start | bytes 6291464 | tf_op jit(solution)/shard_map/ppermute | solution.py:61
  1.2 2.6 %collective-permute-start = (bf16[4,1024]{1,0:T(4,128)(2,1)}, bf16[4,1024]{1,0:T(4,128)(2,1)S(1)}, u32[]{:S(2)}, u32[]{:S(2)}) collective-permute-start(bf16[4,1024]{1,0:T(4,128)(2,1)} %refs_0_.1), channel_id=1, source_target_pairs={{4,0},{0,4},{12,8},{8,12},{5,1},{1,5},{13,9},{9,13},{6,2},{2,6},{1... | collective-permute-start | bytes 24584 | tf_op jit(solution)/shard_map/ppermute | solution.py:32
  3.8 2.6 %collective-permute-start.1 = (bf16[4,1024]{1,0:T(4,128)(2,1)}, bf16[4,1024]{1,0:T(4,128)(2,1)S(1)}, u32[]{:S(2)}, u32[]{:S(2)}) collective-permute-start(bf16[4,1024]{1,0:T(4,128)(2,1)} %refs_0_.1), channel_id=1, source_target_pairs={{8,0},{12,4},{0,8},{4,12},{9,1},{13,5},{1,9},{5,13},{10,2},{14,6},... | collective-permute-start | bytes 24584 | tf_op jit(solution)/shard_map/ppermute | solution.py:32
  6.4 1.6 %copy-done = f32[2,4,4,128,128]{4,3,2,1,0:T(8,128)S(1)} copy-done((f32[2,4,4,128,128]{4,3,2,1,0:T(8,128)S(1)}, f32[2,4,4,128,128]{4,3,2,1,0:T(8,128)}, u32[]{:S(2)}) %copy-start) | copy-done | bytes 2097176
  8.3 0.6 %collective-permute-start.15 = (bf16[4,4,128,128]{3,2,1,0:T(8,128)(2,1)S(1)}, bf16[4,4,128,128]{3,2,1,0:T(8,128)(2,1)S(1)}, u32[]{:S(2)}, u32[]{:S(2)}) collective-permute-start(bf16[4,4,128,128]{3,2,1,0:T(8,128)(2,1)S(1)} %shard_map.120.refs_6_), channel_id=1, source_target_pairs={{0,1},{1,0},{2,3},{3,2},{4,5},{5,4},{6,7},{7,6},{8,9},{9,8},{10,11... | collective-permute-start | bytes 1572872 | tf_op jit(solution)/shard_map/ppermute | solution.py:61
  8.9 3.2 %collective-permute-done.2.refs_3_ = bf16[4,1024]{1,0:T(4,128)(2,1)S(1)} collective-permute-done((bf16[4,1024]{1,0:T(4,128)(2,1)}, bf16[4,1024]{1,0:T(4,128)(2,1)S(1)}, u32[]{:S(2)}, u32[]{:S(2)}) %collective-permute-start.2) | collective-permute-done | bytes 8224 | tf_op jit(solution)/shard_map/ppermute | solution.py:32
  12.1 0.8 %shard_map.114 = (bf16[16,1024]{1,0:T(8,128)(2,1)S(1)}, f32[8,2176]{1,0:T(8,128)S(1)}, bf16[8,2176]{1,0:T(8,128)(2,1)S(1)}, bf16[8,2176]{1,0:T(8,128)(2,1)S(1)}, bf16[8,2176]{1,0:T(8,128)(2,1)S(1)}) custom-call(bf16[4,1024]{1,0:T(4,128)(2,1)S(1)} %copy-done.9, bf16[4,1024]{1,0:T(4,128)(2,1)S(1)} %collective-permute-done.refs_1_, ...), custom_call_target="tpu_custom_call" | custom-call | tf_op jit(solution)/shard_map/pallas_call | solution.py:287
  13.0 1.7 %collective-permute-start.4 = (bf16[8,2176]{1,0:T(8,128)(2,1)S(1)}, bf16[8,2176]{1,0:T(8,128)(2,1)S(1)}, u32[]{:S(2)}, u32[]{:S(2)}) collective-permute-start(bf16[8,2176]{1,0:T(8,128)(2,1)S(1)} %get-tuple-element.24), channel_id=1, source_target_pairs={{0,2},{1,3},{2,0},{3,1},{4,6},{5,7},{6,4},{7,5},{8,10},{9,11},{10,... | collective-permute-start | bytes 104456 | tf_op jit(solution)/shard_map/ppermute | solution.py:32
  14.7 0.8 %collective-permute-start.5 = (bf16[8,2176]{1,0:T(8,128)(2,1)S(1)}, bf16[8,2176]{1,0:T(8,128)(2,1)S(1)}, u32[]{:S(2)}, u32[]{:S(2)}) collective-permute-start(bf16[8,2176]{1,0:T(8,128)(2,1)S(1)} %get-tuple-element.25), channel_id=1, source_target_pairs={{0,3},{1,2},{2,1},{3,0},{4,7},{5,6},{6,5},{7,4},{8,11},{9,10},{10,... | collective-permute-start | bytes 104456 | tf_op jit(solution)/shard_map/ppermute | solution.py:32
  15.5 1.4 %collective-permute-done.4.refs_2_ = bf16[8,2176]{1,0:T(8,128)(2,1)S(1)} collective-permute-done((bf16[8,2176]{1,0:T(8,128)(2,1)S(1)}, bf16[8,2176]{1,0:T(8,128)(2,1)S(1)}, u32[]{:S(2)}, u32[]{:S(2)}) %collective-permute-start.4) | collective-permute-done | bytes 34848 | tf_op jit(solution)/shard_map/ppermute | solution.py:32
  16.9 1.4 %collective-permute-done.5.refs_3_ = bf16[8,2176]{1,0:T(8,128)(2,1)S(1)} collective-permute-done((bf16[8,2176]{1,0:T(8,128)(2,1)S(1)}, bf16[8,2176]{1,0:T(8,128)(2,1)S(1)}, u32[]{:S(2)}, u32[]{:S(2)}) %collective-permute-start.5) | collective-permute-done | bytes 34848 | tf_op jit(solution)/shard_map/ppermute | solution.py:32
  18.3 0.4 shard_map.116
  18.8 0.6 %collective-permute-start.7 = (bf16[8,512]{1,0:T(8,128)(2,1)S(1)}, bf16[8,512]{1,0:T(8,128)(2,1)S(1)}, u32[]{:S(2)}, u32[]{:S(2)}) collective-permute-start(bf16[8,512]{1,0:T(8,128)(2,1)S(1)} %get-tuple-element.26.refs_0_), channel_id=1, source_target_pairs={{3,0},{2,1},{1,2},{0,3},{7,4},{6,5},{5,6},{4,7},{11,8},{10,9},{9,1... | collective-permute-start | bytes 24584 | tf_op jit(solution)/shard_map/ppermute | solution.py:32
  19.4 2.5 %collective-permute-done.7.refs_1_ = bf16[8,512]{1,0:T(8,128)(2,1)S(1)} collective-permute-done((bf16[8,512]{1,0:T(8,128)(2,1)S(1)}, bf16[8,512]{1,0:T(8,128)(2,1)S(1)}, u32[]{:S(2)}, u32[]{:S(2)}) %collective-permute-start.7) | collective-permute-done | bytes 8224 | tf_op jit(solution)/shard_map/ppermute | solution.py:32
  22.2 0.5 %collective-permute-start.9 = (bf16[16,1024]{1,0:T(8,128)(2,1)S(1)}, bf16[16,1024]{1,0:T(8,128)(2,1)S(1)}, u32[]{:S(2)}, u32[]{:S(2)}) collective-permute-start(bf16[16,1024]{1,0:T(8,128)(2,1)S(1)} %shard_map.118), channel_id=1, source_target_pairs={{0,5},{1,4},{2,7},{3,6},{4,1},{5,0},{6,3},{7,2},{8,13},{9,12},{10,... | collective-permute-start | bytes 98312 | tf_op jit(solution)/shard_map/ppermute | solution.py:52
  22.7 3.5 %collective-permute-start.10 = (bf16[16,1024]{1,0:T(8,128)(2,1)S(1)}, bf16[16,1024]{1,0:T(8,128)(2,1)S(1)}, u32[]{:S(2)}, u32[]{:S(2)}) collective-permute-start(bf16[16,1024]{1,0:T(8,128)(2,1)S(1)} %shard_map.118), channel_id=1, source_target_pairs={{0,9},{1,8},{2,11},{3,10},{4,13},{5,12},{6,15},{7,14},{8,1},{9,0},... | collective-permute-start | bytes 98312 | tf_op jit(solution)/shard_map/ppermute | solution.py:52
  26.4 2.1 %collective-permute-done.10.refs_2_ = bf16[16,1024]{1,0:T(8,128)(2,1)S(1)} collective-permute-done((bf16[16,1024]{1,0:T(8,128)(2,1)S(1)}, bf16[16,1024]{1,0:T(8,128)(2,1)S(1)}, u32[]{:S(2)}, u32[]{:S(2)}) %collective-permute-start.10) | collective-permute-done | bytes 32800 | tf_op jit(solution)/shard_map/ppermute | solution.py:52
  28.5 2.9 %collective-permute-done.11.refs_3_ = bf16[16,1024]{1,0:T(8,128)(2,1)S(1)} collective-permute-done((bf16[16,1024]{1,0:T(8,128)(2,1)S(1)}, bf16[16,1024]{1,0:T(8,128)(2,1)S(1)}, u32[]{:S(2)}, u32[]{:S(2)}) %collective-permute-start.11) | collective-permute-done | bytes 32800 | tf_op jit(solution)/shard_map/ppermute | solution.py:52
  31.4 0.7 %shard_map.119 = (bf16[16,1024]{1,0:T(8,128)(2,1)S(1)}, f32[8,2176]{1,0:T(8,128)S(1)}, bf16[8,2176]{1,0:T(8,128)(2,1)S(1)}, bf16[8,2176]{1,0:T(8,128)(2,1)S(1)}, bf16[8,2176]{1,0:T(8,128)(2,1)S(1)}) custom-call(f32[16,1024]{1,0:T(8,128)S(1)} %shard_map.117.refs_0_, bf16[16,1024]{1,0:T(8,128)(2,1)S(1)} %collective-permute-done.9.refs_1_, ...), custom_call_target="tpu_custom_call" | custom-call | tf_op jit(solution)/shard_map/pallas_call | solution.py:287
  32.2 0.7 %collective-permute-start.13 = (bf16[8,2176]{1,0:T(8,128)(2,1)S(1)}, bf16[8,2176]{1,0:T(8,128)(2,1)S(1)}, u32[]{:S(2)}, u32[]{:S(2)}) collective-permute-start(bf16[8,2176]{1,0:T(8,128)(2,1)S(1)} %get-tuple-element.30), channel_id=1, source_target_pairs={{0,2},{1,3},{2,0},{3,1},{4,6},{5,7},{6,4},{7,5},{8,10},{9,11},{10,... | collective-permute-start | bytes 104456 | tf_op jit(solution)/shard_map/ppermute | solution.py:32
  32.8 1.1 %collective-permute-start.14 = (bf16[8,2176]{1,0:T(8,128)(2,1)S(1)}, bf16[8,2176]{1,0:T(8,128)(2,1)S(1)}, u32[]{:S(2)}, u32[]{:S(2)}) collective-permute-start(bf16[8,2176]{1,0:T(8,128)(2,1)S(1)} %get-tuple-element.31), channel_id=1, source_target_pairs={{0,3},{1,2},{2,1},{3,0},{4,7},{5,6},{6,5},{7,4},{8,11},{9,10},{10,... | collective-permute-start | bytes 104456 | tf_op jit(solution)/shard_map/ppermute | solution.py:32
  33.9 2.4 %collective-permute-done.13.refs_2_ = bf16[8,2176]{1,0:T(8,128)(2,1)S(1)} collective-permute-done((bf16[8,2176]{1,0:T(8,128)(2,1)S(1)}, bf16[8,2176]{1,0:T(8,128)(2,1)S(1)}, u32[]{:S(2)}, u32[]{:S(2)}) %collective-permute-start.13) | collective-permute-done | bytes 34848 | tf_op jit(solution)/shard_map/ppermute | solution.py:32
  36.6 0.4 shard_map.121
  37.0 0.8 %collective-permute-start.16 = (bf16[8,512]{1,0:T(8,128)(2,1)S(1)}, bf16[8,512]{1,0:T(8,128)(2,1)S(1)}, u32[]{:S(2)}, u32[]{:S(2)}) collective-permute-start(bf16[8,512]{1,0:T(8,128)(2,1)S(1)} %get-tuple-element.32.refs_0_), channel_id=1, source_target_pairs={{3,0},{2,1},{1,2},{0,3},{7,4},{6,5},{5,6},{4,7},{11,8},{10,9},{9,1... | collective-permute-start | bytes 24584 | tf_op jit(solution)/shard_map/ppermute | solution.py:32
  37.9 2.3 %collective-permute-done.16.refs_1_ = bf16[8,512]{1,0:T(8,128)(2,1)S(1)} collective-permute-done((bf16[8,512]{1,0:T(8,128)(2,1)S(1)}, bf16[8,512]{1,0:T(8,128)(2,1)S(1)}, u32[]{:S(2)}, u32[]{:S(2)}) %collective-permute-start.16) | collective-permute-done | bytes 8224 | tf_op jit(solution)/shard_map/ppermute | solution.py:32
  40.2 0.3 shard_map.123
  40.5 1.1 %collective-permute-start.18 = (bf16[4,1024]{1,0:T(4,128)(2,1)S(1)}, bf16[4,1024]{1,0:T(4,128)(2,1)S(1)}, u32[]{:S(2)}, u32[]{:S(2)}) collective-permute-start(bf16[4,1024]{1,0:T(4,128)(2,1)S(1)} %get-tuple-element.36), channel_id=1, source_target_pairs={{0,9},{1,8},{2,11},{3,10},{4,13},{5,12},{6,15},{7,14},{8,1},{9,0},... | collective-permute-start | bytes 24584 | tf_op jit(solution)/shard_map/ppermute | solution.py:52
  41.7 2.7 %collective-permute-start.19 = (bf16[4,1024]{1,0:T(4,128)(2,1)S(1)}, bf16[4,1024]{1,0:T(4,128)(2,1)S(1)}, u32[]{:S(2)}, u32[]{:S(2)}) collective-permute-start(bf16[4,1024]{1,0:T(4,128)(2,1)S(1)} %get-tuple-element.37), channel_id=1, source_target_pairs={{0,13},{1,12},{2,15},{3,14},{4,9},{5,8},{6,11},{7,10},{8,5},{9,4},... | collective-permute-start | bytes 24584 | tf_op jit(solution)/shard_map/ppermute | solution.py:52
  44.4 1.3 %update.2.refs_0_ = f32[2,4,4,128,128]{4,3,2,1,0:T(8,128)} custom-call(f32[4,3,512]{2,1,0:T(4,128)S(1)} %get-tuple-element.39.gates, f32[2,4,4,128,128]{4,3,2,1,0:T(8,128)S(1)} %copy-done.1), custom_call_target="tpu_custom_call" | custom-call | tf_op jit(solution)/shard_map/update/pallas_call | solution.py:366
  45.7 1.4 %update.3 = f32[2,4,4,128,128]{4,3,2,1,0:T(8,128)} custom-call(f32[4,3,512]{2,1,0:T(4,128)S(1)} %get-tuple-element.38.gates, f32[2,4,4,128,128]{4,3,2,1,0:T(8,128)S(1)} %copy-done.1, f32[2,4,4,128,128]{4,3,2,1,0:T(8,128)} %update.2.refs_0_), custom_call_target="tpu_custom_call", output_to_operand_aliasing={{}: (2, {})} | custom-call | tf_op jit(solution)/shard_map/update/pallas_call | solution.py:366
  47.1 0.3 shard_map.122.own
  47.4 0.6 %close.1 = bf16[4,1024]{1,0:T(4,128)(2,1)} custom-call(f32[4,1024]{1,0:T(4,128)S(1)} %shard_map.122.own, bf16[4,1024]{1,0:T(4,128)(2,1)S(1)} %collective-permute-done.17.refs_0_, bf16[4,1024]{1,0:T(4,128)(2,1)S(1)} %collective-permute-done.18.refs_1_, bf16[4,1024]{1,0:T(4,128)(2,1)S(1)} %collective-permute-done.19.refs_2_), custom_call_target="tpu_custom_call" | custom-call | tf_op jit(solution)/shard_map/close/pallas_call | solution.py:411
  (44 shorter events, 1.2 us)
Async XLA Ops:
  0.6 21.3 %collective-permute-start.8 = (bf16[2,512,1024]{2,1,0:T(8,128)(2,1)}, bf16[2,512,1024]{2,1,0:T(8,128)(2,1)S(1)}, u32[]{:S(2)}, u32[]{:S(2)}) collective-permute-start(bf16[2,512,1024]{2,1,0:T(8,128)(2,1)} %refs_2_.3), channel_id=1, source_target_pairs={{0,1},{1,0},{2,3},{3,2},{4,5},{5,4},{6,7},{7,6},{8,9},{9,8},{10,11... | collective-permute-start | bytes 6291464 | tf_op jit(solution)/shard_map/ppermute | solution.py:61
  1.2 7.1 %collective-permute-start = (bf16[4,1024]{1,0:T(4,128)(2,1)}, bf16[4,1024]{1,0:T(4,128)(2,1)S(1)}, u32[]{:S(2)}, u32[]{:S(2)}) collective-permute-start(bf16[4,1024]{1,0:T(4,128)(2,1)} %refs_0_.1), channel_id=1, source_target_pairs={{4,0},{0,4},{12,8},{8,12},{5,1},{1,5},{13,9},{9,13},{6,2},{2,6},{1... | collective-permute-start | bytes 24584 | tf_op jit(solution)/shard_map/ppermute | solution.py:32
  3.8 5.0 %collective-permute-start.1 = (bf16[4,1024]{1,0:T(4,128)(2,1)}, bf16[4,1024]{1,0:T(4,128)(2,1)S(1)}, u32[]{:S(2)}, u32[]{:S(2)}) collective-permute-start(bf16[4,1024]{1,0:T(4,128)(2,1)} %refs_0_.1), channel_id=1, source_target_pairs={{8,0},{12,4},{0,8},{4,12},{9,1},{13,5},{1,9},{5,13},{10,2},{14,6},... | collective-permute-start | bytes 24584 | tf_op jit(solution)/shard_map/ppermute | solution.py:32
  6.4 5.7 %collective-permute-start.2 = (bf16[4,1024]{1,0:T(4,128)(2,1)}, bf16[4,1024]{1,0:T(4,128)(2,1)S(1)}, u32[]{:S(2)}, u32[]{:S(2)}) collective-permute-start(bf16[4,1024]{1,0:T(4,128)(2,1)} %refs_0_.1), channel_id=1, source_target_pairs={{12,0},{8,4},{4,8},{0,12},{13,1},{9,5},{5,9},{1,13},{14,2},{10,6},... | collective-permute-start | bytes 24584 | tf_op jit(solution)/shard_map/ppermute | solution.py:32
  6.4 1.6 %copy-start = (f32[2,4,4,128,128]{4,3,2,1,0:T(8,128)S(1)}, f32[2,4,4,128,128]{4,3,2,1,0:T(8,128)}, u32[]{:S(2)}) copy-start(f32[2,4,4,128,128]{4,3,2,1,0:T(8,128)} %state.7) | copy-start | bytes 6291460
  8.1 10.2 %collective-permute-start.6 = (bf16[4,4,128,128]{3,2,1,0:T(8,128)(2,1)S(1)}, bf16[4,4,128,128]{3,2,1,0:T(8,128)(2,1)S(1)}, u32[]{:S(2)}, u32[]{:S(2)}) collective-permute-start(bf16[4,4,128,128]{3,2,1,0:T(8,128)(2,1)S(1)} %shard_map.115.refs_6_), channel_id=1, source_target_pairs={{0,1},{1,0},{2,3},{3,2},{4,5},{5,4},{6,7},{7,6},{8,9},{9,8},{10,11... | collective-permute-start | bytes 1572872 | tf_op jit(solution)/shard_map/ppermute | solution.py:61
  8.2 3.9 %copy-start.2 = (bf16[2,1024,512]{2,1,0:T(8,128)(2,1)S(1)}, bf16[2,1024,512]{2,1,0:T(8,128)(2,1)}, u32[]{:S(2)}) copy-start(bf16[2,1024,512]{2,1,0:T(8,128)(2,1)} %refs_5_.6) | copy-start | bytes 6291460
  8.2 3.9 %copy-start.3 = (bf16[2,1024,512]{2,1,0:T(8,128)(2,1)S(1)}, bf16[2,1024,512]{2,1,0:T(8,128)(2,1)}, u32[]{:S(2)}) copy-start(bf16[2,1024,512]{2,1,0:T(8,128)(2,1)} %refs_6_.3) | copy-start | bytes 6291460
  8.2 3.9 %copy-start.4 = (bf16[2,1024,512]{2,1,0:T(8,128)(2,1)S(1)}, bf16[2,1024,512]{2,1,0:T(8,128)(2,1)}, u32[]{:S(2)}) copy-start(bf16[2,1024,512]{2,1,0:T(8,128)(2,1)} %refs_7_.3) | copy-start | bytes 6291460
  8.2 3.8 %copy-start.5 = (bf16[2,1024,512]{2,1,0:T(8,128)(2,1)S(1)}, bf16[2,1024,512]{2,1,0:T(8,128)(2,1)}, u32[]{:S(2)}) copy-start(bf16[2,1024,512]{2,1,0:T(8,128)(2,1)} %refs_8_.3) | copy-start | bytes 6291460
  8.3 3.8 %copy-start.7 = (f32[2,1024]{1,0:T(2,128)S(1)}, f32[2,1024]{1,0:T(2,128)}, u32[]{:S(2)}) copy-start(f32[2,1024]{1,0:T(2,128)} %refs_4_.4) | copy-start | bytes 24580
  8.3 3.8 %copy-start.9 = (bf16[4,1024]{1,0:T(4,128)(2,1)S(1)}, bf16[4,1024]{1,0:T(4,128)(2,1)}, u32[]{:S(2)}) copy-start(bf16[4,1024]{1,0:T(4,128)(2,1)} %refs_0_.1) | copy-start | bytes 24580
  8.3 25.6 %collective-permute-start.15 = (bf16[4,4,128,128]{3,2,1,0:T(8,128)(2,1)S(1)}, bf16[4,4,128,128]{3,2,1,0:T(8,128)(2,1)S(1)}, u32[]{:S(2)}, u32[]{:S(2)}) collective-permute-start(bf16[4,4,128,128]{3,2,1,0:T(8,128)(2,1)S(1)} %shard_map.120.refs_6_), channel_id=1, source_target_pairs={{0,1},{1,0},{2,3},{3,2},{4,5},{5,4},{6,7},{7,6},{8,9},{9,8},{10,11... | collective-permute-start | bytes 1572872 | tf_op jit(solution)/shard_map/ppermute | solution.py:61
  12.1 6.2 %copy-start.8 = (f32[2,512]{1,0:T(2,128)S(1)}, f32[2,512]{1,0:T(2,128)}, u32[]{:S(2)}) copy-start(f32[2,512]{1,0:T(2,128)} %refs_4_.5) | copy-start | bytes 12292
  12.1 6.2 %copy-start.10 = (f32[2,128]{1,0:T(2,128)S(1)}, f32[2,128]{1,0:T(2,128)}, u32[]{:S(2)}) copy-start(f32[2,128]{1,0:T(2,128)} %refs_5_.7) | copy-start | bytes 3076
  12.9 13.3 %copy-start.6 = (bf16[2,512,1024]{2,1,0:T(8,128)(2,1)S(1)}, bf16[2,512,1024]{2,1,0:T(8,128)(2,1)}, u32[]{:S(2)}) copy-start(bf16[2,512,1024]{2,1,0:T(8,128)(2,1)} %refs_2_.3) | copy-start | bytes 6291460
  12.9 1.8 %collective-permute-start.3 = (bf16[8,2176]{1,0:T(8,128)(2,1)S(1)}, bf16[8,2176]{1,0:T(8,128)(2,1)S(1)}, u32[]{:S(2)}, u32[]{:S(2)}) collective-permute-start(bf16[8,2176]{1,0:T(8,128)(2,1)S(1)} %get-tuple-element.23), channel_id=1, source_target_pairs={{0,1},{1,0},{2,3},{3,2},{4,5},{5,4},{6,7},{7,6},{8,9},{9,8},{10,11... | collective-permute-start | bytes 104456 | tf_op jit(solution)/shard_map/ppermute | solution.py:32
  13.0 4.0 %collective-permute-start.4 = (bf16[8,2176]{1,0:T(8,128)(2,1)S(1)}, bf16[8,2176]{1,0:T(8,128)(2,1)S(1)}, u32[]{:S(2)}, u32[]{:S(2)}) collective-permute-start(bf16[8,2176]{1,0:T(8,128)(2,1)S(1)} %get-tuple-element.24), channel_id=1, source_target_pairs={{0,2},{1,3},{2,0},{3,1},{4,6},{5,7},{6,4},{7,5},{8,10},{9,11},{10,... | collective-permute-start | bytes 104456 | tf_op jit(solution)/shard_map/ppermute | solution.py:32
  14.7 3.6 %collective-permute-start.5 = (bf16[8,2176]{1,0:T(8,128)(2,1)S(1)}, bf16[8,2176]{1,0:T(8,128)(2,1)S(1)}, u32[]{:S(2)}, u32[]{:S(2)}) collective-permute-start(bf16[8,2176]{1,0:T(8,128)(2,1)S(1)} %get-tuple-element.25), channel_id=1, source_target_pairs={{0,3},{1,2},{2,1},{3,0},{4,7},{5,6},{6,5},{7,4},{8,11},{9,10},{10,... | collective-permute-start | bytes 104456 | tf_op jit(solution)/shard_map/ppermute | solution.py:32
  18.8 3.1 %collective-permute-start.7 = (bf16[8,512]{1,0:T(8,128)(2,1)S(1)}, bf16[8,512]{1,0:T(8,128)(2,1)S(1)}, u32[]{:S(2)}, u32[]{:S(2)}) collective-permute-start(bf16[8,512]{1,0:T(8,128)(2,1)S(1)} %get-tuple-element.26.refs_0_), channel_id=1, source_target_pairs={{3,0},{2,1},{1,2},{0,3},{7,4},{6,5},{5,6},{4,7},{11,8},{10,9},{9,1... | collective-permute-start | bytes 24584 | tf_op jit(solution)/shard_map/ppermute | solution.py:32
  22.2 4.3 %collective-permute-start.9 = (bf16[16,1024]{1,0:T(8,128)(2,1)S(1)}, bf16[16,1024]{1,0:T(8,128)(2,1)S(1)}, u32[]{:S(2)}, u32[]{:S(2)}) collective-permute-start(bf16[16,1024]{1,0:T(8,128)(2,1)S(1)} %shard_map.118), channel_id=1, source_target_pairs={{0,5},{1,4},{2,7},{3,6},{4,1},{5,0},{6,3},{7,2},{8,13},{9,12},{10,... | collective-permute-start | bytes 98312 | tf_op jit(solution)/shard_map/ppermute | solution.py:52
  22.7 5.8 %collective-permute-start.10 = (bf16[16,1024]{1,0:T(8,128)(2,1)S(1)}, bf16[16,1024]{1,0:T(8,128)(2,1)S(1)}, u32[]{:S(2)}, u32[]{:S(2)}) collective-permute-start(bf16[16,1024]{1,0:T(8,128)(2,1)S(1)} %shard_map.118), channel_id=1, source_target_pairs={{0,9},{1,8},{2,11},{3,10},{4,13},{5,12},{6,15},{7,14},{8,1},{9,0},... | collective-permute-start | bytes 98312 | tf_op jit(solution)/shard_map/ppermute | solution.py:52
  26.2 5.2 %collective-permute-start.11 = (bf16[16,1024]{1,0:T(8,128)(2,1)S(1)}, bf16[16,1024]{1,0:T(8,128)(2,1)S(1)}, u32[]{:S(2)}, u32[]{:S(2)}) collective-permute-start(bf16[16,1024]{1,0:T(8,128)(2,1)S(1)} %shard_map.118), channel_id=1, source_target_pairs={{0,13},{1,12},{2,15},{3,14},{4,9},{5,8},{6,11},{7,10},{8,5},{9,4},... | collective-permute-start | bytes 98312 | tf_op jit(solution)/shard_map/ppermute | solution.py:52
  32.0 12.3 %copy-start.1 = (f32[2,4,4,128,128]{4,3,2,1,0:T(8,128)S(1)}, f32[2,4,4,128,128]{4,3,2,1,0:T(8,128)}, u32[]{:S(2)}) copy-start(f32[2,4,4,128,128]{4,3,2,1,0:T(8,128)} %state.7) | copy-start | bytes 6291460
  32.0 1.9 %collective-permute-start.12 = (bf16[8,2176]{1,0:T(8,128)(2,1)S(1)}, bf16[8,2176]{1,0:T(8,128)(2,1)S(1)}, u32[]{:S(2)}, u32[]{:S(2)}) collective-permute-start(bf16[8,2176]{1,0:T(8,128)(2,1)S(1)} %get-tuple-element.29), channel_id=1, source_target_pairs={{0,1},{1,0},{2,3},{3,2},{4,5},{5,4},{6,7},{7,6},{8,9},{9,8},{10,11... | collective-permute-start | bytes 104456 | tf_op jit(solution)/shard_map/ppermute | solution.py:32
  32.2 4.2 %collective-permute-start.13 = (bf16[8,2176]{1,0:T(8,128)(2,1)S(1)}, bf16[8,2176]{1,0:T(8,128)(2,1)S(1)}, u32[]{:S(2)}, u32[]{:S(2)}) collective-permute-start(bf16[8,2176]{1,0:T(8,128)(2,1)S(1)} %get-tuple-element.30), channel_id=1, source_target_pairs={{0,2},{1,3},{2,0},{3,1},{4,6},{5,7},{6,4},{7,5},{8,10},{9,11},{10,... | collective-permute-start | bytes 104456 | tf_op jit(solution)/shard_map/ppermute | solution.py:32
  32.8 3.7 %collective-permute-start.14 = (bf16[8,2176]{1,0:T(8,128)(2,1)S(1)}, bf16[8,2176]{1,0:T(8,128)(2,1)S(1)}, u32[]{:S(2)}, u32[]{:S(2)}) collective-permute-start(bf16[8,2176]{1,0:T(8,128)(2,1)S(1)} %get-tuple-element.31), channel_id=1, source_target_pairs={{0,3},{1,2},{2,1},{3,0},{4,7},{5,6},{6,5},{7,4},{8,11},{9,10},{10,... | collective-permute-start | bytes 104456 | tf_op jit(solution)/shard_map/ppermute | solution.py:32
  37.0 3.1 %collective-permute-start.16 = (bf16[8,512]{1,0:T(8,128)(2,1)S(1)}, bf16[8,512]{1,0:T(8,128)(2,1)S(1)}, u32[]{:S(2)}, u32[]{:S(2)}) collective-permute-start(bf16[8,512]{1,0:T(8,128)(2,1)S(1)} %get-tuple-element.32.refs_0_), channel_id=1, source_target_pairs={{3,0},{2,1},{1,2},{0,3},{7,4},{6,5},{5,6},{4,7},{11,8},{10,9},{9,1... | collective-permute-start | bytes 24584 | tf_op jit(solution)/shard_map/ppermute | solution.py:32
  40.5 6.9 %collective-permute-start.17 = (bf16[4,1024]{1,0:T(4,128)(2,1)S(1)}, bf16[4,1024]{1,0:T(4,128)(2,1)S(1)}, u32[]{:S(2)}, u32[]{:S(2)}) collective-permute-start(bf16[4,1024]{1,0:T(4,128)(2,1)S(1)} %get-tuple-element.35), channel_id=1, source_target_pairs={{0,5},{1,4},{2,7},{3,6},{4,1},{5,0},{6,3},{7,2},{8,13},{9,12},{10,... | collective-permute-start | bytes 24584 | tf_op jit(solution)/shard_map/ppermute | solution.py:52
  40.5 6.9 %collective-permute-start.18 = (bf16[4,1024]{1,0:T(4,128)(2,1)S(1)}, bf16[4,1024]{1,0:T(4,128)(2,1)S(1)}, u32[]{:S(2)}, u32[]{:S(2)}) collective-permute-start(bf16[4,1024]{1,0:T(4,128)(2,1)S(1)} %get-tuple-element.36), channel_id=1, source_target_pairs={{0,9},{1,8},{2,11},{3,10},{4,13},{5,12},{6,15},{7,14},{8,1},{9,0},... | collective-permute-start | bytes 24584 | tf_op jit(solution)/shard_map/ppermute | solution.py:52
  41.7 5.8 %collective-permute-start.19 = (bf16[4,1024]{1,0:T(4,128)(2,1)S(1)}, bf16[4,1024]{1,0:T(4,128)(2,1)S(1)}, u32[]{:S(2)}, u32[]{:S(2)}) collective-permute-start(bf16[4,1024]{1,0:T(4,128)(2,1)S(1)} %get-tuple-element.37), channel_id=1, source_target_pairs={{0,13},{1,12},{2,15},{3,14},{4,9},{5,8},{6,11},{7,10},{8,5},{9,4},... | collective-permute-start | bytes 24584 | tf_op jit(solution)/shard_map/ppermute | solution.py:52

commit v10 on v9

--- a/solution.py
+++ b/solution.py
@@ -24,10 +24,18 @@
     return list(range(3, n_dp, 2)) if core_flip(n_dp) else list(range(1, n_dp))
 
 
+def start_order(axis, rounds):
+    order = list(reversed(rounds))
+    if axis == "tp" and len(order) > 2:
+        order[:2] = order[1], order[0]
+    return order
+
+
 def exchange(axis, n, arrays, inward=False, rounds=None):
     rounds = rounds or list(range(1, n))
-    parts = {}
-    for k, array in reversed(list(zip(rounds, arrays))):
+    held, parts = dict(zip(rounds, arrays)), {}
+    for k in start_order(axis, rounds):
+        array = held[k]
         pairs = [(i, peer_of(n, k, i)) for i in range(n)]
         parts[k] = lax.ppermute(array, axis, [(b, a) for a, b in pairs] if inward else pairs)
     return [parts[k] for k in rounds]
@@ -48,7 +56,7 @@
 
 def cross_exchange(n_tp, n_dp, arrays):
     parts = [None] * (n_tp - 1)
-    for k in reversed(range(1, n_tp)):
+    for k in start_order("tp", list(range(1, n_tp))):
         parts[k - 1] = lax.ppermute(
             arrays[k - 1], ("tp", "dp"), cross_pairs(n_tp, n_dp, k)
         )

time: 48.2 us -> 48.2 us (level)
  no operation moved by 1% of the time
where the time goes in v10:
time: 48.2 us; the launch traced here: 48.1 us
  starting transfers between devices  20.2 us (42%)
  waiting for transfers between devices  18.4 us (38%)
  Pallas kernels  6.91 us (14%)
  local copies, waits for them, and re-layouts  1.65 us (3%)
  between operations  0.85 us (2%)
    ppermute x11, waiting for transfers between devices, exchange(): lax.ppermute(array, axis, [(b, a) for a, b in pairs] if inward else pairs)  13.5 us
    ppermute x11, starting transfers between devices, exchange(): lax.ppermute(array, axis, [(b, a) for a, b in pairs] if inward else pairs)  11.2 us
    ppermute x6, starting transfers between devices, cross_exchange(): lax.ppermute(arrays[k - 1], ('tp', 'dp'), cross_pairs(n_tp, n_dp, k))  7.85 us
    ppermute x6, waiting for transfers between devices, cross_exchange(): lax.ppermute(arrays[k - 1], ('tp', 'dp'), cross_pairs(n_tp, n_dp, k))  4.95 us
    pallas_call x11, Pallas kernels, call(): pl.pallas_call(body, out_shape=[pltpu.VMEM(shape, dtype) for shape, dtype...  3.6 us
    pallas_call x2, Pallas kernels, per_device(): pl.pallas_call(functools.partial(update, layer), name='update', out_shape...  2.7 us
    unnamed x22, local copies, waits for them, and re-layouts  1.65 us
    ppermute x3, starting transfers between devices, cross_copy(): return lax.ppermute(array, 'dp', [(d, d ^ 1) for d in range(n_dp)])  1.19 us
  transfers between devices with their start and end apart: 20, of which 9 were waited for; matrix products, arithmetic and copies ran while one was open for 0% of the time, Pallas kernels for 11%

profile of v10, /device:TPU:0, one launch (start us, length us, event | category | flops | bytes accessed | tf_op | source)
XLA Modules:
  0.0 48.1 jit_solution(12433535796641692090)
XLA Ops:
  0.6 0.6 %collective-permute-start.8 = (bf16[2,512,1024]{2,1,0:T(8,128)(2,1)}, bf16[2,512,1024]{2,1,0:T(8,128)(2,1)S(1)}, u32[]{:S(2)}, u32[]{:S(2)}) collective-permute-start(bf16[2,512,1024]{2,1,0:T(8,128)(2,1)} %refs_2_.3), channel_id=1, source_target_pairs={{0,1},{1,0},{2,3},{3,2},{4,5},{5,4},{6,7},{7,6},{8,9},{9,8},{10,11... | collective-permute-start | bytes 6291464 | tf_op jit(solution)/shard_map/ppermute | solution.py:69
  1.2 2.6 %collective-permute-start = (bf16[4,1024]{1,0:T(4,128)(2,1)}, bf16[4,1024]{1,0:T(4,128)(2,1)S(1)}, u32[]{:S(2)}, u32[]{:S(2)}) collective-permute-start(bf16[4,1024]{1,0:T(4,128)(2,1)} %refs_0_.1), channel_id=1, source_target_pairs={{4,0},{0,4},{12,8},{8,12},{5,1},{1,5},{13,9},{9,13},{6,2},{2,6},{1... | collective-permute-start | bytes 24584 | tf_op jit(solution)/shard_map/ppermute | solution.py:40
  3.8 2.6 %collective-permute-start.1 = (bf16[4,1024]{1,0:T(4,128)(2,1)}, bf16[4,1024]{1,0:T(4,128)(2,1)S(1)}, u32[]{:S(2)}, u32[]{:S(2)}) collective-permute-start(bf16[4,1024]{1,0:T(4,128)(2,1)} %refs_0_.1), channel_id=1, source_target_pairs={{8,0},{12,4},{0,8},{4,12},{9,1},{13,5},{1,9},{5,13},{10,2},{14,6},... | collective-permute-start | bytes 24584 | tf_op jit(solution)/shard_map/ppermute | solution.py:40
  6.4 1.6 %copy-done = f32[2,4,4,128,128]{4,3,2,1,0:T(8,128)S(1)} copy-done((f32[2,4,4,128,128]{4,3,2,1,0:T(8,128)S(1)}, f32[2,4,4,128,128]{4,3,2,1,0:T(8,128)}, u32[]{:S(2)}) %copy-start) | copy-done | bytes 2097176
  8.3 0.6 %collective-permute-start.15 = (bf16[4,4,128,128]{3,2,1,0:T(8,128)(2,1)S(1)}, bf16[4,4,128,128]{3,2,1,0:T(8,128)(2,1)S(1)}, u32[]{:S(2)}, u32[]{:S(2)}) collective-permute-start(bf16[4,4,128,128]{3,2,1,0:T(8,128)(2,1)S(1)} %shard_map.120.refs_6_), channel_id=1, source_target_pairs={{0,1},{1,0},{2,3},{3,2},{4,5},{5,4},{6,7},{7,6},{8,9},{9,8},{10,11... | collective-permute-start | bytes 1572872 | tf_op jit(solution)/shard_map/ppermute | solution.py:69
  8.9 3.2 %collective-permute-done.2.refs_3_ = bf16[4,1024]{1,0:T(4,128)(2,1)S(1)} collective-permute-done((bf16[4,1024]{1,0:T(4,128)(2,1)}, bf16[4,1024]{1,0:T(4,128)(2,1)S(1)}, u32[]{:S(2)}, u32[]{:S(2)}) %collective-permute-start.2) | collective-permute-done | bytes 8224 | tf_op jit(solution)/shard_map/ppermute | solution.py:40
  12.1 0.8 %shard_map.114 = (bf16[16,1024]{1,0:T(8,128)(2,1)S(1)}, f32[8,2176]{1,0:T(8,128)S(1)}, bf16[8,2176]{1,0:T(8,128)(2,1)S(1)}, bf16[8,2176]{1,0:T(8,128)(2,1)S(1)}, bf16[8,2176]{1,0:T(8,128)(2,1)S(1)}) custom-call(bf16[4,1024]{1,0:T(4,128)(2,1)S(1)} %copy-done.9, bf16[4,1024]{1,0:T(4,128)(2,1)S(1)} %collective-permute-done.refs_1_, ...), custom_call_target="tpu_custom_call" | custom-call | tf_op jit(solution)/shard_map/pallas_call | solution.py:295
  13.0 1.7 %collective-permute-start.4 = (bf16[8,2176]{1,0:T(8,128)(2,1)S(1)}, bf16[8,2176]{1,0:T(8,128)(2,1)S(1)}, u32[]{:S(2)}, u32[]{:S(2)}) collective-permute-start(bf16[8,2176]{1,0:T(8,128)(2,1)S(1)} %get-tuple-element.24), channel_id=1, source_target_pairs={{0,2},{1,3},{2,0},{3,1},{4,6},{5,7},{6,4},{7,5},{8,10},{9,11},{10,... | collective-permute-start | bytes 104456 | tf_op jit(solution)/shard_map/ppermute | solution.py:40
  14.7 0.8 %collective-permute-start.5 = (bf16[8,2176]{1,0:T(8,128)(2,1)S(1)}, bf16[8,2176]{1,0:T(8,128)(2,1)S(1)}, u32[]{:S(2)}, u32[]{:S(2)}) collective-permute-start(bf16[8,2176]{1,0:T(8,128)(2,1)S(1)} %get-tuple-element.25), channel_id=1, source_target_pairs={{0,3},{1,2},{2,1},{3,0},{4,7},{5,6},{6,5},{7,4},{8,11},{9,10},{10,... | collective-permute-start | bytes 104456 | tf_op jit(solution)/shard_map/ppermute | solution.py:40
  15.5 1.4 %collective-permute-done.4.refs_2_ = bf16[8,2176]{1,0:T(8,128)(2,1)S(1)} collective-permute-done((bf16[8,2176]{1,0:T(8,128)(2,1)S(1)}, bf16[8,2176]{1,0:T(8,128)(2,1)S(1)}, u32[]{:S(2)}, u32[]{:S(2)}) %collective-permute-start.4) | collective-permute-done | bytes 34848 | tf_op jit(solution)/shard_map/ppermute | solution.py:40
  16.9 1.4 %collective-permute-done.5.refs_3_ = bf16[8,2176]{1,0:T(8,128)(2,1)S(1)} collective-permute-done((bf16[8,2176]{1,0:T(8,128)(2,1)S(1)}, bf16[8,2176]{1,0:T(8,128)(2,1)S(1)}, u32[]{:S(2)}, u32[]{:S(2)}) %collective-permute-start.5) | collective-permute-done | bytes 34848 | tf_op jit(solution)/shard_map/ppermute | solution.py:40
  18.3 0.4 shard_map.116
  18.8 0.6 %collective-permute-start.7 = (bf16[8,512]{1,0:T(8,128)(2,1)S(1)}, bf16[8,512]{1,0:T(8,128)(2,1)S(1)}, u32[]{:S(2)}, u32[]{:S(2)}) collective-permute-start(bf16[8,512]{1,0:T(8,128)(2,1)S(1)} %get-tuple-element.26.refs_0_), channel_id=1, source_target_pairs={{3,0},{2,1},{1,2},{0,3},{7,4},{6,5},{5,6},{4,7},{11,8},{10,9},{9,1... | collective-permute-start | bytes 24584 | tf_op jit(solution)/shard_map/ppermute | solution.py:40
  19.4 2.5 %collective-permute-done.7.refs_1_ = bf16[8,512]{1,0:T(8,128)(2,1)S(1)} collective-permute-done((bf16[8,512]{1,0:T(8,128)(2,1)S(1)}, bf16[8,512]{1,0:T(8,128)(2,1)S(1)}, u32[]{:S(2)}, u32[]{:S(2)}) %collective-permute-start.7) | collective-permute-done | bytes 8224 | tf_op jit(solution)/shard_map/ppermute | solution.py:40
  22.2 0.5 %collective-permute-start.9 = (bf16[16,1024]{1,0:T(8,128)(2,1)S(1)}, bf16[16,1024]{1,0:T(8,128)(2,1)S(1)}, u32[]{:S(2)}, u32[]{:S(2)}) collective-permute-start(bf16[16,1024]{1,0:T(8,128)(2,1)S(1)} %shard_map.118), channel_id=1, source_target_pairs={{0,5},{1,4},{2,7},{3,6},{4,1},{5,0},{6,3},{7,2},{8,13},{9,12},{10,... | collective-permute-start | bytes 98312 | tf_op jit(solution)/shard_map/ppermute | solution.py:60
  22.7 3.5 %collective-permute-start.10 = (bf16[16,1024]{1,0:T(8,128)(2,1)S(1)}, bf16[16,1024]{1,0:T(8,128)(2,1)S(1)}, u32[]{:S(2)}, u32[]{:S(2)}) collective-permute-start(bf16[16,1024]{1,0:T(8,128)(2,1)S(1)} %shard_map.118), channel_id=1, source_target_pairs={{0,9},{1,8},{2,11},{3,10},{4,13},{5,12},{6,15},{7,14},{8,1},{9,0},... | collective-permute-start | bytes 98312 | tf_op jit(solution)/shard_map/ppermute | solution.py:60
  26.4 2.1 %collective-permute-done.10.refs_2_ = bf16[16,1024]{1,0:T(8,128)(2,1)S(1)} collective-permute-done((bf16[16,1024]{1,0:T(8,128)(2,1)S(1)}, bf16[16,1024]{1,0:T(8,128)(2,1)S(1)}, u32[]{:S(2)}, u32[]{:S(2)}) %collective-permute-start.10) | collective-permute-done | bytes 32800 | tf_op jit(solution)/shard_map/ppermute | solution.py:60
  28.5 2.9 %collective-permute-done.11.refs_3_ = bf16[16,1024]{1,0:T(8,128)(2,1)S(1)} collective-permute-done((bf16[16,1024]{1,0:T(8,128)(2,1)S(1)}, bf16[16,1024]{1,0:T(8,128)(2,1)S(1)}, u32[]{:S(2)}, u32[]{:S(2)}) %collective-permute-start.11) | collective-permute-done | bytes 32800 | tf_op jit(solution)/shard_map/ppermute | solution.py:60
  31.4 0.7 %shard_map.119 = (bf16[16,1024]{1,0:T(8,128)(2,1)S(1)}, f32[8,2176]{1,0:T(8,128)S(1)}, bf16[8,2176]{1,0:T(8,128)(2,1)S(1)}, bf16[8,2176]{1,0:T(8,128)(2,1)S(1)}, bf16[8,2176]{1,0:T(8,128)(2,1)S(1)}) custom-call(f32[16,1024]{1,0:T(8,128)S(1)} %shard_map.117.refs_0_, bf16[16,1024]{1,0:T(8,128)(2,1)S(1)} %collective-permute-done.9.refs_1_, ...), custom_call_target="tpu_custom_call" | custom-call | tf_op jit(solution)/shard_map/pallas_call | solution.py:295
  32.2 0.7 %collective-permute-start.13 = (bf16[8,2176]{1,0:T(8,128)(2,1)S(1)}, bf16[8,2176]{1,0:T(8,128)(2,1)S(1)}, u32[]{:S(2)}, u32[]{:S(2)}) collective-permute-start(bf16[8,2176]{1,0:T(8,128)(2,1)S(1)} %get-tuple-element.30), channel_id=1, source_target_pairs={{0,2},{1,3},{2,0},{3,1},{4,6},{5,7},{6,4},{7,5},{8,10},{9,11},{10,... | collective-permute-start | bytes 104456 | tf_op jit(solution)/shard_map/ppermute | solution.py:40
  32.8 1.1 %collective-permute-start.14 = (bf16[8,2176]{1,0:T(8,128)(2,1)S(1)}, bf16[8,2176]{1,0:T(8,128)(2,1)S(1)}, u32[]{:S(2)}, u32[]{:S(2)}) collective-permute-start(bf16[8,2176]{1,0:T(8,128)(2,1)S(1)} %get-tuple-element.31), channel_id=1, source_target_pairs={{0,3},{1,2},{2,1},{3,0},{4,7},{5,6},{6,5},{7,4},{8,11},{9,10},{10,... | collective-permute-start | bytes 104456 | tf_op jit(solution)/shard_map/ppermute | solution.py:40
  33.9 2.4 %collective-permute-done.13.refs_2_ = bf16[8,2176]{1,0:T(8,128)(2,1)S(1)} collective-permute-done((bf16[8,2176]{1,0:T(8,128)(2,1)S(1)}, bf16[8,2176]{1,0:T(8,128)(2,1)S(1)}, u32[]{:S(2)}, u32[]{:S(2)}) %collective-permute-start.13) | collective-permute-done | bytes 34848 | tf_op jit(solution)/shard_map/ppermute | solution.py:40
  36.6 0.4 shard_map.121
  37.0 0.8 %collective-permute-start.16 = (bf16[8,512]{1,0:T(8,128)(2,1)S(1)}, bf16[8,512]{1,0:T(8,128)(2,1)S(1)}, u32[]{:S(2)}, u32[]{:S(2)}) collective-permute-start(bf16[8,512]{1,0:T(8,128)(2,1)S(1)} %get-tuple-element.32.refs_0_), channel_id=1, source_target_pairs={{3,0},{2,1},{1,2},{0,3},{7,4},{6,5},{5,6},{4,7},{11,8},{10,9},{9,1... | collective-permute-start | bytes 24584 | tf_op jit(solution)/shard_map/ppermute | solution.py:40
  37.9 2.3 %collective-permute-done.16.refs_1_ = bf16[8,512]{1,0:T(8,128)(2,1)S(1)} collective-permute-done((bf16[8,512]{1,0:T(8,128)(2,1)S(1)}, bf16[8,512]{1,0:T(8,128)(2,1)S(1)}, u32[]{:S(2)}, u32[]{:S(2)}) %collective-permute-start.16) | collective-permute-done | bytes 8224 | tf_op jit(solution)/shard_map/ppermute | solution.py:40
  40.2 0.3 shard_map.123
  40.5 1.1 %collective-permute-start.18 = (bf16[4,1024]{1,0:T(4,128)(2,1)S(1)}, bf16[4,1024]{1,0:T(4,128)(2,1)S(1)}, u32[]{:S(2)}, u32[]{:S(2)}) collective-permute-start(bf16[4,1024]{1,0:T(4,128)(2,1)S(1)} %get-tuple-element.36), channel_id=1, source_target_pairs={{0,9},{1,8},{2,11},{3,10},{4,13},{5,12},{6,15},{7,14},{8,1},{9,0},... | collective-permute-start | bytes 24584 | tf_op jit(solution)/shard_map/ppermute | solution.py:60
  41.7 2.7 %collective-permute-start.19 = (bf16[4,1024]{1,0:T(4,128)(2,1)S(1)}, bf16[4,1024]{1,0:T(4,128)(2,1)S(1)}, u32[]{:S(2)}, u32[]{:S(2)}) collective-permute-start(bf16[4,1024]{1,0:T(4,128)(2,1)S(1)} %get-tuple-element.37), channel_id=1, source_target_pairs={{0,13},{1,12},{2,15},{3,14},{4,9},{5,8},{6,11},{7,10},{8,5},{9,4},... | collective-permute-start | bytes 24584 | tf_op jit(solution)/shard_map/ppermute | solution.py:60
  44.4 1.3 %update.2.refs_0_ = f32[2,4,4,128,128]{4,3,2,1,0:T(8,128)} custom-call(f32[4,3,512]{2,1,0:T(4,128)S(1)} %get-tuple-element.39.gates, f32[2,4,4,128,128]{4,3,2,1,0:T(8,128)S(1)} %copy-done.1), custom_call_target="tpu_custom_call" | custom-call | tf_op jit(solution)/shard_map/update/pallas_call | solution.py:374
  45.7 1.4 %update.3 = f32[2,4,4,128,128]{4,3,2,1,0:T(8,128)} custom-call(f32[4,3,512]{2,1,0:T(4,128)S(1)} %get-tuple-element.38.gates, f32[2,4,4,128,128]{4,3,2,1,0:T(8,128)S(1)} %copy-done.1, f32[2,4,4,128,128]{4,3,2,1,0:T(8,128)} %update.2.refs_0_), custom_call_target="tpu_custom_call", output_to_operand_aliasing={{}: (2, {})} | custom-call | tf_op jit(solution)/shard_map/update/pallas_call | solution.py:374
  47.1 0.3 shard_map.122.own
  47.4 0.6 %close.1 = bf16[4,1024]{1,0:T(4,128)(2,1)} custom-call(f32[4,1024]{1,0:T(4,128)S(1)} %shard_map.122.own, bf16[4,1024]{1,0:T(4,128)(2,1)S(1)} %collective-permute-done.17.refs_0_, bf16[4,1024]{1,0:T(4,128)(2,1)S(1)} %collective-permute-done.18.refs_1_, bf16[4,1024]{1,0:T(4,128)(2,1)S(1)} %collective-permute-done.19.refs_2_), custom_call_target="tpu_custom_call" | custom-call | tf_op jit(solution)/shard_map/close/pallas_call | solution.py:419
  (44 shorter events, 1.2 us)
Async XLA Ops:
  0.6 21.3 %collective-permute-start.8 = (bf16[2,512,1024]{2,1,0:T(8,128)(2,1)}, bf16[2,512,1024]{2,1,0:T(8,128)(2,1)S(1)}, u32[]{:S(2)}, u32[]{:S(2)}) collective-permute-start(bf16[2,512,1024]{2,1,0:T(8,128)(2,1)} %refs_2_.3), channel_id=1, source_target_pairs={{0,1},{1,0},{2,3},{3,2},{4,5},{5,4},{6,7},{7,6},{8,9},{9,8},{10,11... | collective-permute-start | bytes 6291464 | tf_op jit(solution)/shard_map/ppermute | solution.py:69
  1.2 7.1 %collective-permute-start = (bf16[4,1024]{1,0:T(4,128)(2,1)}, bf16[4,1024]{1,0:T(4,128)(2,1)S(1)}, u32[]{:S(2)}, u32[]{:S(2)}) collective-permute-start(bf16[4,1024]{1,0:T(4,128)(2,1)} %refs_0_.1), channel_id=1, source_target_pairs={{4,0},{0,4},{12,8},{8,12},{5,1},{1,5},{13,9},{9,13},{6,2},{2,6},{1... | collective-permute-start | bytes 24584 | tf_op jit(solution)/shard_map/ppermute | solution.py:40
  3.8 5.0 %collective-permute-start.1 = (bf16[4,1024]{1,0:T(4,128)(2,1)}, bf16[4,1024]{1,0:T(4,128)(2,1)S(1)}, u32[]{:S(2)}, u32[]{:S(2)}) collective-permute-start(bf16[4,1024]{1,0:T(4,128)(2,1)} %refs_0_.1), channel_id=1, source_target_pairs={{8,0},{12,4},{0,8},{4,12},{9,1},{13,5},{1,9},{5,13},{10,2},{14,6},... | collective-permute-start | bytes 24584 | tf_op jit(solution)/shard_map/ppermute | solution.py:40
  6.4 5.7 %collective-permute-start.2 = (bf16[4,1024]{1,0:T(4,128)(2,1)}, bf16[4,1024]{1,0:T(4,128)(2,1)S(1)}, u32[]{:S(2)}, u32[]{:S(2)}) collective-permute-start(bf16[4,1024]{1,0:T(4,128)(2,1)} %refs_0_.1), channel_id=1, source_target_pairs={{12,0},{8,4},{4,8},{0,12},{13,1},{9,5},{5,9},{1,13},{14,2},{10,6},... | collective-permute-start | bytes 24584 | tf_op jit(solution)/shard_map/ppermute | solution.py:40
  6.4 1.6 %copy-start = (f32[2,4,4,128,128]{4,3,2,1,0:T(8,128)S(1)}, f32[2,4,4,128,128]{4,3,2,1,0:T(8,128)}, u32[]{:S(2)}) copy-start(f32[2,4,4,128,128]{4,3,2,1,0:T(8,128)} %state.7) | copy-start | bytes 6291460
  8.1 10.2 %collective-permute-start.6 = (bf16[4,4,128,128]{3,2,1,0:T(8,128)(2,1)S(1)}, bf16[4,4,128,128]{3,2,1,0:T(8,128)(2,1)S(1)}, u32[]{:S(2)}, u32[]{:S(2)}) collective-permute-start(bf16[4,4,128,128]{3,2,1,0:T(8,128)(2,1)S(1)} %shard_map.115.refs_6_), channel_id=1, source_target_pairs={{0,1},{1,0},{2,3},{3,2},{4,5},{5,4},{6,7},{7,6},{8,9},{9,8},{10,11... | collective-permute-start | bytes 1572872 | tf_op jit(solution)/shard_map/ppermute | solution.py:69
  8.2 3.9 %copy-start.2 = (bf16[2,1024,512]{2,1,0:T(8,128)(2,1)S(1)}, bf16[2,1024,512]{2,1,0:T(8,128)(2,1)}, u32[]{:S(2)}) copy-start(bf16[2,1024,512]{2,1,0:T(8,128)(2,1)} %refs_5_.6) | copy-start | bytes 6291460
  8.2 3.9 %copy-start.3 = (bf16[2,1024,512]{2,1,0:T(8,128)(2,1)S(1)}, bf16[2,1024,512]{2,1,0:T(8,128)(2,1)}, u32[]{:S(2)}) copy-start(bf16[2,1024,512]{2,1,0:T(8,128)(2,1)} %refs_6_.3) | copy-start | bytes 6291460
  8.2 3.9 %copy-start.4 = (bf16[2,1024,512]{2,1,0:T(8,128)(2,1)S(1)}, bf16[2,1024,512]{2,1,0:T(8,128)(2,1)}, u32[]{:S(2)}) copy-start(bf16[2,1024,512]{2,1,0:T(8,128)(2,1)} %refs_7_.3) | copy-start | bytes 6291460
  8.2 3.8 %copy-start.5 = (bf16[2,1024,512]{2,1,0:T(8,128)(2,1)S(1)}, bf16[2,1024,512]{2,1,0:T(8,128)(2,1)}, u32[]{:S(2)}) copy-start(bf16[2,1024,512]{2,1,0:T(8,128)(2,1)} %refs_8_.3) | copy-start | bytes 6291460
  8.3 3.8 %copy-start.7 = (f32[2,1024]{1,0:T(2,128)S(1)}, f32[2,1024]{1,0:T(2,128)}, u32[]{:S(2)}) copy-start(f32[2,1024]{1,0:T(2,128)} %refs_4_.4) | copy-start | bytes 24580
  8.3 3.8 %copy-start.9 = (bf16[4,1024]{1,0:T(4,128)(2,1)S(1)}, bf16[4,1024]{1,0:T(4,128)(2,1)}, u32[]{:S(2)}) copy-start(bf16[4,1024]{1,0:T(4,128)(2,1)} %refs_0_.1) | copy-start | bytes 24580
  8.3 25.6 %collective-permute-start.15 = (bf16[4,4,128,128]{3,2,1,0:T(8,128)(2,1)S(1)}, bf16[4,4,128,128]{3,2,1,0:T(8,128)(2,1)S(1)}, u32[]{:S(2)}, u32[]{:S(2)}) collective-permute-start(bf16[4,4,128,128]{3,2,1,0:T(8,128)(2,1)S(1)} %shard_map.120.refs_6_), channel_id=1, source_target_pairs={{0,1},{1,0},{2,3},{3,2},{4,5},{5,4},{6,7},{7,6},{8,9},{9,8},{10,11... | collective-permute-start | bytes 1572872 | tf_op jit(solution)/shard_map/ppermute | solution.py:69
  12.1 6.2 %copy-start.8 = (f32[2,512]{1,0:T(2,128)S(1)}, f32[2,512]{1,0:T(2,128)}, u32[]{:S(2)}) copy-start(f32[2,512]{1,0:T(2,128)} %refs_4_.5) | copy-start | bytes 12292
  12.1 6.2 %copy-start.10 = (f32[2,128]{1,0:T(2,128)S(1)}, f32[2,128]{1,0:T(2,128)}, u32[]{:S(2)}) copy-start(f32[2,128]{1,0:T(2,128)} %refs_5_.7) | copy-start | bytes 3076
  12.9 13.3 %copy-start.6 = (bf16[2,512,1024]{2,1,0:T(8,128)(2,1)S(1)}, bf16[2,512,1024]{2,1,0:T(8,128)(2,1)}, u32[]{:S(2)}) copy-start(bf16[2,512,1024]{2,1,0:T(8,128)(2,1)} %refs_2_.3) | copy-start | bytes 6291460
  12.9 1.8 %collective-permute-start.3 = (bf16[8,2176]{1,0:T(8,128)(2,1)S(1)}, bf16[8,2176]{1,0:T(8,128)(2,1)S(1)}, u32[]{:S(2)}, u32[]{:S(2)}) collective-permute-start(bf16[8,2176]{1,0:T(8,128)(2,1)S(1)} %get-tuple-element.23), channel_id=1, source_target_pairs={{0,1},{1,0},{2,3},{3,2},{4,5},{5,4},{6,7},{7,6},{8,9},{9,8},{10,11... | collective-permute-start | bytes 104456 | tf_op jit(solution)/shard_map/ppermute | solution.py:40
  13.0 4.0 %collective-permute-start.4 = (bf16[8,2176]{1,0:T(8,128)(2,1)S(1)}, bf16[8,2176]{1,0:T(8,128)(2,1)S(1)}, u32[]{:S(2)}, u32[]{:S(2)}) collective-permute-start(bf16[8,2176]{1,0:T(8,128)(2,1)S(1)} %get-tuple-element.24), channel_id=1, source_target_pairs={{0,2},{1,3},{2,0},{3,1},{4,6},{5,7},{6,4},{7,5},{8,10},{9,11},{10,... | collective-permute-start | bytes 104456 | tf_op jit(solution)/shard_map/ppermute | solution.py:40
  14.7 3.6 %collective-permute-start.5 = (bf16[8,2176]{1,0:T(8,128)(2,1)S(1)}, bf16[8,2176]{1,0:T(8,128)(2,1)S(1)}, u32[]{:S(2)}, u32[]{:S(2)}) collective-permute-start(bf16[8,2176]{1,0:T(8,128)(2,1)S(1)} %get-tuple-element.25), channel_id=1, source_target_pairs={{0,3},{1,2},{2,1},{3,0},{4,7},{5,6},{6,5},{7,4},{8,11},{9,10},{10,... | collective-permute-start | bytes 104456 | tf_op jit(solution)/shard_map/ppermute | solution.py:40
  18.8 3.1 %collective-permute-start.7 = (bf16[8,512]{1,0:T(8,128)(2,1)S(1)}, bf16[8,512]{1,0:T(8,128)(2,1)S(1)}, u32[]{:S(2)}, u32[]{:S(2)}) collective-permute-start(bf16[8,512]{1,0:T(8,128)(2,1)S(1)} %get-tuple-element.26.refs_0_), channel_id=1, source_target_pairs={{3,0},{2,1},{1,2},{0,3},{7,4},{6,5},{5,6},{4,7},{11,8},{10,9},{9,1... | collective-permute-start | bytes 24584 | tf_op jit(solution)/shard_map/ppermute | solution.py:40
  22.2 4.3 %collective-permute-start.9 = (bf16[16,1024]{1,0:T(8,128)(2,1)S(1)}, bf16[16,1024]{1,0:T(8,128)(2,1)S(1)}, u32[]{:S(2)}, u32[]{:S(2)}) collective-permute-start(bf16[16,1024]{1,0:T(8,128)(2,1)S(1)} %shard_map.118), channel_id=1, source_target_pairs={{0,5},{1,4},{2,7},{3,6},{4,1},{5,0},{6,3},{7,2},{8,13},{9,12},{10,... | collective-permute-start | bytes 98312 | tf_op jit(solution)/shard_map/ppermute | solution.py:60
  22.7 5.8 %collective-permute-start.10 = (bf16[16,1024]{1,0:T(8,128)(2,1)S(1)}, bf16[16,1024]{1,0:T(8,128)(2,1)S(1)}, u32[]{:S(2)}, u32[]{:S(2)}) collective-permute-start(bf16[16,1024]{1,0:T(8,128)(2,1)S(1)} %shard_map.118), channel_id=1, source_target_pairs={{0,9},{1,8},{2,11},{3,10},{4,13},{5,12},{6,15},{7,14},{8,1},{9,0},... | collective-permute-start | bytes 98312 | tf_op jit(solution)/shard_map/ppermute | solution.py:60
  26.2 5.2 %collective-permute-start.11 = (bf16[16,1024]{1,0:T(8,128)(2,1)S(1)}, bf16[16,1024]{1,0:T(8,128)(2,1)S(1)}, u32[]{:S(2)}, u32[]{:S(2)}) collective-permute-start(bf16[16,1024]{1,0:T(8,128)(2,1)S(1)} %shard_map.118), channel_id=1, source_target_pairs={{0,13},{1,12},{2,15},{3,14},{4,9},{5,8},{6,11},{7,10},{8,5},{9,4},... | collective-permute-start | bytes 98312 | tf_op jit(solution)/shard_map/ppermute | solution.py:60
  32.0 12.3 %copy-start.1 = (f32[2,4,4,128,128]{4,3,2,1,0:T(8,128)S(1)}, f32[2,4,4,128,128]{4,3,2,1,0:T(8,128)}, u32[]{:S(2)}) copy-start(f32[2,4,4,128,128]{4,3,2,1,0:T(8,128)} %state.7) | copy-start | bytes 6291460
  32.0 1.9 %collective-permute-start.12 = (bf16[8,2176]{1,0:T(8,128)(2,1)S(1)}, bf16[8,2176]{1,0:T(8,128)(2,1)S(1)}, u32[]{:S(2)}, u32[]{:S(2)}) collective-permute-start(bf16[8,2176]{1,0:T(8,128)(2,1)S(1)} %get-tuple-element.29), channel_id=1, source_target_pairs={{0,1},{1,0},{2,3},{3,2},{4,5},{5,4},{6,7},{7,6},{8,9},{9,8},{10,11... | collective-permute-start | bytes 104456 | tf_op jit(solution)/shard_map/ppermute | solution.py:40
  32.2 4.2 %collective-permute-start.13 = (bf16[8,2176]{1,0:T(8,128)(2,1)S(1)}, bf16[8,2176]{1,0:T(8,128)(2,1)S(1)}, u32[]{:S(2)}, u32[]{:S(2)}) collective-permute-start(bf16[8,2176]{1,0:T(8,128)(2,1)S(1)} %get-tuple-element.30), channel_id=1, source_target_pairs={{0,2},{1,3},{2,0},{3,1},{4,6},{5,7},{6,4},{7,5},{8,10},{9,11},{10,... | collective-permute-start | bytes 104456 | tf_op jit(solution)/shard_map/ppermute | solution.py:40
  32.8 3.7 %collective-permute-start.14 = (bf16[8,2176]{1,0:T(8,128)(2,1)S(1)}, bf16[8,2176]{1,0:T(8,128)(2,1)S(1)}, u32[]{:S(2)}, u32[]{:S(2)}) collective-permute-start(bf16[8,2176]{1,0:T(8,128)(2,1)S(1)} %get-tuple-element.31), channel_id=1, source_target_pairs={{0,3},{1,2},{2,1},{3,0},{4,7},{5,6},{6,5},{7,4},{8,11},{9,10},{10,... | collective-permute-start | bytes 104456 | tf_op jit(solution)/shard_map/ppermute | solution.py:40
  37.0 3.1 %collective-permute-start.16 = (bf16[8,512]{1,0:T(8,128)(2,1)S(1)}, bf16[8,512]{1,0:T(8,128)(2,1)S(1)}, u32[]{:S(2)}, u32[]{:S(2)}) collective-permute-start(bf16[8,512]{1,0:T(8,128)(2,1)S(1)} %get-tuple-element.32.refs_0_), channel_id=1, source_target_pairs={{3,0},{2,1},{1,2},{0,3},{7,4},{6,5},{5,6},{4,7},{11,8},{10,9},{9,1... | collective-permute-start | bytes 24584 | tf_op jit(solution)/shard_map/ppermute | solution.py:40
  40.5 6.9 %collective-permute-start.17 = (bf16[4,1024]{1,0:T(4,128)(2,1)S(1)}, bf16[4,1024]{1,0:T(4,128)(2,1)S(1)}, u32[]{:S(2)}, u32[]{:S(2)}) collective-permute-start(bf16[4,1024]{1,0:T(4,128)(2,1)S(1)} %get-tuple-element.35), channel_id=1, source_target_pairs={{0,5},{1,4},{2,7},{3,6},{4,1},{5,0},{6,3},{7,2},{8,13},{9,12},{10,... | collective-permute-start | bytes 24584 | tf_op jit(solution)/shard_map/ppermute | solution.py:60
  40.5 6.9 %collective-permute-start.18 = (bf16[4,1024]{1,0:T(4,128)(2,1)S(1)}, bf16[4,1024]{1,0:T(4,128)(2,1)S(1)}, u32[]{:S(2)}, u32[]{:S(2)}) collective-permute-start(bf16[4,1024]{1,0:T(4,128)(2,1)S(1)} %get-tuple-element.36), channel_id=1, source_target_pairs={{0,9},{1,8},{2,11},{3,10},{4,13},{5,12},{6,15},{7,14},{8,1},{9,0},... | collective-permute-start | bytes 24584 | tf_op jit(solution)/shard_map/ppermute | solution.py:60
  41.7 5.8 %collective-permute-start.19 = (bf16[4,1024]{1,0:T(4,128)(2,1)S(1)}, bf16[4,1024]{1,0:T(4,128)(2,1)S(1)}, u32[]{:S(2)}, u32[]{:S(2)}) collective-permute-start(bf16[4,1024]{1,0:T(4,128)(2,1)S(1)} %get-tuple-element.37), channel_id=1, source_target_pairs={{0,13},{1,12},{2,15},{3,14},{4,9},{5,8},{6,11},{7,10},{8,5},{9,4},... | collective-permute-start | bytes 24584 | tf_op jit(solution)/shard_map/ppermute | solution.py:60

commit v11 on v10

--- a/solution.py
+++ b/solution.py
@@ -24,17 +24,17 @@
     return list(range(3, n_dp, 2)) if core_flip(n_dp) else list(range(1, n_dp))
 
 
-def start_order(axis, rounds):
+def start_order(tag, rounds):
     order = list(reversed(rounds))
-    if axis == "tp" and len(order) > 2:
+    if tag in "ade" and len(order) > 2:
         order[:2] = order[1], order[0]
     return order
 
 
-def exchange(axis, n, arrays, inward=False, rounds=None):
+def exchange(tag, axis, n, arrays, inward=False, rounds=None):
     rounds = rounds or list(range(1, n))
     held, parts = dict(zip(rounds, arrays)), {}
-    for k in start_order(axis, rounds):
+    for k in start_order(tag, rounds):
         array = held[k]
         pairs = [(i, peer_of(n, k, i)) for i in range(n)]
         parts[k] = lax.ppermute(array, axis, [(b, a) for a, b in pairs] if inward else pairs)
@@ -54,9 +54,9 @@
     ]
 
 
-def cross_exchange(n_tp, n_dp, arrays):
+def cross_exchange(tag, n_tp, n_dp, arrays):
     parts = [None] * (n_tp - 1)
-    for k in start_order("tp", list(range(1, n_tp))):
+    for k in start_order(tag, list(range(1, n_tp))):
         parts[k - 1] = lax.ppermute(
             arrays[k - 1], ("tp", "dp"), cross_pairs(n_tp, n_dp, k)
         )
@@ -69,11 +69,11 @@
     return lax.ppermute(array, "dp", [(d, d ^ 1) for d in range(n_dp)])
 
 
-def gather(axis, n, array, rounds=None):
+def gather(tag, axis, n, array, rounds=None):
     rounds = list(range(1, n)) if rounds is None else rounds
     if not rounds:
         return [array]
-    return [array] + exchange(axis, n, [array] * len(rounds), True, rounds)
+    return [array] + exchange(tag, axis, n, [array] * len(rounds), True, rounds)
 
 
 def split(array):
@@ -330,7 +330,7 @@
         [((total, total), BF16)] * 2,
         flops=20_000_000_000,
     )
-    parts = gather("tp", n_tp, tokens)
+    parts = gather("a", "tp", n_tp, tokens)
     flip = core_flip(n_dp)
     group, n_chip = flip + 1, n_dp // (flip + 1)
     crossed = cross_copy(n_dp, w_out)
@@ -361,7 +361,7 @@
                 [VMEM] * (n_tp + 1) + specs,
                 outs,
             )
-        parts = exchange("dp", n_dp, sent)
+        parts = exchange("eb"[layer == 0], "dp", n_dp, sent)
         normed, gates = call(
             functools.partial(recur, n_dp, layer, features, group),
             (own, *parts, lower_bound, head_gain, *states[layer]),
@@ -369,7 +369,7 @@
             [((group * seqs, width), BF16), ((seqs, 3, width), F32)],
             [((4 * group * seqs, group * seqs * hd), F32)],
         )
-        read = gather("dp", n_dp, normed, chip_rounds(n_dp))
+        read = gather("fc"[layer == 0], "dp", n_dp, normed, chip_rounds(n_dp))
         slots = [((total, width), F32)]
         new_state = pl.pallas_call(
             functools.partial(update, layer),
@@ -392,7 +392,7 @@
                 [((total, local), BF16)],
                 slots,
             )
-            parts = cross_exchange(n_tp, n_dp, [sent] * (n_tp - 1))
+            parts = cross_exchange("d", n_tp, n_dp, [sent] * (n_tp - 1))
             (held,) = call(
                 functools.partial(own_next, n_chip, group, layer),
                 (*read, w_out, base),
@@ -408,7 +408,7 @@
                 [((rows, local), BF16)] * (n_tp - 1),
                 slots,
             )
-            parts = cross_exchange(n_tp, n_dp, sent)
+            parts = cross_exchange("g", n_tp, n_dp, sent)
             (own,) = call(
                 functools.partial(own_last, n_chip, group, layer),
                 (*read, w_out, base, order_out),

time: 48.2 us -> 48.2 us (level)
  no operation moved by 1% of the time
where the time goes in v11:
time: 48.2 us; the launch traced here: 48.1 us
  starting transfers between devices  20.2 us (42%)
  waiting for transfers between devices  18.4 us (38%)
  Pallas kernels  6.91 us (14%)
  local copies, waits for them, and re-layouts  1.65 us (3%)
  between operations  0.85 us (2%)
    ppermute x11, waiting for transfers between devices, exchange(): lax.ppermute(array, axis, [(b, a) for a, b in pairs] if inward else pairs)  13.5 us
    ppermute x11, starting transfers between devices, exchange(): lax.ppermute(array, axis, [(b, a) for a, b in pairs] if inward else pairs)  11.2 us
    ppermute x6, starting transfers between devices, cross_exchange(): lax.ppermute(arrays[k - 1], ('tp', 'dp'), cross_pairs(n_tp, n_dp, k))  7.85 us
    ppermute x6, waiting for transfers between devices, cross_exchange(): lax.ppermute(arrays[k - 1], ('tp', 'dp'), cross_pairs(n_tp, n_dp, k))  4.95 us
    pallas_call x11, Pallas kernels, call(): pl.pallas_call(body, out_shape=[pltpu.VMEM(shape, dtype) for shape, dtype...  3.6 us
    pallas_call x2, Pallas kernels, per_device(): pl.pallas_call(functools.partial(update, layer), name='update', out_shape...  2.7 us
    unnamed x22, local copies, waits for them, and re-layouts  1.65 us
    ppermute x3, starting transfers between devices, cross_copy(): return lax.ppermute(array, 'dp', [(d, d ^ 1) for d in range(n_dp)])  1.19 us
  transfers between devices with their start and end apart: 20, of which 9 were waited for; matrix products, arithmetic and copies ran while one was open for 0% of the time, Pallas kernels for 11%

profile of v11, /device:TPU:0, one launch (start us, length us, event | category | flops | bytes accessed | tf_op | source)
XLA Modules:
  0.0 48.1 jit_solution(12433535796641692090)
XLA Ops:
  0.6 0.6 %collective-permute-start.8 = (bf16[2,512,1024]{2,1,0:T(8,128)(2,1)}, bf16[2,512,1024]{2,1,0:T(8,128)(2,1)S(1)}, u32[]{:S(2)}, u32[]{:S(2)}) collective-permute-start(bf16[2,512,1024]{2,1,0:T(8,128)(2,1)} %refs_2_.3), channel_id=1, source_target_pairs={{0,1},{1,0},{2,3},{3,2},{4,5},{5,4},{6,7},{7,6},{8,9},{9,8},{10,11... | collective-permute-start | bytes 6291464 | tf_op jit(solution)/shard_map/ppermute | solution.py:69
  1.2 2.6 %collective-permute-start = (bf16[4,1024]{1,0:T(4,128)(2,1)}, bf16[4,1024]{1,0:T(4,128)(2,1)S(1)}, u32[]{:S(2)}, u32[]{:S(2)}) collective-permute-start(bf16[4,1024]{1,0:T(4,128)(2,1)} %refs_0_.1), channel_id=1, source_target_pairs={{4,0},{0,4},{12,8},{8,12},{5,1},{1,5},{13,9},{9,13},{6,2},{2,6},{1... | collective-permute-start | bytes 24584 | tf_op jit(solution)/shard_map/ppermute | solution.py:40
  3.8 2.6 %collective-permute-start.1 = (bf16[4,1024]{1,0:T(4,128)(2,1)}, bf16[4,1024]{1,0:T(4,128)(2,1)S(1)}, u32[]{:S(2)}, u32[]{:S(2)}) collective-permute-start(bf16[4,1024]{1,0:T(4,128)(2,1)} %refs_0_.1), channel_id=1, source_target_pairs={{8,0},{12,4},{0,8},{4,12},{9,1},{13,5},{1,9},{5,13},{10,2},{14,6},... | collective-permute-start | bytes 24584 | tf_op jit(solution)/shard_map/ppermute | solution.py:40
  6.4 1.6 %copy-done = f32[2,4,4,128,128]{4,3,2,1,0:T(8,128)S(1)} copy-done((f32[2,4,4,128,128]{4,3,2,1,0:T(8,128)S(1)}, f32[2,4,4,128,128]{4,3,2,1,0:T(8,128)}, u32[]{:S(2)}) %copy-start) | copy-done | bytes 2097176
  8.3 0.6 %collective-permute-start.15 = (bf16[4,4,128,128]{3,2,1,0:T(8,128)(2,1)S(1)}, bf16[4,4,128,128]{3,2,1,0:T(8,128)(2,1)S(1)}, u32[]{:S(2)}, u32[]{:S(2)}) collective-permute-start(bf16[4,4,128,128]{3,2,1,0:T(8,128)(2,1)S(1)} %shard_map.120.refs_6_), channel_id=1, source_target_pairs={{0,1},{1,0},{2,3},{3,2},{4,5},{5,4},{6,7},{7,6},{8,9},{9,8},{10,11... | collective-permute-start | bytes 1572872 | tf_op jit(solution)/shard_map/ppermute | solution.py:69
  8.9 3.2 %collective-permute-done.2.refs_3_ = bf16[4,1024]{1,0:T(4,128)(2,1)S(1)} collective-permute-done((bf16[4,1024]{1,0:T(4,128)(2,1)}, bf16[4,1024]{1,0:T(4,128)(2,1)S(1)}, u32[]{:S(2)}, u32[]{:S(2)}) %collective-permute-start.2) | collective-permute-done | bytes 8224 | tf_op jit(solution)/shard_map/ppermute | solution.py:40
  12.1 0.8 %shard_map.114 = (bf16[16,1024]{1,0:T(8,128)(2,1)S(1)}, f32[8,2176]{1,0:T(8,128)S(1)}, bf16[8,2176]{1,0:T(8,128)(2,1)S(1)}, bf16[8,2176]{1,0:T(8,128)(2,1)S(1)}, bf16[8,2176]{1,0:T(8,128)(2,1)S(1)}) custom-call(bf16[4,1024]{1,0:T(4,128)(2,1)S(1)} %copy-done.9, bf16[4,1024]{1,0:T(4,128)(2,1)S(1)} %collective-permute-done.refs_1_, ...), custom_call_target="tpu_custom_call" | custom-call | tf_op jit(solution)/shard_map/pallas_call | solution.py:295
  13.0 1.7 %collective-permute-start.4 = (bf16[8,2176]{1,0:T(8,128)(2,1)S(1)}, bf16[8,2176]{1,0:T(8,128)(2,1)S(1)}, u32[]{:S(2)}, u32[]{:S(2)}) collective-permute-start(bf16[8,2176]{1,0:T(8,128)(2,1)S(1)} %get-tuple-element.24), channel_id=1, source_target_pairs={{0,2},{1,3},{2,0},{3,1},{4,6},{5,7},{6,4},{7,5},{8,10},{9,11},{10,... | collective-permute-start | bytes 104456 | tf_op jit(solution)/shard_map/ppermute | solution.py:40
  14.7 0.8 %collective-permute-start.5 = (bf16[8,2176]{1,0:T(8,128)(2,1)S(1)}, bf16[8,2176]{1,0:T(8,128)(2,1)S(1)}, u32[]{:S(2)}, u32[]{:S(2)}) collective-permute-start(bf16[8,2176]{1,0:T(8,128)(2,1)S(1)} %get-tuple-element.25), channel_id=1, source_target_pairs={{0,3},{1,2},{2,1},{3,0},{4,7},{5,6},{6,5},{7,4},{8,11},{9,10},{10,... | collective-permute-start | bytes 104456 | tf_op jit(solution)/shard_map/ppermute | solution.py:40
  15.5 1.4 %collective-permute-done.4.refs_2_ = bf16[8,2176]{1,0:T(8,128)(2,1)S(1)} collective-permute-done((bf16[8,2176]{1,0:T(8,128)(2,1)S(1)}, bf16[8,2176]{1,0:T(8,128)(2,1)S(1)}, u32[]{:S(2)}, u32[]{:S(2)}) %collective-permute-start.4) | collective-permute-done | bytes 34848 | tf_op jit(solution)/shard_map/ppermute | solution.py:40
  16.9 1.4 %collective-permute-done.5.refs_3_ = bf16[8,2176]{1,0:T(8,128)(2,1)S(1)} collective-permute-done((bf16[8,2176]{1,0:T(8,128)(2,1)S(1)}, bf16[8,2176]{1,0:T(8,128)(2,1)S(1)}, u32[]{:S(2)}, u32[]{:S(2)}) %collective-permute-start.5) | collective-permute-done | bytes 34848 | tf_op jit(solution)/shard_map/ppermute | solution.py:40
  18.3 0.4 shard_map.116
  18.8 0.6 %collective-permute-start.7 = (bf16[8,512]{1,0:T(8,128)(2,1)S(1)}, bf16[8,512]{1,0:T(8,128)(2,1)S(1)}, u32[]{:S(2)}, u32[]{:S(2)}) collective-permute-start(bf16[8,512]{1,0:T(8,128)(2,1)S(1)} %get-tuple-element.26.refs_0_), channel_id=1, source_target_pairs={{3,0},{2,1},{1,2},{0,3},{7,4},{6,5},{5,6},{4,7},{11,8},{10,9},{9,1... | collective-permute-start | bytes 24584 | tf_op jit(solution)/shard_map/ppermute | solution.py:40
  19.4 2.5 %collective-permute-done.7.refs_1_ = bf16[8,512]{1,0:T(8,128)(2,1)S(1)} collective-permute-done((bf16[8,512]{1,0:T(8,128)(2,1)S(1)}, bf16[8,512]{1,0:T(8,128)(2,1)S(1)}, u32[]{:S(2)}, u32[]{:S(2)}) %collective-permute-start.7) | collective-permute-done | bytes 8224 | tf_op jit(solution)/shard_map/ppermute | solution.py:40
  22.2 0.5 %collective-permute-start.9 = (bf16[16,1024]{1,0:T(8,128)(2,1)S(1)}, bf16[16,1024]{1,0:T(8,128)(2,1)S(1)}, u32[]{:S(2)}, u32[]{:S(2)}) collective-permute-start(bf16[16,1024]{1,0:T(8,128)(2,1)S(1)} %shard_map.118), channel_id=1, source_target_pairs={{0,5},{1,4},{2,7},{3,6},{4,1},{5,0},{6,3},{7,2},{8,13},{9,12},{10,... | collective-permute-start | bytes 98312 | tf_op jit(solution)/shard_map/ppermute | solution.py:60
  22.7 3.5 %collective-permute-start.10 = (bf16[16,1024]{1,0:T(8,128)(2,1)S(1)}, bf16[16,1024]{1,0:T(8,128)(2,1)S(1)}, u32[]{:S(2)}, u32[]{:S(2)}) collective-permute-start(bf16[16,1024]{1,0:T(8,128)(2,1)S(1)} %shard_map.118), channel_id=1, source_target_pairs={{0,9},{1,8},{2,11},{3,10},{4,13},{5,12},{6,15},{7,14},{8,1},{9,0},... | collective-permute-start | bytes 98312 | tf_op jit(solution)/shard_map/ppermute | solution.py:60
  26.4 2.1 %collective-permute-done.10.refs_2_ = bf16[16,1024]{1,0:T(8,128)(2,1)S(1)} collective-permute-done((bf16[16,1024]{1,0:T(8,128)(2,1)S(1)}, bf16[16,1024]{1,0:T(8,128)(2,1)S(1)}, u32[]{:S(2)}, u32[]{:S(2)}) %collective-permute-start.10) | collective-permute-done | bytes 32800 | tf_op jit(solution)/shard_map/ppermute | solution.py:60
  28.5 2.9 %collective-permute-done.11.refs_3_ = bf16[16,1024]{1,0:T(8,128)(2,1)S(1)} collective-permute-done((bf16[16,1024]{1,0:T(8,128)(2,1)S(1)}, bf16[16,1024]{1,0:T(8,128)(2,1)S(1)}, u32[]{:S(2)}, u32[]{:S(2)}) %collective-permute-start.11) | collective-permute-done | bytes 32800 | tf_op jit(solution)/shard_map/ppermute | solution.py:60
  31.4 0.7 %shard_map.119 = (bf16[16,1024]{1,0:T(8,128)(2,1)S(1)}, f32[8,2176]{1,0:T(8,128)S(1)}, bf16[8,2176]{1,0:T(8,128)(2,1)S(1)}, bf16[8,2176]{1,0:T(8,128)(2,1)S(1)}, bf16[8,2176]{1,0:T(8,128)(2,1)S(1)}) custom-call(f32[16,1024]{1,0:T(8,128)S(1)} %shard_map.117.refs_0_, bf16[16,1024]{1,0:T(8,128)(2,1)S(1)} %collective-permute-done.9.refs_1_, ...), custom_call_target="tpu_custom_call" | custom-call | tf_op jit(solution)/shard_map/pallas_call | solution.py:295
  32.2 0.7 %collective-permute-start.13 = (bf16[8,2176]{1,0:T(8,128)(2,1)S(1)}, bf16[8,2176]{1,0:T(8,128)(2,1)S(1)}, u32[]{:S(2)}, u32[]{:S(2)}) collective-permute-start(bf16[8,2176]{1,0:T(8,128)(2,1)S(1)} %get-tuple-element.30), channel_id=1, source_target_pairs={{0,2},{1,3},{2,0},{3,1},{4,6},{5,7},{6,4},{7,5},{8,10},{9,11},{10,... | collective-permute-start | bytes 104456 | tf_op jit(solution)/shard_map/ppermute | solution.py:40
  32.8 1.1 %collective-permute-start.14 = (bf16[8,2176]{1,0:T(8,128)(2,1)S(1)}, bf16[8,2176]{1,0:T(8,128)(2,1)S(1)}, u32[]{:S(2)}, u32[]{:S(2)}) collective-permute-start(bf16[8,2176]{1,0:T(8,128)(2,1)S(1)} %get-tuple-element.31), channel_id=1, source_target_pairs={{0,3},{1,2},{2,1},{3,0},{4,7},{5,6},{6,5},{7,4},{8,11},{9,10},{10,... | collective-permute-start | bytes 104456 | tf_op jit(solution)/shard_map/ppermute | solution.py:40
  33.9 2.4 %collective-permute-done.13.refs_2_ = bf16[8,2176]{1,0:T(8,128)(2,1)S(1)} collective-permute-done((bf16[8,2176]{1,0:T(8,128)(2,1)S(1)}, bf16[8,2176]{1,0:T(8,128)(2,1)S(1)}, u32[]{:S(2)}, u32[]{:S(2)}) %collective-permute-start.13) | collective-permute-done | bytes 34848 | tf_op jit(solution)/shard_map/ppermute | solution.py:40
  36.6 0.4 shard_map.121
  37.0 0.8 %collective-permute-start.16 = (bf16[8,512]{1,0:T(8,128)(2,1)S(1)}, bf16[8,512]{1,0:T(8,128)(2,1)S(1)}, u32[]{:S(2)}, u32[]{:S(2)}) collective-permute-start(bf16[8,512]{1,0:T(8,128)(2,1)S(1)} %get-tuple-element.32.refs_0_), channel_id=1, source_target_pairs={{3,0},{2,1},{1,2},{0,3},{7,4},{6,5},{5,6},{4,7},{11,8},{10,9},{9,1... | collective-permute-start | bytes 24584 | tf_op jit(solution)/shard_map/ppermute | solution.py:40
  37.9 2.3 %collective-permute-done.16.refs_1_ = bf16[8,512]{1,0:T(8,128)(2,1)S(1)} collective-permute-done((bf16[8,512]{1,0:T(8,128)(2,1)S(1)}, bf16[8,512]{1,0:T(8,128)(2,1)S(1)}, u32[]{:S(2)}, u32[]{:S(2)}) %collective-permute-start.16) | collective-permute-done | bytes 8224 | tf_op jit(solution)/shard_map/ppermute | solution.py:40
  40.2 0.3 shard_map.123
  40.5 1.1 %collective-permute-start.18 = (bf16[4,1024]{1,0:T(4,128)(2,1)S(1)}, bf16[4,1024]{1,0:T(4,128)(2,1)S(1)}, u32[]{:S(2)}, u32[]{:S(2)}) collective-permute-start(bf16[4,1024]{1,0:T(4,128)(2,1)S(1)} %get-tuple-element.36), channel_id=1, source_target_pairs={{0,9},{1,8},{2,11},{3,10},{4,13},{5,12},{6,15},{7,14},{8,1},{9,0},... | collective-permute-start | bytes 24584 | tf_op jit(solution)/shard_map/ppermute | solution.py:60
  41.7 2.7 %collective-permute-start.19 = (bf16[4,1024]{1,0:T(4,128)(2,1)S(1)}, bf16[4,1024]{1,0:T(4,128)(2,1)S(1)}, u32[]{:S(2)}, u32[]{:S(2)}) collective-permute-start(bf16[4,1024]{1,0:T(4,128)(2,1)S(1)} %get-tuple-element.37), channel_id=1, source_target_pairs={{0,13},{1,12},{2,15},{3,14},{4,9},{5,8},{6,11},{7,10},{8,5},{9,4},... | collective-permute-start | bytes 24584 | tf_op jit(solution)/shard_map/ppermute | solution.py:60
  44.4 1.3 %update.2.refs_0_ = f32[2,4,4,128,128]{4,3,2,1,0:T(8,128)} custom-call(f32[4,3,512]{2,1,0:T(4,128)S(1)} %get-tuple-element.39.gates, f32[2,4,4,128,128]{4,3,2,1,0:T(8,128)S(1)} %copy-done.1), custom_call_target="tpu_custom_call" | custom-call | tf_op jit(solution)/shard_map/update/pallas_call | solution.py:374
  45.7 1.4 %update.3 = f32[2,4,4,128,128]{4,3,2,1,0:T(8,128)} custom-call(f32[4,3,512]{2,1,0:T(4,128)S(1)} %get-tuple-element.38.gates, f32[2,4,4,128,128]{4,3,2,1,0:T(8,128)S(1)} %copy-done.1, f32[2,4,4,128,128]{4,3,2,1,0:T(8,128)} %update.2.refs_0_), custom_call_target="tpu_custom_call", output_to_operand_aliasing={{}: (2, {})} | custom-call | tf_op jit(solution)/shard_map/update/pallas_call | solution.py:374
  47.1 0.3 shard_map.122.own
  47.4 0.6 %close.1 = bf16[4,1024]{1,0:T(4,128)(2,1)} custom-call(f32[4,1024]{1,0:T(4,128)S(1)} %shard_map.122.own, bf16[4,1024]{1,0:T(4,128)(2,1)S(1)} %collective-permute-done.17.refs_0_, bf16[4,1024]{1,0:T(4,128)(2,1)S(1)} %collective-permute-done.18.refs_1_, bf16[4,1024]{1,0:T(4,128)(2,1)S(1)} %collective-permute-done.19.refs_2_), custom_call_target="tpu_custom_call" | custom-call | tf_op jit(solution)/shard_map/close/pallas_call | solution.py:419
  (44 shorter events, 1.2 us)
Async XLA Ops:
  0.6 21.3 %collective-permute-start.8 = (bf16[2,512,1024]{2,1,0:T(8,128)(2,1)}, bf16[2,512,1024]{2,1,0:T(8,128)(2,1)S(1)}, u32[]{:S(2)}, u32[]{:S(2)}) collective-permute-start(bf16[2,512,1024]{2,1,0:T(8,128)(2,1)} %refs_2_.3), channel_id=1, source_target_pairs={{0,1},{1,0},{2,3},{3,2},{4,5},{5,4},{6,7},{7,6},{8,9},{9,8},{10,11... | collective-permute-start | bytes 6291464 | tf_op jit(solution)/shard_map/ppermute | solution.py:69
  1.2 7.1 %collective-permute-start = (bf16[4,1024]{1,0:T(4,128)(2,1)}, bf16[4,1024]{1,0:T(4,128)(2,1)S(1)}, u32[]{:S(2)}, u32[]{:S(2)}) collective-permute-start(bf16[4,1024]{1,0:T(4,128)(2,1)} %refs_0_.1), channel_id=1, source_target_pairs={{4,0},{0,4},{12,8},{8,12},{5,1},{1,5},{13,9},{9,13},{6,2},{2,6},{1... | collective-permute-start | bytes 24584 | tf_op jit(solution)/shard_map/ppermute | solution.py:40
  3.8 5.0 %collective-permute-start.1 = (bf16[4,1024]{1,0:T(4,128)(2,1)}, bf16[4,1024]{1,0:T(4,128)(2,1)S(1)}, u32[]{:S(2)}, u32[]{:S(2)}) collective-permute-start(bf16[4,1024]{1,0:T(4,128)(2,1)} %refs_0_.1), channel_id=1, source_target_pairs={{8,0},{12,4},{0,8},{4,12},{9,1},{13,5},{1,9},{5,13},{10,2},{14,6},... | collective-permute-start | bytes 24584 | tf_op jit(solution)/shard_map/ppermute | solution.py:40
  6.4 5.7 %collective-permute-start.2 = (bf16[4,1024]{1,0:T(4,128)(2,1)}, bf16[4,1024]{1,0:T(4,128)(2,1)S(1)}, u32[]{:S(2)}, u32[]{:S(2)}) collective-permute-start(bf16[4,1024]{1,0:T(4,128)(2,1)} %refs_0_.1), channel_id=1, source_target_pairs={{12,0},{8,4},{4,8},{0,12},{13,1},{9,5},{5,9},{1,13},{14,2},{10,6},... | collective-permute-start | bytes 24584 | tf_op jit(solution)/shard_map/ppermute | solution.py:40
  6.4 1.6 %copy-start = (f32[2,4,4,128,128]{4,3,2,1,0:T(8,128)S(1)}, f32[2,4,4,128,128]{4,3,2,1,0:T(8,128)}, u32[]{:S(2)}) copy-start(f32[2,4,4,128,128]{4,3,2,1,0:T(8,128)} %state.7) | copy-start | bytes 6291460
  8.1 10.2 %collective-permute-start.6 = (bf16[4,4,128,128]{3,2,1,0:T(8,128)(2,1)S(1)}, bf16[4,4,128,128]{3,2,1,0:T(8,128)(2,1)S(1)}, u32[]{:S(2)}, u32[]{:S(2)}) collective-permute-start(bf16[4,4,128,128]{3,2,1,0:T(8,128)(2,1)S(1)} %shard_map.115.refs_6_), channel_id=1, source_target_pairs={{0,1},{1,0},{2,3},{3,2},{4,5},{5,4},{6,7},{7,6},{8,9},{9,8},{10,11... | collective-permute-start | bytes 1572872 | tf_op jit(solution)/shard_map/ppermute | solution.py:69
  8.2 3.9 %copy-start.2 = (bf16[2,1024,512]{2,1,0:T(8,128)(2,1)S(1)}, bf16[2,1024,512]{2,1,0:T(8,128)(2,1)}, u32[]{:S(2)}) copy-start(bf16[2,1024,512]{2,1,0:T(8,128)(2,1)} %refs_5_.6) | copy-start | bytes 6291460
  8.2 3.9 %copy-start.3 = (bf16[2,1024,512]{2,1,0:T(8,128)(2,1)S(1)}, bf16[2,1024,512]{2,1,0:T(8,128)(2,1)}, u32[]{:S(2)}) copy-start(bf16[2,1024,512]{2,1,0:T(8,128)(2,1)} %refs_6_.3) | copy-start | bytes 6291460
  8.2 3.9 %copy-start.4 = (bf16[2,1024,512]{2,1,0:T(8,128)(2,1)S(1)}, bf16[2,1024,512]{2,1,0:T(8,128)(2,1)}, u32[]{:S(2)}) copy-start(bf16[2,1024,512]{2,1,0:T(8,128)(2,1)} %refs_7_.3) | copy-start | bytes 6291460
  8.2 3.8 %copy-start.5 = (bf16[2,1024,512]{2,1,0:T(8,128)(2,1)S(1)}, bf16[2,1024,512]{2,1,0:T(8,128)(2,1)}, u32[]{:S(2)}) copy-start(bf16[2,1024,512]{2,1,0:T(8,128)(2,1)} %refs_8_.3) | copy-start | bytes 6291460
  8.3 3.8 %copy-start.7 = (f32[2,1024]{1,0:T(2,128)S(1)}, f32[2,1024]{1,0:T(2,128)}, u32[]{:S(2)}) copy-start(f32[2,1024]{1,0:T(2,128)} %refs_4_.4) | copy-start | bytes 24580
  8.3 3.8 %copy-start.9 = (bf16[4,1024]{1,0:T(4,128)(2,1)S(1)}, bf16[4,1024]{1,0:T(4,128)(2,1)}, u32[]{:S(2)}) copy-start(bf16[4,1024]{1,0:T(4,128)(2,1)} %refs_0_.1) | copy-start | bytes 24580
  8.3 25.6 %collective-permute-start.15 = (bf16[4,4,128,128]{3,2,1,0:T(8,128)(2,1)S(1)}, bf16[4,4,128,128]{3,2,1,0:T(8,128)(2,1)S(1)}, u32[]{:S(2)}, u32[]{:S(2)}) collective-permute-start(bf16[4,4,128,128]{3,2,1,0:T(8,128)(2,1)S(1)} %shard_map.120.refs_6_), channel_id=1, source_target_pairs={{0,1},{1,0},{2,3},{3,2},{4,5},{5,4},{6,7},{7,6},{8,9},{9,8},{10,11... | collective-permute-start | bytes 1572872 | tf_op jit(solution)/shard_map/ppermute | solution.py:69
  12.1 6.2 %copy-start.8 = (f32[2,512]{1,0:T(2,128)S(1)}, f32[2,512]{1,0:T(2,128)}, u32[]{:S(2)}) copy-start(f32[2,512]{1,0:T(2,128)} %refs_4_.5) | copy-start | bytes 12292
  12.1 6.2 %copy-start.10 = (f32[2,128]{1,0:T(2,128)S(1)}, f32[2,128]{1,0:T(2,128)}, u32[]{:S(2)}) copy-start(f32[2,128]{1,0:T(2,128)} %refs_5_.7) | copy-start | bytes 3076
  12.9 13.3 %copy-start.6 = (bf16[2,512,1024]{2,1,0:T(8,128)(2,1)S(1)}, bf16[2,512,1024]{2,1,0:T(8,128)(2,1)}, u32[]{:S(2)}) copy-start(bf16[2,512,1024]{2,1,0:T(8,128)(2,1)} %refs_2_.3) | copy-start | bytes 6291460
  12.9 1.8 %collective-permute-start.3 = (bf16[8,2176]{1,0:T(8,128)(2,1)S(1)}, bf16[8,2176]{1,0:T(8,128)(2,1)S(1)}, u32[]{:S(2)}, u32[]{:S(2)}) collective-permute-start(bf16[8,2176]{1,0:T(8,128)(2,1)S(1)} %get-tuple-element.23), channel_id=1, source_target_pairs={{0,1},{1,0},{2,3},{3,2},{4,5},{5,4},{6,7},{7,6},{8,9},{9,8},{10,11... | collective-permute-start | bytes 104456 | tf_op jit(solution)/shard_map/ppermute | solution.py:40
  13.0 4.0 %collective-permute-start.4 = (bf16[8,2176]{1,0:T(8,128)(2,1)S(1)}, bf16[8,2176]{1,0:T(8,128)(2,1)S(1)}, u32[]{:S(2)}, u32[]{:S(2)}) collective-permute-start(bf16[8,2176]{1,0:T(8,128)(2,1)S(1)} %get-tuple-element.24), channel_id=1, source_target_pairs={{0,2},{1,3},{2,0},{3,1},{4,6},{5,7},{6,4},{7,5},{8,10},{9,11},{10,... | collective-permute-start | bytes 104456 | tf_op jit(solution)/shard_map/ppermute | solution.py:40
  14.7 3.6 %collective-permute-start.5 = (bf16[8,2176]{1,0:T(8,128)(2,1)S(1)}, bf16[8,2176]{1,0:T(8,128)(2,1)S(1)}, u32[]{:S(2)}, u32[]{:S(2)}) collective-permute-start(bf16[8,2176]{1,0:T(8,128)(2,1)S(1)} %get-tuple-element.25), channel_id=1, source_target_pairs={{0,3},{1,2},{2,1},{3,0},{4,7},{5,6},{6,5},{7,4},{8,11},{9,10},{10,... | collective-permute-start | bytes 104456 | tf_op jit(solution)/shard_map/ppermute | solution.py:40
  18.8 3.1 %collective-permute-start.7 = (bf16[8,512]{1,0:T(8,128)(2,1)S(1)}, bf16[8,512]{1,0:T(8,128)(2,1)S(1)}, u32[]{:S(2)}, u32[]{:S(2)}) collective-permute-start(bf16[8,512]{1,0:T(8,128)(2,1)S(1)} %get-tuple-element.26.refs_0_), channel_id=1, source_target_pairs={{3,0},{2,1},{1,2},{0,3},{7,4},{6,5},{5,6},{4,7},{11,8},{10,9},{9,1... | collective-permute-start | bytes 24584 | tf_op jit(solution)/shard_map/ppermute | solution.py:40
  22.2 4.3 %collective-permute-start.9 = (bf16[16,1024]{1,0:T(8,128)(2,1)S(1)}, bf16[16,1024]{1,0:T(8,128)(2,1)S(1)}, u32[]{:S(2)}, u32[]{:S(2)}) collective-permute-start(bf16[16,1024]{1,0:T(8,128)(2,1)S(1)} %shard_map.118), channel_id=1, source_target_pairs={{0,5},{1,4},{2,7},{3,6},{4,1},{5,0},{6,3},{7,2},{8,13},{9,12},{10,... | collective-permute-start | bytes 98312 | tf_op jit(solution)/shard_map/ppermute | solution.py:60
  22.7 5.8 %collective-permute-start.10 = (bf16[16,1024]{1,0:T(8,128)(2,1)S(1)}, bf16[16,1024]{1,0:T(8,128)(2,1)S(1)}, u32[]{:S(2)}, u32[]{:S(2)}) collective-permute-start(bf16[16,1024]{1,0:T(8,128)(2,1)S(1)} %shard_map.118), channel_id=1, source_target_pairs={{0,9},{1,8},{2,11},{3,10},{4,13},{5,12},{6,15},{7,14},{8,1},{9,0},... | collective-permute-start | bytes 98312 | tf_op jit(solution)/shard_map/ppermute | solution.py:60
  26.2 5.2 %collective-permute-start.11 = (bf16[16,1024]{1,0:T(8,128)(2,1)S(1)}, bf16[16,1024]{1,0:T(8,128)(2,1)S(1)}, u32[]{:S(2)}, u32[]{:S(2)}) collective-permute-start(bf16[16,1024]{1,0:T(8,128)(2,1)S(1)} %shard_map.118), channel_id=1, source_target_pairs={{0,13},{1,12},{2,15},{3,14},{4,9},{5,8},{6,11},{7,10},{8,5},{9,4},... | collective-permute-start | bytes 98312 | tf_op jit(solution)/shard_map/ppermute | solution.py:60
  32.0 12.3 %copy-start.1 = (f32[2,4,4,128,128]{4,3,2,1,0:T(8,128)S(1)}, f32[2,4,4,128,128]{4,3,2,1,0:T(8,128)}, u32[]{:S(2)}) copy-start(f32[2,4,4,128,128]{4,3,2,1,0:T(8,128)} %state.7) | copy-start | bytes 6291460
  32.0 1.9 %collective-permute-start.12 = (bf16[8,2176]{1,0:T(8,128)(2,1)S(1)}, bf16[8,2176]{1,0:T(8,128)(2,1)S(1)}, u32[]{:S(2)}, u32[]{:S(2)}) collective-permute-start(bf16[8,2176]{1,0:T(8,128)(2,1)S(1)} %get-tuple-element.29), channel_id=1, source_target_pairs={{0,1},{1,0},{2,3},{3,2},{4,5},{5,4},{6,7},{7,6},{8,9},{9,8},{10,11... | collective-permute-start | bytes 104456 | tf_op jit(solution)/shard_map/ppermute | solution.py:40
  32.2 4.2 %collective-permute-start.13 = (bf16[8,2176]{1,0:T(8,128)(2,1)S(1)}, bf16[8,2176]{1,0:T(8,128)(2,1)S(1)}, u32[]{:S(2)}, u32[]{:S(2)}) collective-permute-start(bf16[8,2176]{1,0:T(8,128)(2,1)S(1)} %get-tuple-element.30), channel_id=1, source_target_pairs={{0,2},{1,3},{2,0},{3,1},{4,6},{5,7},{6,4},{7,5},{8,10},{9,11},{10,... | collective-permute-start | bytes 104456 | tf_op jit(solution)/shard_map/ppermute | solution.py:40
  32.8 3.7 %collective-permute-start.14 = (bf16[8,2176]{1,0:T(8,128)(2,1)S(1)}, bf16[8,2176]{1,0:T(8,128)(2,1)S(1)}, u32[]{:S(2)}, u32[]{:S(2)}) collective-permute-start(bf16[8,2176]{1,0:T(8,128)(2,1)S(1)} %get-tuple-element.31), channel_id=1, source_target_pairs={{0,3},{1,2},{2,1},{3,0},{4,7},{5,6},{6,5},{7,4},{8,11},{9,10},{10,... | collective-permute-start | bytes 104456 | tf_op jit(solution)/shard_map/ppermute | solution.py:40
  37.0 3.1 %collective-permute-start.16 = (bf16[8,512]{1,0:T(8,128)(2,1)S(1)}, bf16[8,512]{1,0:T(8,128)(2,1)S(1)}, u32[]{:S(2)}, u32[]{:S(2)}) collective-permute-start(bf16[8,512]{1,0:T(8,128)(2,1)S(1)} %get-tuple-element.32.refs_0_), channel_id=1, source_target_pairs={{3,0},{2,1},{1,2},{0,3},{7,4},{6,5},{5,6},{4,7},{11,8},{10,9},{9,1... | collective-permute-start | bytes 24584 | tf_op jit(solution)/shard_map/ppermute | solution.py:40
  40.5 6.9 %collective-permute-start.17 = (bf16[4,1024]{1,0:T(4,128)(2,1)S(1)}, bf16[4,1024]{1,0:T(4,128)(2,1)S(1)}, u32[]{:S(2)}, u32[]{:S(2)}) collective-permute-start(bf16[4,1024]{1,0:T(4,128)(2,1)S(1)} %get-tuple-element.35), channel_id=1, source_target_pairs={{0,5},{1,4},{2,7},{3,6},{4,1},{5,0},{6,3},{7,2},{8,13},{9,12},{10,... | collective-permute-start | bytes 24584 | tf_op jit(solution)/shard_map/ppermute | solution.py:60
  40.5 6.9 %collective-permute-start.18 = (bf16[4,1024]{1,0:T(4,128)(2,1)S(1)}, bf16[4,1024]{1,0:T(4,128)(2,1)S(1)}, u32[]{:S(2)}, u32[]{:S(2)}) collective-permute-start(bf16[4,1024]{1,0:T(4,128)(2,1)S(1)} %get-tuple-element.36), channel_id=1, source_target_pairs={{0,9},{1,8},{2,11},{3,10},{4,13},{5,12},{6,15},{7,14},{8,1},{9,0},... | collective-permute-start | bytes 24584 | tf_op jit(solution)/shard_map/ppermute | solution.py:60
  41.7 5.8 %collective-permute-start.19 = (bf16[4,1024]{1,0:T(4,128)(2,1)S(1)}, bf16[4,1024]{1,0:T(4,128)(2,1)S(1)}, u32[]{:S(2)}, u32[]{:S(2)}) collective-permute-start(bf16[4,1024]{1,0:T(4,128)(2,1)S(1)} %get-tuple-element.37), channel_id=1, source_target_pairs={{0,13},{1,12},{2,15},{3,14},{4,9},{5,8},{6,11},{7,10},{8,5},{9,4},... | collective-permute-start | bytes 24584 | tf_op jit(solution)/shard_map/ppermute | solution.py:60
